TPU v7x, 32 devices: a whole 2x2x4 slice. The times are simulated.
32 devices in a mesh: sp: 8 (over z, x), tp: 4 (over y, core).
Axes of the slice: x: 2, y: 2, z: 4, core: 2. Of those that a mesh axis runs over, the one named last changes fastest.
Arguments:
- moe_input: bfloat16 [1024, 2048], P('sp'), may hold values from -6 to 6
- out_grad: bfloat16 [1024, 2048], P('sp'), may hold values from -6 to 6
- routes: int32 [1024, 2], P('sp'), may hold values from 0 to 7, all different within a row; in each aligned block of 128 rows (0 to 127, 128 to 255, ...) at most 40 rows name the same one
- route_weight: float32 [1024, 2], P('sp'), may hold values from 0.2 to 1.2
- w_gate: bfloat16 [8, 2048, 2048], P('sp', None, 'tp'), may hold values from -0.125 to 0.125
- w_up: bfloat16 [8, 2048, 2048], P('sp', None, 'tp'), may hold values from -0.125 to 0.125
- w_down: bfloat16 [8, 2048, 2048], P('sp', 'tp'), may hold values from -0.125 to 0.125
- w_out: bfloat16 [2048, 4096], P(None, 'tp'), may hold values from -0.09375 to 0.09375
- query_heads: bfloat16 [16, 1024, 128], P('tp', 'sp'), may hold values from -6 to 6
- key_heads: bfloat16 [16, 1024, 128], P('tp', 'sp'), may hold values from -6 to 6
- value_heads: bfloat16 [16, 1024, 256], P('tp', 'sp'), may hold values from -6 to 6
- log_decay: float32 [16, 1024], P('tp', 'sp'), may hold values from -0.6 to 0
- state_in: float32 [16, 8, 128, 256], P('tp', 'sp'), may hold values from -4 to 4
Outputs:
- gate_grad: bfloat16 [8, 2048, 2048], P('sp', None, 'tp')
- up_grad: bfloat16 [8, 2048, 2048], P('sp', None, 'tp')
- down_grad: bfloat16 [8, 2048, 2048], P('sp', 'tp')
- out_proj_grad: float32 [2048, 4096], P('sp', 'tp')
- query_gradient: bfloat16 [16, 1024, 128], P('tp', 'sp')
- key_grad: bfloat16 [16, 1024, 128], P('tp', 'sp')
- value_grad: bfloat16 [16, 1024, 256], P('tp', 'sp')
Inputs may be any that keep to these rules, and one draw needn't show every extreme that they name: `routes`: each row names 2 different experts; within each aligned block of 128 tokens no expert is named more than 40 times, and exactly 40 times for some expert in some blocks.
All inputs are finite; a program needn't handle non-finite values.
Results may differ from a plain program's by a relative error of at most 0.025.
Values may be sent and summed in bfloat16 or wider, within the bound.
No kernel may reach another device: no remote copies, remote signals or barrier semaphores. Data moves between devices by JAX's collectives and lax.ppermute only.
A program may use at most 64 MiB of HBM per device.

v0:
```python
import jax
import jax.numpy as jnp
from jax import lax
from jax.sharding import PartitionSpec as P

BLOCK = 64


exact_precision = lax.Precision.HIGHEST


def entering(shard, axis, join, neutral):
    count = lax.axis_size(axis)
    place = lax.axis_index(axis)
    ahead = count - 1 - place
    gathered = jax.tree.map(
        lambda a, kind: lax.all_gather(a.astype(kind), axis), shard, (jnp.bfloat16, jnp.bfloat16)
    )
    state = jax.tree.map(lambda a, e: jnp.zeros_like(a) + jnp.asarray(e, a.dtype), shard, neutral)

    def one(lap, state):
        source = count - 1 - lap
        return join(
            state,
            jax.tree.map(
                lambda a, own: lax.dynamic_index_in_dim(a, source, 0, False).astype(own.dtype),
                gathered,
                shard,
            ),
        )

    return lax.fori_loop(0, ahead, one, state)


def silu_slope(gate_pre):
    sigmoid_v = jax.nn.sigmoid(gate_pre)
    return sigmoid_v * (1.0 + gate_pre * (1.0 - sigmoid_v))


def decay_table(log_sums):
    block_size = log_sums.shape[-1]
    token_positions = jnp.arange(block_size)
    lower_mask = (token_positions[:, None] >= token_positions[None, :])[None]
    log_diff = jnp.where(lower_mask, log_sums[:, :, None] - log_sums[:, None, :], 0.0)
    return jnp.where(lower_mask, jnp.exp(log_diff), 0.0)


def forward_block(forwarded_state, inputs):
    query_rows, rescaled_keys, value_rows, head_gradients, log_sums = inputs
    decay_mat = decay_table(log_sums)
    scores = (
        jnp.einsum("htk,hsk->hts", query_rows, rescaled_keys, precision=exact_precision) * decay_mat
    )
    leading_decay = jnp.exp(log_sums)[:, :, None]
    trailing_decay = jnp.exp(log_sums[:, -1:] - log_sums)[:, :, None]
    blended_heads = jnp.einsum("hts,hsv->htv", scores, value_rows, precision=exact_precision)
    blended_heads = blended_heads + jnp.einsum(
        "imj,iju->imu", query_rows * leading_decay, forwarded_state, precision=exact_precision
    )
    back_scores = (
        jnp.einsum("htv,hsv->hts", head_gradients, value_rows, precision=exact_precision)
        * decay_mat
    )
    query_gradient = jnp.einsum(
        "hts,hsk->htk", back_scores, rescaled_keys, precision=exact_precision
    )
    query_gradient = query_gradient + jnp.einsum(
        "fqg,fug->fqu", head_gradients * leading_decay, forwarded_state, precision=exact_precision
    )
    forwarded_state = jnp.exp(log_sums[:, -1])[:, None, None] * forwarded_state + jnp.einsum(
        "nbq,nbc->nqc", rescaled_keys * trailing_decay, value_rows, precision=exact_precision
    )
    return (forwarded_state, (blended_heads, query_gradient))


def reverse_block(forwarded_state, inputs):
    query_rows, rescaled_keys, value_rows, head_gradients, log_sums = inputs
    decay_mat = decay_table(log_sums)
    scores = (
        jnp.einsum("htk,hsk->hts", query_rows, rescaled_keys, precision=exact_precision) * decay_mat
    )
    back_scores = (
        jnp.einsum("htv,hsv->hts", head_gradients, value_rows, precision=exact_precision)
        * decay_mat
    )
    leading_decay = jnp.exp(log_sums)[:, :, None]
    trailing_decay = jnp.exp(log_sums[:, -1:] - log_sums)[:, :, None]
    key_portion = jnp.einsum("hts,htk->hsk", back_scores, query_rows, precision=exact_precision)
    key_portion = key_portion + jnp.einsum(
        "lbg,ljg->lbj", value_rows * trailing_decay, forwarded_state, precision=exact_precision
    )
    value_portion = jnp.einsum("hts,htv->hsv", scores, head_gradients, precision=exact_precision)
    value_portion = value_portion + jnp.einsum(
        "bea,baz->bez", rescaled_keys * trailing_decay, forwarded_state, precision=exact_precision
    )
    forwarded_state = jnp.exp(log_sums[:, -1])[:, None, None] * forwarded_state + jnp.einsum(
        "byj,byg->bjg", query_rows * leading_decay, head_gradients, precision=exact_precision
    )
    return (forwarded_state, (key_portion, value_portion))


def link_states(higher_part, lower_part):
    return (
        higher_part[0] * lower_part[0],
        lower_part[1] + lower_part[0][:, None, None] * higher_part[1],
    )


def expert_backward(rows_in, grad_in, w_gate, w_up, w_down):
    gate_pre = jnp.einsum("erd,edf->erf", rows_in, w_gate, preferred_element_type=jnp.float32)
    up_pre = jnp.einsum("erd,edf->erf", rows_in, w_up, preferred_element_type=jnp.float32)
    active = jax.nn.silu(gate_pre)
    hidden = (active * up_pre).astype(jnp.bfloat16)
    hidden_back = jnp.einsum("erd,efd->erf", grad_in, w_down, preferred_element_type=jnp.float32)
    down_part = jnp.einsum("erf,erd->efd", hidden, grad_in, preferred_element_type=jnp.float32)
    gate_back = (hidden_back * up_pre * silu_slope(gate_pre)).astype(jnp.bfloat16)
    up_back = (hidden_back * active).astype(jnp.bfloat16)
    gate_part = jnp.einsum("erd,erf->edf", rows_in, gate_back, preferred_element_type=jnp.float32)
    up_part = jnp.einsum("erd,erf->edf", rows_in, up_back, preferred_element_type=jnp.float32)
    partial_value = jnp.einsum(
        "erf,edf->erd", gate_back, w_gate, preferred_element_type=jnp.float32
    )
    partial_value = partial_value + jnp.einsum(
        "erf,edf->erd", up_back, w_up, preferred_element_type=jnp.float32
    )
    return (
        gate_part.astype(jnp.bfloat16),
        up_part.astype(jnp.bfloat16),
        down_part.astype(jnp.bfloat16),
        partial_value.astype(jnp.bfloat16),
    )


def body(
    moe_input,
    out_grad,
    routes,
    route_weight,
    w_gate,
    w_up,
    w_down,
    w_out,
    query_heads,
    key_heads,
    value_heads,
    log_decay,
    state_in,
):
    tok_rows, model_width = moe_input.shape
    picks = routes.shape[1]
    experts = w_gate.shape[0] * lax.axis_size("sp")
    capacity = 5 * tok_rows * picks // (4 * experts)
    route_ids = routes.reshape(-1)
    routed = route_ids.shape[0]
    onehot = (route_ids[:, None] == jnp.arange(experts, dtype=jnp.int32)[None, :]).astype(jnp.int32)
    slot_index = jnp.sum(jnp.cumsum(onehot, axis=0) * onehot, axis=1) - 1
    target = route_ids * capacity + slot_index
    source = (
        jnp.full((experts * capacity,), routed, jnp.int32)
        .at[target]
        .set(jnp.arange(routed, dtype=jnp.int32))
    )
    filled = source < routed
    picked = jnp.where(filled, source, 0)
    token_idx = picked // picks
    weight_slot = jnp.where(filled, route_weight.reshape(-1)[picked], 0.0)
    send_rows = jnp.where(filled[:, None], moe_input[token_idx], jnp.zeros((), jnp.bfloat16))
    send_rows = send_rows.reshape(experts, capacity, model_width)
    send_grad = (weight_slot[:, None] * out_grad[token_idx].astype(jnp.float32)).astype(
        jnp.bfloat16
    )
    send_grad = send_grad.reshape(experts, capacity, model_width)
    group_count = lax.axis_size("tp")
    slice_width = model_width // group_count
    rows_in, grad_in = (
        lax.all_to_all(send_rows, "sp", split_axis=0, concat_axis=1, tiled=True),
        lax.all_to_all(send_grad, "sp", split_axis=0, concat_axis=1, tiled=True),
    )
    gate_grad, up_grad, down_grad, partial_value = expert_backward(
        rows_in, grad_in, w_gate, w_up, w_down
    )
    local_rows = partial_value.shape[1]
    grouped = partial_value.reshape(partial_value.shape[0], local_rows, group_count, slice_width)
    spread_parts = lax.all_to_all(grouped, "tp", split_axis=2, concat_axis=2, tiled=True)
    feature_part = jnp.sum(spread_parts.astype(jnp.float32), axis=2).astype(jnp.bfloat16)
    returned_part = lax.all_to_all(feature_part, "sp", split_axis=1, concat_axis=0, tiled=True)
    returned = lax.all_gather(returned_part, "tp", axis=2, tiled=True)
    gathered = returned.reshape(experts * capacity, model_width)[target].reshape(
        tok_rows, picks, model_width
    )
    mixed_grad = (
        out_grad.astype(jnp.float32) + jnp.sum(gathered.astype(jnp.float32), axis=1)
    ).astype(jnp.bfloat16)
    head_count = query_heads.shape[0]
    key_size = key_heads.shape[-1]
    value_size = value_heads.shape[-1]
    head_grad = jnp.dot(mixed_grad, w_out, preferred_element_type=jnp.float32).astype(jnp.bfloat16)
    head_gradients = (
        head_grad.reshape(tok_rows, head_count, value_size).transpose(1, 0, 2).astype(jnp.float32)
    )
    query_rows = query_heads.astype(jnp.float32)
    rescaled_keys = key_heads.astype(jnp.float32) * key_size ** (-0.5)
    value_rows = value_heads.astype(jnp.float32)
    block_count = tok_rows // BLOCK

    def to_blocks(array):
        return array.reshape(head_count, block_count, BLOCK, array.shape[-1]).transpose(1, 0, 2, 3)

    def from_blocks(array):
        return array.transpose(1, 0, 2, 3).reshape(head_count, tok_rows, array.shape[-1])

    log_sums = jnp.cumsum(log_decay.reshape(head_count, block_count, BLOCK), axis=2).transpose(
        1, 0, 2
    )
    inputs = (
        to_blocks(query_rows),
        to_blocks(rescaled_keys),
        to_blocks(value_rows),
        to_blocks(head_gradients),
        log_sums,
    )
    _, (blended_heads, query_gradient) = lax.scan(forward_block, state_in[:, 0], inputs)
    running_total = jnp.cumsum(log_decay, axis=1)
    carried = jnp.einsum(
        "byj,byg->bjg",
        query_rows * jnp.exp(running_total)[:, :, None],
        head_gradients,
        precision=exact_precision,
    )
    span_keep = jnp.exp(running_total[:, -1])
    incoming = entering(
        (span_keep, carried), "sp", link_states, (jnp.ones_like(span_keep), jnp.zeros_like(carried))
    )[1]
    _, (key_grad, value_grad) = lax.scan(reverse_block, incoming, inputs, reverse=True)
    mixed_flat = (
        from_blocks(blended_heads)
        .astype(jnp.bfloat16)
        .transpose(1, 0, 2)
        .reshape(tok_rows, head_count * value_size)
    )
    out_proj_grad = lax.psum_scatter(
        lax.dot_general(
            mixed_grad, mixed_flat, (((0,), (0,)), ((), ())), preferred_element_type=jnp.float32
        ).astype(jnp.bfloat16),
        "sp",
        scatter_dimension=0,
        tiled=True,
    ).astype(jnp.float32)
    query_gradient = from_blocks(query_gradient).astype(jnp.bfloat16)
    key_grad = (from_blocks(key_grad) * key_size ** (-0.5)).astype(jnp.bfloat16)
    value_grad = from_blocks(value_grad).astype(jnp.bfloat16)
    return (gate_grad, up_grad, down_grad, out_proj_grad, query_gradient, key_grad, value_grad)


def solution(mesh):
    return jax.shard_map(
        body,
        mesh=mesh,
        in_specs=(
            P("sp", None),
            P("sp", None),
            P("sp", None),
            P("sp", None),
            P("sp", None, "tp"),
            P("sp", None, "tp"),
            P("sp", "tp", None),
            P(None, "tp"),
            P("tp", "sp", None),
            P("tp", "sp", None),
            P("tp", "sp", None),
            P("tp", "sp"),
            P("tp", "sp", None, None),
        ),
        out_specs=(
            P("sp", None, "tp"),
            P("sp", None, "tp"),
            P("sp", "tp", None),
            P("sp", "tp"),
            P("tp", "sp", None),
            P("tp", "sp", None),
            P("tp", "sp", None),
        ),
        check_vma=False,
    )
```

profile of v0, /device:TPU:0, one launch (start us, length us, event | category | flops | bytes accessed | tf_op | source)
XLA Modules:
  0.0 334.4 jit_solution(13286429424124512285)
XLA Ops:
  10.3 1.4 scatter_custom_fusion
  11.9 3.0 gather_fusion
  14.9 2.6 broadcast_select_fusion
  17.5 7.3 %all-to-all-start = ((bf16[8,40,2048]{2,1,0:T(8,128)(2,1)}), bf16[8,40,2048]{2,1,0:T(8,128)(2,1)}, u32[]{:S(2)}, u32[]{:S(2)}) async-start(bf16[8,40,2048]{2,1,0:T(8,128)(2,1)} %broadcast_select_fusion), calls=%async_computation | async-start | bytes 2621440 | tf_op jit(solution)/shard_map/all_to_all | solution.py:176
  24.8 3.0 gather_fusion.2
  28.1 2.5 gather_fusion.1
  30.6 2.7 fusion.70
  33.3 23.0 %all-to-all-done = bf16[8,40,2048]{2,1,0:T(8,128)(2,1)} async-done(((bf16[8,40,2048]{2,1,0:T(8,128)(2,1)}), bf16[8,40,2048]{2,1,0:T(8,128)(2,1)}, u32[]{:S(2)}, u32[]{:S(2)}) %all-to-all-start) | async-done | bytes 1310752 | tf_op jit(solution)/shard_map/all_to_all | solution.py:176
  56.3 4.3 %all-to-all-start.1 = ((bf16[8,40,2048]{2,1,0:T(8,128)(2,1)}), bf16[8,40,2048]{2,1,0:T(8,128)(2,1)}, u32[]{:S(2)}, u32[]{:S(2)}) async-start(bf16[8,40,2048]{2,1,0:T(8,128)(2,1)} %fusion.70), calls=%async_computation.1 | async-start | bytes 2621440 | tf_op jit(solution)/shard_map/all_to_all | solution.py:177
  60.6 2.3 fusion.73
  63.0 3.3 fusion.76
  66.2 25.3 %all-to-all-done.1 = bf16[8,40,2048]{2,1,0:T(8,128)(2,1)} async-done(((bf16[8,40,2048]{2,1,0:T(8,128)(2,1)}), bf16[8,40,2048]{2,1,0:T(8,128)(2,1)}, u32[]{:S(2)}, u32[]{:S(2)}) %all-to-all-start.1) | async-done | bytes 1310752 | tf_op jit(solution)/shard_map/all_to_all | solution.py:177
  91.6 3.2 multiply_convert_fusion.1
  96.6 1.9 fusion.69
  98.5 4.1 %reshape.353 = bf16[1,320,4,512]{3,2,1,0:T(4,128)(2,1)} reshape(bf16[320,2048]{1,0:T(8,128)(2,1)} %fusion.69) | data formatting | bytes 2621440 | tf_op jit(solution)/shard_map/reshape | solution.py:183
  102.6 1.6 copy.168
  104.2 20.4 %all_to_all.35 = bf16[1,320,4,512]{3,1,0,2:T(8,128)(2,1)} all-to-all(bf16[1,320,4,512]{3,1,0,2:T(8,128)(2,1)S(1)} %copy.168), channel_id=1, replica_groups=mesh['sp'=8,'tp'=4] {'tp'}, dimensions={2} | all-to-all | bytes 2621440 | tf_op jit(solution)/shard_map/all_to_all | solution.py:184
  124.6 2.3 reduce_sum.33
  126.9 1.5 copy.203
  128.9 3.4 %reduce.10 = bf16[320,512]{1,0:T(8,128)(2,1)} reduce(bf16[320,1,512]{2,1,0:T(2,128)(2,1)S(1)} %bitcast.257, bf16[]{:T(256)} %broadcast.193), dimensions={1}, to_apply=%bitcast.184.reduce_sub_computation | reduce | bytes 655362
  133.5 14.1 %all_to_all.36 = bf16[8,2,10240]{2,1,0:T(2,128)(2,1)} all-to-all(bf16[8,2,10240]{2,1,0:T(2,128)(2,1)S(1)} %reshape.425), channel_id=1, replica_groups=mesh['sp'=8,'tp'=4] {'sp'}, dimensions={0} | all-to-all | bytes 655360 | tf_op jit(solution)/shard_map/all_to_all | solution.py:186
  147.6 2.5 reshape.426
  155.7 11.0 %all-gather.5.cloned.1.call-done = bf16[8,40,2048]{2,1,0:T(8,128)(2,1)} async-done(((bf16[8,40,512]{2,1,0:T(8,128)(2,1)}), bf16[8,40,2048]{2,1,0:T(8,128)(2,1)}) %all-gather.5.cloned.1.call-update) | async-done | bytes 1310736 | tf_op jit(solution)/shard_map/all_gather | solution.py:187
  166.7 4.8 %gather_fusion.3 = bf16[256,2048]{1,0:T(8,128)(2,1)} fusion(bf16[320,2048]{1,0:T(8,128)(2,1)} %bitcast.254, s32[1024]{0:T(1024)S(1)} %pad_clamp_fusion), kind=kCustom, calls=%fused_computation.3 | custom fusion | bytes 2098176 | tf_op jit(solution)/shard_map/gather | solution.py:188
  171.5 3.3 reshape.365
  174.8 5.1 %reduce_sum.35 = f32[128,2048]{1,0:T(8,128)} reduce(f32[128,2,2048]{2,1,0:T(2,128)} %reshape.365, f32[]{:T(128)} %constant.152.clone.1), dimensions={1}, to_apply=%region_5.6 | reduce | flops 262144 | bytes 3145732 | tf_op jit(solution)/shard_map/reduce_sum | solution.py:192
  179.9 3.3 convolution_convert_fusion.5
  187.3 14.4 %while.46 = (s32[]{:T(128)}, f32[4,128,256]{2,1,0:T(8,128)S(1)}, bf16[2,4,64,256]{3,2,0,1:T(8,128)(2,1)}, bf16[2,4,64,128]{3,2,1,0:T(8,128)(2,1)}, f32[2,4,64]{2...) while((s32[]{:T(128)}, f32[4,128,256]{2,1,0:T(8,128)S(1)}, ...), condition=%wide.region_8.9_spmd, body=%wide.region_7.8_spmd.sunk | while | flops 453611776 | bytes 10858797 | solution.py:222
  187.3 1.3 convolution_multiply_fusion.8
  188.6 1.3 fusion.161
  190.0 2.0 fusion.162
  194.5 1.3 convolution_multiply_fusion.8
  195.9 1.3 fusion.161
  197.2 2.0 fusion.162
  202.8 4.5 %convolution_convert_fusion = bf16[2048,1024]{1,0:T(8,128)(2,1)} fusion(bf16[128,1024]{0,1:T(8,128)(2,1)S(1)} %bitcast.264, f32[128,2048]{1,0:T(8,128)} %reduce_sum.35, bf16[128,2048]{1,0:T(8,128)(2,1)S(1)} %copy-done.1), kind=kOutput, calls=%fused_computation.99 | convolution fusion | flops 539754496 | bytes 6029312 | tf_op jit(solution)/shard_map/dot_general | solution.py:242
  209.6 21.8 %all-reduce = bf16[32]{0:T(256)(128)(2,1)S(1)} all-reduce(bf16[32]{0:T(256)(128)(2,1)S(1)} %dynamic-update-slice), channel_id=3, replica_groups=mesh['sp'=8,'tp'=4] {'sp'}, use_global_device_ids=true, to_apply=%add | all-reduce | flops 32 | bytes 128
  231.5 4.0 %fusion.67 = bf16[1,2048,512]{2,1,0:T(8,128)(2,1)} fusion(bf16[320,2048]{1,0:T(8,128)(2,1)} %bitcast.21, bf16[320,512]{1,0:T(8,128)(2,1)S(1)} %copy-done.20), kind=kOutput, calls=%fused_computation.105 | convolution fusion | flops 672137216 | bytes 3735552 | tf_op jit(solution)/shard_map/erd,erf->edf/dot_general | solution.py:119
  235.5 4.0 %fusion.66 = bf16[1,2048,512]{2,1,0:T(8,128)(2,1)} fusion(bf16[320,2048]{1,0:T(8,128)(2,1)} %bitcast.21, bf16[320,512]{1,0:T(8,128)(2,1)S(1)} %copy-done.14), kind=kOutput, calls=%fused_computation.104 | convolution fusion | flops 672137216 | bytes 3735552 | tf_op jit(solution)/shard_map/erd,erf->edf/dot_general | solution.py:118
  239.5 4.0 %fusion.68 = bf16[1,512,2048]{2,1,0:T(8,128)(2,1)} fusion(bf16[320,2048]{1,0:T(8,128)(2,1)} %bitcast.23, f32[320,512]{1,0:T(8,128)S(1)} %copy-done.29, f32[320,512]{1,0:T(8,128)S(1)} %copy-done.28), kind=kOutput, calls=%fused_computation.106 | convolution fusion | flops 673120256 | bytes 4718592 | tf_op jit(solution)/shard_map/erf,erd->efd/dot_general | solution.py:115
  244.2 8.3 %while.47 = (s32[]{:T(128)}, f32[4,128,256]{2,1,0:T(8,128)S(1)}, s32[]{:T(128)}, bf16[8,4,128,256]{3,2,1,0:T(8,128)(2,1)}, bf16[8,4]{1,0:T(8,128)(2,1)S(1)}, /*index=5*/s32[]{:T(128)}, s32[]{:T(128)}, s32[]{:T(128)}, s32[]{:T(128)}) while((s32[]{:T(128)}, f32[4,128,256]{2,1,0:T(8,128)S(1)}, s32[]{:T(128)}, ...), condition=%wide.region_12.13_spmd, body=%wide.region_11.12_spmd.sunk | while | flops 393226 | bytes 1310907 | solution.py:32
  253.9 14.3 %while.48 = (s32[]{:T(128)}, f32[4,128,256]{2,1,0:T(8,128)S(1)}, f32[2,4,64,128]{3,2,1,0:T(8,128)}, bf16[2,4,64,256]{3,2,1,0:T(8,128)(2,1)}, f32[2,4,64]{2,1,0:T...) while((s32[]{:T(128)}, f32[4,128,256]{2,1,0:T(8,128)S(1)}, ...), condition=%wide.region_14.15_spmd, body=%wide.region_13.14_spmd.sunk | while | flops 453611776 | bytes 10859325 | solution.py:234
  254.0 1.3 convolution_multiply_fusion.11
  255.3 1.4 fusion.179
  261.2 1.3 convolution_multiply_fusion.11
  262.5 1.4 fusion.179
  269.9 1.7 copy.186
  271.6 54.1 %reduce-scatter.2.cloned.1.call-done = bf16[256,1024]{1,0:T(8,128)(2,1)} async-done(((bf16[2048,1024]{1,0:T(8,128)(2,1)}), bf16[256,1024]{1,0:T(8,128)(2,1)}) %reduce-scatter.2.cloned.1.call-update) | async-done | bytes 524304 | tf_op jit(solution)/shard_map/reduce_scatter | solution.py:241
  325.7 2.1 convert_element_type.182
  (193 shorter events, 44.8 us)
Async XLA Ops:
  7.2 53.4 %copy-start = (bf16[1,2048,512]{2,1,0:T(8,128)(2,1)S(1)}, bf16[1,2048,512]{2,1,0:T(8,128)(2,1)}, u32[]{:S(2)}) copy-start(bf16[1,2048,512]{2,1,0:T(8,128)(2,1)} %param.23) | copy-start | bytes 6291460
  7.2 4.7 %copy-start.2 = (bf16[128,2048]{1,0:T(8,128)(2,1)S(1)}, bf16[128,2048]{1,0:T(8,128)(2,1)}, u32[]{:S(2)}) copy-start(bf16[128,2048]{1,0:T(8,128)(2,1)} %param.19) | copy-start | bytes 1572868
  10.3 1.5 copy-start.23
  14.9 9.9 %copy-start.1 = (bf16[128,2048]{1,0:T(8,128)(2,1)S(1)}, bf16[128,2048]{1,0:T(8,128)(2,1)}, u32[]{:S(2)}) copy-start(bf16[128,2048]{1,0:T(8,128)(2,1)} %param.20) | copy-start | bytes 1572868
  17.5 38.8 %all-to-all-start = ((bf16[8,40,2048]{2,1,0:T(8,128)(2,1)}), bf16[8,40,2048]{2,1,0:T(8,128)(2,1)}, u32[]{:S(2)}, u32[]{:S(2)}) async-start(bf16[8,40,2048]{2,1,0:T(8,128)(2,1)} %broadcast_select_fusion), calls=%async_computation | async-start | bytes 2621440 | tf_op jit(solution)/shard_map/all_to_all | solution.py:176
  24.8 3.0 copy-start.25
  56.3 35.3 %all-to-all-start.1 = ((bf16[8,40,2048]{2,1,0:T(8,128)(2,1)}), bf16[8,40,2048]{2,1,0:T(8,128)(2,1)}, u32[]{:S(2)}, u32[]{:S(2)}) async-start(bf16[8,40,2048]{2,1,0:T(8,128)(2,1)} %fusion.70), calls=%async_computation.1 | async-start | bytes 2621440 | tf_op jit(solution)/shard_map/all_to_all | solution.py:177
  60.6 106.1 %all-gather.5.cloned.1.call-start = ((), (), s32[]{:S(2)}) async-start(), calls=%async_computation.5 | async-start | bytes 1638400 | tf_op jit(solution)/shard_map/all_gather | solution.py:187
  60.6 2.3 copy-start.9
  62.9 28.6 %copy-start.27 = (f32[320,512]{1,0:T(8,128)}, f32[320,512]{1,0:T(8,128)S(1)}, u32[]{:S(2)}) copy-start(f32[320,512]{1,0:T(8,128)S(1)} %fusion.73) | copy-start | bytes 1966084
  94.7 0.9 copy-start.13
  94.8 0.9 copy-start.19
  94.8 1.8 copy-start.10
  128.9 22.0 %copy-start.22 = (f32[4,128]{1,0:T(4,128)S(1)}, f32[4,128]{1,0:T(4,128)}, u32[]{:S(2)}) copy-start(f32[4,128]{1,0:T(4,128)} %param.30) | copy-start | bytes 6148
  147.6 5.6 %copy-start.21 = (bf16[4,128,128]{2,1,0:T(8,128)(2,1)S(1)}, bf16[4,128,128]{2,1,0:T(8,128)(2,1)}, u32[]{:S(2)}) copy-start(bf16[4,128,128]{2,1,0:T(8,128)(2,1)} %param.28) | copy-start | bytes 393220
  150.1 3.2 copy-start.15
  150.9 4.1 %copy-start.24 = (s32[256,1]{0,1:T(1,128)S(1)}, s32[256,1]{0,1:T(1,128)}, u32[]{:S(2)}) copy-start(s32[256,1]{0,1:T(1,128)} %copy-done.23) | copy-start | bytes 3076
  150.9 93.3 %all-gather.7.cloned.1.call-start = ((), (), s32[]{:S(2)}) async-start(), calls=%async_computation.7 | async-start | bytes 2359296 | tf_op jit(solution)/shard_map/all_gather | solution.py:17
  183.2 4.1 %copy-start.3 = (f32[4,1,128,256]{3,2,1,0:T(8,128)S(1)}, f32[4,1,128,256]{3,2,1,0:T(8,128)}, u32[]{:S(2)}) copy-start(f32[4,1,128,256]{3,2,1,0:T(8,128)} %param.31) | copy-start | bytes 1572868
  185.2 140.6 %reduce-scatter.2.cloned.1.call-start = ((), (), s32[]{:S(2)}) async-start(), calls=%async_computation.6 | async-start | bytes 4718592 | tf_op jit(solution)/shard_map/reduce_scatter | solution.py:241
  187.3 4.7 %copy-start.4 = (f32[2,4,64,256]{3,2,1,0:T(8,128)S(1)}, f32[2,4,64,256]{3,2,1,0:T(8,128)}, u32[]{:S(2)}) copy-start(f32[2,4,64,256]{3,2,1,0:T(8,128)} %get-tuple-element.662) | copy-start | bytes 1572868 | tf_op jit(solution)/shard_map/while
  187.3 4.7 %copy-start.6 = (f32[2,4,64,256]{3,2,1,0:T(8,128)S(1)}, f32[2,4,64,256]{3,2,1,0:T(8,128)}, u32[]{:S(2)}) copy-start(f32[2,4,64,256]{3,2,1,0:T(8,128)} %get-tuple-element.664) | copy-start | bytes 1572868 | tf_op jit(solution)/shard_map/while
  187.3 5.4 %copy-start.16 = (bf16[2,4,64,128]{3,2,1,0:T(8,128)(2,1)S(1)}, bf16[2,4,64,128]{3,2,1,0:T(8,128)(2,1)}, u32[]{:S(2)}) copy-start(bf16[2,4,64,128]{3,2,1,0:T(8,128)(2,1)} %get-tuple-element.649) | copy-start | bytes 393220 | tf_op jit(solution)/shard_map/while
  193.4 1.1 copy-start.17
  194.5 4.7 %copy-start.4 = (f32[2,4,64,256]{3,2,1,0:T(8,128)S(1)}, f32[2,4,64,256]{3,2,1,0:T(8,128)}, u32[]{:S(2)}) copy-start(f32[2,4,64,256]{3,2,1,0:T(8,128)} %get-tuple-element.662) | copy-start | bytes 1572868 | tf_op jit(solution)/shard_map/while
  194.5 4.7 %copy-start.6 = (f32[2,4,64,256]{3,2,1,0:T(8,128)S(1)}, f32[2,4,64,256]{3,2,1,0:T(8,128)}, u32[]{:S(2)}) copy-start(f32[2,4,64,256]{3,2,1,0:T(8,128)} %get-tuple-element.664) | copy-start | bytes 1572868 | tf_op jit(solution)/shard_map/while
  194.5 5.4 %copy-start.16 = (bf16[2,4,64,128]{3,2,1,0:T(8,128)(2,1)S(1)}, bf16[2,4,64,128]{3,2,1,0:T(8,128)(2,1)}, u32[]{:S(2)}) copy-start(bf16[2,4,64,128]{3,2,1,0:T(8,128)(2,1)} %get-tuple-element.649) | copy-start | bytes 393220 | tf_op jit(solution)/shard_map/while
  200.6 1.1 copy-start.17
  207.3 0.7 copy-start.26
  207.3 24.2 %copy-start.20 = (bf16[320,512]{1,0:T(8,128)(2,1)S(1)}, bf16[320,512]{1,0:T(8,128)(2,1)}, u32[]{:S(2)}) copy-start(bf16[320,512]{1,0:T(8,128)(2,1)} %copy-done.19) | copy-start | bytes 983044
  231.5 4.0 %copy-start.14 = (bf16[320,512]{1,0:T(8,128)(2,1)S(1)}, bf16[320,512]{1,0:T(8,128)(2,1)}, u32[]{:S(2)}) copy-start(bf16[320,512]{1,0:T(8,128)(2,1)} %copy-done.13) | copy-start | bytes 983044
  235.5 4.0 %copy-start.28 = (f32[320,512]{1,0:T(8,128)S(1)}, f32[320,512]{1,0:T(8,128)}, u32[]{:S(2)}) copy-start(f32[320,512]{1,0:T(8,128)} %copy-done.27) | copy-start | bytes 1966084
  235.5 4.0 %copy-start.29 = (f32[320,512]{1,0:T(8,128)S(1)}, f32[320,512]{1,0:T(8,128)}, u32[]{:S(2)}) copy-start(f32[320,512]{1,0:T(8,128)} %fusion.76) | copy-start | bytes 1966084
  239.5 4.0 %copy-start.18 = (bf16[2,4,64,128]{3,2,1,0:T(8,128)(2,1)S(1)}, bf16[2,4,64,128]{3,2,1,0:T(8,128)(2,1)}, u32[]{:S(2)}) copy-start(bf16[2,4,64,128]{3,2,1,0:T(8,128)(2,1)} %get-tuple-element.320) | copy-start | bytes 393220
  244.2 9.7 %copy-start.5 = (f32[2,4,64,256]{3,2,1,0:T(8,128)S(1)}, f32[2,4,64,256]{3,2,1,0:T(8,128)}, u32[]{:S(2)}) copy-start(f32[2,4,64,256]{3,2,1,0:T(8,128)} %get-tuple-element.726) | copy-start | bytes 1572868
  253.9 4.1 %copy-start.7 = (f32[2,4,64,256]{3,2,1,0:T(8,128)S(1)}, f32[2,4,64,256]{3,2,1,0:T(8,128)}, u32[]{:S(2)}) copy-start(f32[2,4,64,256]{3,2,1,0:T(8,128)} %get-tuple-element.719) | copy-start | bytes 1572868 | tf_op jit(solution)/shard_map/while
  253.9 4.5 %copy-start.8 = (f32[2,4,64,128]{3,2,1,0:T(8,128)S(1)}, f32[2,4,64,128]{3,2,1,0:T(8,128)}, u32[]{:S(2)}) copy-start(f32[2,4,64,128]{3,2,1,0:T(8,128)} %get-tuple-element.718) | copy-start | bytes 786436 | tf_op jit(solution)/shard_map/while
  253.9 4.9 %copy-start.11 = (f32[2,4,64,128]{3,2,1,0:T(8,128)S(1)}, f32[2,4,64,128]{3,2,1,0:T(8,128)}, u32[]{:S(2)}) copy-start(f32[2,4,64,128]{3,2,1,0:T(8,128)} %get-tuple-element.705) | copy-start | bytes 786436 | tf_op jit(solution)/shard_map/while
  259.6 0.7 copy-start.12
  261.1 4.2 %copy-start.7 = (f32[2,4,64,256]{3,2,1,0:T(8,128)S(1)}, f32[2,4,64,256]{3,2,1,0:T(8,128)}, u32[]{:S(2)}) copy-start(f32[2,4,64,256]{3,2,1,0:T(8,128)} %get-tuple-element.719) | copy-start | bytes 1572868 | tf_op jit(solution)/shard_map/while
  261.1 4.6 %copy-start.8 = (f32[2,4,64,128]{3,2,1,0:T(8,128)S(1)}, f32[2,4,64,128]{3,2,1,0:T(8,128)}, u32[]{:S(2)}) copy-start(f32[2,4,64,128]{3,2,1,0:T(8,128)} %get-tuple-element.718) | copy-start | bytes 786436 | tf_op jit(solution)/shard_map/while
  261.1 5.0 %copy-start.11 = (f32[2,4,64,128]{3,2,1,0:T(8,128)S(1)}, f32[2,4,64,128]{3,2,1,0:T(8,128)}, u32[]{:S(2)}) copy-start(f32[2,4,64,128]{3,2,1,0:T(8,128)} %get-tuple-element.705) | copy-start | bytes 786436 | tf_op jit(solution)/shard_map/while
  266.8 0.7 copy-start.12
Sparse Core Ops, SparseCore 0:
  151.0 15.5 all-gather.4
  185.3 49.9 all-gather.6
  238.9 86.7 reduce-scatter.1
where the time goes:
time: 336 us; the launch traced here: 334 us
  waiting for transfers between devices  113 us (34%)
  matrix products  58.2 us (17%)
  blocking collectives  56.3 us (17%)
  local copies, waits for them, and re-layouts  45.8 us (14%)
  other arithmetic  33.1 us (10%)
  between operations  14.8 us (4%)
  starting transfers between devices  11.9 us (4%)
    reduce_scatter x1, waiting for transfers between devices, body(): lax.psum_scatter(lax.dot_general(mixed_grad, mixed_flat, (((0,), (0,)), (...  54.1 us
    all_to_all x1, waiting for transfers between devices, body(): lax.all_to_all(send_grad, 'sp', split_axis=0, concat_axis=1, tiled=True)  25.3 us
    all_to_all x1, waiting for transfers between devices, body(): lax.all_to_all(send_rows, 'sp', split_axis=0, concat_axis=1, tiled=True)  23 us
    unnamed x1, blocking collectives  21.8 us
    all_to_all x1, blocking collectives, body(): lax.all_to_all(grouped, 'tp', split_axis=2, concat_axis=2, tiled=True)  20.4 us
    all_to_all x1, blocking collectives, body(): lax.all_to_all(feature_part, 'sp', split_axis=1, concat_axis=0, tiled=True)  14.1 us
    all_gather x1, waiting for transfers between devices, body(): returned = lax.all_gather(returned_part, 'tp', axis=2, tiled=True)  11 us
    unnamed x53, local copies, waits for them, and re-layouts  8.41 us
  transfers between devices with their start and end apart: 5, of which 4 were waited for; matrix products, arithmetic and copies ran while one was open for 24% of the time, Pallas kernels for 0%

commit v1 on v0

v1 whole, which is shorter than its diff:
```python
import functools

import jax
import jax.numpy as jnp
from jax import lax
from jax.experimental import pallas as pl
from jax.experimental.pallas import tpu as pltpu
from jax.sharding import PartitionSpec as P

F32 = jnp.float32
BF16 = jnp.bfloat16
EXACT = lax.Precision.HIGHEST


def dot(a, b, ca=1, cb=0, precision=None):
    return lax.dot_general(
        a, b, (((ca,), (cb,)), ((), ())), preferred_element_type=F32, precision=precision
    )


def iota(shape, axis):
    return lax.broadcasted_iota(jnp.int32, shape, axis)


def dispatch_kernel(core, routes, weight, x, g, rows, grads, place, *, experts, cap):
    tokens = routes.shape[0]
    slots = experts * cap
    expert = iota((tokens, experts), 1)
    first = routes[:, 0:1] == expert
    second = routes[:, 1:2] == expert
    named = jnp.where(first | second, 1.0, 0.0)
    share = jnp.where(first, weight[:, 0:1], 0.0) + jnp.where(second, weight[:, 1:2], 0.0)
    before = jnp.where(iota((tokens, tokens), 0) < iota((tokens, tokens), 1), 1.0, 0.0)
    same = jnp.where(iota((tokens, tokens), 0) == iota((tokens, tokens), 1), 1.0, 0.0)
    rank_t = dot(named.astype(BF16), before.astype(BF16), 0, 0)
    named_t = dot(named.astype(BF16), same.astype(BF16), 0, 0)
    slot = iota((slots, experts), 0)
    base = iota((slots, experts), 1) * cap
    owner = (slot >= base) & (slot < base + cap)
    owner_f = jnp.where(owner, 1.0, 0.0).astype(BF16)
    number = jnp.sum(jnp.where(owner, slot - base, 0).astype(F32), axis=1, keepdims=True)
    rank = dot(owner_f, rank_t.astype(BF16))
    hit = dot(owner_f, named_t.astype(BF16))
    picked = jnp.where((rank == number) & (hit > 0.5), 1.0, 0.0)
    picked_b = picked.astype(BF16)
    share_slot = jnp.sum(
        jnp.where(owner, dot(picked, share, precision=EXACT), 0.0), axis=1, keepdims=True
    )
    place[...] = picked_b
    rows[...] = dot(picked_b, x[...]).astype(BF16)
    grads[...] = (share_slot * dot(picked_b, g[...])).astype(BF16)


def dispatch(core, routes, weight, x, g, experts, cap):
    tokens, width = x.shape
    half = width // 2
    slots = experts * cap
    whole = lambda i, c: (0, 0)
    return pl.pallas_call(
        functools.partial(dispatch_kernel, experts=experts, cap=cap),
        grid_spec=pltpu.PrefetchScalarGridSpec(
            num_scalar_prefetch=1,
            grid=(1,),
            in_specs=[
                pl.BlockSpec(routes.shape, whole),
                pl.BlockSpec(weight.shape, whole),
                pl.BlockSpec((tokens, half), lambda i, c: (0, c[0])),
                pl.BlockSpec((tokens, half), lambda i, c: (0, c[0])),
            ],
            out_specs=[
                pl.BlockSpec((slots, half), whole),
                pl.BlockSpec((slots, half), whole),
                pl.BlockSpec((slots, tokens), whole),
            ],
        ),
        out_shape=[
            jax.ShapeDtypeStruct((slots, half), BF16),
            jax.ShapeDtypeStruct((slots, half), BF16),
            jax.ShapeDtypeStruct((slots, tokens), BF16),
        ],
        name="dispatch",
    )(core, routes, weight, x, g)


def expert_kernel(
    core, ra, rb, ga, gb, wga, wgb, wua, wub, wda, wdb, hidden, gback, uback, pa, pb, acca, accb
):
    step = pl.program_id(0)
    gate = dot(ra[...], wga[...]) + dot(rb[...], wgb[...])
    up = dot(ra[...], wua[...]) + dot(rb[...], wub[...])
    back = dot(ga[...], wda[...], 1, 1) + dot(gb[...], wdb[...], 1, 1)
    sig = 1.0 / (1.0 + jnp.exp(-gate))
    active = gate * sig
    hidden[...] = (active * up).astype(BF16)
    gb_v = (back * up * (sig * (1.0 + gate * (1.0 - sig)))).astype(BF16)
    ub_v = (back * active).astype(BF16)
    gback[...] = gb_v
    uback[...] = ub_v
    part_a = dot(gb_v, wga[...], 1, 1) + dot(ub_v, wua[...], 1, 1)
    part_b = dot(gb_v, wgb[...], 1, 1) + dot(ub_v, wub[...], 1, 1)

    @pl.when(step == 0)
    def _():
        acca[...] = part_a
        accb[...] = part_b

    @pl.when(step > 0)
    def _():
        acca[...] += part_a
        accb[...] += part_b

    @pl.when(step == pl.num_programs(0) - 1)
    def _():
        pa[...] = acca[...].astype(BF16)
        pb[...] = accb[...].astype(BF16)


def expert_back(core, ra, rb, ga, gb, w_gate, w_up, w_down):
    rows, half = ra.shape
    units = w_gate.shape[2]
    chunk = min(units, 256)
    whole = lambda f, c: (0, 0)
    mine = pl.BlockSpec((None, half, chunk), lambda f, c: (0, c[0], f))
    other = pl.BlockSpec((None, half, chunk), lambda f, c: (0, 1 - c[0], f))
    mine_d = pl.BlockSpec((None, chunk, half), lambda f, c: (0, f, c[0]))
    other_d = pl.BlockSpec((None, chunk, half), lambda f, c: (0, f, 1 - c[0]))
    full = pl.BlockSpec((rows, half), whole)
    part = pl.BlockSpec((rows, chunk), lambda f, c: (0, f))
    return pl.pallas_call(
        expert_kernel,
        grid_spec=pltpu.PrefetchScalarGridSpec(
            num_scalar_prefetch=1,
            grid=(units // chunk,),
            in_specs=[full] * 4 + [mine, other, mine, other, mine_d, other_d],
            out_specs=[part, part, part, full, full],
            scratch_shapes=[pltpu.VMEM((rows, half), F32), pltpu.VMEM((rows, half), F32)],
        ),
        out_shape=[jax.ShapeDtypeStruct((rows, units), BF16)] * 3
        + [jax.ShapeDtypeStruct((rows, half), BF16)] * 2,
        name="expert",
    )(core, ra, rb, ga, gb, w_gate, w_gate, w_up, w_up, w_down, w_down)


def weights_kernel(core, ra, rb, ga, gb, hidden, gback, uback, gate_out, up_out, down_out):
    step = pl.program_id(0)
    turn = pl.num_programs(0) // 2

    def write(r, g):
        gate_out[...] = dot(r[...], gback[...], 0, 0).astype(BF16)
        up_out[...] = dot(r[...], uback[...], 0, 0).astype(BF16)
        down_out[...] = dot(hidden[...], g[...], 0, 0).astype(BF16)

    @pl.when(step < turn)
    def _():
        write(ra, ga)

    @pl.when(step >= turn)
    def _():
        write(rb, gb)


def weight_grads(core, ra, rb, ga, gb, hidden, gback, uback):
    rows, half = ra.shape
    units = hidden.shape[1]
    chunk = min(half, 512)
    turn = half // chunk
    whole = lambda i, c: (0, 0)
    left = pl.BlockSpec((rows, chunk), lambda i, c: (0, jnp.minimum(i, turn - 1)))
    right = pl.BlockSpec((rows, chunk), lambda i, c: (0, jnp.maximum(i - turn, 0)))
    at = lambda i, c: jnp.where(i < turn, c[0] * turn + i, (1 - c[0]) * turn + i - turn)
    full = pl.BlockSpec((rows, units), whole)
    tall = pl.BlockSpec((None, chunk, units), lambda i, c: (0, at(i, c), 0))
    wide = pl.BlockSpec((None, units, chunk), lambda i, c: (0, 0, at(i, c)))
    return pl.pallas_call(
        weights_kernel,
        grid_spec=pltpu.PrefetchScalarGridSpec(
            num_scalar_prefetch=1,
            grid=(2 * turn,),
            in_specs=[left, right, left, right, full, full, full],
            out_specs=[tall, tall, wide],
        ),
        out_shape=[
            jax.ShapeDtypeStruct((1, 2 * half, units), BF16),
            jax.ShapeDtypeStruct((1, 2 * half, units), BF16),
            jax.ShapeDtypeStruct((1, units, 2 * half), BF16),
        ],
        name="weight_grads",
    )(core, ra, rb, ga, gb, hidden, gback, uback)


def combine_kernel(place, back, out):
    out[...] = dot(place[...], back[...], 0, 0).astype(BF16)


def combine(place, back):
    return pl.pallas_call(
        combine_kernel,
        out_shape=jax.ShapeDtypeStruct((place.shape[1], back.shape[1]), BF16),
        name="combine",
    )(place, back)


def decays(log_decay, head):
    span = log_decay.shape[-1]
    row = iota((span, span), 0)
    col = iota((span, span), 1)
    keep = row >= col
    lower = jnp.where(keep, 1.0, 0.0)
    own = log_decay[head : head + 1, :]
    down = jnp.sum(lower * own, axis=1, keepdims=True)
    across = jnp.sum(jnp.where(row <= col, 1.0, 0.0) * jnp.sum(
        jnp.where(row == col, own, 0.0), axis=1, keepdims=True), axis=0, keepdims=True)
    total = jnp.sum(own, axis=1, keepdims=True)
    table = jnp.where(keep, jnp.exp(jnp.where(keep, down - across, 0.0)), 0.0)
    return table, jnp.exp(down), jnp.exp(total - down), total


def mixed_kernel(q, k, v, log_decay, state, mixed, totals):
    heads, span, size = q.shape
    width = v.shape[2]
    scale = size**-0.5
    for h in range(heads):
        table, lead, _, total = decays(log_decay[...], h)
        scores = (dot(q[h], k[h], 1, 1) * (scale * table)).astype(BF16)
        out = dot(scores, v[h]) + lead * dot(q[h], state[h, 0].astype(BF16))
        mixed[:, h * width : (h + 1) * width] = out.astype(BF16)
        totals[h : h + 1, :] = jnp.broadcast_to(total, (1, totals.shape[1]))


def mixed_heads(q, k, v, log_decay, state):
    heads, span, _ = q.shape
    return pl.pallas_call(
        mixed_kernel,
        out_shape=[
            jax.ShapeDtypeStruct((span, heads * v.shape[2]), BF16),
            jax.ShapeDtypeStruct((heads, 128), F32),
        ],
        name="mixed_heads",
    )(q, k, v, log_decay, state)


def carry_kernel(core, ma, mb, wa, wb, q, log_decay, hg, carried, slices, *, groups):
    head = pl.program_id(0)
    h_grad = (dot(ma[...], wa[...]) + dot(mb[...], wb[...])).astype(BF16)
    hg[...] = h_grad
    span = log_decay.shape[-1]
    lower = jnp.where(iota((span, span), 0) >= iota((span, span), 1), 1.0, 0.0)
    lead = jnp.exp(jnp.sum(lower * log_decay[pl.ds(head, 1), :], axis=1, keepdims=True))
    carried[...] = dot((q[...].astype(F32) * lead).astype(BF16), h_grad, 0, 0).astype(BF16)

    @pl.when(head == 0)
    def _():
        size = slices.shape[2]
        turn = groups // 2
        for i in range(turn):
            slices[core[0] * turn + i] = ma[:, i * size : (i + 1) * size]
            slices[(1 - core[0]) * turn + i] = mb[:, i * size : (i + 1) * size]


def carry(core, ma, mb, w_out, q, log_decay, groups, value_size):
    span, half = ma.shape
    heads, _, size = q.shape
    whole = lambda h, c: (0, 0)
    by_head = lambda h, c: (h, 0, 0)
    return pl.pallas_call(
        functools.partial(carry_kernel, groups=groups),
        grid_spec=pltpu.PrefetchScalarGridSpec(
            num_scalar_prefetch=1,
            grid=(heads,),
            in_specs=[
                pl.BlockSpec((span, half), whole),
                pl.BlockSpec((span, half), whole),
                pl.BlockSpec((half, value_size), lambda h, c: (c[0], h)),
                pl.BlockSpec((half, value_size), lambda h, c: (1 - c[0], h)),
                pl.BlockSpec((None, span, size), by_head),
                pl.BlockSpec(log_decay.shape, whole),
            ],
            out_specs=[
                pl.BlockSpec((None, span, value_size), by_head),
                pl.BlockSpec((None, size, value_size), by_head),
                pl.BlockSpec((groups, span, 2 * half // groups), lambda h, c: (0, 0, 0)),
            ],
        ),
        out_shape=[
            jax.ShapeDtypeStruct((heads, span, value_size), BF16),
            jax.ShapeDtypeStruct((heads, size, value_size), BF16),
            jax.ShapeDtypeStruct((groups, span, 2 * half // groups), BF16),
        ],
        name="carry",
    )(core, ma, mb, w_out, w_out, q, log_decay)


def local_kernel(q, k, v, log_decay, state, hg, q_grad, k_part, v_part):
    heads, span, size = q.shape
    scale = size**-0.5
    for h in range(heads):
        table, lead, _, _ = decays(log_decay[...], h)
        scores = (dot(q[h], k[h], 1, 1) * (scale * table)).astype(BF16)
        back = (dot(hg[h], v[h], 1, 1) * table).astype(BF16)
        from_state = dot(hg[h], state[h, 0].astype(BF16), 1, 1)
        q_grad[h] = (scale * dot(back, k[h]) + lead * from_state).astype(BF16)
        k_part[h] = dot(back, q[h], 0, 0)
        v_part[h] = dot(scores, hg[h], 0, 0)


def local_grads(q, k, v, log_decay, state, hg):
    return pl.pallas_call(
        local_kernel,
        out_shape=[
            jax.ShapeDtypeStruct(q.shape, BF16),
            jax.ShapeDtypeStruct(k.shape, F32),
            jax.ShapeDtypeStruct(v.shape, F32),
        ],
        name="local_grads",
    )(q, k, v, log_decay, state, hg)


def final_kernel(k, v, log_decay, later, last, factor, k_part, v_part, k_grad, v_grad):
    heads, span, size = k.shape
    scale = size**-0.5
    for h in range(heads):
        _, _, trail, _ = decays(log_decay[...], h)
        state = (later[h] + factor[h : h + 1, 0:1] * last[h].astype(F32)).astype(BF16)
        k_grad[h] = (scale * (k_part[h] + trail * dot(v[h], state, 1, 1))).astype(BF16)
        v_grad[h] = (v_part[h] + (scale * trail) * dot(k[h], state)).astype(BF16)


def final_grads(k, v, log_decay, later, last, factor, k_part, v_part):
    return pl.pallas_call(
        final_kernel,
        out_shape=[jax.ShapeDtypeStruct(k.shape, BF16), jax.ShapeDtypeStruct(v.shape, BF16)],
        name="final_grads",
    )(k, v, log_decay, later, last, factor, k_part, v_part)


def project_kernel(order, x, y, out):
    part = dot(x[...], y[...], 0, 0)

    @pl.when(pl.program_id(0) == 0)
    def _():
        out[...] = part

    @pl.when(pl.program_id(0) > 0)
    def _():
        out[...] += part


def project(order, x, y):
    groups, span, size = x.shape
    width = y.shape[2]
    return pl.pallas_call(
        project_kernel,
        grid_spec=pltpu.PrefetchScalarGridSpec(
            num_scalar_prefetch=1,
            grid=(groups,),
            in_specs=[
                pl.BlockSpec((None, span, size), lambda i, o: (o[i], 0, 0)),
                pl.BlockSpec((None, span, width), lambda i, o: (i, 0, 0)),
            ],
            out_specs=pl.BlockSpec((size, width), lambda i, o: (0, 0)),
        ),
        out_shape=jax.ShapeDtypeStruct((size, width), F32),
        name="project",
    )(order, x, y)


def swap(a, axis, bit):
    count = lax.axis_size(axis)
    return lax.ppermute(a, axis, [(i, i ^ bit) for i in range(count)])


def bits_of(count):
    return [1 << i for i in range(count.bit_length() - 1)]


def join_factors(totals, place, count):
    spans = jnp.arange(count)
    rows = []
    for bit in bits_of(count):
        start = (place // bit) * bit
        rows.append((spans > place) & (spans < start + bit))
        rows.append((spans >= start) & (spans < start + bit))
        other = start ^ bit
        rows.append((spans >= other) & (spans < other + bit))
    sums = jnp.dot(jnp.stack(rows).astype(F32), totals, precision=EXACT)
    scales = jnp.exp(sums)
    out = []
    for n, bit in enumerate(bits_of(count)):
        low = (place & bit) == 0
        one = jnp.ones_like(scales[0])
        out.append((
            jnp.where(low, scales[3 * n], 0.0),
            jnp.where(low, one, scales[3 * n + 2]),
            jnp.where(low, scales[3 * n + 1], one),
        ))
    return out


def body(
    moe_input,
    out_grad,
    routes,
    route_weight,
    w_gate,
    w_up,
    w_down,
    w_out,
    query_heads,
    key_heads,
    value_heads,
    log_decay,
    state_in,
):
    tokens, width = moe_input.shape
    half = width // 2
    sp = lax.axis_size("sp")
    tp = lax.axis_size("tp")
    place = lax.axis_index("sp")
    core = lax.axis_index("tp") & 1
    core_at = core.reshape(1).astype(jnp.int32)
    experts = w_gate.shape[0] * sp
    cap = 5 * tokens * routes.shape[1] // (4 * experts)
    value_size = value_heads.shape[-1]

    rows, grads, picked = dispatch(
        core_at, routes, route_weight, moe_input, out_grad, experts, cap
    )
    mixed, totals = mixed_heads(query_heads, key_heads, value_heads, log_decay, state_in)
    span_totals = lax.all_gather(totals[:, 0], "sp")
    factors = join_factors(span_totals, place, sp)

    def exchange(a):
        a = a.reshape(experts, cap, half)
        return lax.all_to_all(a, "sp", split_axis=0, concat_axis=0, tiled=True).reshape(-1, half)

    rows_a = exchange(rows)
    grads_a = exchange(grads)
    rows_b = swap(rows_a, "tp", 1)
    grads_b = swap(grads_a, "tp", 1)

    hidden, gate_back, up_back, part_a, part_b = expert_back(
        core_at, rows_a, rows_b, grads_a, grads_b, w_gate, w_up, w_down
    )
    part = (part_a.astype(F32) + swap(part_b, "tp", 1).astype(F32)).astype(BF16)
    gate_grad, up_grad, down_grad = weight_grads(
        core_at, rows_a, rows_b, grads_a, grads_b, hidden, gate_back, up_back
    )

    mixed, rows_b2 = lax.optimization_barrier((mixed, rows_b))
    gathered = mixed[None]
    for bit in reversed(bits_of(sp)):
        gathered = jnp.concatenate([gathered, swap(gathered, "sp", bit)], axis=0)

    returned = exchange(part)
    token_part = combine(picked, returned)
    for bit in bits_of(tp)[1:]:
        token_part = token_part.astype(F32) + swap(token_part, "tp", bit).astype(F32)
        if bit * 2 < tp:
            token_part = token_part.astype(BF16)
    own_grad = lax.dynamic_slice_in_dim(out_grad, core * half, half, axis=1)
    mixed_a = (own_grad.astype(F32) + token_part.astype(F32)).astype(BF16)
    mixed_b = swap(mixed_a, "tp", 1)

    head_grad, carried, slices = carry(
        core_at, mixed_a, mixed_b, w_out, query_heads, log_decay, sp, value_size
    )
    q_grad, k_part, v_part = local_grads(
        query_heads, key_heads, value_heads, log_decay, state_in, head_grad
    )
    later = jnp.zeros(carried.shape, F32)
    whole = carried
    for n, bit in enumerate(bits_of(sp)):
        came = swap(whole, "sp", bit)
        f_later, f_own, f_came = factors[n]
        if bit * 2 < sp:
            later = later + f_later[:, None, None] * came.astype(F32)
            whole = (
                f_own[:, None, None] * whole.astype(F32) + f_came[:, None, None] * came.astype(F32)
            ).astype(BF16)
    k_grad, v_grad = final_grads(
        key_heads, value_heads, log_decay, later, came,
        jnp.broadcast_to(factors[-1][0][:, None], (factors[-1][0].shape[0], 128)),
        k_part, v_part,
    )
    slices = lax.all_to_all(slices, "sp", split_axis=0, concat_axis=0, tiled=True)
    offsets = [0]
    for bit in reversed(bits_of(sp)):
        offsets = offsets + [o ^ bit for o in offsets]
    order = (place ^ jnp.array(offsets, jnp.int32)).astype(jnp.int32)
    out_proj_grad = project(order, slices, gathered)
    return gate_grad, up_grad, down_grad, out_proj_grad, q_grad, k_grad, v_grad


def solution(mesh):
    return jax.shard_map(
        body,
        mesh=mesh,
        in_specs=(
            P("sp", None),
            P("sp", None),
            P("sp", None),
            P("sp", None),
            P("sp", None, "tp"),
            P("sp", None, "tp"),
            P("sp", "tp", None),
            P(None, "tp"),
            P("tp", "sp", None),
            P("tp", "sp", None),
            P("tp", "sp", None),
            P("tp", "sp"),
            P("tp", "sp", None, None),
        ),
        out_specs=(
            P("sp", None, "tp"),
            P("sp", None, "tp"),
            P("sp", "tp", None),
            P("sp", "tp"),
            P("tp", "sp", None),
            P("tp", "sp", None),
            P("tp", "sp", None),
        ),
        check_vma=False,
    )
```

time: 336 us -> 188 us (0.56)
  matrix products: 58.2 us -> 0.18 us
  waiting for transfers between devices: 113 us -> 58.5 us
  Pallas kernels: 0 us -> 44.2 us
  local copies, waits for them, and re-layouts: 45.8 us -> 9.23 us
  other arithmetic: 33.1 us -> 10.2 us
  between operations: 14.8 us -> 1.53 us
  blocking collectives: 56.3 us -> 45.2 us
  starting transfers between devices: 11.9 us -> 17.9 us
    dot_general x39 -> x1, matrix products: 58.2 us -> 0.18 us  [join_factors(): sums = jnp.dot(jnp.stack(rows).astype(F32), totals, precision=EXACT)]
    reduce_scatter x1 -> x0, waiting for transfers between devices: 54.1 us -> none  [body(): lax.psum_scatter(lax.dot_general(mixed_grad, mixed_flat, (((0,), (0,)), (...]
    pallas_call x0 -> x9, Pallas kernels: none -> 44.2 us  [the longest x1 10.1 us: expert_back(): pl.pallas_call(expert_kernel, grid_spec=pltpu.PrefetchScalarGridSpec(num_...]
    ppermute x0 -> x11, waiting for transfers between devices: none -> 22.8 us  [swap(): return lax.ppermute(a, axis, [(i, i ^ bit) for i in range(count)])]
    gather x4 -> x0, local copies, waits for them, and re-layouts: 13.3 us -> none  [the longest x1 4.82 us: body(): returned.reshape(experts * capacity, model_width)[target]]
    all_to_all x2 -> x3, waiting for transfers between devices: 48.3 us -> 35.6 us  [the longest x2 35.6 us: exchange(): lax.all_to_all(a, 'sp', split_axis=0, concat_axis=0, tiled=True)]
    all_gather x2 -> x0, waiting for transfers between devices: 11 us -> none  [the longest x1 11 us: body(): returned = lax.all_gather(returned_part, 'tp', axis=2, tiled=True)]
    all_to_all x2 -> x1, blocking collectives: 34.5 us -> 24.9 us  [exchange(): lax.all_to_all(a, 'sp', split_axis=0, concat_axis=0, tiled=True)]
  transfers between devices with their start and end apart: 5 -> 14, of which waited for: 4 -> 8; matrix products, arithmetic and copies ran while one was open for 24% -> 6% of each run, Pallas kernels for 0% -> 12%
where the time goes in v1:
time: 188 us; the launch traced here: 187 us
  waiting for transfers between devices  58.5 us (31%)
  blocking collectives  45.2 us (24%)
  Pallas kernels  44.2 us (24%)
  starting transfers between devices  17.9 us (10%)
  other arithmetic  10.2 us (5%)
  local copies, waits for them, and re-layouts  9.23 us (5%)
    all_to_all x2, waiting for transfers between devices, exchange(): lax.all_to_all(a, 'sp', split_axis=0, concat_axis=0, tiled=True)  35.6 us
    all_to_all x1, blocking collectives, exchange(): lax.all_to_all(a, 'sp', split_axis=0, concat_axis=0, tiled=True)  24.9 us
    ppermute x11, waiting for transfers between devices, swap(): return lax.ppermute(a, axis, [(i, i ^ bit) for i in range(count)])  22.8 us
    unnamed x1, blocking collectives  20.3 us
    pallas_call x1, Pallas kernels, expert_back(): pl.pallas_call(expert_kernel, grid_spec=pltpu.PrefetchScalarGridSpec(num_...  10.1 us
    pallas_call x1, Pallas kernels, project(): pl.pallas_call(project_kernel, grid_spec=pltpu.PrefetchScalarGridSpec(num...  7.75 us
    unnamed x35, local copies, waits for them, and re-layouts  7.63 us
    pallas_call x1, Pallas kernels, weight_grads(): pl.pallas_call(weights_kernel, grid_spec=pltpu.PrefetchScalarGridSpec(num...  7.46 us
  transfers between devices with their start and end apart: 14, of which 8 were waited for; matrix products, arithmetic and copies ran while one was open for 6% of the time, Pallas kernels for 12%

profile of v1, /device:TPU:0, one launch (start us, length us, event | category | flops | bytes accessed | tf_op | source)
XLA Modules:
  0.0 186.9 jit_solution(9979861368661206360)
XLA Ops:
  0.6 1.4 copy.23.routes
  2.0 1.4 copy.24.weight
  3.5 3.0 %dispatch.1 = (bf16[320,1024]{1,0:T(8,128)(2,1)}, bf16[320,1024]{1,0:T(8,128)(2,1)}, bf16[320,128]{1,0:T(8,128)(2,1)}) custom-call(s32[1]{0:T(128)} %bitcast.core, s32[128,2]{1,0:T(8,128)} %copy.23.routes, f32[128,2]{1,0:T(8,128)} %copy.24.weight, bf16[128,2048]{1,0:T(8,128)(2,1)} %x.2, bf16[128,2048]{1,0:T(8,128)(2,1)} %g.1), custom_call_target="tpu_custom_call" | custom-call | tf_op jit(solution)/shard_map/dispatch/pallas_call | solution.py:59
  6.5 24.9 %all_to_all.20 = bf16[8,40,1024]{2,1,0:T(8,128)(2,1)S(1)} all-to-all(bf16[8,40,1024]{2,1,0:T(8,128)(2,1)} %bitcast.23), channel_id=1, replica_groups=mesh['sp'=8,'tp'=4] {'sp'}, dimensions={0} | all-to-all | bytes 1310720 | tf_op jit(solution)/shard_map/all_to_all | solution.py:434
  31.4 3.5 %all-to-all-start.1 = ((bf16[8,40,1024]{2,1,0:T(8,128)(2,1)}), bf16[8,40,1024]{2,1,0:T(8,128)(2,1)S(1)}, u32[]{:S(2)}, u32[]{:S(2)}) async-start(bf16[8,40,1024]{2,1,0:T(8,128)(2,1)} %bitcast.22), calls=%async_computation.1 | async-start | bytes 1310720 | tf_op jit(solution)/shard_map/all_to_all | solution.py:434
  35.1 16.8 %all-to-all-done.1 = bf16[8,40,1024]{2,1,0:T(8,128)(2,1)S(1)} async-done(((bf16[8,40,1024]{2,1,0:T(8,128)(2,1)}), bf16[8,40,1024]{2,1,0:T(8,128)(2,1)S(1)}, u32[]{:S(2)}, u32[]{:S(2)}) %all-to-all-start.1) | async-done | bytes 655392 | tf_op jit(solution)/shard_map/all_to_all | solution.py:434
  51.8 2.1 %collective-permute-done.1.gb = bf16[320,1024]{1,0:T(8,128)(2,1)S(1)} collective-permute-done((bf16[320,1024]{1,0:T(8,128)(2,1)S(1)}, bf16[320,1024]{1,0:T(8,128)(2,1)S(1)}, u32[]{:S(2)}, u32[]{:S(2)}) %collective-permute-start.1) | collective-permute-done | bytes 655392 | tf_op jit(solution)/shard_map/ppermute | solution.py:369
  53.9 0.8 copy-done.3
  54.8 10.1 %expert.1 = (bf16[320,512]{1,0:T(8,128)(2,1)}, bf16[320,512]{1,0:T(8,128)(2,1)}, bf16[320,512]{1,0:T(8,128)(2,1)}, bf16[320,1024]{1,0:T(8,128)(2,1)}, bf16[320,1024]{1,0:T(8,128)(2,1)}) custom-call(s32[1]{0:T(128)} %bitcast.core, bf16[320,1024]{1,0:T(8,128)(2,1)} %bitcast.12, bf16[320,1024]{1,0:T(8,128)(2,1)} %copy-done.2, bf16[320,1024]{1,0:T(8,128)(2,1)} %bitcast.15, ...), custom_call_target="tpu_custom_call" | custom-call | tf_op jit(solution)/shard_map/expert/pallas_call | solution.py:129
  64.9 0.2 collective-permute-start.2
  65.1 2.2 %collective-permute-done.2 = bf16[320,1024]{1,0:T(8,128)(2,1)S(1)} collective-permute-done((bf16[320,1024]{1,0:T(8,128)(2,1)}, bf16[320,1024]{1,0:T(8,128)(2,1)S(1)}, u32[]{:S(2)}, u32[]{:S(2)}) %collective-permute-start.2) | collective-permute-done | bytes 655392 | tf_op jit(solution)/shard_map/ppermute | solution.py:369
  67.3 2.2 %add_convert_fusion = bf16[320,1024]{1,0:T(8,128)(2,1)} fusion(bf16[320,1024]{1,0:T(8,128)(2,1)S(1)} %collective-permute-done.2, bf16[320,1024]{1,0:T(8,128)(2,1)} %get-tuple-element.38), kind=kLoop, calls=%fused_computation.1 | loop fusion | flops 1310720 | bytes 1966080 | tf_op jit(solution)/shard_map/convert_element_type | solution.py:444
  69.4 3.8 %all-to-all-start.2 = ((bf16[8,40,1024]{2,1,0:T(8,128)(2,1)}), bf16[8,40,1024]{2,1,0:T(8,128)(2,1)S(1)}, u32[]{:S(2)}, u32[]{:S(2)}) async-start(bf16[8,40,1024]{2,1,0:T(8,128)(2,1)} %bitcast.5), calls=%async_computation.2 | async-start | bytes 1310720 | tf_op jit(solution)/shard_map/all_to_all | solution.py:434
  73.2 2.5 %mixed_heads.1 = (bf16[128,1024]{1,0:T(8,128)(2,1)}, f32[4,128]{1,0:T(4,128)}) custom-call(bf16[4,128,128]{2,1,0:T(8,128)(2,1)} %q.5, bf16[4,128,128]{2,1,0:T(8,128)(2,1)} %k.5, bf16[4,128,256]{2,1,0:T(8,128)(2,1)} %v.5, f32[4,128]{1,0:T(4,128)} %log_decay.7, f32[4,1,128,256]{3,2,1,0:T(8,128)} %state.3), custom_call_target="tpu_custom_call" | custom-call | tf_op jit(solution)/shard_map/mixed_heads/pallas_call | solution.py:232
  75.7 2.9 %collective-permute-start.5 = (bf16[1,128,1024]{2,1,0:T(8,128)(2,1)}, bf16[1,128,1024]{2,1,0:T(8,128)(2,1)S(1)}, u32[]{:S(2)}, u32[]{:S(2)}) collective-permute-start(bf16[1,128,1024]{2,1,0:T(8,128)(2,1)} %bitcast.18), channel_id=1, source_target_pairs={{0,16},{4,20},{8,24},{12,28},{16,0},{20,4},{24,8},{28,12},{1,17},{... | collective-permute-start | bytes 786440 | tf_op jit(solution)/shard_map/ppermute | solution.py:369
  78.6 18.9 %all-to-all-done.2 = bf16[8,40,1024]{2,1,0:T(8,128)(2,1)S(1)} async-done(((bf16[8,40,1024]{2,1,0:T(8,128)(2,1)}), bf16[8,40,1024]{2,1,0:T(8,128)(2,1)S(1)}, u32[]{:S(2)}, u32[]{:S(2)}) %all-to-all-start.2) | async-done | bytes 655392 | tf_op jit(solution)/shard_map/all_to_all | solution.py:434
  97.5 0.8 copy-done.4
  98.4 2.2 %combine.1 = bf16[128,1024]{1,0:T(8,128)(2,1)} custom-call(bf16[320,128]{1,0:T(8,128)(2,1)} %get-tuple-element.37.place, bf16[320,1024]{1,0:T(8,128)(2,1)} %bitcast.17), custom_call_target="tpu_custom_call" | custom-call | tf_op jit(solution)/shard_map/combine/pallas_call | solution.py:196
  100.5 1.5 collective-permute-start.3
  102.0 0.8 slice_reduce_fusion
  102.8 1.0 pad_maximum_fusion.2
  103.9 3.2 %collective-permute-done.3 = bf16[128,1024]{1,0:T(8,128)(2,1)S(1)} collective-permute-done((bf16[128,1024]{1,0:T(8,128)(2,1)}, bf16[128,1024]{1,0:T(8,128)(2,1)S(1)}, u32[]{:S(2)}, u32[]{:S(2)}) %collective-permute-start.3) | collective-permute-done | bytes 262176 | tf_op jit(solution)/shard_map/ppermute | solution.py:369
  107.1 1.1 add_convert_fusion.1.ma
  108.3 0.6 dynamic-slice
  109.6 0.2 dynamic-update-slice
  109.8 20.3 %all-reduce = f32[32]{0:T(128)S(1)} all-reduce(f32[32]{0:T(128)S(1)} %dynamic-update-slice), channel_id=2, replica_groups=mesh['sp'=8,'tp'=4] {'sp'}, use_global_device_ids=true, to_apply=%add | all-reduce | flops 32 | bytes 256
  130.1 0.1 reshape.212
  130.3 0.7 copy-done.9
  131.0 5.3 %carry.1 = (bf16[4,128,256]{2,1,0:T(8,128)(2,1)}, bf16[4,128,256]{2,1,0:T(8,128)(2,1)}, bf16[8,128,256]{2,1,0:T(8,128)(2,1)}) custom-call(s32[1]{0:T(128)} %bitcast.core, bf16[128,1024]{1,0:T(8,128)(2,1)} %copy-done.8, bf16[128,1024]{1,0:T(8,128)(2,1)} %copy-done.9, bf16[2048,1024]{1,0:T(8,128)(2,1)} %wb.1, bf16[2048,1024]{1,0:T(8,128)(2,1)} %wb.1, ...), custom_call_target="tpu_custom_call" | custom-call | tf_op jit(solution)/shard_map/carry/pallas_call | solution.py:265
  136.4 0.2 convolution_exponential_fusion
  136.6 0.1 pad_maximum_fusion.1
  136.8 2.1 %collective-permute-start.7 = (bf16[4,128,1024]{2,1,0:T(8,128)(2,1)S(1)}, bf16[4,128,1024]{2,1,0:T(8,128)(2,1)}, u32[]{:S(2)}, u32[]{:S(2)}) collective-permute-start(bf16[4,128,1024]{2,1,0:T(8,128)(2,1)S(1)} %pad_maximum_fusion.1), channel_id=1, source_target_pairs={{0,4},{4,0},{8,12},{12,8},{16,20},{20,16},{24,28},{28,24},{1,5},{5... | collective-permute-start | bytes 3145736 | tf_op jit(solution)/shard_map/ppermute | solution.py:369
  138.8 0.3 select_reduce_fusion
  139.1 6.7 %collective-permute-done.8 = bf16[4,128,256]{2,1,0:T(8,128)(2,1)S(1)} collective-permute-done((bf16[4,128,256]{2,1,0:T(8,128)(2,1)}, bf16[4,128,256]{2,1,0:T(8,128)(2,1)S(1)}, u32[]{:S(2)}, u32[]{:S(2)}) %collective-permute-start.8) | collective-permute-done | bytes 262176 | tf_op jit(solution)/shard_map/ppermute | solution.py:369
  145.8 0.2 fusion.2
  146.1 3.5 %all-to-all-start.3 = ((bf16[8,128,256]{2,1,0:T(8,128)(2,1)}), bf16[8,128,256]{2,1,0:T(8,128)(2,1)S(1)}, u32[]{:S(2)}, u32[]{:S(2)}) async-start(bf16[8,128,256]{2,1,0:T(8,128)(2,1)} %get-tuple-element.40), calls=%async_computation.3 | async-start | bytes 1048576 | tf_op jit(solution)/shard_map/all_to_all | solution.py:485
  149.6 4.4 %collective-permute-done.9 = bf16[4,128,256]{2,1,0:T(8,128)(2,1)S(1)} collective-permute-done((bf16[4,128,256]{2,1,0:T(8,128)(2,1)S(1)}, bf16[4,128,256]{2,1,0:T(8,128)(2,1)S(1)}, u32[]{:S(2)}, u32[]{:S(2)}) %collective-permute-start.9) | collective-permute-done | bytes 262176 | tf_op jit(solution)/shard_map/ppermute | solution.py:369
  154.0 0.7 copy-done.12
  154.7 2.0 %fusion.4 = (bf16[4,128,256]{2,1,0:T(8,128)(2,1)S(1)}, f32[4,128,256]{2,1,0:T(8,128)}) fusion(bf16[4,128,256]{2,1,0:T(8,128)(2,1)} %copy-done.12, bf16[4,128,256]{2,1,0:T(8,128)(2,1)S(1)} %fusion.2, f32[4]{0:T(128)S(1)} %get-tuple-element.52, f32[4]{0:T(128)S(1)} %get-tuple-element.53, f32[4]{0:T(128)S(1)} %get-tuple-element.56, ...), kind=kLoop, calls=%fused_computation.12 | loop fusion | flops 1310720 | bytes 1572928 | tf_op jit(solution)/shard_map/convert_element_type | solution.py:479
  156.7 0.6 broadcast_xor_fusion.order
  157.3 7.5 %weight_grads.1 = (bf16[1,2048,512]{2,1,0:T(8,128)(2,1)}, bf16[1,2048,512]{2,1,0:T(8,128)(2,1)}, bf16[1,512,2048]{2,1,0:T(8,128)(2,1)}) custom-call(s32[1]{0:T(128)} %bitcast.core, bf16[320,1024]{1,0:T(8,128)(2,1)} %bitcast.13, bf16[320,1024]{1,0:T(8,128)(2,1)} %copy-done.2, bf16[320,1024]{1,0:T(8,128)(2,1)} %bitcast.16, bf16[320,1024]{1,0:T(8,128)(2,1)} %copy-done.3, ...), custom_call_target="tpu_custom_call" | custom-call | tf_op jit(solution)/shard_map/weight_grads/pallas_call | solution.py:174
  164.8 4.3 %collective-permute-done.7 = bf16[4,128,1024]{2,1,0:T(8,128)(2,1)} collective-permute-done((bf16[4,128,1024]{2,1,0:T(8,128)(2,1)S(1)}, bf16[4,128,1024]{2,1,0:T(8,128)(2,1)}, u32[]{:S(2)}, u32[]{:S(2)}) %collective-permute-start.7) | collective-permute-done | bytes 1048608 | tf_op jit(solution)/shard_map/ppermute | solution.py:369
  169.0 2.7 %pad_maximum_fusion.y = bf16[8,128,1024]{2,1,0:T(8,128)(2,1)} fusion(bf16[4,128,1024]{2,1,0:T(8,128)(2,1)} %collective-permute-done.7, bf16[2,128,1024]{2,1,0:T(8,128)(2,1)S(1)} %collective-permute-done.6, bf16[1,128,1024]{2,1,0:T(8,128)(2,1)S(1)} %collective-permute-done.5, bf16[1,128,1024]{2,1,0:T(8,128)(2,1)S(1)} %bitcast.21), kind=kLoop, calls=%fused_computation | loop fusion | flops 3145728 | bytes 4194304 | tf_op jit(solution)/shard_map/concatenate | solution.py:452
  171.8 3.3 %local_grads.1 = (bf16[4,128,128]{2,1,0:T(8,128)(2,1)}, f32[4,128,128]{2,1,0:T(8,128)}, f32[4,128,256]{2,1,0:T(8,128)}) custom-call(bf16[4,128,128]{2,1,0:T(8,128)(2,1)} %q.5, bf16[4,128,128]{2,1,0:T(8,128)(2,1)} %k.5, bf16[4,128,256]{2,1,0:T(8,128)(2,1)} %v.5, f32[4,128]{1,0:T(4,128)} %log_decay.7, f32[4,1,128,256]{3,2,1,0:T(8,128)} %state.3, ...), custom_call_target="tpu_custom_call" | custom-call | tf_op jit(solution)/shard_map/local_grads/pallas_call | solution.py:307
  175.0 0.7 broadcast_in_dim.12.factor
  175.8 2.6 %final_grads.1 = (bf16[4,128,128]{2,1,0:T(8,128)(2,1)}, bf16[4,128,256]{2,1,0:T(8,128)(2,1)}) custom-call(bf16[4,128,128]{2,1,0:T(8,128)(2,1)} %k.5, bf16[4,128,256]{2,1,0:T(8,128)(2,1)} %v.5, f32[4,128]{1,0:T(4,128)} %log_decay.7, f32[4,128,256]{2,1,0:T(8,128)} %get-tuple-element.59.later, bf16[4,128,256]{2,1,0:T(8,128)(2,1)} %copy-done.10, ...), custom_call_target="tpu_custom_call" | custom-call | tf_op jit(solution)/shard_map/final_grads/pallas_call | solution.py:329
  178.3 0.8 copy-done.6
  179.1 7.7 %project.1 = f32[256,1024]{1,0:T(8,128)} custom-call(s32[8]{0:T(128)} %broadcast_xor_fusion.order, bf16[8,128,256]{2,1,0:T(8,128)(2,1)} %copy-done.6, bf16[8,128,1024]{2,1,0:T(8,128)(2,1)} %pad_maximum_fusion.y), custom_call_target="tpu_custom_call" | custom-call | tf_op jit(solution)/shard_map/project/pallas_call | solution.py:351
  (45 shorter events, 0.6 us)
Async XLA Ops:
  31.4 22.5 %copy-start = (bf16[8,40,1024]{2,1,0:T(8,128)(2,1)}, bf16[8,40,1024]{2,1,0:T(8,128)(2,1)S(1)}, u32[]{:S(2)}) copy-start(bf16[8,40,1024]{2,1,0:T(8,128)(2,1)S(1)} %all_to_all.20) | copy-start | bytes 1966084
  31.4 20.4 %all-to-all-start.1 = ((bf16[8,40,1024]{2,1,0:T(8,128)(2,1)}), bf16[8,40,1024]{2,1,0:T(8,128)(2,1)S(1)}, u32[]{:S(2)}, u32[]{:S(2)}) async-start(bf16[8,40,1024]{2,1,0:T(8,128)(2,1)} %bitcast.22), calls=%async_computation.1 | async-start | bytes 1310720 | tf_op jit(solution)/shard_map/all_to_all | solution.py:434
  35.0 16.8 %collective-permute-start = (bf16[320,1024]{1,0:T(8,128)(2,1)S(1)}, bf16[320,1024]{1,0:T(8,128)(2,1)S(1)}, u32[]{:S(2)}, u32[]{:S(2)}) collective-permute-start(bf16[320,1024]{1,0:T(8,128)(2,1)S(1)} %bitcast.11), channel_id=1, source_target_pairs={{0,1},{1,0},{2,3},{3,2},{4,5},{5,4},{6,7},{7,6},{8,9},{9,8},{10,11... | collective-permute-start | bytes 1966088 | tf_op jit(solution)/shard_map/ppermute | solution.py:369
  51.8 2.1 %copy-start.1 = (bf16[8,40,1024]{2,1,0:T(8,128)(2,1)}, bf16[8,40,1024]{2,1,0:T(8,128)(2,1)S(1)}, u32[]{:S(2)}) copy-start(bf16[8,40,1024]{2,1,0:T(8,128)(2,1)S(1)} %all-to-all-done.1) | copy-start | bytes 1966084
  51.8 2.1 %collective-permute-start.1 = (bf16[320,1024]{1,0:T(8,128)(2,1)S(1)}, bf16[320,1024]{1,0:T(8,128)(2,1)S(1)}, u32[]{:S(2)}, u32[]{:S(2)}) collective-permute-start(bf16[320,1024]{1,0:T(8,128)(2,1)S(1)} %bitcast.14), channel_id=1, source_target_pairs={{0,1},{1,0},{2,3},{3,2},{4,5},{5,4},{6,7},{7,6},{8,9},{9,8},{10,11... | collective-permute-start | bytes 1966088 | tf_op jit(solution)/shard_map/ppermute | solution.py:369
  51.8 2.1 %copy-start.2 = (bf16[320,1024]{1,0:T(8,128)(2,1)}, bf16[320,1024]{1,0:T(8,128)(2,1)S(1)}, u32[]{:S(2)}) copy-start(bf16[320,1024]{1,0:T(8,128)(2,1)S(1)} %collective-permute-done.rb) | copy-start | bytes 1966084
  53.9 0.8 copy-start.3
  64.9 2.4 %collective-permute-start.2 = (bf16[320,1024]{1,0:T(8,128)(2,1)}, bf16[320,1024]{1,0:T(8,128)(2,1)S(1)}, u32[]{:S(2)}, u32[]{:S(2)}) collective-permute-start(bf16[320,1024]{1,0:T(8,128)(2,1)} %get-tuple-element.39), channel_id=1, source_target_pairs={{0,1},{1,0},{2,3},{3,2},{4,5},{5,4},{6,7},{7,6},{8,9},{9,8},{10,11... | collective-permute-start | bytes 1966088 | tf_op jit(solution)/shard_map/ppermute | solution.py:369
  69.4 37.7 %copy-start.7 = (bf16[128,2048]{1,0:T(8,128)(2,1)S(1)}, bf16[128,2048]{1,0:T(8,128)(2,1)}, u32[]{:S(2)}) copy-start(bf16[128,2048]{1,0:T(8,128)(2,1)} %g.1) | copy-start | bytes 1572868
  69.4 28.1 %all-to-all-start.2 = ((bf16[8,40,1024]{2,1,0:T(8,128)(2,1)}), bf16[8,40,1024]{2,1,0:T(8,128)(2,1)S(1)}, u32[]{:S(2)}, u32[]{:S(2)}) async-start(bf16[8,40,1024]{2,1,0:T(8,128)(2,1)} %bitcast.5), calls=%async_computation.2 | async-start | bytes 1310720 | tf_op jit(solution)/shard_map/all_to_all | solution.py:434
  73.2 35.1 %copy-start.14 = (u32[32]{0:T(128)S(1)}, u32[32]{0:T(128)}, u32[]{:S(2)}) copy-start(u32[32]{0:T(128)} %constant.62) | copy-start | bytes 388
  75.7 27.1 %collective-permute-start.5 = (bf16[1,128,1024]{2,1,0:T(8,128)(2,1)}, bf16[1,128,1024]{2,1,0:T(8,128)(2,1)S(1)}, u32[]{:S(2)}, u32[]{:S(2)}) collective-permute-start(bf16[1,128,1024]{2,1,0:T(8,128)(2,1)} %bitcast.18), channel_id=1, source_target_pairs={{0,16},{4,20},{8,24},{12,28},{16,0},{20,4},{24,8},{28,12},{1,17},{... | collective-permute-start | bytes 786440 | tf_op jit(solution)/shard_map/ppermute | solution.py:369
  97.5 0.8 copy-start.4
  100.5 6.6 %collective-permute-start.3 = (bf16[128,1024]{1,0:T(8,128)(2,1)}, bf16[128,1024]{1,0:T(8,128)(2,1)S(1)}, u32[]{:S(2)}, u32[]{:S(2)}) collective-permute-start(bf16[128,1024]{1,0:T(8,128)(2,1)} %combine.1), channel_id=1, source_target_pairs={{0,2},{1,3},{2,0},{3,1},{4,6},{5,7},{6,4},{7,5},{8,10},{9,11},{10,... | collective-permute-start | bytes 786440 | tf_op jit(solution)/shard_map/ppermute | solution.py:369
  103.8 32.8 %collective-permute-start.6 = (bf16[2,128,1024]{2,1,0:T(8,128)(2,1)S(1)}, bf16[2,128,1024]{2,1,0:T(8,128)(2,1)S(1)}, u32[]{:S(2)}, u32[]{:S(2)}) collective-permute-start(bf16[2,128,1024]{2,1,0:T(8,128)(2,1)S(1)} %pad_maximum_fusion.2), channel_id=1, source_target_pairs={{0,8},{4,12},{8,0},{12,4},{16,24},{20,28},{24,16},{28,20},{1,9},{5... | collective-permute-start | bytes 1572872 | tf_op jit(solution)/shard_map/ppermute | solution.py:369
  108.2 22.1 %copy-start.8 = (bf16[128,1024]{1,0:T(8,128)(2,1)}, bf16[128,1024]{1,0:T(8,128)(2,1)S(1)}, u32[]{:S(2)}) copy-start(bf16[128,1024]{1,0:T(8,128)(2,1)S(1)} %add_convert_fusion.1.ma) | copy-start | bytes 786436
  108.2 22.1 %collective-permute-start.4 = (bf16[128,1024]{1,0:T(8,128)(2,1)S(1)}, bf16[128,1024]{1,0:T(8,128)(2,1)S(1)}, u32[]{:S(2)}, u32[]{:S(2)}) collective-permute-start(bf16[128,1024]{1,0:T(8,128)(2,1)S(1)} %add_convert_fusion.1.ma), channel_id=1, source_target_pairs={{0,1},{1,0},{2,3},{3,2},{4,5},{5,4},{6,7},{7,6},{8,9},{9,8},{10,11... | collective-permute-start | bytes 786440 | tf_op jit(solution)/shard_map/ppermute | solution.py:369
  130.3 6.3 %copy-start.5 = (bf16[128,1024]{1,0:T(8,128)(2,1)S(1)}, bf16[128,1024]{1,0:T(8,128)(2,1)}, u32[]{:S(2)}) copy-start(bf16[128,1024]{1,0:T(8,128)(2,1)} %get-tuple-element.42) | copy-start | bytes 786436
  130.3 0.7 copy-start.9
  136.3 9.5 %copy-start.11 = (bf16[4,128,256]{2,1,0:T(8,128)(2,1)S(1)}, bf16[4,128,256]{2,1,0:T(8,128)(2,1)}, u32[]{:S(2)}) copy-start(bf16[4,128,256]{2,1,0:T(8,128)(2,1)} %get-tuple-element.46) | copy-start | bytes 786436
  136.3 9.5 %collective-permute-start.8 = (bf16[4,128,256]{2,1,0:T(8,128)(2,1)}, bf16[4,128,256]{2,1,0:T(8,128)(2,1)S(1)}, u32[]{:S(2)}, u32[]{:S(2)}) collective-permute-start(bf16[4,128,256]{2,1,0:T(8,128)(2,1)} %get-tuple-element.46), channel_id=1, source_target_pairs={{0,4},{4,0},{8,12},{12,8},{16,20},{20,16},{24,28},{28,24},{1,5},{5... | collective-permute-start | bytes 786440 | tf_op jit(solution)/shard_map/ppermute | solution.py:369
  136.7 20.0 %copy-start.13 = (s32[8]{0:T(128)S(1)}, s32[8]{0:T(128)}, u32[]{:S(2)}) copy-start(s32[8]{0:T(128)} %constant.55.clone) | copy-start | bytes 100
  136.8 32.3 %collective-permute-start.7 = (bf16[4,128,1024]{2,1,0:T(8,128)(2,1)S(1)}, bf16[4,128,1024]{2,1,0:T(8,128)(2,1)}, u32[]{:S(2)}, u32[]{:S(2)}) collective-permute-start(bf16[4,128,1024]{2,1,0:T(8,128)(2,1)S(1)} %pad_maximum_fusion.1), channel_id=1, source_target_pairs={{0,4},{4,0},{8,12},{12,8},{16,20},{20,16},{24,28},{28,24},{1,5},{5... | collective-permute-start | bytes 3145736 | tf_op jit(solution)/shard_map/ppermute | solution.py:369
  146.0 8.0 %collective-permute-start.9 = (bf16[4,128,256]{2,1,0:T(8,128)(2,1)S(1)}, bf16[4,128,256]{2,1,0:T(8,128)(2,1)S(1)}, u32[]{:S(2)}, u32[]{:S(2)}) collective-permute-start(bf16[4,128,256]{2,1,0:T(8,128)(2,1)S(1)} %fusion.2), channel_id=1, source_target_pairs={{0,8},{4,12},{8,0},{12,4},{16,24},{20,28},{24,16},{28,20},{1,9},{5... | collective-permute-start | bytes 786440 | tf_op jit(solution)/shard_map/ppermute | solution.py:369
  146.1 32.3 %all-to-all-start.3 = ((bf16[8,128,256]{2,1,0:T(8,128)(2,1)}), bf16[8,128,256]{2,1,0:T(8,128)(2,1)S(1)}, u32[]{:S(2)}, u32[]{:S(2)}) async-start(bf16[8,128,256]{2,1,0:T(8,128)(2,1)} %get-tuple-element.40), calls=%async_computation.3 | async-start | bytes 1048576 | tf_op jit(solution)/shard_map/all_to_all | solution.py:485
  154.0 0.7 copy-start.12
  156.7 18.3 %collective-permute-start.10 = (bf16[4,128,256]{2,1,0:T(8,128)(2,1)S(1)}, bf16[4,128,256]{2,1,0:T(8,128)(2,1)S(1)}, u32[]{:S(2)}, u32[]{:S(2)}) collective-permute-start(bf16[4,128,256]{2,1,0:T(8,128)(2,1)S(1)} %get-tuple-element.58), channel_id=1, source_target_pairs={{0,16},{4,20},{8,24},{12,28},{16,0},{20,4},{24,8},{28,12},{1,17},{... | collective-permute-start | bytes 786440 | tf_op jit(solution)/shard_map/ppermute | solution.py:369
  175.0 0.7 copy-start.10
  178.3 0.8 copy-start.6

commit v2 on v1

v2 whole, which is shorter than its diff:
```python
import functools

import jax
import jax.numpy as jnp
from jax import lax
from jax.experimental import pallas as pl
from jax.experimental.pallas import tpu as pltpu
from jax.sharding import PartitionSpec as P

F32 = jnp.float32
BF16 = jnp.bfloat16
EXACT = lax.Precision.HIGHEST


def dot(a, b, ca=1, cb=0, precision=None):
    return lax.dot_general(
        a, b, (((ca,), (cb,)), ((), ())), preferred_element_type=F32, precision=precision
    )


def iota(shape, axis):
    return lax.broadcasted_iota(jnp.int32, shape, axis)


def limit(mib):
    return pltpu.CompilerParams(vmem_limit_bytes=mib << 20)


def dispatch_kernel(core, routes, weight, x, g, out, place, *, experts, cap):
    tokens, half = x.shape
    slots = experts * cap
    expert = iota((experts, tokens), 0)
    first = routes[0:1, :] == expert
    second = routes[1:2, :] == expert
    named = jnp.where(first | second, 1.0, 0.0)
    share = jnp.where(first, weight[0:1, :], 0.0) + jnp.where(second, weight[1:2, :], 0.0)
    before = jnp.where(iota((tokens, tokens), 0) < iota((tokens, tokens), 1), 1.0, 0.0)
    rank_t = dot(named.astype(BF16), before.astype(BF16))
    rank_t = jnp.where(named > 0.5, rank_t, 2.0 * cap)
    slot = iota((slots, experts), 0)
    base = iota((slots, experts), 1) * cap
    owner = (slot >= base) & (slot < base + cap)
    owner_f = jnp.where(owner, 1.0, 0.0)
    number = jnp.sum(jnp.where(owner, slot - base, 0).astype(F32), axis=1, keepdims=True)
    rank = dot(owner_f.astype(BF16), rank_t.astype(BF16))
    hit = rank == number
    picked = jnp.where(hit, 1.0, 0.0).astype(BF16)
    share_slot = jnp.sum(
        jnp.where(hit, dot(owner_f, share, precision=EXACT), 0.0), axis=1, keepdims=True
    )
    place[...] = picked
    out[:, :half] = dot(picked, x[...]).astype(BF16)
    out[:, half:] = (share_slot * dot(picked, g[...])).astype(BF16)


def dispatch(core, routes, weight, x, g, experts, cap):
    tokens, width = x.shape
    half = width // 2
    slots = experts * cap
    whole = lambda i, c: (0, 0)
    return pl.pallas_call(
        functools.partial(dispatch_kernel, experts=experts, cap=cap),
        grid_spec=pltpu.PrefetchScalarGridSpec(
            num_scalar_prefetch=1,
            grid=(1,),
            in_specs=[
                pl.BlockSpec(routes.shape, whole),
                pl.BlockSpec(weight.shape, whole),
                pl.BlockSpec((tokens, half), lambda i, c: (0, c[0])),
                pl.BlockSpec((tokens, half), lambda i, c: (0, c[0])),
            ],
            out_specs=[
                pl.BlockSpec((slots, width), whole),
                pl.BlockSpec((slots, tokens), whole),
            ],
        ),
        out_shape=[
            jax.ShapeDtypeStruct((slots, width), BF16),
            jax.ShapeDtypeStruct((slots, tokens), BF16),
        ],
        compiler_params=limit(16),
        name="dispatch",
    )(core, routes, weight, x, g)


def expert_kernel(
    core, ra, rb, ga, gb, wga, wgb, wua, wub, wda, wdb, hidden, gback, uback, pb, accb
):
    step = pl.program_id(0)
    gate = dot(ra[...], wga[...]) + dot(rb[...], wgb[...])
    up = dot(ra[...], wua[...]) + dot(rb[...], wub[...])
    back = dot(ga[...], wda[...], 1, 1) + dot(gb[...], wdb[...], 1, 1)
    sig = 1.0 / (1.0 + jnp.exp(-gate))
    active = gate * sig
    hidden[...] = (active * up).astype(BF16)
    gb_v = (back * up * (sig * (1.0 + gate * (1.0 - sig)))).astype(BF16)
    ub_v = (back * active).astype(BF16)
    gback[...] = gb_v
    uback[...] = ub_v
    part_b = dot(gb_v, wgb[...], 1, 1) + dot(ub_v, wub[...], 1, 1)
    last = pl.num_programs(0) - 1

    @pl.when((step == 0) & (last > 0))
    def _():
        accb[...] = part_b

    @pl.when((step > 0) & (step < last))
    def _():
        accb[...] += part_b

    @pl.when((step == last) & (last > 0))
    def _():
        pb[...] = (accb[...] + part_b).astype(BF16)

    @pl.when((step == last) & (last == 0))
    def _():
        pb[...] = part_b.astype(BF16)


def expert_back(core, own, other, w_gate, w_up, w_down):
    rows, width = own.shape
    half = width // 2
    units = w_gate.shape[2]
    chunk = min(units, 256)
    left = pl.BlockSpec((rows, half), lambda f, c: (0, 0))
    right = pl.BlockSpec((rows, half), lambda f, c: (0, 1))
    near = pl.BlockSpec((None, half, chunk), lambda f, c: (0, c[0], f))
    far = pl.BlockSpec((None, half, chunk), lambda f, c: (0, 1 - c[0], f))
    near_d = pl.BlockSpec((None, chunk, half), lambda f, c: (0, f, c[0]))
    far_d = pl.BlockSpec((None, chunk, half), lambda f, c: (0, f, 1 - c[0]))
    part = pl.BlockSpec((rows, chunk), lambda f, c: (0, f))
    return pl.pallas_call(
        expert_kernel,
        grid_spec=pltpu.PrefetchScalarGridSpec(
            num_scalar_prefetch=1,
            grid=(units // chunk,),
            in_specs=[left, left, right, right, near, far, near, far, near_d, far_d],
            out_specs=[part, part, part, left],
            scratch_shapes=[pltpu.VMEM((rows, half), F32)],
        ),
        out_shape=[jax.ShapeDtypeStruct((rows, units), BF16)] * 3
        + [jax.ShapeDtypeStruct((rows, half), BF16)],
        compiler_params=limit(28),
        name="expert",
    )(core, own, other, own, other, w_gate, w_gate, w_up, w_up, w_down, w_down)


def partial_kernel(core, gback, uback, wg, wu, out):
    out[...] = (dot(gback[...], wg[...], 1, 1) + dot(uback[...], wu[...], 1, 1)).astype(BF16)


def expert_part(core, gback, uback, w_gate, w_up):
    rows, units = gback.shape
    half = w_gate.shape[1] // 2
    chunk = half // 2
    full = pl.BlockSpec((rows, units), lambda i, c: (0, 0))
    near = pl.BlockSpec((None, chunk, units), lambda i, c: (0, 2 * c[0] + i, 0))
    return pl.pallas_call(
        partial_kernel,
        grid_spec=pltpu.PrefetchScalarGridSpec(
            num_scalar_prefetch=1,
            grid=(2,),
            in_specs=[full, full, near, near],
            out_specs=pl.BlockSpec((rows, chunk), lambda i, c: (0, i)),
        ),
        out_shape=jax.ShapeDtypeStruct((rows, half), BF16),
        compiler_params=limit(12),
        name="expert_part",
    )(core, gback, uback, w_gate, w_up)


def weights_kernel(core, ra, rb, ga, gb, hidden, gback, uback, gate_out, up_out, down_out):
    step = pl.program_id(0)
    turn = pl.num_programs(0) // 2

    def write(r, g):
        gate_out[...] = dot(r[...], gback[...], 0, 0).astype(BF16)
        up_out[...] = dot(r[...], uback[...], 0, 0).astype(BF16)
        down_out[...] = dot(hidden[...], g[...], 0, 0).astype(BF16)

    @pl.when(step < turn)
    def _():
        write(ra, ga)

    @pl.when(step >= turn)
    def _():
        write(rb, gb)


def weight_grads(core, own, other, hidden, gback, uback):
    rows, width = own.shape
    half = width // 2
    units = hidden.shape[1]
    chunk = min(half, 512)
    turn = half // chunk
    near = lambda i: jnp.minimum(i, turn - 1)
    far = lambda i: jnp.maximum(i - turn, 0)
    at = lambda i, c: jnp.where(i < turn, c[0] * turn + i, (1 - c[0]) * turn + i - turn)
    full = pl.BlockSpec((rows, units), lambda i, c: (0, 0))
    tall = pl.BlockSpec((None, chunk, units), lambda i, c: (0, at(i, c), 0))
    wide = pl.BlockSpec((None, units, chunk), lambda i, c: (0, 0, at(i, c)))
    return pl.pallas_call(
        weights_kernel,
        grid_spec=pltpu.PrefetchScalarGridSpec(
            num_scalar_prefetch=1,
            grid=(2 * turn,),
            in_specs=[
                pl.BlockSpec((rows, chunk), lambda i, c: (0, near(i))),
                pl.BlockSpec((rows, chunk), lambda i, c: (0, far(i))),
                pl.BlockSpec((rows, chunk), lambda i, c: (0, turn + near(i))),
                pl.BlockSpec((rows, chunk), lambda i, c: (0, turn + far(i))),
                full, full, full,
            ],
            out_specs=[tall, tall, wide],
        ),
        out_shape=[
            jax.ShapeDtypeStruct((1, width, units), BF16),
            jax.ShapeDtypeStruct((1, width, units), BF16),
            jax.ShapeDtypeStruct((1, units, width), BF16),
        ],
        compiler_params=limit(20),
        name="weight_grads",
    )(core, own, other, own, other, hidden, gback, uback)


def combine_kernel(place, back, out):
    out[...] = dot(place[...], back[...], 0, 0).astype(BF16)


def combine(place, back):
    return pl.pallas_call(
        combine_kernel,
        out_shape=jax.ShapeDtypeStruct((place.shape[1], back.shape[1]), BF16),
        compiler_params=limit(8),
        name="combine",
    )(place, back)


def decays(log_decay, head):
    span = log_decay.shape[-1]
    row = iota((span, span), 0)
    col = iota((span, span), 1)
    keep = row >= col
    lower = jnp.where(keep, 1.0, 0.0)
    own = log_decay[head : head + 1, :]
    down = jnp.sum(lower * own, axis=1, keepdims=True)
    across = jnp.sum(jnp.where(row <= col, 1.0, 0.0) * jnp.sum(
        jnp.where(row == col, own, 0.0), axis=1, keepdims=True), axis=0, keepdims=True)
    total = jnp.sum(own, axis=1, keepdims=True)
    table = jnp.where(keep, jnp.exp(jnp.where(keep, down - across, 0.0)), 0.0)
    return table, jnp.exp(down), jnp.exp(total - down), total


def mixed_kernel(q, k, v, log_decay, state, mixed):
    heads, span, size = q.shape
    width = v.shape[2]
    scale = size**-0.5
    for h in range(heads):
        table, lead, _, _ = decays(log_decay[...], h)
        scores = (dot(q[h], k[h], 1, 1) * (scale * table)).astype(BF16)
        out = dot(scores, v[h]) + lead * dot(q[h], state[h, 0].astype(BF16))
        mixed[:, h * width : (h + 1) * width] = out.astype(BF16)


def mixed_heads(q, k, v, log_decay, state):
    heads, span, _ = q.shape
    return pl.pallas_call(
        mixed_kernel,
        out_shape=jax.ShapeDtypeStruct((span, heads * v.shape[2]), BF16),
        compiler_params=limit(8),
        name="mixed_heads",
    )(q, k, v, log_decay, state)


PIECES = 16


def pieces(decay, shape):
    row = iota(shape, 0)
    high = decay.astype(BF16).astype(F32)
    rest = decay - high
    middle = rest.astype(BF16).astype(F32)
    low = rest - middle
    return jnp.where(row == 0, high, jnp.where(row == 1, middle, jnp.where(row == 2, low, 0.0)))


def put_message(ref, h, body, decay):
    size = body.shape[0]
    ref[h, :size, :] = body.astype(BF16)
    ref[h, size:, :] = pieces(decay, (PIECES, body.shape[1])).astype(BF16)


def get_message(ref, h):
    size = ref.shape[1] - PIECES
    decay = jnp.sum(ref[h, size:, :].astype(F32), axis=0, keepdims=True)[:, 0:1]
    return ref[h, :size, :].astype(F32), decay


def carry_kernel(at, ma, mb, wa, wb, q, log_decay, hg, keep, send, slices, *, groups):
    head = pl.program_id(0)
    h_grad = (dot(ma[...], wa[...]) + dot(mb[...], wb[...])).astype(BF16)
    hg[...] = h_grad
    span = log_decay.shape[-1]
    own = log_decay[pl.ds(head, 1), :]
    lower = jnp.where(iota((span, span), 0) >= iota((span, span), 1), 1.0, 0.0)
    lead = jnp.exp(jnp.sum(lower * own, axis=1, keepdims=True))
    total = jnp.exp(jnp.sum(own, axis=1, keepdims=True))
    part = dot((q[...].astype(F32) * lead).astype(BF16), h_grad, 0, 0)
    half = part.shape[1] // 2
    upper = (at[1] & 1) == 1
    put_message(keep, 0, jnp.where(upper, part[:, half:], part[:, :half]), total)
    put_message(send, 0, jnp.where(upper, part[:, :half], part[:, half:]), total)

    @pl.when(head == 0)
    def _():
        size = slices.shape[2]
        turn = groups // 2
        for i in range(turn):
            slices[at[0] * turn + i] = ma[:, i * size : (i + 1) * size]
            slices[(1 - at[0]) * turn + i] = mb[:, i * size : (i + 1) * size]


def carry(at, ma, mb, w_out, q, log_decay, groups, value_size):
    span, half = ma.shape
    heads, _, size = q.shape
    whole = lambda h, c: (0, 0)
    by_head = lambda h, c: (h, 0, 0)
    message = (size + PIECES, value_size // 2)
    return pl.pallas_call(
        functools.partial(carry_kernel, groups=groups),
        grid_spec=pltpu.PrefetchScalarGridSpec(
            num_scalar_prefetch=1,
            grid=(heads,),
            in_specs=[
                pl.BlockSpec((span, half), whole),
                pl.BlockSpec((span, half), whole),
                pl.BlockSpec((half, value_size), lambda h, c: (c[0], h)),
                pl.BlockSpec((half, value_size), lambda h, c: (1 - c[0], h)),
                pl.BlockSpec((None, span, size), by_head),
                pl.BlockSpec(log_decay.shape, whole),
            ],
            out_specs=[
                pl.BlockSpec((None, span, value_size), by_head),
                pl.BlockSpec((1,) + message, by_head),
                pl.BlockSpec((1,) + message, by_head),
                pl.BlockSpec((groups, span, 2 * half // groups), lambda h, c: (0, 0, 0)),
            ],
        ),
        out_shape=[
            jax.ShapeDtypeStruct((heads, span, value_size), BF16),
            jax.ShapeDtypeStruct((heads,) + message, BF16),
            jax.ShapeDtypeStruct((heads,) + message, BF16),
            jax.ShapeDtypeStruct((groups, span, 2 * half // groups), BF16),
        ],
        compiler_params=limit(12),
        name="carry",
    )(at, ma, mb, w_out, w_out, q, log_decay)


def pair_kernel(at, keep, came, out):
    upper = (at[1] & 1) == 1
    for h in range(keep.shape[0]):
        mine, mine_decay = get_message(keep, h)
        theirs, their_decay = get_message(came, h)
        first = jnp.where(upper, theirs, mine)
        second = jnp.where(upper, mine, theirs)
        decay = jnp.where(upper, their_decay, mine_decay)
        put_message(out, h, first + decay * second, mine_decay * their_decay)


def join_kernel(at, group, came, later, reach, out, later_out, reach_out, *, bit):
    upper = (at[1] & bit) != 0
    for h in range(group.shape[0]):
        mine, mine_decay = get_message(group, h)
        theirs, their_decay = get_message(came, h)
        first = jnp.where(upper, theirs, mine)
        second = jnp.where(upper, mine, theirs)
        decay = jnp.where(upper, their_decay, mine_decay)
        put_message(out, h, first + decay * second, mine_decay * their_decay)
        old = reach[h : h + 1, :]
        later_out[h] = later[h] + jnp.where(upper, 0.0, old[:, 0:1]) * theirs
        reach_out[h : h + 1, :] = old * jnp.where(upper, 1.0, their_decay)


def close_kernel(at, came, later, reach, keep, first_came, own, send, *, bit):
    upper = (at[1] & bit) != 0
    right = (at[1] & 1) == 1
    for h in range(keep.shape[0]):
        theirs, _ = get_message(came, h)
        after = later[h] + jnp.where(upper, 0.0, reach[h : h + 1, 0:1]) * theirs
        mine, mine_decay = get_message(keep, h)
        pair, pair_decay = get_message(first_came, h)
        second = jnp.where(right, mine, pair)
        decay = jnp.where(right, mine_decay, pair_decay)
        through = second + decay * after
        own[h] = jnp.where(right, after, through).astype(BF16)
        send[h] = jnp.where(right, through, after).astype(BF16)


def small(kernel, name, outs, at, *operands):
    spec = pl.BlockSpec(memory_space=pltpu.VMEM)
    return pl.pallas_call(
        kernel,
        in_specs=[pl.BlockSpec(memory_space=pltpu.SMEM)] + [spec] * len(operands),
        out_shape=outs,
        compiler_params=limit(8),
        name=name,
    )(at, *operands)


def local_kernel(q, k, v, log_decay, state, hg, q_grad, k_part, v_part):
    heads, span, size = q.shape
    scale = size**-0.5
    for h in range(heads):
        table, lead, _, _ = decays(log_decay[...], h)
        scores = (dot(q[h], k[h], 1, 1) * (scale * table)).astype(BF16)
        back = (dot(hg[h], v[h], 1, 1) * table).astype(BF16)
        from_state = dot(hg[h], state[h, 0].astype(BF16), 1, 1)
        q_grad[h] = (scale * dot(back, k[h]) + lead * from_state).astype(BF16)
        k_part[h] = dot(back, q[h], 0, 0)
        v_part[h] = dot(scores, hg[h], 0, 0)


def local_grads(q, k, v, log_decay, state, hg):
    return pl.pallas_call(
        local_kernel,
        out_shape=[
            jax.ShapeDtypeStruct(q.shape, BF16),
            jax.ShapeDtypeStruct(k.shape, F32),
            jax.ShapeDtypeStruct(v.shape, F32),
        ],
        compiler_params=limit(12),
        name="local_grads",
    )(q, k, v, log_decay, state, hg)


def final_kernel(at, k, v, log_decay, own, came, k_part, v_part, k_grad, v_grad):
    heads, span, size = k.shape
    half = v.shape[2] // 2
    scale = size**-0.5
    right = (at[1] & 1) == 1
    for h in range(heads):
        _, _, trail, _ = decays(log_decay[...], h)
        low = jnp.where(right, came[h].astype(F32), own[h].astype(F32)).astype(BF16)
        high = jnp.where(right, own[h].astype(F32), came[h].astype(F32)).astype(BF16)
        back = dot(v[h, :, :half], low, 1, 1) + dot(v[h, :, half:], high, 1, 1)
        k_grad[h] = (scale * (k_part[h] + trail * back)).astype(BF16)
        strength = scale * trail
        v_grad[h, :, :half] = (v_part[h, :, :half] + strength * dot(k[h], low)).astype(BF16)
        v_grad[h, :, half:] = (v_part[h, :, half:] + strength * dot(k[h], high)).astype(BF16)


def project_kernel(order, x, ya, yb, out):
    turn = ya.shape[0]
    span, width = ya.shape[1], ya.shape[2]
    left = jnp.concatenate([x[order[i]] for i in range(turn)], axis=0)
    right = jnp.concatenate([x[order[turn + i]] for i in range(turn)], axis=0)
    out[...] = dot(left, ya[...].reshape(turn * span, width), 0, 0) + dot(
        right, yb[...].reshape(turn * span, width), 0, 0
    )


def project(order, x, ya, yb):
    groups, span, size = x.shape
    turn, _, width = ya.shape
    chunk = min(width, 512)
    return pl.pallas_call(
        project_kernel,
        grid_spec=pltpu.PrefetchScalarGridSpec(
            num_scalar_prefetch=1,
            grid=(width // chunk,),
            in_specs=[
                pl.BlockSpec((groups, span, size), lambda i, o: (0, 0, 0)),
                pl.BlockSpec((turn, span, chunk), lambda i, o: (0, 0, i)),
                pl.BlockSpec((turn, span, chunk), lambda i, o: (0, 0, i)),
            ],
            out_specs=pl.BlockSpec((size, chunk), lambda i, o: (0, i)),
        ),
        out_shape=jax.ShapeDtypeStruct((size, width), F32),
        compiler_params=limit(16),
        name="project",
    )(order, x, ya, yb)


def swap(a, axis, bit):
    count = lax.axis_size(axis)
    return lax.ppermute(a, axis, [(i, i ^ bit) for i in range(count)])


def bits_of(count):
    return [1 << i for i in range(count.bit_length() - 1)]


def body(
    moe_input,
    out_grad,
    routes,
    route_weight,
    w_gate,
    w_up,
    w_down,
    w_out,
    query_heads,
    key_heads,
    value_heads,
    log_decay,
    state_in,
):
    tokens, width = moe_input.shape
    half = width // 2
    sp = lax.axis_size("sp")
    tp = lax.axis_size("tp")
    place = lax.axis_index("sp").astype(jnp.int32)
    core = (lax.axis_index("tp") & 1).astype(jnp.int32)
    at = jnp.stack([core, place])
    experts = w_gate.shape[0] * sp
    cap = 5 * tokens * routes.shape[1] // (4 * experts)
    heads, _, size = query_heads.shape
    value_size = value_heads.shape[-1]

    def exchange(a):
        wide = a.shape[1]
        a = a.reshape(experts, cap, wide)
        return lax.all_to_all(a, "sp", split_axis=0, concat_axis=0, tiled=True).reshape(-1, wide)

    sent, picked = dispatch(at, routes.T, route_weight.T, moe_input, out_grad, experts, cap)
    own = exchange(sent)
    other = swap(own, "tp", 1)
    mixed = mixed_heads(query_heads, key_heads, value_heads, log_decay, state_in)
    mixed, _ = lax.optimization_barrier((mixed, own))

    hidden, gate_back, up_back, part_b = expert_back(at, own, other, w_gate, w_up, w_down)
    part_came = swap(part_b, "tp", 1)
    part_a = expert_part(at, gate_back, up_back, w_gate, w_up)
    part = (part_a.astype(F32) + part_came.astype(F32)).astype(BF16)
    gate_grad, up_grad, down_grad = weight_grads(at, own, other, hidden, gate_back, up_back)

    returned = exchange(part)

    gathered = mixed[None]
    offsets = [0]
    for bit in reversed(bits_of(sp)):
        came = swap(gathered, "sp", bit)
        if bit > 1:
            gathered = jnp.concatenate([gathered, came], axis=0)
        offsets = offsets + [o ^ bit for o in offsets]
    order = (place ^ jnp.array(offsets, jnp.int32)).astype(jnp.int32)

    token_part = combine(picked, returned)
    for bit in bits_of(tp)[1:]:
        token_part = token_part.astype(F32) + swap(token_part, "tp", bit).astype(F32)
        if bit * 2 < tp:
            token_part = token_part.astype(BF16)
    own_grad = lax.dynamic_slice_in_dim(out_grad, core * half, half, axis=1)
    mixed_a = (own_grad.astype(F32) + token_part.astype(F32)).astype(BF16)
    mixed_b = swap(mixed_a, "tp", 1)

    head_grad, keep, send, slices = carry(
        at, mixed_a, mixed_b, w_out, query_heads, log_decay, sp, value_size
    )
    first_came = swap(send, "sp", 1)
    q_grad, k_part, v_part = local_grads(
        query_heads, key_heads, value_heads, log_decay, state_in, head_grad
    )
    message = jax.ShapeDtypeStruct(keep.shape, BF16)
    state_shape = (heads, size, value_size // 2)
    group = small(pair_kernel, "pair", message, at, keep, first_came)
    later = jnp.zeros(state_shape, F32)
    reach = jnp.ones((heads, 128), F32)
    for bit in bits_of(sp)[1:]:
        came_state = swap(group, "sp", bit)
        if bit * 2 < sp:
            group, later, reach = small(
                functools.partial(join_kernel, bit=bit),
                "join",
                [message, jax.ShapeDtypeStruct(state_shape, F32),
                 jax.ShapeDtypeStruct((heads, 128), F32)],
                at, group, came_state, later, reach,
            )
    state_out = jax.ShapeDtypeStruct(state_shape, BF16)
    own_state, send_state = small(
        functools.partial(close_kernel, bit=bit),
        "close", [state_out, state_out], at, came_state, later, reach, keep, first_came,
    )
    other_state = swap(send_state, "sp", 1)
    k_grad, v_grad = small(
        final_kernel,
        "final",
        [jax.ShapeDtypeStruct(key_heads.shape, BF16), jax.ShapeDtypeStruct(value_heads.shape, BF16)],
        at, key_heads, value_heads, log_decay, own_state, other_state, k_part, v_part,
    )
    slices = lax.all_to_all(slices, "sp", split_axis=0, concat_axis=0, tiled=True)
    out_proj_grad = project(order, slices, gathered, came)
    return gate_grad, up_grad, down_grad, out_proj_grad, q_grad, k_grad, v_grad


def solution(mesh):
    return jax.shard_map(
        body,
        mesh=mesh,
        in_specs=(
            P("sp", None),
            P("sp", None),
            P("sp", None),
            P("sp", None),
            P("sp", None, "tp"),
            P("sp", None, "tp"),
            P("sp", "tp", None),
            P(None, "tp"),
            P("tp", "sp", None),
            P("tp", "sp", None),
            P("tp", "sp", None),
            P("tp", "sp"),
            P("tp", "sp", None, None),
        ),
        out_specs=(
            P("sp", None, "tp"),
            P("sp", None, "tp"),
            P("sp", "tp", None),
            P("sp", "tp"),
            P("tp", "sp", None),
            P("tp", "sp", None),
            P("tp", "sp", None),
        ),
        check_vma=False,
    )
```

time: 188 us -> 174 us (0.926)
  Pallas kernels: 44.2 us -> 29 us
  local copies, waits for them, and re-layouts: 9.23 us -> 18 us
  blocking collectives: 45.2 us -> 38.4 us
  other arithmetic: 10.2 us -> 5.5 us
  starting transfers between devices: 17.9 us -> 20.6 us
  waiting for transfers between devices: 58.5 us -> 60.8 us
    ppermute x11, waiting for transfers between devices: 22.8 us -> 60.8 us  [swap(): return lax.ppermute(a, axis, [(i, i ^ bit) for i in range(count)])]
    all_to_all x2 -> x1, waiting for transfers between devices: 35.6 us -> 0.01 us  [exchange(): lax.all_to_all(a, 'sp', split_axis=0, concat_axis=0, tiled=True)]
    unnamed x1 -> x0, blocking collectives: 20.3 us -> none
    all_to_all x1, blocking collectives: 24.9 us -> 38.4 us  [exchange(): lax.all_to_all(a, 'sp', split_axis=0, concat_axis=0, tiled=True)]
    unnamed x35 -> x68, local copies, waits for them, and re-layouts: 7.63 us -> 18 us
    ppermute x11, starting transfers between devices: 7.07 us -> 13.4 us  [swap(): return lax.ppermute(a, axis, [(i, i ^ bit) for i in range(count)])]
    pallas_call x1, Pallas kernels: 7.75 us -> 3.5 us  [project(): pl.pallas_call(project_kernel, grid_spec=pltpu.PrefetchScalarGridSpec(num...]
    pallas_call x1, Pallas kernels: 10.1 us -> 6.15 us  [expert_back(): pl.pallas_call(expert_kernel, grid_spec=pltpu.PrefetchScalarGridSpec(num_...]
  transfers between devices with their start and end apart: 14 -> 13, of which waited for: 8 -> 8; matrix products, arithmetic and copies ran while one was open for 6% -> 3% of each run, Pallas kernels for 12% -> 10%
where the time goes in v2:
time: 174 us; the launch traced here: 173 us
  waiting for transfers between devices  60.8 us (35%)
  blocking collectives  38.4 us (22%)
  Pallas kernels  29 us (17%)
  starting transfers between devices  20.6 us (12%)
  local copies, waits for them, and re-layouts  18 us (10%)
  other arithmetic  5.5 us (3%)
    ppermute x11, waiting for transfers between devices, swap(): return lax.ppermute(a, axis, [(i, i ^ bit) for i in range(count)])  60.8 us
    all_to_all x1, blocking collectives, exchange(): lax.all_to_all(a, 'sp', split_axis=0, concat_axis=0, tiled=True)  38.4 us
    unnamed x68, local copies, waits for them, and re-layouts  18 us
    ppermute x11, starting transfers between devices, swap(): return lax.ppermute(a, axis, [(i, i ^ bit) for i in range(count)])  13.4 us
    pallas_call x1, Pallas kernels, weight_grads(): pl.pallas_call(weights_kernel, grid_spec=pltpu.PrefetchScalarGridSpec(num...  6.26 us
    pallas_call x1, Pallas kernels, expert_back(): pl.pallas_call(expert_kernel, grid_spec=pltpu.PrefetchScalarGridSpec(num_...  6.15 us
    pallas_call x4, Pallas kernels, small(): pl.pallas_call(kernel, in_specs=[pl.BlockSpec(memory_space=pltpu.SMEM)] +...  3.65 us
    all_to_all x1, starting transfers between devices, body(): lax.all_to_all(slices, 'sp', split_axis=0, concat_axis=0, tiled=True)  3.65 us
  transfers between devices with their start and end apart: 13, of which 8 were waited for; matrix products, arithmetic and copies ran while one was open for 3% of the time, Pallas kernels for 10%

profile of v2, /device:TPU:0, one launch (start us, length us, event | category | flops | bytes accessed | tf_op | source)
XLA Modules:
  0.0 173.4 jit_solution(2735009200701423150)
XLA Ops:
  0.7 1.2 copy-done.16
  1.9 1.0 copy-done.21
  2.9 0.7 copy-done.29
  3.6 0.7 copy-done.30
  4.3 1.3 dispatch.1
  6.3 38.4 %all_to_all.15 = bf16[8,40,2048]{2,1,0:T(8,128)(2,1)S(1)} all-to-all(bf16[8,40,2048]{2,1,0:T(8,128)(2,1)S(1)} %bitcast.18), channel_id=1, replica_groups=mesh['sp'=8,'tp'=4] {'sp'}, dimensions={0} | all-to-all | bytes 2621440 | tf_op jit(solution)/shard_map/all_to_all | solution.py:524
  44.7 3.0 %collective-permute-done.rb.gb = bf16[320,2048]{1,0:T(8,128)(2,1)S(1)} collective-permute-done((bf16[320,2048]{1,0:T(8,128)(2,1)S(1)}, bf16[320,2048]{1,0:T(8,128)(2,1)S(1)}, u32[]{:S(2)}, u32[]{:S(2)}) %collective-permute-start) | collective-permute-done | bytes 1310752 | tf_op jit(solution)/shard_map/ppermute | solution.py:487
  47.8 1.6 copy-done.1
  49.4 1.6 copy-done.3
  51.0 6.2 %expert.1 = (bf16[320,512]{1,0:T(8,128)(2,1)S(1)}, bf16[320,512]{1,0:T(8,128)(2,1)S(1)}, bf16[320,512]{1,0:T(8,128)(2,1)S(1)}, bf16[320,1024]{1,0:T(8,128)(2,1)S(1)}) custom-call(s32[2]{0:T(128)S(1)} %pad_add_fusion.core.at, bf16[320,2048]{1,0:T(8,128)(2,1)S(1)} %bitcast.10, bf16[320,2048]{1,0:T(8,128)(2,1)S(1)} %collective-permute-done.rb.gb, ...), custom_call_target="tpu_custom_call" | custom-call | tf_op jit(solution)/shard_map/expert/pallas_call | solution.py:132
  57.4 1.7 expert_part.1
  59.3 1.1 add_convert_fusion
  60.4 3.6 %all-to-all-start.1 = ((bf16[8,40,1024]{2,1,0:T(8,128)(2,1)}), bf16[8,40,1024]{2,1,0:T(8,128)(2,1)S(1)}, u32[]{:S(2)}, u32[]{:S(2)}) async-start(bf16[8,40,1024]{2,1,0:T(8,128)(2,1)} %bitcast.21), calls=%async_computation.1 | async-start | bytes 1310720 | tf_op jit(solution)/shard_map/all_to_all | solution.py:524
  64.0 1.0 copy-done.6
  65.1 0.9 copy-done.12
  66.0 0.9 copy-done.14
  67.4 3.0 %collective-permute-start.4 = (bf16[1,128,1024]{2,1,0:T(8,128)(2,1)S(1)}, bf16[1,128,1024]{2,1,0:T(8,128)(2,1)S(1)}, u32[]{:S(2)}, u32[]{:S(2)}) collective-permute-start(bf16[1,128,1024]{2,1,0:T(8,128)(2,1)S(1)} %bitcast.15), channel_id=1, source_target_pairs={{0,16},{4,20},{8,24},{12,28},{16,0},{20,4},{24,8},{28,12},{1,17},{... | collective-permute-start | bytes 786440 | tf_op jit(solution)/shard_map/ppermute | solution.py:487
  70.4 22.6 %collective-permute-done.4 = bf16[1,128,1024]{2,1,0:T(8,128)(2,1)S(1)} collective-permute-done((bf16[1,128,1024]{2,1,0:T(8,128)(2,1)S(1)}, bf16[1,128,1024]{2,1,0:T(8,128)(2,1)S(1)}, u32[]{:S(2)}, u32[]{:S(2)}) %collective-permute-start.4) | collective-permute-done | bytes 262176 | tf_op jit(solution)/shard_map/ppermute | solution.py:487
  93.0 0.9 pad_maximum_fusion.1
  93.9 0.9 copy-done.27
  94.8 1.0 combine.1
  95.8 1.5 collective-permute-start.2
  97.4 6.1 %collective-permute-done.2 = bf16[128,1024]{1,0:T(8,128)(2,1)S(1)} collective-permute-done((bf16[128,1024]{1,0:T(8,128)(2,1)}, bf16[128,1024]{1,0:T(8,128)(2,1)S(1)}, u32[]{:S(2)}, u32[]{:S(2)}) %collective-permute-start.2) | collective-permute-done | bytes 262176 | tf_op jit(solution)/shard_map/ppermute | solution.py:487
  103.4 1.2 add_convert_fusion.1.ma
  104.7 2.5 %collective-permute-done.5 = bf16[2,128,1024]{2,1,0:T(8,128)(2,1)} collective-permute-done((bf16[2,128,1024]{2,1,0:T(8,128)(2,1)}, bf16[2,128,1024]{2,1,0:T(8,128)(2,1)}, u32[]{:S(2)}, u32[]{:S(2)}) %collective-permute-start.5) | collective-permute-done | bytes 524320 | tf_op jit(solution)/shard_map/ppermute | solution.py:487
  107.2 2.3 %pad_maximum_fusion.ya = bf16[4,128,1024]{2,1,0:T(8,128)(2,1)} fusion(bf16[2,128,1024]{2,1,0:T(8,128)(2,1)} %collective-permute-done.5, bf16[1,128,1024]{2,1,0:T(8,128)(2,1)} %copy-done.32, bf16[1,128,1024]{2,1,0:T(8,128)(2,1)} %bitcast.17), kind=kLoop, calls=%fused_computation.1 | loop fusion | flops 1048576 | bytes 2097152 | tf_op jit(solution)/shard_map/concatenate | solution.py:545
  109.5 1.5 collective-permute-start.6
  111.0 2.2 %copy-done.2 = bf16[2048,1024]{1,0:T(8,128)(2,1)S(1)} copy-done((bf16[2048,1024]{1,0:T(8,128)(2,1)S(1)}, bf16[2048,1024]{1,0:T(8,128)(2,1)}, u32[]{:S(2)}) %copy-start.2) | copy-done | bytes 4194328
  113.2 3.2 %carry.1 = (bf16[4,128,256]{2,1,0:T(8,128)(2,1)S(1)}, bf16[4,144,128]{2,1,0:T(8,128)(2,1)S(1)}, bf16[4,144,128]{2,1,0:T(8,128)(2,1)S(1)}, bf16[8,128,256]{2,1,0:T(8,128)(2,1)S(1)}) custom-call(s32[2]{0:T(128)S(1)} %pad_add_fusion.core.at, bf16[128,1024]{1,0:T(8,128)(2,1)S(1)} %add_convert_fusion.1.ma, bf16[128,1024]{1,0:T(8,128)(2,1)S(1)} %collective-permute-done.3.mb, ...), custom_call_target="tpu_custom_call" | custom-call | tf_op jit(solution)/shard_map/carry/pallas_call | solution.py:329
  116.5 0.7 copy-done.17
  117.1 0.8 copy-done.20
  117.9 0.7 copy-done.24
  119.3 3.6 %all-to-all-start.2 = ((bf16[8,128,256]{2,1,0:T(8,128)(2,1)}), bf16[8,128,256]{2,1,0:T(8,128)(2,1)S(1)}, u32[]{:S(2)}, u32[]{:S(2)}) async-start(bf16[8,128,256]{2,1,0:T(8,128)(2,1)} %copy-done.20), calls=%async_computation.2 | async-start | bytes 1048576 | tf_op jit(solution)/shard_map/all_to_all | solution.py:592
  122.9 2.0 %collective-permute-start.7 = (bf16[4,144,128]{2,1,0:T(8,128)(2,1)}, bf16[4,144,128]{2,1,0:T(8,128)(2,1)S(1)}, u32[]{:S(2)}, u32[]{:S(2)}) collective-permute-start(bf16[4,144,128]{2,1,0:T(8,128)(2,1)} %copy-done.31), channel_id=1, source_target_pairs={{0,4},{4,0},{8,12},{12,8},{16,20},{20,16},{24,28},{28,24},{1,5},{5... | collective-permute-start | bytes 442376 | tf_op jit(solution)/shard_map/ppermute | solution.py:487
  124.9 16.9 %collective-permute-done.7.came.first_came = bf16[4,144,128]{2,1,0:T(8,128)(2,1)S(1)} collective-permute-done((bf16[4,144,128]{2,1,0:T(8,128)(2,1)}, bf16[4,144,128]{2,1,0:T(8,128)(2,1)S(1)}, u32[]{:S(2)}, u32[]{:S(2)}) %collective-permute-start.7) | collective-permute-done | bytes 147488 | tf_op jit(solution)/shard_map/ppermute | solution.py:487
  141.9 0.9 copy-done.18
  143.4 1.4 collective-permute-start.8
  144.9 3.8 %collective-permute-done.8.came = bf16[4,144,128]{2,1,0:T(8,128)(2,1)S(1)} collective-permute-done((bf16[4,144,128]{2,1,0:T(8,128)(2,1)S(1)}, bf16[4,144,128]{2,1,0:T(8,128)(2,1)S(1)}, u32[]{:S(2)}, u32[]{:S(2)}) %collective-permute-start.8) | collective-permute-done | bytes 147488 | tf_op jit(solution)/shard_map/ppermute | solution.py:487
  148.7 0.7 join.1
  149.4 2.1 %collective-permute-start.9 = (bf16[4,144,128]{2,1,0:T(8,128)(2,1)S(1)}, bf16[4,144,128]{2,1,0:T(8,128)(2,1)S(1)}, u32[]{:S(2)}, u32[]{:S(2)}) collective-permute-start(bf16[4,144,128]{2,1,0:T(8,128)(2,1)S(1)} %get-tuple-element.46), channel_id=1, source_target_pairs={{0,16},{4,20},{8,24},{12,28},{16,0},{20,4},{24,8},{28,12},{1,17},{... | collective-permute-start | bytes 442376 | tf_op jit(solution)/shard_map/ppermute | solution.py:487
  151.4 5.6 %collective-permute-done.9.came = bf16[4,144,128]{2,1,0:T(8,128)(2,1)S(1)} collective-permute-done((bf16[4,144,128]{2,1,0:T(8,128)(2,1)S(1)}, bf16[4,144,128]{2,1,0:T(8,128)(2,1)S(1)}, u32[]{:S(2)}, u32[]{:S(2)}) %collective-permute-start.9) | collective-permute-done | bytes 147488 | tf_op jit(solution)/shard_map/ppermute | solution.py:487
  157.0 0.9 copy-done.19
  158.0 0.7 close.1
  158.6 1.6 collective-permute-start.10
  160.3 6.3 %weight_grads.1 = (bf16[1,2048,512]{2,1,0:T(8,128)(2,1)}, bf16[1,2048,512]{2,1,0:T(8,128)(2,1)}, bf16[1,512,2048]{2,1,0:T(8,128)(2,1)}) custom-call(s32[2]{0:T(128)S(1)} %pad_add_fusion.core.at, bf16[320,2048]{1,0:T(8,128)(2,1)S(1)} %bitcast.12, bf16[320,2048]{1,0:T(8,128)(2,1)S(1)} %collective-permute-done.rb.gb, bf16[320,2048]{1,0:T(8,128)(2,1)S(1)} %bitcast.13, ...), custom_call_target="tpu_custom_call" | custom-call | tf_op jit(solution)/shard_map/weight_grads/pallas_call | solution.py:202
  166.5 1.6 local_grads.1
  168.2 1.7 final.1
  169.9 3.5 %project.1 = f32[256,1024]{1,0:T(8,128)} custom-call(s32[8]{0:T(128)S(1)} %broadcast_xor_fusion.order, bf16[8,128,256]{2,1,0:T(8,128)(2,1)S(1)} %all-to-all-done.2.x, bf16[4,128,1024]{2,1,0:T(8,128)(2,1)} %pad_maximum_fusion.ya, bf16[4,128,1024]{2,1,0:T(8,128)(2,1)} %collective-permute-done.6.yb), custom_call_target="tpu_custom_call" | custom-call | tf_op jit(solution)/shard_map/project/pallas_call | solution.py:467
  (68 shorter events, 3.2 us)
Async XLA Ops:
  0.6 47.1 %copy-start = (bf16[1,2048,512]{2,1,0:T(8,128)(2,1)S(1)}, bf16[1,2048,512]{2,1,0:T(8,128)(2,1)}, u32[]{:S(2)}) copy-start(bf16[1,2048,512]{2,1,0:T(8,128)(2,1)} %wg.1) | copy-start | bytes 6291460
  0.7 1.2 copy-start.16
  1.9 1.0 copy-start.21
  2.9 0.7 copy-start.29
  3.6 0.7 copy-start.30
  5.6 0.6 copy-start.26
  44.7 3.0 %collective-permute-start = (bf16[320,2048]{1,0:T(8,128)(2,1)S(1)}, bf16[320,2048]{1,0:T(8,128)(2,1)S(1)}, u32[]{:S(2)}, u32[]{:S(2)}) collective-permute-start(bf16[320,2048]{1,0:T(8,128)(2,1)S(1)} %bitcast.9), channel_id=1, source_target_pairs={{0,1},{1,0},{2,3},{3,2},{4,5},{5,4},{6,7},{7,6},{8,9},{9,8},{10,11... | collective-permute-start | bytes 3932168 | tf_op jit(solution)/shard_map/ppermute | solution.py:487
  47.8 1.6 copy-start.1
  49.4 1.6 copy-start.3
  57.1 1.9 %copy-start.8 = (bf16[320,512]{1,0:T(8,128)(2,1)}, bf16[320,512]{1,0:T(8,128)(2,1)S(1)}, u32[]{:S(2)}) copy-start(bf16[320,512]{1,0:T(8,128)(2,1)S(1)} %get-tuple-element.33.gback) | copy-start | bytes 983044
  57.1 1.9 %copy-start.10 = (bf16[320,512]{1,0:T(8,128)(2,1)}, bf16[320,512]{1,0:T(8,128)(2,1)S(1)}, u32[]{:S(2)}) copy-start(bf16[320,512]{1,0:T(8,128)(2,1)S(1)} %get-tuple-element.34.uback) | copy-start | bytes 983044
  57.1 1.9 %copy-start.22 = (bf16[320,512]{1,0:T(8,128)(2,1)}, bf16[320,512]{1,0:T(8,128)(2,1)S(1)}, u32[]{:S(2)}) copy-start(bf16[320,512]{1,0:T(8,128)(2,1)S(1)} %get-tuple-element.32.hidden) | copy-start | bytes 983044
  57.1 2.2 %collective-permute-start.1 = (bf16[320,1024]{1,0:T(8,128)(2,1)S(1)}, bf16[320,1024]{1,0:T(8,128)(2,1)S(1)}, u32[]{:S(2)}, u32[]{:S(2)}) collective-permute-start(bf16[320,1024]{1,0:T(8,128)(2,1)S(1)} %get-tuple-element.39), channel_id=1, source_target_pairs={{0,1},{1,0},{2,3},{3,2},{4,5},{5,4},{6,7},{7,6},{8,9},{9,8},{10,11... | collective-permute-start | bytes 1966088 | tf_op jit(solution)/shard_map/ppermute | solution.py:487
  59.1 4.9 %copy-start.4 = (bf16[4,128,256]{2,1,0:T(8,128)(2,1)S(1)}, bf16[4,128,256]{2,1,0:T(8,128)(2,1)}, u32[]{:S(2)}) copy-start(bf16[4,128,256]{2,1,0:T(8,128)(2,1)} %v.5) | copy-start | bytes 786436
  59.1 4.9 %copy-start.28 = (f32[4,128]{1,0:T(4,128)S(1)}, f32[4,128]{1,0:T(4,128)}, u32[]{:S(2)}) copy-start(f32[4,128]{1,0:T(4,128)} %log_decay.7) | copy-start | bytes 6148
  60.4 33.5 %all-to-all-start.1 = ((bf16[8,40,1024]{2,1,0:T(8,128)(2,1)}), bf16[8,40,1024]{2,1,0:T(8,128)(2,1)S(1)}, u32[]{:S(2)}, u32[]{:S(2)}) async-start(bf16[8,40,1024]{2,1,0:T(8,128)(2,1)} %bitcast.21), calls=%async_computation.1 | async-start | bytes 1310720 | tf_op jit(solution)/shard_map/all_to_all | solution.py:524
  64.0 1.0 copy-start.6
  65.1 0.9 copy-start.12
  66.0 0.9 copy-start.14
  67.4 26.5 %copy-start.5 = (bf16[128,1024]{1,0:T(8,128)(2,1)}, bf16[128,1024]{1,0:T(8,128)(2,1)S(1)}, u32[]{:S(2)}) copy-start(bf16[128,1024]{1,0:T(8,128)(2,1)S(1)} %mixed_heads.1) | copy-start | bytes 786436
  67.4 25.6 %collective-permute-start.4 = (bf16[1,128,1024]{2,1,0:T(8,128)(2,1)S(1)}, bf16[1,128,1024]{2,1,0:T(8,128)(2,1)S(1)}, u32[]{:S(2)}, u32[]{:S(2)}) collective-permute-start(bf16[1,128,1024]{2,1,0:T(8,128)(2,1)S(1)} %bitcast.15), channel_id=1, source_target_pairs={{0,16},{4,20},{8,24},{12,28},{16,0},{20,4},{24,8},{28,12},{1,17},{... | collective-permute-start | bytes 786440 | tf_op jit(solution)/shard_map/ppermute | solution.py:487
  93.0 0.9 copy-start.32
  93.9 13.3 %collective-permute-start.5 = (bf16[2,128,1024]{2,1,0:T(8,128)(2,1)}, bf16[2,128,1024]{2,1,0:T(8,128)(2,1)}, u32[]{:S(2)}, u32[]{:S(2)}) collective-permute-start(bf16[2,128,1024]{2,1,0:T(8,128)(2,1)} %pad_maximum_fusion.1), channel_id=1, source_target_pairs={{0,8},{4,12},{8,0},{12,4},{16,24},{20,28},{24,16},{28,20},{1,9},{5... | collective-permute-start | bytes 1572872 | tf_op jit(solution)/shard_map/ppermute | solution.py:487
  93.9 0.9 copy-start.27
  95.8 15.2 %copy-start.13 = (bf16[4,128,128]{2,1,0:T(8,128)(2,1)S(1)}, bf16[4,128,128]{2,1,0:T(8,128)(2,1)}, u32[]{:S(2)}) copy-start(bf16[4,128,128]{2,1,0:T(8,128)(2,1)} %q.5) | copy-start | bytes 393220
  95.8 7.6 %collective-permute-start.2 = (bf16[128,1024]{1,0:T(8,128)(2,1)}, bf16[128,1024]{1,0:T(8,128)(2,1)S(1)}, u32[]{:S(2)}, u32[]{:S(2)}) collective-permute-start(bf16[128,1024]{1,0:T(8,128)(2,1)} %combine.1), channel_id=1, source_target_pairs={{0,2},{1,3},{2,0},{3,1},{4,6},{5,7},{6,4},{7,5},{8,10},{9,11},{10,... | collective-permute-start | bytes 786440 | tf_op jit(solution)/shard_map/ppermute | solution.py:487
  104.6 6.4 %collective-permute-start.3 = (bf16[128,1024]{1,0:T(8,128)(2,1)S(1)}, bf16[128,1024]{1,0:T(8,128)(2,1)S(1)}, u32[]{:S(2)}, u32[]{:S(2)}) collective-permute-start(bf16[128,1024]{1,0:T(8,128)(2,1)S(1)} %add_convert_fusion.1.ma), channel_id=1, source_target_pairs={{0,1},{1,0},{2,3},{3,2},{4,5},{5,4},{6,7},{7,6},{8,9},{9,8},{10,11... | collective-permute-start | bytes 786440 | tf_op jit(solution)/shard_map/ppermute | solution.py:487
  109.5 60.4 %collective-permute-start.6 = (bf16[4,128,1024]{2,1,0:T(8,128)(2,1)}, bf16[4,128,1024]{2,1,0:T(8,128)(2,1)}, u32[]{:S(2)}, u32[]{:S(2)}) collective-permute-start(bf16[4,128,1024]{2,1,0:T(8,128)(2,1)} %pad_maximum_fusion.ya), channel_id=1, source_target_pairs={{0,4},{4,0},{8,12},{12,8},{16,20},{20,16},{24,28},{28,24},{1,5},{5... | collective-permute-start | bytes 3145736 | tf_op jit(solution)/shard_map/ppermute | solution.py:487
  111.0 2.2 %copy-start.2 = (bf16[2048,1024]{1,0:T(8,128)(2,1)S(1)}, bf16[2048,1024]{1,0:T(8,128)(2,1)}, u32[]{:S(2)}) copy-start(bf16[2048,1024]{1,0:T(8,128)(2,1)} %wb.1) | copy-start | bytes 12582916
  116.4 0.7 copy-start.17
  117.1 0.8 copy-start.20
  117.9 0.7 copy-start.24
  118.6 0.7 copy-start.31
  119.3 40.9 %copy-start.33 = (s32[8]{0:T(128)S(1)}, s32[8]{0:T(128)}, u32[]{:S(2)}) copy-start(s32[8]{0:T(128)} %constant.23.clone) | copy-start | bytes 100
  119.3 50.6 %all-to-all-start.2 = ((bf16[8,128,256]{2,1,0:T(8,128)(2,1)}), bf16[8,128,256]{2,1,0:T(8,128)(2,1)S(1)}, u32[]{:S(2)}, u32[]{:S(2)}) async-start(bf16[8,128,256]{2,1,0:T(8,128)(2,1)} %copy-done.20), calls=%async_computation.2 | async-start | bytes 1048576 | tf_op jit(solution)/shard_map/all_to_all | solution.py:592
  122.9 37.3 %copy-start.9 = (bf16[320,512]{1,0:T(8,128)(2,1)S(1)}, bf16[320,512]{1,0:T(8,128)(2,1)}, u32[]{:S(2)}) copy-start(bf16[320,512]{1,0:T(8,128)(2,1)} %copy-done.8) | copy-start | bytes 983044
  122.9 37.3 %copy-start.11 = (bf16[320,512]{1,0:T(8,128)(2,1)S(1)}, bf16[320,512]{1,0:T(8,128)(2,1)}, u32[]{:S(2)}) copy-start(bf16[320,512]{1,0:T(8,128)(2,1)} %copy-done.10) | copy-start | bytes 983044
  122.9 19.0 %collective-permute-start.7 = (bf16[4,144,128]{2,1,0:T(8,128)(2,1)}, bf16[4,144,128]{2,1,0:T(8,128)(2,1)S(1)}, u32[]{:S(2)}, u32[]{:S(2)}) collective-permute-start(bf16[4,144,128]{2,1,0:T(8,128)(2,1)} %copy-done.31), channel_id=1, source_target_pairs={{0,4},{4,0},{8,12},{12,8},{16,20},{20,16},{24,28},{28,24},{1,5},{5... | collective-permute-start | bytes 442376 | tf_op jit(solution)/shard_map/ppermute | solution.py:487
  141.9 0.9 copy-start.18
  142.8 17.4 %copy-start.23 = (bf16[320,512]{1,0:T(8,128)(2,1)S(1)}, bf16[320,512]{1,0:T(8,128)(2,1)}, u32[]{:S(2)}) copy-start(bf16[320,512]{1,0:T(8,128)(2,1)} %copy-done.22) | copy-start | bytes 983044
  143.4 5.2 %collective-permute-start.8 = (bf16[4,144,128]{2,1,0:T(8,128)(2,1)S(1)}, bf16[4,144,128]{2,1,0:T(8,128)(2,1)S(1)}, u32[]{:S(2)}, u32[]{:S(2)}) collective-permute-start(bf16[4,144,128]{2,1,0:T(8,128)(2,1)S(1)} %pair.1.group), channel_id=1, source_target_pairs={{0,8},{4,12},{8,0},{12,4},{16,24},{20,28},{24,16},{28,20},{1,9},{5... | collective-permute-start | bytes 442376 | tf_op jit(solution)/shard_map/ppermute | solution.py:487
  149.4 7.7 %collective-permute-start.9 = (bf16[4,144,128]{2,1,0:T(8,128)(2,1)S(1)}, bf16[4,144,128]{2,1,0:T(8,128)(2,1)S(1)}, u32[]{:S(2)}, u32[]{:S(2)}) collective-permute-start(bf16[4,144,128]{2,1,0:T(8,128)(2,1)S(1)} %get-tuple-element.46), channel_id=1, source_target_pairs={{0,16},{4,20},{8,24},{12,28},{16,0},{20,4},{24,8},{28,12},{1,17},{... | collective-permute-start | bytes 442376 | tf_op jit(solution)/shard_map/ppermute | solution.py:487
  157.0 0.9 copy-start.19
  158.6 9.6 %collective-permute-start.10 = (bf16[4,128,128]{2,1,0:T(8,128)(2,1)S(1)}, bf16[4,128,128]{2,1,0:T(8,128)(2,1)S(1)}, u32[]{:S(2)}, u32[]{:S(2)}) collective-permute-start(bf16[4,128,128]{2,1,0:T(8,128)(2,1)S(1)} %get-tuple-element.50), channel_id=1, source_target_pairs={{0,4},{4,0},{8,12},{12,8},{16,20},{20,16},{24,28},{28,24},{1,5},{5... | collective-permute-start | bytes 393224 | tf_op jit(solution)/shard_map/ppermute | solution.py:487
  160.2 6.3 %copy-start.7 = (f32[4,1,128,256]{3,2,1,0:T(8,128)S(1)}, f32[4,1,128,256]{3,2,1,0:T(8,128)}, u32[]{:S(2)}) copy-start(f32[4,1,128,256]{3,2,1,0:T(8,128)} %state.3) | copy-start | bytes 1572868
  160.2 6.3 %copy-start.15 = (bf16[4,128,128]{2,1,0:T(8,128)(2,1)S(1)}, bf16[4,128,128]{2,1,0:T(8,128)(2,1)}, u32[]{:S(2)}) copy-start(bf16[4,128,128]{2,1,0:T(8,128)(2,1)} %k.5) | copy-start | bytes 393220
  160.2 6.3 %copy-start.25 = (bf16[4,128,256]{2,1,0:T(8,128)(2,1)S(1)}, bf16[4,128,256]{2,1,0:T(8,128)(2,1)}, u32[]{:S(2)}) copy-start(bf16[4,128,256]{2,1,0:T(8,128)(2,1)} %copy-done.24) | copy-start | bytes 786436

commit v3 on v2

--- a/solution.py
+++ b/solution.py
@@ -7,6 +7,7 @@
 from jax.experimental.pallas import tpu as pltpu
 from jax.sharding import PartitionSpec as P
 
+
 F32 = jnp.float32
 BF16 = jnp.bfloat16
 EXACT = lax.Precision.HIGHEST
@@ -20,6 +21,10 @@
 
 def iota(shape, axis):
     return lax.broadcasted_iota(jnp.int32, shape, axis)
+
+
+def in_hbm(a):
+    return pltpu.with_memory_space_constraint(a, pltpu.HBM)
 
 
 def limit(mib):
@@ -76,11 +81,11 @@
         ),
         out_shape=[
             jax.ShapeDtypeStruct((slots, width), BF16),
-            jax.ShapeDtypeStruct((slots, tokens), BF16),
+            pltpu.HBM((slots, tokens), BF16),
         ],
         compiler_params=limit(16),
         name="dispatch",
-    )(core, routes, weight, x, g)
+    )(core, in_hbm(routes), in_hbm(weight), in_hbm(x), in_hbm(g))
 
 
 def expert_kernel(
@@ -142,7 +147,7 @@
         + [jax.ShapeDtypeStruct((rows, half), BF16)],
         compiler_params=limit(28),
         name="expert",
-    )(core, own, other, own, other, w_gate, w_gate, w_up, w_up, w_down, w_down)
+    )(core, own, other, own, other, w_gate, w_gate, *[in_hbm(w) for w in (w_up, w_up, w_down, w_down)])
 
 
 def partial_kernel(core, gback, uback, wg, wu, out):
@@ -252,7 +257,7 @@
 
 
 def mixed_kernel(q, k, v, log_decay, state, mixed):
-    heads, span, size = q.shape
+    heads, _, size = q.shape
     width = v.shape[2]
     scale = size**-0.5
     for h in range(heads):
@@ -347,14 +352,14 @@
             ],
         ),
         out_shape=[
-            jax.ShapeDtypeStruct((heads, span, value_size), BF16),
+            pltpu.HBM((heads, span, value_size), BF16),
+            pltpu.HBM((heads,) + message, BF16),
             jax.ShapeDtypeStruct((heads,) + message, BF16),
-            jax.ShapeDtypeStruct((heads,) + message, BF16),
-            jax.ShapeDtypeStruct((groups, span, 2 * half // groups), BF16),
+            pltpu.HBM((groups, span, 2 * half // groups), BF16),
         ],
         compiler_params=limit(12),
         name="carry",
-    )(at, ma, mb, w_out, w_out, q, log_decay)
+    )(at, ma, mb, in_hbm(w_out), in_hbm(w_out), in_hbm(q), log_decay)
 
 
 def pair_kernel(at, keep, came, out):
@@ -397,19 +402,18 @@
         send[h] = jnp.where(right, through, after).astype(BF16)
 
 
-def small(kernel, name, outs, at, *operands):
+def small(kernel, outs, at, *operands):
     spec = pl.BlockSpec(memory_space=pltpu.VMEM)
     return pl.pallas_call(
         kernel,
         in_specs=[pl.BlockSpec(memory_space=pltpu.SMEM)] + [spec] * len(operands),
         out_shape=outs,
         compiler_params=limit(8),
-        name=name,
     )(at, *operands)
 
 
 def local_kernel(q, k, v, log_decay, state, hg, q_grad, k_part, v_part):
-    heads, span, size = q.shape
+    heads, _, size = q.shape
     scale = size**-0.5
     for h in range(heads):
         table, lead, _, _ = decays(log_decay[...], h)
@@ -435,7 +439,7 @@
 
 
 def final_kernel(at, k, v, log_decay, own, came, k_part, v_part, k_grad, v_grad):
-    heads, span, size = k.shape
+    heads, _, size = k.shape
     half = v.shape[2] // 2
     scale = size**-0.5
     right = (at[1] & 1) == 1
@@ -450,36 +454,35 @@
         v_grad[h, :, half:] = (v_part[h, :, half:] + strength * dot(k[h], high)).astype(BF16)
 
 
-def project_kernel(order, x, ya, yb, out):
-    turn = ya.shape[0]
-    span, width = ya.shape[1], ya.shape[2]
-    left = jnp.concatenate([x[order[i]] for i in range(turn)], axis=0)
-    right = jnp.concatenate([x[order[turn + i]] for i in range(turn)], axis=0)
-    out[...] = dot(left, ya[...].reshape(turn * span, width), 0, 0) + dot(
-        right, yb[...].reshape(turn * span, width), 0, 0
-    )
-
-
-def project(order, x, ya, yb):
+def project_kernel(order, x, *refs):
+    out = refs[-1]
+    total, at = None, 0
+    for y in refs[:-1]:
+        blocks, span, width = y.shape
+        rows = jnp.concatenate([x[order[at + i]] for i in range(blocks)], axis=0)
+        part = dot(rows, y[...].reshape(blocks * span, width), 0, 0)
+        total = part if total is None else total + part
+        at += blocks
+    out[...] = total
+
+
+def project(order, x, parts):
     groups, span, size = x.shape
-    turn, _, width = ya.shape
+    width = parts[0].shape[2]
     chunk = min(width, 512)
     return pl.pallas_call(
         project_kernel,
         grid_spec=pltpu.PrefetchScalarGridSpec(
             num_scalar_prefetch=1,
             grid=(width // chunk,),
-            in_specs=[
-                pl.BlockSpec((groups, span, size), lambda i, o: (0, 0, 0)),
-                pl.BlockSpec((turn, span, chunk), lambda i, o: (0, 0, i)),
-                pl.BlockSpec((turn, span, chunk), lambda i, o: (0, 0, i)),
-            ],
+            in_specs=[pl.BlockSpec((groups, span, size), lambda i, o: (0, 0, 0))]
+            + [pl.BlockSpec(y.shape[:2] + (chunk,), lambda i, o: (0, 0, i)) for y in parts],
             out_specs=pl.BlockSpec((size, chunk), lambda i, o: (0, i)),
         ),
         out_shape=jax.ShapeDtypeStruct((size, width), F32),
         compiler_params=limit(16),
         name="project",
-    )(order, x, ya, yb)
+    )(order, x, *parts)
 
 
 def swap(a, axis, bit):
@@ -491,7 +494,7 @@
     return [1 << i for i in range(count.bit_length() - 1)]
 
 
-def body(
+def step(
     moe_input,
     out_grad,
     routes,
@@ -527,32 +530,35 @@
     own = exchange(sent)
     other = swap(own, "tp", 1)
     mixed = mixed_heads(query_heads, key_heads, value_heads, log_decay, state_in)
-    mixed, _ = lax.optimization_barrier((mixed, own))
-
     hidden, gate_back, up_back, part_b = expert_back(at, own, other, w_gate, w_up, w_down)
     part_came = swap(part_b, "tp", 1)
     part_a = expert_part(at, gate_back, up_back, w_gate, w_up)
     part = (part_a.astype(F32) + part_came.astype(F32)).astype(BF16)
+    returned = exchange(part)
     gate_grad, up_grad, down_grad = weight_grads(at, own, other, hidden, gate_back, up_back)
 
-    returned = exchange(part)
-
-    gathered = mixed[None]
-    offsets = [0]
+    blocks = mixed[None]
+    parts, offsets = [], [0]
     for bit in reversed(bits_of(sp)):
-        came = swap(gathered, "sp", bit)
-        if bit > 1:
-            gathered = jnp.concatenate([gathered, came], axis=0)
+        if not parts:
+            parts = [jnp.concatenate([blocks, swap(blocks, "sp", bit)], axis=0)]
+        else:
+            came = []
+            for piece in parts:
+                came.append(swap(piece, "sp", bit))
+            parts = parts + came
         offsets = offsets + [o ^ bit for o in offsets]
     order = (place ^ jnp.array(offsets, jnp.int32)).astype(jnp.int32)
 
     token_part = combine(picked, returned)
     for bit in bits_of(tp)[1:]:
-        token_part = token_part.astype(F32) + swap(token_part, "tp", bit).astype(F32)
+        came = swap(token_part, "tp", bit)
+        token_part = token_part.astype(F32) + came.astype(F32)
         if bit * 2 < tp:
             token_part = token_part.astype(BF16)
-    own_grad = lax.dynamic_slice_in_dim(out_grad, core * half, half, axis=1)
-    mixed_a = (own_grad.astype(F32) + token_part.astype(F32)).astype(BF16)
+        else:
+            own_grad = lax.dynamic_slice_in_dim(out_grad, core * half, half, axis=1)
+            mixed_a = (own_grad.astype(F32) + token_part).astype(BF16)
     mixed_b = swap(mixed_a, "tp", 1)
 
     head_grad, keep, send, slices = carry(
@@ -564,7 +570,7 @@
     )
     message = jax.ShapeDtypeStruct(keep.shape, BF16)
     state_shape = (heads, size, value_size // 2)
-    group = small(pair_kernel, "pair", message, at, keep, first_came)
+    group = small(pair_kernel, message, at, keep, first_came)
     later = jnp.zeros(state_shape, F32)
     reach = jnp.ones((heads, 128), F32)
     for bit in bits_of(sp)[1:]:
@@ -572,7 +578,6 @@
         if bit * 2 < sp:
             group, later, reach = small(
                 functools.partial(join_kernel, bit=bit),
-                "join",
                 [message, jax.ShapeDtypeStruct(state_shape, F32),
                  jax.ShapeDtypeStruct((heads, 128), F32)],
                 at, group, came_state, later, reach,
@@ -580,23 +585,23 @@
     state_out = jax.ShapeDtypeStruct(state_shape, BF16)
     own_state, send_state = small(
         functools.partial(close_kernel, bit=bit),
-        "close", [state_out, state_out], at, came_state, later, reach, keep, first_came,
+        [state_out, state_out], at, came_state, later, reach, keep, first_came,
     )
     other_state = swap(send_state, "sp", 1)
+    slices = lax.all_to_all(slices, "sp", split_axis=0, concat_axis=0, tiled=True)
+    out_proj_grad = project(order, slices, parts)
     k_grad, v_grad = small(
         final_kernel,
-        "final",
-        [jax.ShapeDtypeStruct(key_heads.shape, BF16), jax.ShapeDtypeStruct(value_heads.shape, BF16)],
+        [jax.ShapeDtypeStruct(key_heads.shape, BF16),
+         jax.ShapeDtypeStruct(value_heads.shape, BF16)],
         at, key_heads, value_heads, log_decay, own_state, other_state, k_part, v_part,
     )
-    slices = lax.all_to_all(slices, "sp", split_axis=0, concat_axis=0, tiled=True)
-    out_proj_grad = project(order, slices, gathered, came)
     return gate_grad, up_grad, down_grad, out_proj_grad, q_grad, k_grad, v_grad
 
 
 def solution(mesh):
     return jax.shard_map(
-        body,
+        step,
         mesh=mesh,
         in_specs=(
             P("sp", None),

time: 174 us -> 154 us (0.89)
  waiting for transfers between devices: 60.8 us -> 31.7 us
  blocking collectives: 38.4 us -> 60 us
  local copies, waits for them, and re-layouts: 18 us -> 7.39 us
  starting transfers between devices: 20.6 us -> 15 us
  Pallas kernels: 29 us -> 34.2 us
    ppermute x11 -> x12, waiting for transfers between devices: 60.8 us -> 31.7 us  [swap(): return lax.ppermute(a, axis, [(i, i ^ bit) for i in range(count)])]
    all_to_all x1 -> x2, blocking collectives: 38.4 us -> 60 us  [exchange(): lax.all_to_all(a, 'sp', split_axis=0, concat_axis=0, tiled=True)]
    unnamed x68 -> x58, local copies, waits for them, and re-layouts: 18 us -> 7.37 us
    all_to_all x2 -> x1, starting transfers between devices: 7.24 us -> 4.28 us  [step(): lax.all_to_all(slices, 'sp', split_axis=0, concat_axis=0, tiled=True)]
    ppermute x11 -> x12, starting transfers between devices: 13.4 us -> 10.8 us  [swap(): return lax.ppermute(a, axis, [(i, i ^ bit) for i in range(count)])]
    pallas_call x1, Pallas kernels: 3.25 us -> 5.52 us  [carry(): pl.pallas_call(functools.partial(carry_kernel, groups=groups), grid_spec=...]
  transfers between devices with their start and end apart: 13 -> 13, of which waited for: 8 -> 8; matrix products, arithmetic and copies ran while one was open for 3% -> 2% of each run, Pallas kernels for 10% -> 13%
where the time goes in v3:
time: 154 us; the launch traced here: 153 us
  blocking collectives  60 us (39%)
  Pallas kernels  34.2 us (22%)
  waiting for transfers between devices  31.7 us (21%)
  starting transfers between devices  15 us (10%)
  local copies, waits for them, and re-layouts  7.39 us (5%)
  other arithmetic  4.08 us (3%)
    all_to_all x2, blocking collectives, exchange(): lax.all_to_all(a, 'sp', split_axis=0, concat_axis=0, tiled=True)  60 us
    ppermute x12, waiting for transfers between devices, swap(): return lax.ppermute(a, axis, [(i, i ^ bit) for i in range(count)])  31.7 us
    ppermute x12, starting transfers between devices, swap(): return lax.ppermute(a, axis, [(i, i ^ bit) for i in range(count)])  10.8 us
    unnamed x58, local copies, waits for them, and re-layouts  7.37 us
    pallas_call x1, Pallas kernels, expert_back(): pl.pallas_call(expert_kernel, grid_spec=pltpu.PrefetchScalarGridSpec(num_...  7.11 us
    pallas_call x1, Pallas kernels, weight_grads(): pl.pallas_call(weights_kernel, grid_spec=pltpu.PrefetchScalarGridSpec(num...  6.27 us
    pallas_call x1, Pallas kernels, carry(): pl.pallas_call(functools.partial(carry_kernel, groups=groups), grid_spec=...  5.52 us
    all_to_all x1, starting transfers between devices, step(): lax.all_to_all(slices, 'sp', split_axis=0, concat_axis=0, tiled=True)  4.28 us
  transfers between devices with their start and end apart: 13, of which 8 were waited for; matrix products, arithmetic and copies ran while one was open for 2% of the time, Pallas kernels for 13%

profile of v3, /device:TPU:0, one launch (start us, length us, event | category | flops | bytes accessed | tf_op | source)
XLA Modules:
  0.0 153.4 jit_solution(1214030685081528068)
XLA Ops:
  0.6 0.1 pad_add_fusion.core.at
  0.7 2.6 %dispatch.1 = (bf16[320,2048]{1,0:T(8,128)(2,1)S(1)}, bf16[320,128]{1,0:T(8,128)(2,1)}) custom-call(s32[2]{0:T(128)S(1)} %pad_add_fusion.core.at, s32[2,128]{1,0:T(2,128)} %bitcast.17, f32[2,128]{1,0:T(2,128)} %bitcast.18, bf16[128,2048]{1,0:T(8,128)(2,1)} %x.1, bf16[128,2048]{1,0:T(8,128)(2,1)} %g.1), custom_call_target="tpu_custom_call" | custom-call | tf_op jit(solution)/shard_map/dispatch/pallas_call | solution.py:66
  3.3 38.4 %all_to_all.15 = bf16[8,40,2048]{2,1,0:T(8,128)(2,1)S(1)} all-to-all(bf16[8,40,2048]{2,1,0:T(8,128)(2,1)S(1)} %bitcast.15), channel_id=1, replica_groups=mesh['sp'=8,'tp'=4] {'sp'}, dimensions={0} | all-to-all | bytes 2621440 | tf_op jit(solution)/shard_map/all_to_all | solution.py:527
  41.7 3.0 %collective-permute-done.rb.gb = bf16[320,2048]{1,0:T(8,128)(2,1)S(1)} collective-permute-done((bf16[320,2048]{1,0:T(8,128)(2,1)S(1)}, bf16[320,2048]{1,0:T(8,128)(2,1)S(1)}, u32[]{:S(2)}, u32[]{:S(2)}) %collective-permute-start) | collective-permute-done | bytes 1310752 | tf_op jit(solution)/shard_map/ppermute | solution.py:490
  44.8 7.1 %expert.1 = (bf16[320,512]{1,0:T(8,128)(2,1)S(1)}, bf16[320,512]{1,0:T(8,128)(2,1)S(1)}, bf16[320,512]{1,0:T(8,128)(2,1)S(1)}, bf16[320,1024]{1,0:T(8,128)(2,1)S(1)}) custom-call(s32[2]{0:T(128)S(1)} %pad_add_fusion.core.at, bf16[320,2048]{1,0:T(8,128)(2,1)S(1)} %bitcast.10, bf16[320,2048]{1,0:T(8,128)(2,1)S(1)} %collective-permute-done.rb.gb, ...), custom_call_target="tpu_custom_call" | custom-call | tf_op jit(solution)/shard_map/expert/pallas_call | solution.py:137
  51.9 0.2 collective-permute-start.1
  52.1 1.7 %expert_part.1 = bf16[320,1024]{1,0:T(8,128)(2,1)S(1)} custom-call(s32[2]{0:T(128)S(1)} %pad_add_fusion.core.at, bf16[320,512]{1,0:T(8,128)(2,1)S(1)} %get-tuple-element.32.gback, bf16[320,512]{1,0:T(8,128)(2,1)S(1)} %get-tuple-element.33.uback, bf16[1,2048,512]{2,1,0:T(8,128)(2,1)S(1)} %copy-done, bf16[1,2048,512]{2,1,0:T(8,128)(2,1)S(1)} %copy-done.1), custom_call_target="tpu_custom_call" | custom-call | tf_op jit(solution)/shard_map/expert_part/pallas_call | solution.py:163
  53.9 0.2 collective-permute-done.1
  54.1 0.2 add_convert_fusion
  54.3 21.6 %all_to_all.16 = bf16[8,40,1024]{2,1,0:T(8,128)(2,1)S(1)} all-to-all(bf16[8,40,1024]{2,1,0:T(8,128)(2,1)S(1)} %bitcast.16), channel_id=1, replica_groups=mesh['sp'=8,'tp'=4] {'sp'}, dimensions={0} | all-to-all | bytes 1310720 | tf_op jit(solution)/shard_map/all_to_all | solution.py:527
  75.9 1.0 combine.1
  76.9 1.5 collective-permute-start.2
  78.5 1.2 mixed_heads.1
  79.7 0.9 collective-permute-start.4
  80.6 3.7 %collective-permute-done.2 = bf16[128,1024]{1,0:T(8,128)(2,1)} collective-permute-done((bf16[128,1024]{1,0:T(8,128)(2,1)}, bf16[128,1024]{1,0:T(8,128)(2,1)}, u32[]{:S(2)}, u32[]{:S(2)}) %collective-permute-start.2) | collective-permute-done | bytes 262176 | tf_op jit(solution)/shard_map/ppermute | solution.py:490
  84.3 1.2 add_convert_fusion.1.ma
  85.5 0.1 collective-permute-start.3
  85.6 7.7 %collective-permute-done.4 = bf16[1,128,1024]{2,1,0:T(8,128)(2,1)} collective-permute-done((bf16[1,128,1024]{2,1,0:T(8,128)(2,1)}, bf16[1,128,1024]{2,1,0:T(8,128)(2,1)}, u32[]{:S(2)}, u32[]{:S(2)}) %collective-permute-start.4) | collective-permute-done | bytes 262176 | tf_op jit(solution)/shard_map/ppermute | solution.py:490
  93.3 1.9 %pad_maximum_fusion.refs_0_ = bf16[2,128,1024]{2,1,0:T(8,128)(2,1)} fusion(bf16[1,128,1024]{2,1,0:T(8,128)(2,1)} %collective-permute-done.4, bf16[1,128,1024]{2,1,0:T(8,128)(2,1)} %bitcast.8), kind=kLoop, calls=%fused_computation.1 | loop fusion | flops 262144 | bytes 1048576 | tf_op jit(solution)/shard_map/concatenate | solution.py:544
  95.2 5.5 %carry.1 = (bf16[4,128,256]{2,1,0:T(8,128)(2,1)}, bf16[4,144,128]{2,1,0:T(8,128)(2,1)}, bf16[4,144,128]{2,1,0:T(8,128)(2,1)S(1)}, bf16[8,128,256]{2,1,0:T(8,128)(2,1)}) custom-call(s32[2]{0:T(128)S(1)} %pad_add_fusion.core.at, bf16[128,1024]{1,0:T(8,128)(2,1)S(1)} %add_convert_fusion.1.ma, bf16[128,1024]{1,0:T(8,128)(2,1)S(1)} %collective-permute-done.3.mb, ...), custom_call_target="tpu_custom_call" | custom-call | tf_op jit(solution)/shard_map/carry/pallas_call | solution.py:334
  100.8 0.6 copy-done.28
  101.4 4.3 %all-to-all-start.2 = ((bf16[8,128,256]{2,1,0:T(8,128)(2,1)}), bf16[8,128,256]{2,1,0:T(8,128)(2,1)}, u32[]{:S(2)}, u32[]{:S(2)}) async-start(bf16[8,128,256]{2,1,0:T(8,128)(2,1)} %get-tuple-element.39), calls=%async_computation.2 | async-start | bytes 1048576 | tf_op jit(solution)/shard_map/all_to_all | solution.py:591
  105.7 2.0 %collective-permute-start.8 = (bf16[4,144,128]{2,1,0:T(8,128)(2,1)}, bf16[4,144,128]{2,1,0:T(8,128)(2,1)S(1)}, u32[]{:S(2)}, u32[]{:S(2)}) collective-permute-start(bf16[4,144,128]{2,1,0:T(8,128)(2,1)} %copy-done.28), channel_id=1, source_target_pairs={{0,4},{4,0},{8,12},{12,8},{16,20},{20,16},{24,28},{28,24},{1,5},{5... | collective-permute-start | bytes 442376 | tf_op jit(solution)/shard_map/ppermute | solution.py:490
  107.7 0.1 collective-permute-start.6
  107.8 1.8 %collective-permute-done.5.refs_1_ = bf16[2,128,1024]{2,1,0:T(8,128)(2,1)} collective-permute-done((bf16[2,128,1024]{2,1,0:T(8,128)(2,1)}, bf16[2,128,1024]{2,1,0:T(8,128)(2,1)}, u32[]{:S(2)}, u32[]{:S(2)}) %collective-permute-start.5) | collective-permute-done | bytes 524320 | tf_op jit(solution)/shard_map/ppermute | solution.py:490
  109.6 1.8 %collective-permute-start.7 = (bf16[2,128,1024]{2,1,0:T(8,128)(2,1)}, bf16[2,128,1024]{2,1,0:T(8,128)(2,1)S(1)}, u32[]{:S(2)}, u32[]{:S(2)}) collective-permute-start(bf16[2,128,1024]{2,1,0:T(8,128)(2,1)} %collective-permute-done.5.refs_1_), channel_id=1, source_target_pairs={{0,4},{4,0},{8,12},{12,8},{16,20},{20,16},{24,28},{28,24},{1,5},{5... | collective-permute-start | bytes 1572872 | tf_op jit(solution)/shard_map/ppermute | solution.py:490
  111.4 6.0 %collective-permute-done.8.came.first_came = bf16[4,144,128]{2,1,0:T(8,128)(2,1)S(1)} collective-permute-done((bf16[4,144,128]{2,1,0:T(8,128)(2,1)}, bf16[4,144,128]{2,1,0:T(8,128)(2,1)S(1)}, u32[]{:S(2)}, u32[]{:S(2)}) %collective-permute-start.8) | collective-permute-done | bytes 147488 | tf_op jit(solution)/shard_map/ppermute | solution.py:490
  117.5 0.9 copy-done.12
  118.4 0.7 copy-done.23
  119.1 0.6 shard_map.189.group
  119.7 1.5 collective-permute-start.9
  121.2 3.7 %collective-permute-done.9.came = bf16[4,144,128]{2,1,0:T(8,128)(2,1)S(1)} collective-permute-done((bf16[4,144,128]{2,1,0:T(8,128)(2,1)S(1)}, bf16[4,144,128]{2,1,0:T(8,128)(2,1)S(1)}, u32[]{:S(2)}, u32[]{:S(2)}) %collective-permute-start.9) | collective-permute-done | bytes 147488 | tf_op jit(solution)/shard_map/ppermute | solution.py:490
  125.0 0.7 copy-done.24
  125.6 0.7 shard_map.190
  126.3 2.1 %collective-permute-start.10 = (bf16[4,144,128]{2,1,0:T(8,128)(2,1)S(1)}, bf16[4,144,128]{2,1,0:T(8,128)(2,1)S(1)}, u32[]{:S(2)}, u32[]{:S(2)}) collective-permute-start(bf16[4,144,128]{2,1,0:T(8,128)(2,1)S(1)} %get-tuple-element.44), channel_id=1, source_target_pairs={{0,16},{4,20},{8,24},{12,28},{16,0},{20,4},{24,8},{28,12},{1,17},{... | collective-permute-start | bytes 442376 | tf_op jit(solution)/shard_map/ppermute | solution.py:490
  128.4 5.6 %collective-permute-done.10.came = bf16[4,144,128]{2,1,0:T(8,128)(2,1)S(1)} collective-permute-done((bf16[4,144,128]{2,1,0:T(8,128)(2,1)S(1)}, bf16[4,144,128]{2,1,0:T(8,128)(2,1)S(1)}, u32[]{:S(2)}, u32[]{:S(2)}) %collective-permute-start.10) | collective-permute-done | bytes 147488 | tf_op jit(solution)/shard_map/ppermute | solution.py:490
  134.0 0.7 shard_map.191
  134.7 0.5 collective-permute-start.11
  135.2 0.7 broadcast_xor_fusion.order
  135.9 0.7 copy-done.25
  136.6 6.3 %weight_grads.1 = (bf16[1,2048,512]{2,1,0:T(8,128)(2,1)}, bf16[1,2048,512]{2,1,0:T(8,128)(2,1)}, bf16[1,512,2048]{2,1,0:T(8,128)(2,1)}) custom-call(s32[2]{0:T(128)S(1)} %copy-done.25, bf16[320,2048]{1,0:T(8,128)(2,1)S(1)} %bitcast.12, bf16[320,2048]{1,0:T(8,128)(2,1)S(1)} %collective-permute-done.rb.gb, bf16[320,2048]{1,0:T(8,128)(2,1)S(1)} %bitcast.13, ...), custom_call_target="tpu_custom_call" | custom-call | tf_op jit(solution)/shard_map/weight_grads/pallas_call | solution.py:207
  142.8 1.6 %local_grads.1 = (bf16[4,128,128]{2,1,0:T(8,128)(2,1)}, f32[4,128,128]{2,1,0:T(8,128)S(1)}, f32[4,128,256]{2,1,0:T(8,128)S(1)}) custom-call(bf16[4,128,128]{2,1,0:T(8,128)(2,1)S(1)} %copy-done.9, bf16[4,128,128]{2,1,0:T(8,128)(2,1)S(1)} %copy-done.11, bf16[4,128,256]{2,1,0:T(8,128)(2,1)S(1)} %copy-done.2, f32[4,128]{1,0:T(4,128)S(1)} %copy-done.27, ...), custom_call_target="tpu_custom_call" | custom-call | tf_op jit(solution)/shard_map/local_grads/pallas_call | solution.py:429
  144.5 1.7 %shard_map.192 = (bf16[4,128,128]{2,1,0:T(8,128)(2,1)}, bf16[4,128,256]{2,1,0:T(8,128)(2,1)}) custom-call(s32[2]{0:T(128)S(1)} %copy-done.25, bf16[4,128,128]{2,1,0:T(8,128)(2,1)S(1)} %copy-done.11, bf16[4,128,256]{2,1,0:T(8,128)(2,1)S(1)} %copy-done.2, f32[4,128]{1,0:T(4,128)S(1)} %copy-done.27, bf16[4,128,128]{2,1,0:T(8,128)(2,1)S(1)} %get-tuple-element.47.own, ...), custom_call_target="tpu_custom_call" | custom-call | tf_op jit(solution)/shard_map/pallas_call | solution.py:407
  146.2 0.8 copy-done.14
  147.0 0.8 copy-done.16
  147.8 1.0 copy-done.15
  148.8 1.0 copy-done.17
  149.9 3.5 %project.1 = f32[256,1024]{1,0:T(8,128)} custom-call(s32[8]{0:T(128)S(1)} %broadcast_xor_fusion.order, bf16[8,128,256]{2,1,0:T(8,128)(2,1)} %all-to-all-done.2.x, bf16[2,128,1024]{2,1,0:T(8,128)(2,1)} %pad_maximum_fusion.refs_0_, bf16[2,128,1024]{2,1,0:T(8,128)(2,1)} %collective-permute-done.5.refs_1_, bf16[2,128,1024]{2,1,0:T(8,128)(2,1)S(1)} %copy-done.15, ...), custom_call_target="tpu_custom_call" | custom-call | tf_op jit(solution)/shard_map/project/pallas_call | solution.py:473
  (58 shorter events, 0.2 us)
Async XLA Ops:
  0.6 44.1 %copy-start = (bf16[1,2048,512]{2,1,0:T(8,128)(2,1)S(1)}, bf16[1,2048,512]{2,1,0:T(8,128)(2,1)}, u32[]{:S(2)}) copy-start(bf16[1,2048,512]{2,1,0:T(8,128)(2,1)} %wg.1) | copy-start | bytes 6291460
  0.7 94.5 %copy-start.22 = (s32[2]{0:T(128)}, s32[2]{0:T(128)S(1)}, u32[]{:S(2)}) copy-start(s32[2]{0:T(128)S(1)} %pad_add_fusion.core.at) | copy-start | bytes 28
  41.7 10.4 %copy-start.1 = (bf16[1,2048,512]{2,1,0:T(8,128)(2,1)S(1)}, bf16[1,2048,512]{2,1,0:T(8,128)(2,1)}, u32[]{:S(2)}) copy-start(bf16[1,2048,512]{2,1,0:T(8,128)(2,1)} %wu.1) | copy-start | bytes 6291460
  41.7 3.0 %collective-permute-start = (bf16[320,2048]{1,0:T(8,128)(2,1)S(1)}, bf16[320,2048]{1,0:T(8,128)(2,1)S(1)}, u32[]{:S(2)}, u32[]{:S(2)}) collective-permute-start(bf16[320,2048]{1,0:T(8,128)(2,1)S(1)} %bitcast.9), channel_id=1, source_target_pairs={{0,1},{1,0},{2,3},{3,2},{4,5},{5,4},{6,7},{7,6},{8,9},{9,8},{10,11... | collective-permute-start | bytes 3932168 | tf_op jit(solution)/shard_map/ppermute | solution.py:490
  51.9 1.9 %copy-start.4 = (bf16[320,512]{1,0:T(8,128)(2,1)}, bf16[320,512]{1,0:T(8,128)(2,1)S(1)}, u32[]{:S(2)}) copy-start(bf16[320,512]{1,0:T(8,128)(2,1)S(1)} %get-tuple-element.32.gback) | copy-start | bytes 983044
  51.9 1.9 %copy-start.6 = (bf16[320,512]{1,0:T(8,128)(2,1)}, bf16[320,512]{1,0:T(8,128)(2,1)S(1)}, u32[]{:S(2)}) copy-start(bf16[320,512]{1,0:T(8,128)(2,1)S(1)} %get-tuple-element.33.uback) | copy-start | bytes 983044
  51.9 1.9 %copy-start.18 = (bf16[320,512]{1,0:T(8,128)(2,1)}, bf16[320,512]{1,0:T(8,128)(2,1)S(1)}, u32[]{:S(2)}) copy-start(bf16[320,512]{1,0:T(8,128)(2,1)S(1)} %get-tuple-element.31.hidden) | copy-start | bytes 983044
  51.9 2.2 %collective-permute-start.1 = (bf16[320,1024]{1,0:T(8,128)(2,1)S(1)}, bf16[320,1024]{1,0:T(8,128)(2,1)S(1)}, u32[]{:S(2)}, u32[]{:S(2)}) collective-permute-start(bf16[320,1024]{1,0:T(8,128)(2,1)S(1)} %get-tuple-element.38), channel_id=1, source_target_pairs={{0,1},{1,0},{2,3},{3,2},{4,5},{5,4},{6,7},{7,6},{8,9},{9,8},{10,11... | collective-permute-start | bytes 1966088 | tf_op jit(solution)/shard_map/ppermute | solution.py:490
  53.9 22.1 %copy-start.21 = (bf16[320,128]{1,0:T(8,128)(2,1)S(1)}, bf16[320,128]{1,0:T(8,128)(2,1)}, u32[]{:S(2)}) copy-start(bf16[320,128]{1,0:T(8,128)(2,1)} %get-tuple-element.37.place) | copy-start | bytes 245764
  53.9 24.6 %copy-start.2 = (bf16[4,128,256]{2,1,0:T(8,128)(2,1)S(1)}, bf16[4,128,256]{2,1,0:T(8,128)(2,1)}, u32[]{:S(2)}) copy-start(bf16[4,128,256]{2,1,0:T(8,128)(2,1)} %v.5) | copy-start | bytes 786436
  53.9 24.6 %copy-start.3 = (f32[4,1,128,256]{3,2,1,0:T(8,128)S(1)}, f32[4,1,128,256]{3,2,1,0:T(8,128)}, u32[]{:S(2)}) copy-start(f32[4,1,128,256]{3,2,1,0:T(8,128)} %state.3) | copy-start | bytes 1572868
  53.9 24.6 %copy-start.8 = (bf16[4,128,128]{2,1,0:T(8,128)(2,1)S(1)}, bf16[4,128,128]{2,1,0:T(8,128)(2,1)}, u32[]{:S(2)}) copy-start(bf16[4,128,128]{2,1,0:T(8,128)(2,1)} %q.5) | copy-start | bytes 393220
  53.9 24.6 %copy-start.10 = (bf16[4,128,128]{2,1,0:T(8,128)(2,1)S(1)}, bf16[4,128,128]{2,1,0:T(8,128)(2,1)}, u32[]{:S(2)}) copy-start(bf16[4,128,128]{2,1,0:T(8,128)(2,1)} %k.5) | copy-start | bytes 393220
  53.9 24.6 %copy-start.26 = (f32[4,128]{1,0:T(4,128)S(1)}, f32[4,128]{1,0:T(4,128)}, u32[]{:S(2)}) copy-start(f32[4,128]{1,0:T(4,128)} %log_decay.7) | copy-start | bytes 6148
  76.9 7.4 %collective-permute-start.2 = (bf16[128,1024]{1,0:T(8,128)(2,1)}, bf16[128,1024]{1,0:T(8,128)(2,1)}, u32[]{:S(2)}, u32[]{:S(2)}) collective-permute-start(bf16[128,1024]{1,0:T(8,128)(2,1)} %combine.1), channel_id=1, source_target_pairs={{0,2},{1,3},{2,0},{3,1},{4,6},{5,7},{6,4},{7,5},{8,10},{9,11},{10,... | collective-permute-start | bytes 786440 | tf_op jit(solution)/shard_map/ppermute | solution.py:490
  79.7 13.6 %collective-permute-start.4 = (bf16[1,128,1024]{2,1,0:T(8,128)(2,1)}, bf16[1,128,1024]{2,1,0:T(8,128)(2,1)}, u32[]{:S(2)}, u32[]{:S(2)}) collective-permute-start(bf16[1,128,1024]{2,1,0:T(8,128)(2,1)} %bitcast.8), channel_id=1, source_target_pairs={{0,16},{4,20},{8,24},{12,28},{16,0},{20,4},{24,8},{28,12},{1,17},{... | collective-permute-start | bytes 786440 | tf_op jit(solution)/shard_map/ppermute | solution.py:490
  85.5 9.7 %collective-permute-start.3 = (bf16[128,1024]{1,0:T(8,128)(2,1)S(1)}, bf16[128,1024]{1,0:T(8,128)(2,1)S(1)}, u32[]{:S(2)}, u32[]{:S(2)}) collective-permute-start(bf16[128,1024]{1,0:T(8,128)(2,1)S(1)} %add_convert_fusion.1.ma), channel_id=1, source_target_pairs={{0,1},{1,0},{2,3},{3,2},{4,5},{5,4},{6,7},{7,6},{8,9},{9,8},{10,11... | collective-permute-start | bytes 786440 | tf_op jit(solution)/shard_map/ppermute | solution.py:490
  95.2 14.4 %collective-permute-start.5 = (bf16[2,128,1024]{2,1,0:T(8,128)(2,1)}, bf16[2,128,1024]{2,1,0:T(8,128)(2,1)}, u32[]{:S(2)}, u32[]{:S(2)}) collective-permute-start(bf16[2,128,1024]{2,1,0:T(8,128)(2,1)} %pad_maximum_fusion.refs_0_), channel_id=1, source_target_pairs={{0,8},{4,12},{8,0},{12,4},{16,24},{20,28},{24,16},{28,20},{1,9},{5... | collective-permute-start | bytes 1572872 | tf_op jit(solution)/shard_map/ppermute | solution.py:490
  100.7 0.7 copy-start.28
  101.4 32.6 %copy-start.13 = (bf16[4,144,128]{2,1,0:T(8,128)(2,1)S(1)}, bf16[4,144,128]{2,1,0:T(8,128)(2,1)}, u32[]{:S(2)}) copy-start(bf16[4,144,128]{2,1,0:T(8,128)(2,1)} %get-tuple-element.42.keep) | copy-start | bytes 442372
  101.4 46.4 %all-to-all-start.2 = ((bf16[8,128,256]{2,1,0:T(8,128)(2,1)}), bf16[8,128,256]{2,1,0:T(8,128)(2,1)}, u32[]{:S(2)}, u32[]{:S(2)}) async-start(bf16[8,128,256]{2,1,0:T(8,128)(2,1)} %get-tuple-element.39), calls=%async_computation.2 | async-start | bytes 1048576 | tf_op jit(solution)/shard_map/all_to_all | solution.py:591
  105.7 30.2 %copy-start.5 = (bf16[320,512]{1,0:T(8,128)(2,1)S(1)}, bf16[320,512]{1,0:T(8,128)(2,1)}, u32[]{:S(2)}) copy-start(bf16[320,512]{1,0:T(8,128)(2,1)} %copy-done.4) | copy-start | bytes 983044
  105.7 30.2 %copy-start.7 = (bf16[320,512]{1,0:T(8,128)(2,1)S(1)}, bf16[320,512]{1,0:T(8,128)(2,1)}, u32[]{:S(2)}) copy-start(bf16[320,512]{1,0:T(8,128)(2,1)} %copy-done.6) | copy-start | bytes 983044
  105.7 11.8 %collective-permute-start.8 = (bf16[4,144,128]{2,1,0:T(8,128)(2,1)}, bf16[4,144,128]{2,1,0:T(8,128)(2,1)S(1)}, u32[]{:S(2)}, u32[]{:S(2)}) collective-permute-start(bf16[4,144,128]{2,1,0:T(8,128)(2,1)} %copy-done.28), channel_id=1, source_target_pairs={{0,4},{4,0},{8,12},{12,8},{16,20},{20,16},{24,28},{28,24},{1,5},{5... | collective-permute-start | bytes 442376 | tf_op jit(solution)/shard_map/ppermute | solution.py:490
  107.7 38.5 %collective-permute-start.6 = (bf16[2,128,1024]{2,1,0:T(8,128)(2,1)}, bf16[2,128,1024]{2,1,0:T(8,128)(2,1)S(1)}, u32[]{:S(2)}, u32[]{:S(2)}) collective-permute-start(bf16[2,128,1024]{2,1,0:T(8,128)(2,1)} %pad_maximum_fusion.refs_0_), channel_id=1, source_target_pairs={{0,4},{4,0},{8,12},{12,8},{16,20},{20,16},{24,28},{28,24},{1,5},{5... | collective-permute-start | bytes 1572872 | tf_op jit(solution)/shard_map/ppermute | solution.py:490
  109.6 37.3 %collective-permute-start.7 = (bf16[2,128,1024]{2,1,0:T(8,128)(2,1)}, bf16[2,128,1024]{2,1,0:T(8,128)(2,1)S(1)}, u32[]{:S(2)}, u32[]{:S(2)}) collective-permute-start(bf16[2,128,1024]{2,1,0:T(8,128)(2,1)} %collective-permute-done.5.refs_1_), channel_id=1, source_target_pairs={{0,4},{4,0},{8,12},{12,8},{16,20},{20,16},{24,28},{28,24},{1,5},{5... | collective-permute-start | bytes 1572872 | tf_op jit(solution)/shard_map/ppermute | solution.py:490
  117.5 0.9 copy-start.12
  118.4 0.7 copy-start.23
  119.1 16.8 %copy-start.19 = (bf16[320,512]{1,0:T(8,128)(2,1)S(1)}, bf16[320,512]{1,0:T(8,128)(2,1)}, u32[]{:S(2)}) copy-start(bf16[320,512]{1,0:T(8,128)(2,1)} %copy-done.18) | copy-start | bytes 983044
  119.7 5.2 %collective-permute-start.9 = (bf16[4,144,128]{2,1,0:T(8,128)(2,1)S(1)}, bf16[4,144,128]{2,1,0:T(8,128)(2,1)S(1)}, u32[]{:S(2)}, u32[]{:S(2)}) collective-permute-start(bf16[4,144,128]{2,1,0:T(8,128)(2,1)S(1)} %shard_map.189.group), channel_id=1, source_target_pairs={{0,8},{4,12},{8,0},{12,4},{16,24},{20,28},{24,16},{28,20},{1,9},{5... | collective-permute-start | bytes 442376 | tf_op jit(solution)/shard_map/ppermute | solution.py:490
  125.0 0.7 copy-start.24
  126.3 7.7 %collective-permute-start.10 = (bf16[4,144,128]{2,1,0:T(8,128)(2,1)S(1)}, bf16[4,144,128]{2,1,0:T(8,128)(2,1)S(1)}, u32[]{:S(2)}, u32[]{:S(2)}) collective-permute-start(bf16[4,144,128]{2,1,0:T(8,128)(2,1)S(1)} %get-tuple-element.44), channel_id=1, source_target_pairs={{0,16},{4,20},{8,24},{12,28},{16,0},{20,4},{24,8},{28,12},{1,17},{... | collective-permute-start | bytes 442376 | tf_op jit(solution)/shard_map/ppermute | solution.py:490
  134.7 9.8 %collective-permute-start.11 = (bf16[4,128,128]{2,1,0:T(8,128)(2,1)S(1)}, bf16[4,128,128]{2,1,0:T(8,128)(2,1)S(1)}, u32[]{:S(2)}, u32[]{:S(2)}) collective-permute-start(bf16[4,128,128]{2,1,0:T(8,128)(2,1)S(1)} %get-tuple-element.48), channel_id=1, source_target_pairs={{0,4},{4,0},{8,12},{12,8},{16,20},{20,16},{24,28},{28,24},{1,5},{5... | collective-permute-start | bytes 393224 | tf_op jit(solution)/shard_map/ppermute | solution.py:490
  135.9 0.7 copy-start.25
  136.5 6.3 %copy-start.9 = (bf16[4,128,128]{2,1,0:T(8,128)(2,1)S(1)}, bf16[4,128,128]{2,1,0:T(8,128)(2,1)}, u32[]{:S(2)}) copy-start(bf16[4,128,128]{2,1,0:T(8,128)(2,1)} %q.5) | copy-start | bytes 393220
  136.5 6.3 %copy-start.11 = (bf16[4,128,128]{2,1,0:T(8,128)(2,1)S(1)}, bf16[4,128,128]{2,1,0:T(8,128)(2,1)}, u32[]{:S(2)}) copy-start(bf16[4,128,128]{2,1,0:T(8,128)(2,1)} %k.5) | copy-start | bytes 393220
  136.5 6.3 %copy-start.20 = (bf16[4,128,256]{2,1,0:T(8,128)(2,1)S(1)}, bf16[4,128,256]{2,1,0:T(8,128)(2,1)}, u32[]{:S(2)}) copy-start(bf16[4,128,256]{2,1,0:T(8,128)(2,1)} %get-tuple-element.40.hg) | copy-start | bytes 786436
  136.5 6.3 %copy-start.27 = (f32[4,128]{1,0:T(4,128)S(1)}, f32[4,128]{1,0:T(4,128)}, u32[]{:S(2)}) copy-start(f32[4,128]{1,0:T(4,128)} %log_decay.7) | copy-start | bytes 6148
  146.2 0.8 copy-start.14
  147.0 0.8 copy-start.16
  147.8 1.0 copy-start.15
  148.8 1.0 copy-start.17

commit v4 on v3

--- a/solution.py
+++ b/solution.py
@@ -31,7 +31,7 @@
     return pltpu.CompilerParams(vmem_limit_bytes=mib << 20)
 
 
-def dispatch_kernel(core, routes, weight, x, g, out, place, *, experts, cap):
+def dispatch_kernel(at, routes, weight, x, g, place, *blocks, experts, cap):
     tokens, half = x.shape
     slots = experts * cap
     expert = iota((experts, tokens), 0)
@@ -43,49 +43,70 @@
     rank_t = dot(named.astype(BF16), before.astype(BF16))
     rank_t = jnp.where(named > 0.5, rank_t, 2.0 * cap)
     slot = iota((slots, experts), 0)
-    base = iota((slots, experts), 1) * cap
+    base = (iota((slots, experts), 1) ^ at[1]) * cap
     owner = (slot >= base) & (slot < base + cap)
     owner_f = jnp.where(owner, 1.0, 0.0)
     number = jnp.sum(jnp.where(owner, slot - base, 0).astype(F32), axis=1, keepdims=True)
-    rank = dot(owner_f.astype(BF16), rank_t.astype(BF16))
-    hit = rank == number
+    hit = dot(owner_f.astype(BF16), rank_t.astype(BF16)) == number
     picked = jnp.where(hit, 1.0, 0.0).astype(BF16)
     share_slot = jnp.sum(
         jnp.where(hit, dot(owner_f, share, precision=EXACT), 0.0), axis=1, keepdims=True
     )
     place[...] = picked
-    out[:, :half] = dot(picked, x[...]).astype(BF16)
-    out[:, half:] = (share_slot * dot(picked, g[...])).astype(BF16)
-
-
-def dispatch(core, routes, weight, x, g, experts, cap):
+    rows = dot(picked, x[...]).astype(BF16)
+    grads = (share_slot * dot(picked, g[...])).astype(BF16)
+    for n, block in enumerate(blocks):
+        block[:, :half] = rows[n * cap : (n + 1) * cap]
+        block[:, half:] = grads[n * cap : (n + 1) * cap]
+
+
+def dispatch(at, routes, weight, x, g, experts, cap):
     tokens, width = x.shape
     half = width // 2
     slots = experts * cap
     whole = lambda i, c: (0, 0)
+    mine = pl.BlockSpec((tokens, half), lambda i, c: (0, c[0]))
     return pl.pallas_call(
         functools.partial(dispatch_kernel, experts=experts, cap=cap),
         grid_spec=pltpu.PrefetchScalarGridSpec(
             num_scalar_prefetch=1,
             grid=(1,),
             in_specs=[
-                pl.BlockSpec(routes.shape, whole),
-                pl.BlockSpec(weight.shape, whole),
-                pl.BlockSpec((tokens, half), lambda i, c: (0, c[0])),
-                pl.BlockSpec((tokens, half), lambda i, c: (0, c[0])),
+                pl.BlockSpec(routes.shape, whole), pl.BlockSpec(weight.shape, whole), mine, mine,
             ],
-            out_specs=[
-                pl.BlockSpec((slots, width), whole),
-                pl.BlockSpec((slots, tokens), whole),
-            ],
+            out_specs=[pl.BlockSpec((slots, tokens), whole)]
+            + [pl.BlockSpec((cap, width), whole)] * experts,
         ),
-        out_shape=[
-            jax.ShapeDtypeStruct((slots, width), BF16),
-            pltpu.HBM((slots, tokens), BF16),
-        ],
-        compiler_params=limit(16),
+        out_shape=[pltpu.HBM((slots, tokens), BF16)]
+        + [pltpu.HBM((cap, width), BF16)] * experts,
+        compiler_params=limit(12),
         name="dispatch",
-    )(core, in_hbm(routes), in_hbm(weight), in_hbm(x), in_hbm(g))
+    )(at, in_hbm(routes), in_hbm(weight), in_hbm(x), in_hbm(g))
+
+
+def gather_kernel(*refs):
+    blocks, out, sems = refs[:-2], refs[-2], refs[-1]
+    copies = [
+        pltpu.make_async_copy(block, out.at[n], sems.at[n]) for n, block in enumerate(blocks)
+    ]
+    for each in copies:
+        each.start()
+    for each in copies:
+        each.wait()
+
+
+def gather(blocks):
+    cap, width = blocks[0].shape
+    out = pl.pallas_call(
+        gather_kernel,
+        in_specs=[pl.BlockSpec(memory_space=pltpu.HBM)] * len(blocks),
+        out_specs=pl.BlockSpec(memory_space=pltpu.VMEM),
+        out_shape=jax.ShapeDtypeStruct((len(blocks), cap, width), BF16),
+        scratch_shapes=[pltpu.SemaphoreType.DMA((len(blocks),))],
+        compiler_params=limit(4),
+        name="gather",
+    )(*[in_hbm(block) for block in blocks])
+    return out.reshape(len(blocks) * cap, width)
 
 
 def expert_kernel(
@@ -172,6 +193,17 @@
         compiler_params=limit(12),
         name="expert_part",
     )(core, gback, uback, w_gate, w_up)
+
+
+def add_blocks_kernel(at, a, b, *blocks):
+    cap = blocks[0].shape[0]
+    for n, block in enumerate(blocks):
+        cut = slice(n * cap, (n + 1) * cap)
+        block[...] = (a[cut, :].astype(F32) + b[cut, :].astype(F32)).astype(BF16)
+
+
+def add_kernel(at, a, b, out):
+    out[...] = (a[...].astype(F32) + b[...].astype(F32)).astype(out.dtype)
 
 
 def weights_kernel(core, ra, rb, ga, gb, hidden, gback, uback, gate_out, up_out, down_out):
@@ -228,17 +260,46 @@
     )(core, own, other, own, other, hidden, gback, uback)
 
 
-def combine_kernel(place, back, out):
-    out[...] = dot(place[...], back[...], 0, 0).astype(BF16)
-
-
-def combine(place, back):
+def combine_kernel(at, place, *refs):
+    blocks, out = refs[:-1], refs[-1]
+    cap = blocks[0].shape[0]
+    total = None
+    for n, block in enumerate(blocks):
+        part = dot(place[n * cap : (n + 1) * cap, :], block[...], 0, 0)
+        total = part if total is None else total + part
+    out[...] = total.astype(BF16)
+
+
+def base_kernel(at, g, part, wo, out, near, sem):
+    half = part.shape[1]
+    begin = pl.multiple_of(at[0] * half, half)
+    copy = pltpu.make_async_copy(wo.at[pl.ds(begin, half), :], near, sem)
+    copy.start()
+    out[...] = g[...].astype(F32) + part[...].astype(F32)
+    copy.wait()
+
+
+def base_sum(at, g, part, w_out):
+    tokens, half = part.shape
+    whole = lambda i, c: (0, 0)
+    near = (half, w_out.shape[1])
     return pl.pallas_call(
-        combine_kernel,
-        out_shape=jax.ShapeDtypeStruct((place.shape[1], back.shape[1]), BF16),
-        compiler_params=limit(8),
-        name="combine",
-    )(place, back)
+        base_kernel,
+        grid_spec=pltpu.PrefetchScalarGridSpec(
+            num_scalar_prefetch=1,
+            grid=(1,),
+            in_specs=[
+                pl.BlockSpec((tokens, half), lambda i, c: (0, c[0])),
+                pl.BlockSpec((tokens, half), whole),
+                pl.BlockSpec(memory_space=pltpu.HBM),
+            ],
+            out_specs=[pl.BlockSpec((tokens, half), whole), pl.BlockSpec(memory_space=pltpu.VMEM)],
+            scratch_shapes=[pltpu.SemaphoreType.DMA],
+        ),
+        out_shape=[jax.ShapeDtypeStruct((tokens, half), F32), pltpu.VMEM(near, BF16)],
+        compiler_params=limit(4),
+        name="base",
+    )(at, in_hbm(g), part, in_hbm(w_out))
 
 
 def decays(log_decay, head):
@@ -256,7 +317,7 @@
     return table, jnp.exp(down), jnp.exp(total - down), total
 
 
-def mixed_kernel(q, k, v, log_decay, state, mixed):
+def mixed_kernel(at, q, k, v, log_decay, state, mixed):
     heads, _, size = q.shape
     width = v.shape[2]
     scale = size**-0.5
@@ -267,16 +328,6 @@
         mixed[:, h * width : (h + 1) * width] = out.astype(BF16)
 
 
-def mixed_heads(q, k, v, log_decay, state):
-    heads, span, _ = q.shape
-    return pl.pallas_call(
-        mixed_kernel,
-        out_shape=jax.ShapeDtypeStruct((span, heads * v.shape[2]), BF16),
-        compiler_params=limit(8),
-        name="mixed_heads",
-    )(q, k, v, log_decay, state)
-
-
 PIECES = 16
 
 
@@ -301,65 +352,74 @@
     return ref[h, :size, :].astype(F32), decay
 
 
-def carry_kernel(at, ma, mb, wa, wb, q, log_decay, hg, keep, send, slices, *, groups):
-    head = pl.program_id(0)
-    h_grad = (dot(ma[...], wa[...]) + dot(mb[...], wb[...])).astype(BF16)
-    hg[...] = h_grad
-    span = log_decay.shape[-1]
-    own = log_decay[pl.ds(head, 1), :]
+def carry_kernel(
+    at, ma, mb, near, q_in, decay_in, wo, hg, keep, send, slices, far, q, log_decay, sems
+):
+    heads, span, _ = q.shape
+    groups, rows, size = slices.shape
+    width = hg.shape[2]
+    half = width // 2
+    tall = ma.shape[1]
+    begin = pl.multiple_of((1 - at[0]) * tall, tall)
+    copies = [
+        pltpu.make_async_copy(decay_in, log_decay, sems.at[heads + 1]),
+        pltpu.make_async_copy(q_in, q, sems.at[heads]),
+    ]
+    for h in range(heads):
+        cut = slice(h * width, (h + 1) * width)
+        copies.append(
+            pltpu.make_async_copy(wo.at[pl.ds(begin, tall), cut], far.at[:, cut], sems.at[h])
+        )
+    for each in copies:
+        each.start()
+    mine = pl.ds(pl.multiple_of(at[0] * rows, rows), rows)
+    turn = groups // 2
+    for i in range(turn):
+        slices[at[0] * turn + i] = ma[mine, i * size : (i + 1) * size]
+        slices[(1 - at[0]) * turn + i] = mb[mine, i * size : (i + 1) * size]
+    upper = (at[1] & 1) == 1
     lower = jnp.where(iota((span, span), 0) >= iota((span, span), 1), 1.0, 0.0)
-    lead = jnp.exp(jnp.sum(lower * own, axis=1, keepdims=True))
-    total = jnp.exp(jnp.sum(own, axis=1, keepdims=True))
-    part = dot((q[...].astype(F32) * lead).astype(BF16), h_grad, 0, 0)
-    half = part.shape[1] // 2
-    upper = (at[1] & 1) == 1
-    put_message(keep, 0, jnp.where(upper, part[:, half:], part[:, :half]), total)
-    put_message(send, 0, jnp.where(upper, part[:, :half], part[:, half:]), total)
-
-    @pl.when(head == 0)
-    def _():
-        size = slices.shape[2]
-        turn = groups // 2
-        for i in range(turn):
-            slices[at[0] * turn + i] = ma[:, i * size : (i + 1) * size]
-            slices[(1 - at[0]) * turn + i] = mb[:, i * size : (i + 1) * size]
-
-
-def carry(at, ma, mb, w_out, q, log_decay, groups, value_size):
+    copies[0].wait()
+    copies[1].wait()
+    for h in range(heads):
+        cut = slice(h * width, (h + 1) * width)
+        first = dot(ma[...], near[:, cut])
+        copies[2 + h].wait()
+        h_grad = (first + dot(mb[...], far[:, cut])).astype(BF16)
+        hg[h] = h_grad
+        own = log_decay[h : h + 1, :]
+        lead = jnp.exp(jnp.sum(lower * own, axis=1, keepdims=True))
+        total = jnp.exp(jnp.sum(own, axis=1, keepdims=True))
+        part = dot((q[h].astype(F32) * lead).astype(BF16), h_grad, 0, 0)
+        put_message(keep, h, jnp.where(upper, part[:, half:], part[:, :half]), total)
+        put_message(send, h, jnp.where(upper, part[:, :half], part[:, half:]), total)
+
+
+def carry(at, ma, mb, near, w_out, q, log_decay, groups, value_size):
     span, half = ma.shape
     heads, _, size = q.shape
-    whole = lambda h, c: (0, 0)
-    by_head = lambda h, c: (h, 0, 0)
-    message = (size + PIECES, value_size // 2)
+    message = (heads, size + PIECES, value_size // 2)
+    inside = pl.BlockSpec(memory_space=pltpu.VMEM)
+    outside = pl.BlockSpec(memory_space=pltpu.HBM)
     return pl.pallas_call(
-        functools.partial(carry_kernel, groups=groups),
-        grid_spec=pltpu.PrefetchScalarGridSpec(
-            num_scalar_prefetch=1,
-            grid=(heads,),
-            in_specs=[
-                pl.BlockSpec((span, half), whole),
-                pl.BlockSpec((span, half), whole),
-                pl.BlockSpec((half, value_size), lambda h, c: (c[0], h)),
-                pl.BlockSpec((half, value_size), lambda h, c: (1 - c[0], h)),
-                pl.BlockSpec((None, span, size), by_head),
-                pl.BlockSpec(log_decay.shape, whole),
-            ],
-            out_specs=[
-                pl.BlockSpec((None, span, value_size), by_head),
-                pl.BlockSpec((1,) + message, by_head),
-                pl.BlockSpec((1,) + message, by_head),
-                pl.BlockSpec((groups, span, 2 * half // groups), lambda h, c: (0, 0, 0)),
-            ],
-        ),
+        carry_kernel,
+        in_specs=[pl.BlockSpec(memory_space=pltpu.SMEM)] + [inside] * 3 + [outside] * 3,
+        out_specs=[pl.BlockSpec()] * 4,
         out_shape=[
             pltpu.HBM((heads, span, value_size), BF16),
-            pltpu.HBM((heads,) + message, BF16),
-            jax.ShapeDtypeStruct((heads,) + message, BF16),
-            pltpu.HBM((groups, span, 2 * half // groups), BF16),
+            jax.ShapeDtypeStruct(message, BF16),
+            jax.ShapeDtypeStruct(message, BF16),
+            pltpu.HBM((groups, span // 2, 2 * half // groups), BF16),
+        ],
+        scratch_shapes=[
+            pltpu.VMEM((half, heads * value_size), BF16),
+            pltpu.VMEM(q.shape, BF16),
+            pltpu.VMEM(log_decay.shape, F32),
+            pltpu.SemaphoreType.DMA((heads + 2,)),
         ],
         compiler_params=limit(12),
         name="carry",
-    )(at, ma, mb, in_hbm(w_out), in_hbm(w_out), in_hbm(q), log_decay)
+    )(at, ma, mb, near, in_hbm(q), in_hbm(log_decay), in_hbm(w_out))
 
 
 def pair_kernel(at, keep, came, out):
@@ -402,17 +462,19 @@
         send[h] = jnp.where(right, through, after).astype(BF16)
 
 
-def small(kernel, outs, at, *operands):
-    spec = pl.BlockSpec(memory_space=pltpu.VMEM)
+def small(kernel, outs, at, *operands, mib=8):
+    spec = pl.BlockSpec()
+    many = isinstance(outs, (list, tuple))
     return pl.pallas_call(
         kernel,
         in_specs=[pl.BlockSpec(memory_space=pltpu.SMEM)] + [spec] * len(operands),
+        out_specs=[spec] * len(outs) if many else spec,
         out_shape=outs,
-        compiler_params=limit(8),
+        compiler_params=limit(mib),
     )(at, *operands)
 
 
-def local_kernel(q, k, v, log_decay, state, hg, q_grad, k_part, v_part):
+def local_kernel(at, q, k, v, log_decay, state, hg, q_grad, k_part, v_part):
     heads, _, size = q.shape
     scale = size**-0.5
     for h in range(heads):
@@ -423,19 +485,6 @@
         q_grad[h] = (scale * dot(back, k[h]) + lead * from_state).astype(BF16)
         k_part[h] = dot(back, q[h], 0, 0)
         v_part[h] = dot(scores, hg[h], 0, 0)
-
-
-def local_grads(q, k, v, log_decay, state, hg):
-    return pl.pallas_call(
-        local_kernel,
-        out_shape=[
-            jax.ShapeDtypeStruct(q.shape, BF16),
-            jax.ShapeDtypeStruct(k.shape, F32),
-            jax.ShapeDtypeStruct(v.shape, F32),
-        ],
-        compiler_params=limit(12),
-        name="local_grads",
-    )(q, k, v, log_decay, state, hg)
 
 
 def final_kernel(at, k, v, log_decay, own, came, k_part, v_part, k_grad, v_grad):
@@ -454,40 +503,53 @@
         v_grad[h, :, half:] = (v_part[h, :, half:] + strength * dot(k[h], high)).astype(BF16)
 
 
-def project_kernel(order, x, *refs):
-    out = refs[-1]
+def project_kernel(order, core, xa, xb, *refs):
+    out, x = refs[-2:]
+    rows = xa.shape[1]
+
+    @pl.when(pl.program_id(0) == 0)
+    def _():
+        x[:, pl.ds(pl.multiple_of(core[0] * rows, rows), rows), :] = xa[...]
+        x[:, pl.ds(pl.multiple_of((1 - core[0]) * rows, rows), rows), :] = xb[...]
+
     total, at = None, 0
-    for y in refs[:-1]:
+    for y in refs[:-2]:
         blocks, span, width = y.shape
-        rows = jnp.concatenate([x[order[at + i]] for i in range(blocks)], axis=0)
-        part = dot(rows, y[...].reshape(blocks * span, width), 0, 0)
+        left = jnp.concatenate([x[order[at + i]] for i in range(blocks)], axis=0)
+        part = dot(left, y[...].reshape(blocks * span, width), 0, 0)
         total = part if total is None else total + part
         at += blocks
     out[...] = total
 
 
-def project(order, x, parts):
-    groups, span, size = x.shape
+def project(order, at, xa, xb, parts):
+    groups, rows, size = xa.shape
     width = parts[0].shape[2]
     chunk = min(width, 512)
+    piece = pl.BlockSpec((groups, rows, size), lambda i, *_: (0, 0, 0))
     return pl.pallas_call(
         project_kernel,
         grid_spec=pltpu.PrefetchScalarGridSpec(
-            num_scalar_prefetch=1,
+            num_scalar_prefetch=2,
             grid=(width // chunk,),
-            in_specs=[pl.BlockSpec((groups, span, size), lambda i, o: (0, 0, 0))]
-            + [pl.BlockSpec(y.shape[:2] + (chunk,), lambda i, o: (0, 0, i)) for y in parts],
-            out_specs=pl.BlockSpec((size, chunk), lambda i, o: (0, i)),
+            in_specs=[piece, piece]
+            + [pl.BlockSpec(y.shape[:2] + (chunk,), lambda i, *_: (0, 0, i)) for y in parts],
+            out_specs=pl.BlockSpec((size, chunk), lambda i, *_: (0, i)),
+            scratch_shapes=[pltpu.VMEM((groups, 2 * rows, size), BF16)],
         ),
         out_shape=jax.ShapeDtypeStruct((size, width), F32),
         compiler_params=limit(16),
         name="project",
-    )(order, x, *parts)
+    )(order, at, xa, xb, *parts)
 
 
 def swap(a, axis, bit):
     count = lax.axis_size(axis)
     return lax.ppermute(a, axis, [(i, i ^ bit) for i in range(count)])
+
+
+def far_first(count):
+    return list(range(count // 2, count)) + list(range(count // 2 - 1, 0, -1))
 
 
 def bits_of(count):
@@ -514,27 +576,31 @@
     sp = lax.axis_size("sp")
     tp = lax.axis_size("tp")
     place = lax.axis_index("sp").astype(jnp.int32)
-    core = (lax.axis_index("tp") & 1).astype(jnp.int32)
-    at = jnp.stack([core, place])
+    column = lax.axis_index("tp").astype(jnp.int32)
+    core = column & 1
+    at = jnp.stack([core, place, (column >> 1) & 1])
     experts = w_gate.shape[0] * sp
     cap = 5 * tokens * routes.shape[1] // (4 * experts)
     heads, _, size = query_heads.shape
     value_size = value_heads.shape[-1]
 
-    def exchange(a):
-        wide = a.shape[1]
-        a = a.reshape(experts, cap, wide)
-        return lax.all_to_all(a, "sp", split_axis=0, concat_axis=0, tiled=True).reshape(-1, wide)
-
-    sent, picked = dispatch(at, routes.T, route_weight.T, moe_input, out_grad, experts, cap)
-    own = exchange(sent)
+    picked, *sent = dispatch(at, routes.T, route_weight.T, moe_input, out_grad, experts, cap)
+    came = {0: sent[0]}
+    for n in far_first(sp):
+        came[n] = swap(sent[n], "sp", n)
+    mixed = small(
+        mixed_kernel, jax.ShapeDtypeStruct((tokens, heads * value_size), BF16),
+        at, *[in_hbm(a) for a in (query_heads, key_heads, value_heads, log_decay, state_in)],
+    )
+    own = gather([came[n] for n in range(sp)])
     other = swap(own, "tp", 1)
-    mixed = mixed_heads(query_heads, key_heads, value_heads, log_decay, state_in)
     hidden, gate_back, up_back, part_b = expert_back(at, own, other, w_gate, w_up, w_down)
     part_came = swap(part_b, "tp", 1)
     part_a = expert_part(at, gate_back, up_back, w_gate, w_up)
-    part = (part_a.astype(F32) + part_came.astype(F32)).astype(BF16)
-    returned = exchange(part)
+    parts_out = small(add_blocks_kernel, [pltpu.HBM((cap, half), BF16)] * sp, at, part_a, part_came)
+    back = {0: parts_out[0]}
+    for n in far_first(sp):
+        back[n] = swap(parts_out[n], "sp", n)
     gate_grad, up_grad, down_grad = weight_grads(at, own, other, hidden, gate_back, up_back)
 
     blocks = mixed[None]
@@ -550,25 +616,32 @@
         offsets = offsets + [o ^ bit for o in offsets]
     order = (place ^ jnp.array(offsets, jnp.int32)).astype(jnp.int32)
 
-    token_part = combine(picked, returned)
+    token_shape = jax.ShapeDtypeStruct((tokens, half), BF16)
+    token_part = small(combine_kernel, token_shape, at, in_hbm(picked), *[in_hbm(back[n]) for n in range(sp)])
     for bit in bits_of(tp)[1:]:
         came = swap(token_part, "tp", bit)
-        token_part = token_part.astype(F32) + came.astype(F32)
         if bit * 2 < tp:
-            token_part = token_part.astype(BF16)
-        else:
-            own_grad = lax.dynamic_slice_in_dim(out_grad, core * half, half, axis=1)
-            mixed_a = (own_grad.astype(F32) + token_part).astype(BF16)
+            token_part = (token_part.astype(F32) + came.astype(F32)).astype(BF16)
+    base, near_out = base_sum(at, out_grad, token_part, w_out)
+    mixed_a = small(add_kernel, token_shape, at, base, came)
     mixed_b = swap(mixed_a, "tp", 1)
 
+    message = jax.ShapeDtypeStruct((heads, size + PIECES, value_size // 2), BF16)
     head_grad, keep, send, slices = carry(
-        at, mixed_a, mixed_b, w_out, query_heads, log_decay, sp, value_size
+        at, mixed_a, mixed_b, near_out, w_out, query_heads, log_decay, sp, value_size
     )
     first_came = swap(send, "sp", 1)
-    q_grad, k_part, v_part = local_grads(
-        query_heads, key_heads, value_heads, log_decay, state_in, head_grad
+    q_grad, k_part, v_part = small(
+        local_kernel,
+        [
+            jax.ShapeDtypeStruct(query_heads.shape, BF16),
+            jax.ShapeDtypeStruct(key_heads.shape, F32),
+            jax.ShapeDtypeStruct(value_heads.shape, F32),
+        ],
+        at,
+        *[in_hbm(a) for a in (query_heads, key_heads, value_heads, log_decay, state_in, head_grad)],
+        mib=12,
     )
-    message = jax.ShapeDtypeStruct(keep.shape, BF16)
     state_shape = (heads, size, value_size // 2)
     group = small(pair_kernel, message, at, keep, first_came)
     later = jnp.zeros(state_shape, F32)
@@ -588,8 +661,9 @@
         [state_out, state_out], at, came_state, later, reach, keep, first_came,
     )
     other_state = swap(send_state, "sp", 1)
-    slices = lax.all_to_all(slices, "sp", split_axis=0, concat_axis=0, tiled=True)
-    out_proj_grad = project(order, slices, parts)
+    slices_a = lax.all_to_all(slices, "sp", split_axis=0, concat_axis=0, tiled=True)
+    slices_b = swap(slices_a, "tp", 1)
+    out_proj_grad = project(order, at, slices_a, slices_b, parts)
     k_grad, v_grad = small(
         final_kernel,
         [jax.ShapeDtypeStruct(key_heads.shape, BF16),

time: 154 us -> 155 us (level)
  blocking collectives: 60 us -> 0 us
  starting transfers between devices: 15 us -> 48.9 us
  waiting for transfers between devices: 31.7 us -> 50.3 us
  Pallas kernels: 34.2 us -> 44.9 us
  other arithmetic: 4.08 us -> 0.13 us
  local copies, waits for them, and re-layouts: 7.39 us -> 9.19 us
    all_to_all x2 -> x0, blocking collectives: 60 us -> none  [exchange(): lax.all_to_all(a, 'sp', split_axis=0, concat_axis=0, tiled=True)]
    ppermute x12 -> x27, starting transfers between devices: 10.8 us -> 43.2 us  [swap(): return lax.ppermute(a, axis, [(i, i ^ bit) for i in range(count)])]
    ppermute x12 -> x27, waiting for transfers between devices: 31.7 us -> 50.3 us  [swap(): return lax.ppermute(a, axis, [(i, i ^ bit) for i in range(count)])]
    pallas_call x4 -> x9, Pallas kernels: 3.65 us -> 13.5 us  [small(): pl.pallas_call(kernel, in_specs=[pl.BlockSpec(memory_space=pltpu.SMEM)] +...]
    concatenate x1, other arithmetic: 1.88 us -> 0.05 us  [step(): parts = [jnp.concatenate([blocks, swap(blocks, 'sp', bit)], axis=0)]]
    unnamed x58 -> x64, local copies, waits for them, and re-layouts: 7.37 us -> 9.17 us
    pallas_call x4 -> x3, Pallas kernels: 9.44 us -> 9.38 us  [the longest x1 4.82 us: carry(): pl.pallas_call(carry_kernel, in_specs=[pl.BlockSpec(memory_space=pltpu.SM...]
  transfers between devices with their start and end apart: 13 -> 28, of which waited for: 8 -> 13; matrix products, arithmetic and copies ran while one was open for 2% -> 0% of each run, Pallas kernels for 13% -> 19%
where the time goes in v4:
time: 155 us; the launch traced here: 154 us
  waiting for transfers between devices  50.3 us (32%)
  starting transfers between devices  48.9 us (32%)
  Pallas kernels  44.9 us (29%)
  local copies, waits for them, and re-layouts  9.19 us (6%)
    ppermute x27, waiting for transfers between devices, swap(): return lax.ppermute(a, axis, [(i, i ^ bit) for i in range(count)])  50.3 us
    ppermute x27, starting transfers between devices, swap(): return lax.ppermute(a, axis, [(i, i ^ bit) for i in range(count)])  43.2 us
    pallas_call x9, Pallas kernels, small(): pl.pallas_call(kernel, in_specs=[pl.BlockSpec(memory_space=pltpu.SMEM)] +...  13.5 us
    unnamed x64, local copies, waits for them, and re-layouts  9.17 us
    pallas_call x1, Pallas kernels, expert_back(): pl.pallas_call(expert_kernel, grid_spec=pltpu.PrefetchScalarGridSpec(num_...  7.1 us
    pallas_call x1, Pallas kernels, weight_grads(): pl.pallas_call(weights_kernel, grid_spec=pltpu.PrefetchScalarGridSpec(num...  6.29 us
    all_to_all x1, starting transfers between devices, step(): lax.all_to_all(slices, 'sp', split_axis=0, concat_axis=0, tiled=True)  5.7 us
    pallas_call x1, Pallas kernels, carry(): pl.pallas_call(carry_kernel, in_specs=[pl.BlockSpec(memory_space=pltpu.SM...  4.82 us
  transfers between devices with their start and end apart: 28, of which 13 were waited for; matrix products, arithmetic and copies ran while one was open for 0% of the time, Pallas kernels for 19%

profile of v4, /device:TPU:0, one launch (start us, length us, event | category | flops | bytes accessed | tf_op | source)
XLA Modules:
  0.0 154.3 jit_solution(11579015698815578651)
XLA Ops:
  0.7 3.4 %dispatch.1 = (bf16[320,128]{1,0:T(8,128)(2,1)}, bf16[40,2048]{1,0:T(8,128)(2,1)}, bf16[40,2048]{1,0:T(8,128)(2,1)}, bf16[40,2048]{1,0:T(8,128)(2,1)}, bf16[40,2...) custom-call(s32[3]{0:T(128)S(1)} %pad_add_fusion.at.core, ...), custom_call_target="tpu_custom_call" | custom-call | tf_op jit(solution)/shard_map/dispatch/pallas_call | solution.py:69
  4.1 3.0 %collective-permute-start = (bf16[40,2048]{1,0:T(8,128)(2,1)}, bf16[40,2048]{1,0:T(8,128)(2,1)S(1)}, u32[]{:S(2)}, u32[]{:S(2)}) collective-permute-start(bf16[40,2048]{1,0:T(8,128)(2,1)} %get-tuple-element.48), channel_id=1, source_target_pairs={{0,4},{4,0},{8,12},{12,8},{16,20},{20,16},{24,28},{28,24},{1,5},{5... | collective-permute-start | bytes 491528 | tf_op jit(solution)/shard_map/ppermute | solution.py:548
  7.1 1.6 %collective-permute-start.1 = (bf16[40,2048]{1,0:T(8,128)(2,1)}, bf16[40,2048]{1,0:T(8,128)(2,1)S(1)}, u32[]{:S(2)}, u32[]{:S(2)}) collective-permute-start(bf16[40,2048]{1,0:T(8,128)(2,1)} %get-tuple-element.49), channel_id=1, source_target_pairs={{0,8},{4,12},{8,0},{12,4},{16,24},{20,28},{24,16},{28,20},{1,9},{5... | collective-permute-start | bytes 491528 | tf_op jit(solution)/shard_map/ppermute | solution.py:548
  8.7 3.0 %collective-permute-start.3 = (bf16[40,2048]{1,0:T(8,128)(2,1)}, bf16[40,2048]{1,0:T(8,128)(2,1)S(1)}, u32[]{:S(2)}, u32[]{:S(2)}) collective-permute-start(bf16[40,2048]{1,0:T(8,128)(2,1)} %get-tuple-element.51), channel_id=1, source_target_pairs={{0,16},{4,20},{8,24},{12,28},{16,0},{20,4},{24,8},{28,12},{1,17},{... | collective-permute-start | bytes 491528 | tf_op jit(solution)/shard_map/ppermute | solution.py:548
  11.7 1.3 collective-permute-start.4
  12.9 3.6 %collective-permute-start.5 = (bf16[40,2048]{1,0:T(8,128)(2,1)}, bf16[40,2048]{1,0:T(8,128)(2,1)S(1)}, u32[]{:S(2)}, u32[]{:S(2)}) collective-permute-start(bf16[40,2048]{1,0:T(8,128)(2,1)} %get-tuple-element.53), channel_id=1, source_target_pairs={{0,24},{4,28},{8,16},{12,20},{16,8},{20,12},{24,0},{28,4},{1,25},{... | collective-permute-start | bytes 491528 | tf_op jit(solution)/shard_map/ppermute | solution.py:548
  16.5 3.8 %collective-permute-done.1.refs_2_ = bf16[40,2048]{1,0:T(8,128)(2,1)S(1)} collective-permute-done((bf16[40,2048]{1,0:T(8,128)(2,1)}, bf16[40,2048]{1,0:T(8,128)(2,1)S(1)}, u32[]{:S(2)}, u32[]{:S(2)}) %collective-permute-start.1) | collective-permute-done | bytes 163872 | tf_op jit(solution)/shard_map/ppermute | solution.py:548
  20.3 1.2 collective-permute-start.6
  21.9 13.6 %collective-permute-done.4.refs_5_ = bf16[40,2048]{1,0:T(8,128)(2,1)S(1)} collective-permute-done((bf16[40,2048]{1,0:T(8,128)(2,1)}, bf16[40,2048]{1,0:T(8,128)(2,1)S(1)}, u32[]{:S(2)}, u32[]{:S(2)}) %collective-permute-start.4) | collective-permute-done | bytes 163872 | tf_op jit(solution)/shard_map/ppermute | solution.py:548
  36.2 1.5 gather.1
  37.8 3.0 %collective-permute-done.7.rb.gb = bf16[320,2048]{1,0:T(8,128)(2,1)S(1)} collective-permute-done((bf16[320,2048]{1,0:T(8,128)(2,1)S(1)}, bf16[320,2048]{1,0:T(8,128)(2,1)S(1)}, u32[]{:S(2)}, u32[]{:S(2)}) %collective-permute-start.7) | collective-permute-done | bytes 1310752 | tf_op jit(solution)/shard_map/ppermute | solution.py:548
  40.8 7.1 %expert.1 = (bf16[320,512]{1,0:T(8,128)(2,1)S(1)}, bf16[320,512]{1,0:T(8,128)(2,1)S(1)}, bf16[320,512]{1,0:T(8,128)(2,1)S(1)}, bf16[320,1024]{1,0:T(8,128)(2,1)S(1)}) custom-call(s32[3]{0:T(128)S(1)} %pad_add_fusion.at.core, bf16[320,2048]{1,0:T(8,128)(2,1)S(1)} %bitcast.8, bf16[320,2048]{1,0:T(8,128)(2,1)S(1)} %collective-permute-done.7.rb.gb, ...), custom_call_target="tpu_custom_call" | custom-call | tf_op jit(solution)/shard_map/expert/pallas_call | solution.py:158
  48.1 1.8 %shard_map.192 = bf16[128,1024]{1,0:T(8,128)(2,1)S(1)} custom-call(s32[3]{0:T(128)S(1)} %pad_add_fusion.at.core, bf16[4,128,128]{2,1,0:T(8,128)(2,1)} %q.3, bf16[4,128,128]{2,1,0:T(8,128)(2,1)} %k.5, bf16[4,128,256]{2,1,0:T(8,128)(2,1)} %v.5, f32[4,128]{1,0:T(4,128)} %log_decay.5, f32[4,1,128,256]{3,2,1,0:T(8,128)} %state.3), custom_call_target="tpu_custom_call" | custom-call | tf_op jit(solution)/shard_map/pallas_call | solution.py:468
  50.0 8.0 %collective-permute-start.19 = (bf16[1,128,1024]{2,1,0:T(8,128)(2,1)S(1)}, bf16[1,128,1024]{2,1,0:T(8,128)(2,1)S(1)}, u32[]{:S(2)}, u32[]{:S(2)}) collective-permute-start(bf16[1,128,1024]{2,1,0:T(8,128)(2,1)S(1)} %bitcast.12), channel_id=1, source_target_pairs={{0,16},{4,20},{8,24},{12,28},{16,0},{20,4},{24,8},{28,12},{1,17},{... | collective-permute-start | bytes 786440 | tf_op jit(solution)/shard_map/ppermute | solution.py:548
  58.0 1.7 %expert_part.1.a = bf16[320,1024]{1,0:T(8,128)(2,1)S(1)} custom-call(s32[3]{0:T(128)S(1)} %pad_add_fusion.at.core, bf16[320,512]{1,0:T(8,128)(2,1)S(1)} %get-tuple-element.56.gback, bf16[320,512]{1,0:T(8,128)(2,1)S(1)} %get-tuple-element.57.uback, bf16[1,2048,512]{2,1,0:T(8,128)(2,1)S(1)} %copy-done, bf16[1,2048,512]{2,1,0:T(8,128)(2,1)S(1)} %copy-done.1), custom_call_target="tpu_custom_call" | custom-call | tf_op jit(solution)/shard_map/expert_part/pallas_call | solution.py:184
  59.7 1.4 shard_map.189
  61.7 3.0 %collective-permute-start.11 = (bf16[40,1024]{1,0:T(8,128)(2,1)}, bf16[40,1024]{1,0:T(8,128)(2,1)S(1)}, u32[]{:S(2)}, u32[]{:S(2)}) collective-permute-start(bf16[40,1024]{1,0:T(8,128)(2,1)} %get-tuple-element.66), channel_id=1, source_target_pairs={{0,12},{4,8},{8,4},{12,0},{16,28},{20,24},{24,20},{28,16},{1,13},{... | collective-permute-start | bytes 245768 | tf_op jit(solution)/shard_map/ppermute | solution.py:548
  64.7 1.1 collective-permute-done.9.refs_1_
  65.8 1.7 %collective-permute-start.13 = (bf16[40,1024]{1,0:T(8,128)(2,1)}, bf16[40,1024]{1,0:T(8,128)(2,1)S(1)}, u32[]{:S(2)}, u32[]{:S(2)}) collective-permute-start(bf16[40,1024]{1,0:T(8,128)(2,1)} %get-tuple-element.68), channel_id=1, source_target_pairs={{0,20},{4,16},{8,28},{12,24},{16,4},{20,0},{24,12},{28,8},{1,21},{... | collective-permute-start | bytes 245768 | tf_op jit(solution)/shard_map/ppermute | solution.py:548
  67.5 2.7 %collective-permute-done.10.refs_2_ = bf16[40,1024]{1,0:T(8,128)(2,1)S(1)} collective-permute-done((bf16[40,1024]{1,0:T(8,128)(2,1)}, bf16[40,1024]{1,0:T(8,128)(2,1)S(1)}, u32[]{:S(2)}, u32[]{:S(2)}) %collective-permute-start.10) | collective-permute-done | bytes 81952 | tf_op jit(solution)/shard_map/ppermute | solution.py:548
  70.2 1.9 %collective-permute-done.11.refs_3_ = bf16[40,1024]{1,0:T(8,128)(2,1)S(1)} collective-permute-done((bf16[40,1024]{1,0:T(8,128)(2,1)}, bf16[40,1024]{1,0:T(8,128)(2,1)S(1)}, u32[]{:S(2)}, u32[]{:S(2)}) %collective-permute-start.11) | collective-permute-done | bytes 81952 | tf_op jit(solution)/shard_map/ppermute | solution.py:548
  72.2 2.2 %collective-permute-start.15 = (bf16[40,1024]{1,0:T(8,128)(2,1)}, bf16[40,1024]{1,0:T(8,128)(2,1)S(1)}, u32[]{:S(2)}, u32[]{:S(2)}) collective-permute-start(bf16[40,1024]{1,0:T(8,128)(2,1)} %get-tuple-element.70), channel_id=1, source_target_pairs={{0,28},{4,24},{8,20},{12,16},{16,12},{20,8},{24,4},{28,0},{1,29},{... | collective-permute-start | bytes 245768 | tf_op jit(solution)/shard_map/ppermute | solution.py:548
  74.4 5.1 %collective-permute-done.12.refs_4_ = bf16[40,1024]{1,0:T(8,128)(2,1)S(1)} collective-permute-done((bf16[40,1024]{1,0:T(8,128)(2,1)}, bf16[40,1024]{1,0:T(8,128)(2,1)S(1)}, u32[]{:S(2)}, u32[]{:S(2)}) %collective-permute-start.12) | collective-permute-done | bytes 81952 | tf_op jit(solution)/shard_map/ppermute | solution.py:548
  79.5 1.8 %collective-permute-done.13.refs_5_ = bf16[40,1024]{1,0:T(8,128)(2,1)S(1)} collective-permute-done((bf16[40,1024]{1,0:T(8,128)(2,1)}, bf16[40,1024]{1,0:T(8,128)(2,1)S(1)}, u32[]{:S(2)}, u32[]{:S(2)}) %collective-permute-start.13) | collective-permute-done | bytes 81952 | tf_op jit(solution)/shard_map/ppermute | solution.py:548
  82.0 1.9 %shard_map.190.part = bf16[128,1024]{1,0:T(8,128)(2,1)S(1)} custom-call(s32[3]{0:T(128)S(1)} %pad_add_fusion.at.core, bf16[320,128]{1,0:T(8,128)(2,1)} %get-tuple-element.61.place, bf16[40,1024]{1,0:T(8,128)(2,1)} %get-tuple-element.63.refs_0_, bf16[40,1024]{1,0:T(8,128)(2,1)} %copy-done.24, bf16[40,1024]{1,0:T(8,128)(2,1)} %copy-done.25, ...), custom_call_target="tpu_custom_call" | custom-call | tf_op jit(solution)/shard_map/pallas_call | solution.py:468
  83.9 1.6 %collective-permute-start.16 = (bf16[128,1024]{1,0:T(8,128)(2,1)S(1)}, bf16[128,1024]{1,0:T(8,128)(2,1)S(1)}, u32[]{:S(2)}, u32[]{:S(2)}) collective-permute-start(bf16[128,1024]{1,0:T(8,128)(2,1)S(1)} %shard_map.190.part), channel_id=1, source_target_pairs={{0,2},{1,3},{2,0},{3,1},{4,6},{5,7},{6,4},{7,5},{8,10},{9,11},{10,... | collective-permute-start | bytes 786440 | tf_op jit(solution)/shard_map/ppermute | solution.py:548
  85.6 3.8 %collective-permute-start.20 = (bf16[2,128,1024]{2,1,0:T(8,128)(2,1)S(1)}, bf16[2,128,1024]{2,1,0:T(8,128)(2,1)}, u32[]{:S(2)}, u32[]{:S(2)}) collective-permute-start(bf16[2,128,1024]{2,1,0:T(8,128)(2,1)S(1)} %pad_maximum_fusion.refs_0_), channel_id=1, source_target_pairs={{0,8},{4,12},{8,0},{12,4},{16,24},{20,28},{24,16},{28,20},{1,9},{5... | collective-permute-start | bytes 1572872 | tf_op jit(solution)/shard_map/ppermute | solution.py:548
  89.3 3.1 %base.1 = (f32[128,1024]{1,0:T(8,128)S(1)}, bf16[1024,1024]{1,0:T(8,128)(2,1)S(1)}) custom-call(s32[3]{0:T(128)S(1)} %pad_add_fusion.at.core, bf16[128,2048]{1,0:T(8,128)(2,1)} %g.3, bf16[128,1024]{1,0:T(8,128)(2,1)S(1)} %shard_map.190.part, bf16[2048,1024]{1,0:T(8,128)(2,1)} %wo.3), custom_call_target="tpu_custom_call" | custom-call | tf_op jit(solution)/shard_map/base/pallas_call | solution.py:286
  93.1 1.5 collective-permute-done.17.mb
  94.7 4.8 %carry.1 = (bf16[4,128,256]{2,1,0:T(8,128)(2,1)}, bf16[4,144,128]{2,1,0:T(8,128)(2,1)S(1)}, bf16[4,144,128]{2,1,0:T(8,128)(2,1)S(1)}, bf16[8,64,256]{2,1,0:T(8,128)(2,1)}) custom-call(s32[3]{0:T(128)S(1)} %pad_add_fusion.at.core, bf16[128,1024]{1,0:T(8,128)(2,1)S(1)} %shard_map.191.ma, bf16[128,1024]{1,0:T(8,128)(2,1)S(1)} %collective-permute-done.17.mb, ...), custom_call_target="tpu_custom_call" | custom-call | tf_op jit(solution)/shard_map/carry/pallas_call | solution.py:404
  100.8 5.7 %all-to-all-start = ((bf16[8,64,256]{2,1,0:T(8,128)(2,1)}), bf16[8,64,256]{2,1,0:T(8,128)(2,1)}, u32[]{:S(2)}, u32[]{:S(2)}) async-start(bf16[8,64,256]{2,1,0:T(8,128)(2,1)} %get-tuple-element.73), calls=%async_computation | async-start | bytes 524288 | tf_op jit(solution)/shard_map/all_to_all | solution.py:664
  106.5 2.0 %collective-permute-start.23 = (bf16[4,144,128]{2,1,0:T(8,128)(2,1)}, bf16[4,144,128]{2,1,0:T(8,128)(2,1)S(1)}, u32[]{:S(2)}, u32[]{:S(2)}) collective-permute-start(bf16[4,144,128]{2,1,0:T(8,128)(2,1)} %copy-done.16), channel_id=1, source_target_pairs={{0,4},{4,0},{8,12},{12,8},{16,20},{20,16},{24,28},{28,24},{1,5},{5... | collective-permute-start | bytes 442376 | tf_op jit(solution)/shard_map/ppermute | solution.py:548
  108.6 2.0 %collective-permute-start.22 = (bf16[2,128,1024]{2,1,0:T(8,128)(2,1)}, bf16[2,128,1024]{2,1,0:T(8,128)(2,1)}, u32[]{:S(2)}, u32[]{:S(2)}) collective-permute-start(bf16[2,128,1024]{2,1,0:T(8,128)(2,1)} %collective-permute-done.20.refs_1_), channel_id=1, source_target_pairs={{0,4},{4,0},{8,12},{12,8},{16,20},{20,16},{24,28},{28,24},{1,5},{5... | collective-permute-start | bytes 1572872 | tf_op jit(solution)/shard_map/ppermute | solution.py:548
  110.6 5.7 %collective-permute-done.23.came.first_came = bf16[4,144,128]{2,1,0:T(8,128)(2,1)S(1)} collective-permute-done((bf16[4,144,128]{2,1,0:T(8,128)(2,1)}, bf16[4,144,128]{2,1,0:T(8,128)(2,1)S(1)}, u32[]{:S(2)}, u32[]{:S(2)}) %collective-permute-start.23) | collective-permute-done | bytes 147488 | tf_op jit(solution)/shard_map/ppermute | solution.py:548
  116.3 1.0 copy-done.7
  117.9 1.5 collective-permute-start.24
  119.4 3.7 %collective-permute-done.24.came = bf16[4,144,128]{2,1,0:T(8,128)(2,1)S(1)} collective-permute-done((bf16[4,144,128]{2,1,0:T(8,128)(2,1)S(1)}, bf16[4,144,128]{2,1,0:T(8,128)(2,1)S(1)}, u32[]{:S(2)}, u32[]{:S(2)}) %collective-permute-start.24) | collective-permute-done | bytes 147488 | tf_op jit(solution)/shard_map/ppermute | solution.py:548
  123.1 1.3 shard_map.195
  125.1 2.0 %collective-permute-start.25 = (bf16[4,144,128]{2,1,0:T(8,128)(2,1)}, bf16[4,144,128]{2,1,0:T(8,128)(2,1)}, u32[]{:S(2)}, u32[]{:S(2)}) collective-permute-start(bf16[4,144,128]{2,1,0:T(8,128)(2,1)} %get-tuple-element.78), channel_id=1, source_target_pairs={{0,16},{4,20},{8,24},{12,28},{16,0},{20,4},{24,8},{28,12},{1,17},{... | collective-permute-start | bytes 442376 | tf_op jit(solution)/shard_map/ppermute | solution.py:548
  127.2 5.9 %collective-permute-done.25.came = bf16[4,144,128]{2,1,0:T(8,128)(2,1)} collective-permute-done((bf16[4,144,128]{2,1,0:T(8,128)(2,1)}, bf16[4,144,128]{2,1,0:T(8,128)(2,1)}, u32[]{:S(2)}, u32[]{:S(2)}) %collective-permute-start.25) | collective-permute-done | bytes 147488 | tf_op jit(solution)/shard_map/ppermute | solution.py:548
  134.9 0.9 copy-done.14
  135.9 1.1 shard_map.196
  137.8 1.0 copy-done.4
  138.7 1.0 copy-done.12
  139.7 6.3 %weight_grads.1 = (bf16[1,2048,512]{2,1,0:T(8,128)(2,1)}, bf16[1,2048,512]{2,1,0:T(8,128)(2,1)}, bf16[1,512,2048]{2,1,0:T(8,128)(2,1)}) custom-call(s32[3]{0:T(128)S(1)} %pad_add_fusion.at.core, bf16[320,2048]{1,0:T(8,128)(2,1)S(1)} %bitcast.10, bf16[320,2048]{1,0:T(8,128)(2,1)S(1)} %collective-permute-done.7.rb.gb, bf16[320,2048]{1,0:T(8,128)(2,1)S(1)} %bitcast.11, ...), custom_call_target="tpu_custom_call" | custom-call | tf_op jit(solution)/shard_map/weight_grads/pallas_call | solution.py:239
  146.0 3.0 %shard_map.193 = (bf16[4,128,128]{2,1,0:T(8,128)(2,1)}, f32[4,128,128]{2,1,0:T(8,128)S(1)}, f32[4,128,256]{2,1,0:T(8,128)S(1)}) custom-call(s32[3]{0:T(128)S(1)} %pad_add_fusion.at.core, bf16[4,128,128]{2,1,0:T(8,128)(2,1)} %q.3, bf16[4,128,128]{2,1,0:T(8,128)(2,1)} %k.5, bf16[4,128,256]{2,1,0:T(8,128)(2,1)} %v.5, f32[4,128]{1,0:T(4,128)} %log_decay.5, ...), custom_call_target="tpu_custom_call" | custom-call | tf_op jit(solution)/shard_map/pallas_call | solution.py:468
  149.0 1.7 %shard_map.197 = (bf16[4,128,128]{2,1,0:T(8,128)(2,1)}, bf16[4,128,256]{2,1,0:T(8,128)(2,1)}) custom-call(s32[3]{0:T(128)S(1)} %pad_add_fusion.at.core, bf16[4,128,128]{2,1,0:T(8,128)(2,1)S(1)} %copy-done.5, bf16[4,128,256]{2,1,0:T(8,128)(2,1)S(1)} %copy-done.2, f32[4,128]{1,0:T(4,128)S(1)} %copy-done.15, bf16[4,128,128]{2,1,0:T(8,128)(2,1)S(1)} %get-tuple-element.81.own, ...), custom_call_target="tpu_custom_call" | custom-call | tf_op jit(solution)/shard_map/pallas_call | solution.py:468
  150.7 3.6 %project.1 = f32[256,1024]{1,0:T(8,128)} custom-call(s32[8]{0:T(128)S(1)} %broadcast_xor_fusion.order, s32[3]{0:T(128)S(1)} %pad_add_fusion.at.core, bf16[8,64,256]{2,1,0:T(8,128)(2,1)} %all-to-all-done.xa, bf16[8,64,256]{2,1,0:T(8,128)(2,1)S(1)} %collective-permute-done.18.xb, bf16[2,128,1024]{2,1,0:T(8,128)(2,1)S(1)} %pad_maximum_fusion.refs_0_, ...), custom_call_target="tpu_custom_call" | custom-call | tf_op jit(solution)/shard_map/project/pallas_call | solution.py:530
  (94 shorter events, 8.9 us)
Async XLA Ops:
  0.6 40.2 %copy-start = (bf16[1,2048,512]{2,1,0:T(8,128)(2,1)S(1)}, bf16[1,2048,512]{2,1,0:T(8,128)(2,1)}, u32[]{:S(2)}) copy-start(bf16[1,2048,512]{2,1,0:T(8,128)(2,1)} %wg.1) | copy-start | bytes 6291460
  4.1 8.8 %collective-permute-start = (bf16[40,2048]{1,0:T(8,128)(2,1)}, bf16[40,2048]{1,0:T(8,128)(2,1)S(1)}, u32[]{:S(2)}, u32[]{:S(2)}) collective-permute-start(bf16[40,2048]{1,0:T(8,128)(2,1)} %get-tuple-element.48), channel_id=1, source_target_pairs={{0,4},{4,0},{8,12},{12,8},{16,20},{20,16},{24,28},{28,24},{1,5},{5... | collective-permute-start | bytes 491528 | tf_op jit(solution)/shard_map/ppermute | solution.py:548
  7.1 13.3 %collective-permute-start.1 = (bf16[40,2048]{1,0:T(8,128)(2,1)}, bf16[40,2048]{1,0:T(8,128)(2,1)S(1)}, u32[]{:S(2)}, u32[]{:S(2)}) collective-permute-start(bf16[40,2048]{1,0:T(8,128)(2,1)} %get-tuple-element.49), channel_id=1, source_target_pairs={{0,8},{4,12},{8,0},{12,4},{16,24},{20,28},{24,16},{28,20},{1,9},{5... | collective-permute-start | bytes 491528 | tf_op jit(solution)/shard_map/ppermute | solution.py:548
  8.6 13.2 %collective-permute-start.2 = (bf16[40,2048]{1,0:T(8,128)(2,1)}, bf16[40,2048]{1,0:T(8,128)(2,1)S(1)}, u32[]{:S(2)}, u32[]{:S(2)}) collective-permute-start(bf16[40,2048]{1,0:T(8,128)(2,1)} %get-tuple-element.50), channel_id=1, source_target_pairs={{0,12},{4,8},{8,4},{12,0},{16,28},{20,24},{24,20},{28,16},{1,13},{... | collective-permute-start | bytes 491528 | tf_op jit(solution)/shard_map/ppermute | solution.py:548
  8.7 13.2 %collective-permute-start.3 = (bf16[40,2048]{1,0:T(8,128)(2,1)}, bf16[40,2048]{1,0:T(8,128)(2,1)S(1)}, u32[]{:S(2)}, u32[]{:S(2)}) collective-permute-start(bf16[40,2048]{1,0:T(8,128)(2,1)} %get-tuple-element.51), channel_id=1, source_target_pairs={{0,16},{4,20},{8,24},{12,28},{16,0},{20,4},{24,8},{28,12},{1,17},{... | collective-permute-start | bytes 491528 | tf_op jit(solution)/shard_map/ppermute | solution.py:548
  11.7 23.8 %collective-permute-start.4 = (bf16[40,2048]{1,0:T(8,128)(2,1)}, bf16[40,2048]{1,0:T(8,128)(2,1)S(1)}, u32[]{:S(2)}, u32[]{:S(2)}) collective-permute-start(bf16[40,2048]{1,0:T(8,128)(2,1)} %get-tuple-element.52), channel_id=1, source_target_pairs={{0,20},{4,16},{8,28},{12,24},{16,4},{20,0},{24,12},{28,8},{1,21},{... | collective-permute-start | bytes 491528 | tf_op jit(solution)/shard_map/ppermute | solution.py:548
  12.9 22.5 %copy-start.17 = (bf16[40,2048]{1,0:T(8,128)(2,1)}, bf16[40,2048]{1,0:T(8,128)(2,1)S(1)}, u32[]{:S(2)}) copy-start(bf16[40,2048]{1,0:T(8,128)(2,1)S(1)} %collective-permute-done.refs_1_) | copy-start | bytes 491524
  12.9 22.5 %collective-permute-start.5 = (bf16[40,2048]{1,0:T(8,128)(2,1)}, bf16[40,2048]{1,0:T(8,128)(2,1)S(1)}, u32[]{:S(2)}, u32[]{:S(2)}) collective-permute-start(bf16[40,2048]{1,0:T(8,128)(2,1)} %get-tuple-element.53), channel_id=1, source_target_pairs={{0,24},{4,28},{8,16},{12,20},{16,8},{20,12},{24,0},{28,4},{1,25},{... | collective-permute-start | bytes 491528 | tf_op jit(solution)/shard_map/ppermute | solution.py:548
  20.3 15.1 %copy-start.18 = (bf16[40,2048]{1,0:T(8,128)(2,1)}, bf16[40,2048]{1,0:T(8,128)(2,1)S(1)}, u32[]{:S(2)}) copy-start(bf16[40,2048]{1,0:T(8,128)(2,1)S(1)} %collective-permute-done.1.refs_2_) | copy-start | bytes 491524
  20.3 15.1 %collective-permute-start.6 = (bf16[40,2048]{1,0:T(8,128)(2,1)}, bf16[40,2048]{1,0:T(8,128)(2,1)S(1)}, u32[]{:S(2)}, u32[]{:S(2)}) collective-permute-start(bf16[40,2048]{1,0:T(8,128)(2,1)} %get-tuple-element.54), channel_id=1, source_target_pairs={{0,28},{4,24},{8,20},{12,16},{16,12},{20,8},{24,4},{28,0},{1,29},{... | collective-permute-start | bytes 491528 | tf_op jit(solution)/shard_map/ppermute | solution.py:548
  21.9 13.6 %copy-start.19 = (bf16[40,2048]{1,0:T(8,128)(2,1)}, bf16[40,2048]{1,0:T(8,128)(2,1)S(1)}, u32[]{:S(2)}) copy-start(bf16[40,2048]{1,0:T(8,128)(2,1)S(1)} %collective-permute-done.2.refs_3_) | copy-start | bytes 491524
  21.9 13.6 %copy-start.20 = (bf16[40,2048]{1,0:T(8,128)(2,1)}, bf16[40,2048]{1,0:T(8,128)(2,1)S(1)}, u32[]{:S(2)}) copy-start(bf16[40,2048]{1,0:T(8,128)(2,1)S(1)} %collective-permute-done.3.refs_4_) | copy-start | bytes 491524
  37.7 3.1 %collective-permute-start.7 = (bf16[320,2048]{1,0:T(8,128)(2,1)S(1)}, bf16[320,2048]{1,0:T(8,128)(2,1)S(1)}, u32[]{:S(2)}, u32[]{:S(2)}) collective-permute-start(bf16[320,2048]{1,0:T(8,128)(2,1)S(1)} %bitcast.7), channel_id=1, source_target_pairs={{0,1},{1,0},{2,3},{3,2},{4,5},{5,4},{6,7},{7,6},{8,9},{9,8},{10,11... | collective-permute-start | bytes 3932168 | tf_op jit(solution)/shard_map/ppermute | solution.py:548
  40.8 17.2 %copy-start.1 = (bf16[1,2048,512]{2,1,0:T(8,128)(2,1)S(1)}, bf16[1,2048,512]{2,1,0:T(8,128)(2,1)}, u32[]{:S(2)}) copy-start(bf16[1,2048,512]{2,1,0:T(8,128)(2,1)} %wu.1) | copy-start | bytes 6291460
  47.9 11.8 %copy-start.3 = (bf16[320,512]{1,0:T(8,128)(2,1)}, bf16[320,512]{1,0:T(8,128)(2,1)S(1)}, u32[]{:S(2)}) copy-start(bf16[320,512]{1,0:T(8,128)(2,1)S(1)} %get-tuple-element.57.uback) | copy-start | bytes 983044
  47.9 11.8 %copy-start.11 = (bf16[320,512]{1,0:T(8,128)(2,1)}, bf16[320,512]{1,0:T(8,128)(2,1)S(1)}, u32[]{:S(2)}) copy-start(bf16[320,512]{1,0:T(8,128)(2,1)S(1)} %get-tuple-element.55.hidden) | copy-start | bytes 983044
  47.9 11.8 %collective-permute-start.8 = (bf16[320,1024]{1,0:T(8,128)(2,1)S(1)}, bf16[320,1024]{1,0:T(8,128)(2,1)S(1)}, u32[]{:S(2)}, u32[]{:S(2)}) collective-permute-start(bf16[320,1024]{1,0:T(8,128)(2,1)S(1)} %get-tuple-element.62), channel_id=1, source_target_pairs={{0,1},{1,0},{2,3},{3,2},{4,5},{5,4},{6,7},{7,6},{8,9},{9,8},{10,11... | collective-permute-start | bytes 1966088 | tf_op jit(solution)/shard_map/ppermute | solution.py:548
  50.0 35.6 %collective-permute-start.19 = (bf16[1,128,1024]{2,1,0:T(8,128)(2,1)S(1)}, bf16[1,128,1024]{2,1,0:T(8,128)(2,1)S(1)}, u32[]{:S(2)}, u32[]{:S(2)}) collective-permute-start(bf16[1,128,1024]{2,1,0:T(8,128)(2,1)S(1)} %bitcast.12), channel_id=1, source_target_pairs={{0,16},{4,20},{8,24},{12,28},{16,0},{20,4},{24,8},{28,12},{1,17},{... | collective-permute-start | bytes 786440 | tf_op jit(solution)/shard_map/ppermute | solution.py:548
  61.2 4.7 %collective-permute-start.9 = (bf16[40,1024]{1,0:T(8,128)(2,1)}, bf16[40,1024]{1,0:T(8,128)(2,1)S(1)}, u32[]{:S(2)}, u32[]{:S(2)}) collective-permute-start(bf16[40,1024]{1,0:T(8,128)(2,1)} %get-tuple-element.64), channel_id=1, source_target_pairs={{0,4},{4,0},{8,12},{12,8},{16,20},{20,16},{24,28},{28,24},{1,5},{5... | collective-permute-start | bytes 245768 | tf_op jit(solution)/shard_map/ppermute | solution.py:548
  61.7 8.5 %collective-permute-start.10 = (bf16[40,1024]{1,0:T(8,128)(2,1)}, bf16[40,1024]{1,0:T(8,128)(2,1)S(1)}, u32[]{:S(2)}, u32[]{:S(2)}) collective-permute-start(bf16[40,1024]{1,0:T(8,128)(2,1)} %get-tuple-element.65), channel_id=1, source_target_pairs={{0,8},{4,12},{8,0},{12,4},{16,24},{20,28},{24,16},{28,20},{1,9},{5... | collective-permute-start | bytes 245768 | tf_op jit(solution)/shard_map/ppermute | solution.py:548
  61.7 10.5 %collective-permute-start.11 = (bf16[40,1024]{1,0:T(8,128)(2,1)}, bf16[40,1024]{1,0:T(8,128)(2,1)S(1)}, u32[]{:S(2)}, u32[]{:S(2)}) collective-permute-start(bf16[40,1024]{1,0:T(8,128)(2,1)} %get-tuple-element.66), channel_id=1, source_target_pairs={{0,12},{4,8},{8,4},{12,0},{16,28},{20,24},{24,20},{28,16},{1,13},{... | collective-permute-start | bytes 245768 | tf_op jit(solution)/shard_map/ppermute | solution.py:548
  64.7 14.8 %collective-permute-start.12 = (bf16[40,1024]{1,0:T(8,128)(2,1)}, bf16[40,1024]{1,0:T(8,128)(2,1)S(1)}, u32[]{:S(2)}, u32[]{:S(2)}) collective-permute-start(bf16[40,1024]{1,0:T(8,128)(2,1)} %get-tuple-element.67), channel_id=1, source_target_pairs={{0,16},{4,20},{8,24},{12,28},{16,0},{20,4},{24,8},{28,12},{1,17},{... | collective-permute-start | bytes 245768 | tf_op jit(solution)/shard_map/ppermute | solution.py:548
  65.8 15.5 %copy-start.24 = (bf16[40,1024]{1,0:T(8,128)(2,1)}, bf16[40,1024]{1,0:T(8,128)(2,1)S(1)}, u32[]{:S(2)}) copy-start(bf16[40,1024]{1,0:T(8,128)(2,1)S(1)} %collective-permute-done.9.refs_1_) | copy-start | bytes 245764
  65.8 15.5 %collective-permute-start.13 = (bf16[40,1024]{1,0:T(8,128)(2,1)}, bf16[40,1024]{1,0:T(8,128)(2,1)S(1)}, u32[]{:S(2)}, u32[]{:S(2)}) collective-permute-start(bf16[40,1024]{1,0:T(8,128)(2,1)} %get-tuple-element.68), channel_id=1, source_target_pairs={{0,20},{4,16},{8,28},{12,24},{16,4},{20,0},{24,12},{28,8},{1,21},{... | collective-permute-start | bytes 245768 | tf_op jit(solution)/shard_map/ppermute | solution.py:548
  70.2 11.1 %copy-start.25 = (bf16[40,1024]{1,0:T(8,128)(2,1)}, bf16[40,1024]{1,0:T(8,128)(2,1)S(1)}, u32[]{:S(2)}) copy-start(bf16[40,1024]{1,0:T(8,128)(2,1)S(1)} %collective-permute-done.10.refs_2_) | copy-start | bytes 245764
  70.2 11.1 %collective-permute-start.14 = (bf16[40,1024]{1,0:T(8,128)(2,1)}, bf16[40,1024]{1,0:T(8,128)(2,1)S(1)}, u32[]{:S(2)}, u32[]{:S(2)}) collective-permute-start(bf16[40,1024]{1,0:T(8,128)(2,1)} %get-tuple-element.69), channel_id=1, source_target_pairs={{0,24},{4,28},{8,16},{12,20},{16,8},{20,12},{24,0},{28,4},{1,25},{... | collective-permute-start | bytes 245768 | tf_op jit(solution)/shard_map/ppermute | solution.py:548
  72.2 9.2 %copy-start.26 = (bf16[40,1024]{1,0:T(8,128)(2,1)}, bf16[40,1024]{1,0:T(8,128)(2,1)S(1)}, u32[]{:S(2)}) copy-start(bf16[40,1024]{1,0:T(8,128)(2,1)S(1)} %collective-permute-done.11.refs_3_) | copy-start | bytes 245764
  72.2 9.1 %collective-permute-start.15 = (bf16[40,1024]{1,0:T(8,128)(2,1)}, bf16[40,1024]{1,0:T(8,128)(2,1)S(1)}, u32[]{:S(2)}, u32[]{:S(2)}) collective-permute-start(bf16[40,1024]{1,0:T(8,128)(2,1)} %get-tuple-element.70), channel_id=1, source_target_pairs={{0,28},{4,24},{8,20},{12,16},{16,12},{20,8},{24,4},{28,0},{1,29},{... | collective-permute-start | bytes 245768 | tf_op jit(solution)/shard_map/ppermute | solution.py:548
  79.5 1.9 %copy-start.27 = (bf16[40,1024]{1,0:T(8,128)(2,1)}, bf16[40,1024]{1,0:T(8,128)(2,1)S(1)}, u32[]{:S(2)}) copy-start(bf16[40,1024]{1,0:T(8,128)(2,1)S(1)} %collective-permute-done.12.refs_4_) | copy-start | bytes 245764
  83.9 8.5 %collective-permute-start.16 = (bf16[128,1024]{1,0:T(8,128)(2,1)S(1)}, bf16[128,1024]{1,0:T(8,128)(2,1)S(1)}, u32[]{:S(2)}, u32[]{:S(2)}) collective-permute-start(bf16[128,1024]{1,0:T(8,128)(2,1)S(1)} %shard_map.190.part), channel_id=1, source_target_pairs={{0,2},{1,3},{2,0},{3,1},{4,6},{5,7},{6,4},{7,5},{8,10},{9,11},{10,... | collective-permute-start | bytes 786440 | tf_op jit(solution)/shard_map/ppermute | solution.py:548
  85.6 23.0 %collective-permute-start.20 = (bf16[2,128,1024]{2,1,0:T(8,128)(2,1)S(1)}, bf16[2,128,1024]{2,1,0:T(8,128)(2,1)}, u32[]{:S(2)}, u32[]{:S(2)}) collective-permute-start(bf16[2,128,1024]{2,1,0:T(8,128)(2,1)S(1)} %pad_maximum_fusion.refs_0_), channel_id=1, source_target_pairs={{0,8},{4,12},{8,0},{12,4},{16,24},{20,28},{24,16},{28,20},{1,9},{5... | collective-permute-start | bytes 1572872 | tf_op jit(solution)/shard_map/ppermute | solution.py:548
  93.0 1.6 %collective-permute-start.17 = (bf16[128,1024]{1,0:T(8,128)(2,1)S(1)}, bf16[128,1024]{1,0:T(8,128)(2,1)S(1)}, u32[]{:S(2)}, u32[]{:S(2)}) collective-permute-start(bf16[128,1024]{1,0:T(8,128)(2,1)S(1)} %shard_map.191.ma), channel_id=1, source_target_pairs={{0,1},{1,0},{2,3},{3,2},{4,5},{5,4},{6,7},{7,6},{8,9},{9,8},{10,11... | collective-permute-start | bytes 786440 | tf_op jit(solution)/shard_map/ppermute | solution.py:548
  100.8 36.9 %copy-start.31 = (s32[8]{0:T(128)S(1)}, s32[8]{0:T(128)}, u32[]{:S(2)}) copy-start(s32[8]{0:T(128)} %constant.17.clone) | copy-start | bytes 100
  100.8 26.3 %all-to-all-start = ((bf16[8,64,256]{2,1,0:T(8,128)(2,1)}), bf16[8,64,256]{2,1,0:T(8,128)(2,1)}, u32[]{:S(2)}, u32[]{:S(2)}) async-start(bf16[8,64,256]{2,1,0:T(8,128)(2,1)} %get-tuple-element.73), calls=%async_computation | async-start | bytes 524288 | tf_op jit(solution)/shard_map/all_to_all | solution.py:664
  106.5 9.7 %collective-permute-start.23 = (bf16[4,144,128]{2,1,0:T(8,128)(2,1)}, bf16[4,144,128]{2,1,0:T(8,128)(2,1)S(1)}, u32[]{:S(2)}, u32[]{:S(2)}) collective-permute-start(bf16[4,144,128]{2,1,0:T(8,128)(2,1)} %copy-done.16), channel_id=1, source_target_pairs={{0,4},{4,0},{8,12},{12,8},{16,20},{20,16},{24,28},{28,24},{1,5},{5... | collective-permute-start | bytes 442376 | tf_op jit(solution)/shard_map/ppermute | solution.py:548
  108.5 42.1 %collective-permute-start.21 = (bf16[2,128,1024]{2,1,0:T(8,128)(2,1)S(1)}, bf16[2,128,1024]{2,1,0:T(8,128)(2,1)}, u32[]{:S(2)}, u32[]{:S(2)}) collective-permute-start(bf16[2,128,1024]{2,1,0:T(8,128)(2,1)S(1)} %pad_maximum_fusion.refs_0_), channel_id=1, source_target_pairs={{0,4},{4,0},{8,12},{12,8},{16,20},{20,16},{24,28},{28,24},{1,5},{5... | collective-permute-start | bytes 1572872 | tf_op jit(solution)/shard_map/ppermute | solution.py:548
  108.6 42.1 %collective-permute-start.22 = (bf16[2,128,1024]{2,1,0:T(8,128)(2,1)}, bf16[2,128,1024]{2,1,0:T(8,128)(2,1)}, u32[]{:S(2)}, u32[]{:S(2)}) collective-permute-start(bf16[2,128,1024]{2,1,0:T(8,128)(2,1)} %collective-permute-done.20.refs_1_), channel_id=1, source_target_pairs={{0,4},{4,0},{8,12},{12,8},{16,20},{20,16},{24,28},{28,24},{1,5},{5... | collective-permute-start | bytes 1572872 | tf_op jit(solution)/shard_map/ppermute | solution.py:548
  116.3 3.2 %copy-start.9 = (bf16[4,144,128]{2,1,0:T(8,128)(2,1)}, bf16[4,144,128]{2,1,0:T(8,128)(2,1)S(1)}, u32[]{:S(2)}) copy-start(bf16[4,144,128]{2,1,0:T(8,128)(2,1)S(1)} %collective-permute-done.23.came.first_came) | copy-start | bytes 442372
  116.3 1.0 copy-start.7
  117.9 5.2 %collective-permute-start.24 = (bf16[4,144,128]{2,1,0:T(8,128)(2,1)S(1)}, bf16[4,144,128]{2,1,0:T(8,128)(2,1)S(1)}, u32[]{:S(2)}, u32[]{:S(2)}) collective-permute-start(bf16[4,144,128]{2,1,0:T(8,128)(2,1)S(1)} %shard_map.194.group), channel_id=1, source_target_pairs={{0,8},{4,12},{8,0},{12,4},{16,24},{20,28},{24,16},{28,20},{1,9},{5... | collective-permute-start | bytes 442376 | tf_op jit(solution)/shard_map/ppermute | solution.py:548
  125.1 7.9 %collective-permute-start.25 = (bf16[4,144,128]{2,1,0:T(8,128)(2,1)}, bf16[4,144,128]{2,1,0:T(8,128)(2,1)}, u32[]{:S(2)}, u32[]{:S(2)}) collective-permute-start(bf16[4,144,128]{2,1,0:T(8,128)(2,1)} %get-tuple-element.78), channel_id=1, source_target_pairs={{0,16},{4,20},{8,24},{12,28},{16,0},{20,4},{24,8},{28,12},{1,17},{... | collective-permute-start | bytes 442376 | tf_op jit(solution)/shard_map/ppermute | solution.py:548
  127.2 23.5 %collective-permute-start.18 = (bf16[8,64,256]{2,1,0:T(8,128)(2,1)}, bf16[8,64,256]{2,1,0:T(8,128)(2,1)S(1)}, u32[]{:S(2)}, u32[]{:S(2)}) collective-permute-start(bf16[8,64,256]{2,1,0:T(8,128)(2,1)} %all-to-all-done.xa), channel_id=1, source_target_pairs={{0,1},{1,0},{2,3},{3,2},{4,5},{5,4},{6,7},{7,6},{8,9},{9,8},{10,11... | collective-permute-start | bytes 786440 | tf_op jit(solution)/shard_map/ppermute | solution.py:548
  136.9 12.1 %collective-permute-start.26 = (bf16[4,128,128]{2,1,0:T(8,128)(2,1)S(1)}, bf16[4,128,128]{2,1,0:T(8,128)(2,1)S(1)}, u32[]{:S(2)}, u32[]{:S(2)}) collective-permute-start(bf16[4,128,128]{2,1,0:T(8,128)(2,1)S(1)} %get-tuple-element.82), channel_id=1, source_target_pairs={{0,4},{4,0},{8,12},{12,8},{16,20},{20,16},{24,28},{28,24},{1,5},{5... | collective-permute-start | bytes 393224 | tf_op jit(solution)/shard_map/ppermute | solution.py:548
  137.8 1.0 copy-start.4
  138.7 1.0 copy-start.12
  139.7 9.3 %copy-start.2 = (bf16[4,128,256]{2,1,0:T(8,128)(2,1)S(1)}, bf16[4,128,256]{2,1,0:T(8,128)(2,1)}, u32[]{:S(2)}) copy-start(bf16[4,128,256]{2,1,0:T(8,128)(2,1)} %v.5) | copy-start | bytes 786436
  139.7 9.3 %copy-start.5 = (bf16[4,128,128]{2,1,0:T(8,128)(2,1)S(1)}, bf16[4,128,128]{2,1,0:T(8,128)(2,1)}, u32[]{:S(2)}) copy-start(bf16[4,128,128]{2,1,0:T(8,128)(2,1)} %k.5) | copy-start | bytes 393220
  139.7 9.3 %copy-start.15 = (f32[4,128]{1,0:T(4,128)S(1)}, f32[4,128]{1,0:T(4,128)}, u32[]{:S(2)}) copy-start(f32[4,128]{1,0:T(4,128)} %log_decay.5) | copy-start | bytes 6148
  (12 other events, 9.0 us)

commit v5 on v4

v5 whole, which is shorter than its diff:
```python
import functools

import jax
import jax.numpy as jnp
from jax import lax
from jax.experimental import pallas as pl
from jax.experimental.pallas import tpu as pltpu
from jax.sharding import PartitionSpec as P


F32 = jnp.float32
BF16 = jnp.bfloat16
EXACT = lax.Precision.HIGHEST


def dot(a, b, ca=1, cb=0, precision=None):
    return lax.dot_general(
        a, b, (((ca,), (cb,)), ((), ())), preferred_element_type=F32, precision=precision
    )


def iota(shape, axis):
    return lax.broadcasted_iota(jnp.int32, shape, axis)


def in_hbm(a):
    return pltpu.with_memory_space_constraint(a, pltpu.HBM)


def limit(mib):
    return pltpu.CompilerParams(vmem_limit_bytes=mib << 20)


def dispatch_kernel(at, routes, weight, x, g, place, *blocks, experts, cap):
    tokens, half = x.shape
    slots = experts * cap
    expert = iota((experts, tokens), 0)
    first = routes[0:1, :] == expert
    second = routes[1:2, :] == expert
    named = jnp.where(first | second, 1.0, 0.0)
    share = jnp.where(first, weight[0:1, :], 0.0) + jnp.where(second, weight[1:2, :], 0.0)
    before = jnp.where(iota((tokens, tokens), 0) < iota((tokens, tokens), 1), 1.0, 0.0)
    rank_t = dot(named.astype(BF16), before.astype(BF16))
    rank_t = jnp.where(named > 0.5, rank_t, 2.0 * cap)
    slot = iota((slots, experts), 0)
    base = (iota((slots, experts), 1) ^ at[1]) * cap
    owner = (slot >= base) & (slot < base + cap)
    owner_f = jnp.where(owner, 1.0, 0.0)
    number = jnp.sum(jnp.where(owner, slot - base, 0).astype(F32), axis=1, keepdims=True)
    hit = dot(owner_f.astype(BF16), rank_t.astype(BF16)) == number
    picked = jnp.where(hit, 1.0, 0.0).astype(BF16)
    share_slot = jnp.sum(
        jnp.where(hit, dot(owner_f, share, precision=EXACT), 0.0), axis=1, keepdims=True
    )
    place[...] = picked
    rows = dot(picked, x[...])
    grads = share_slot * dot(picked, g[...])
    quarter = half // 2
    upper = at[2] == 1
    for n, block in enumerate(blocks):
        cut = slice(n * cap, (n + 1) * cap)
        if block.shape[1] == half:
            for m, a in enumerate((rows, grads)):
                mine = jnp.where(upper, a[cut, quarter:], a[cut, :quarter])
                block[:, m * quarter : (m + 1) * quarter] = mine.astype(BF16)
        else:
            block[:, :half] = rows[cut].astype(BF16)
            block[:, half:] = grads[cut].astype(BF16)


def dispatch(at, routes, weight, x, g, experts, cap):
    tokens, width = x.shape
    half = width // 2
    slots = experts * cap
    whole = lambda i, c: (0, 0)
    mine = pl.BlockSpec((tokens, half), lambda i, c: (0, c[0]))
    wide = [half if n in shared_far(experts) else width for n in range(experts)]
    return pl.pallas_call(
        functools.partial(dispatch_kernel, experts=experts, cap=cap),
        grid_spec=pltpu.PrefetchScalarGridSpec(
            num_scalar_prefetch=1,
            grid=(1,),
            in_specs=[
                pl.BlockSpec(routes.shape, whole), pl.BlockSpec(weight.shape, whole), mine, mine,
            ],
            out_specs=[pl.BlockSpec((slots, tokens), whole)]
            + [pl.BlockSpec((cap, w), whole) for w in wide],
        ),
        out_shape=[jax.ShapeDtypeStruct((slots, tokens), BF16)]
        + [jax.ShapeDtypeStruct((cap, w), BF16) for w in wide],
        compiler_params=limit(12),
        name="dispatch",
    )(at, in_hbm(routes), in_hbm(weight), in_hbm(x), in_hbm(g))


def gather_kernel(at, *refs, homes):
    blocks, out, sems = refs[:-2], refs[-2], refs[-1]
    half = out.shape[2] // 2
    quarter = half // 2
    copies = []

    def copy(source, target):
        copies.append(pltpu.make_async_copy(source, target, sems.at[len(copies)]))
        copies[-1].start()

    for block, (n, side) in zip(blocks, homes):
        if side is None:
            copy(block, out.at[n])
        else:
            place = at[2] if side == 0 else 1 - at[2]
            for m in range(2):
                begin = pl.multiple_of(m * half + place * quarter, quarter)
                copy(
                    block.at[:, m * quarter : (m + 1) * quarter],
                    out.at[n, :, pl.ds(begin, quarter)],
                )
    for each in copies:
        each.wait()


def gather(at, blocks, homes, experts, cap, width):
    out = pl.pallas_call(
        functools.partial(gather_kernel, homes=homes),
        in_specs=[pl.BlockSpec(memory_space=pltpu.SMEM)]
        + [pl.BlockSpec(memory_space=pl.ANY)] * len(blocks),
        out_specs=pl.BlockSpec(memory_space=pltpu.VMEM),
        out_shape=jax.ShapeDtypeStruct((experts, cap, width), BF16),
        scratch_shapes=[pltpu.SemaphoreType.DMA((2 * len(blocks),))],
        compiler_params=limit(4),
        name="gather",
    )(at, *blocks)
    return out.reshape(experts * cap, width)


def stage_kernel(at, *refs, kinds):
    count = len(kinds)
    sources, outs, sems = refs[:count], refs[count:-1], refs[-1]
    copies = []

    def copy(source, target):
        copies.append(pltpu.make_async_copy(source, target, sems.at[len(copies)]))
        copies[-1].start()

    for source, target, kind in zip(sources, outs, kinds):
        if kind == "plain":
            copy(source, target)
            continue
        half = target.shape[1] if kind == "tall" else target.shape[2]
        for side in range(2):
            begin = pl.multiple_of((at[0] if side == 0 else 1 - at[0]) * half, half)
            cut = pl.ds(begin, half)
            copy(source.at[cut, :] if kind == "tall" else source.at[:, cut], target.at[side])
    for each in copies:
        each.wait()


def stage(at, kinds, arrays):
    shapes = []
    for a, kind in zip(arrays, kinds):
        if kind == "tall":
            shapes.append(pltpu.VMEM((2, a.shape[0] // 2, a.shape[1]), a.dtype))
        elif kind == "wide":
            shapes.append(pltpu.VMEM((2, a.shape[0], a.shape[1] // 2), a.dtype))
        else:
            shapes.append(pltpu.VMEM(a.shape, a.dtype))
    count = len(arrays)
    return pl.pallas_call(
        functools.partial(stage_kernel, kinds=kinds),
        in_specs=[pl.BlockSpec(memory_space=pltpu.SMEM)]
        + [pl.BlockSpec(memory_space=pltpu.HBM)] * count,
        out_specs=[pl.BlockSpec(memory_space=pltpu.VMEM)] * count,
        out_shape=shapes,
        scratch_shapes=[pltpu.SemaphoreType.DMA((2 * count,))],
        compiler_params=limit(2),
        name="stage",
    )(at, *[in_hbm(a) for a in arrays])


def expert_kernel(at, own, other, wg, wu, wd, hidden, gback, uback, pb):
    half = own.shape[1] // 2
    units = hidden.shape[1]
    chunk = min(units, 256)
    for f in range(0, units, chunk):
        cut = slice(f, f + chunk)
        gate = dot(own[:, :half], wg[0, :, cut]) + dot(other[:, :half], wg[1, :, cut])
        up = dot(own[:, :half], wu[0, :, cut]) + dot(other[:, :half], wu[1, :, cut])
        back = dot(own[:, half:], wd[0, cut, :], 1, 1) + dot(other[:, half:], wd[1, cut, :], 1, 1)
        sig = 1.0 / (1.0 + jnp.exp(-gate))
        active = gate * sig
        hidden[:, cut] = (active * up).astype(BF16)
        gback[:, cut] = (back * up * (sig * (1.0 + gate * (1.0 - sig)))).astype(BF16)
        uback[:, cut] = (back * active).astype(BF16)
    pb[...] = (dot(gback[...], wg[1], 1, 1) + dot(uback[...], wu[1], 1, 1)).astype(BF16)


def partial_kernel(at, gback, uback, wg, wu, out):
    out[...] = (dot(gback[...], wg[0], 1, 1) + dot(uback[...], wu[0], 1, 1)).astype(BF16)


def add_blocks_kernel(at, a, b, *blocks):
    cap = blocks[0].shape[0]
    for n, block in enumerate(blocks):
        cut = slice(n * cap, (n + 1) * cap)
        block[...] = (a[cut, :].astype(F32) + b[cut, :].astype(F32)).astype(BF16)


def add_kernel(at, a, b, out):
    out[...] = (a[...].astype(F32) + b[...].astype(F32)).astype(out.dtype)


def weights_kernel(core, ra, rb, ga, gb, hidden, gback, uback, gate_out, up_out, down_out):
    step = pl.program_id(0)
    turn = pl.num_programs(0) // 2

    def write(r, g):
        gate_out[...] = dot(r[...], gback[...], 0, 0).astype(BF16)
        up_out[...] = dot(r[...], uback[...], 0, 0).astype(BF16)
        down_out[...] = dot(hidden[...], g[...], 0, 0).astype(BF16)

    @pl.when(step < turn)
    def _():
        write(ra, ga)

    @pl.when(step >= turn)
    def _():
        write(rb, gb)


def weight_grads(core, own, other, hidden, gback, uback):
    rows, width = own.shape
    half = width // 2
    units = hidden.shape[1]
    chunk = min(half, 512)
    turn = half // chunk
    near = lambda i: jnp.minimum(i, turn - 1)
    far = lambda i: jnp.maximum(i - turn, 0)
    at = lambda i, c: jnp.where(i < turn, c[0] * turn + i, (1 - c[0]) * turn + i - turn)
    full = pl.BlockSpec((rows, units), lambda i, c: (0, 0))
    tall = pl.BlockSpec((None, chunk, units), lambda i, c: (0, at(i, c), 0))
    wide = pl.BlockSpec((None, units, chunk), lambda i, c: (0, 0, at(i, c)))
    return pl.pallas_call(
        weights_kernel,
        grid_spec=pltpu.PrefetchScalarGridSpec(
            num_scalar_prefetch=1,
            grid=(2 * turn,),
            in_specs=[
                pl.BlockSpec((rows, chunk), lambda i, c: (0, near(i))),
                pl.BlockSpec((rows, chunk), lambda i, c: (0, far(i))),
                pl.BlockSpec((rows, chunk), lambda i, c: (0, turn + near(i))),
                pl.BlockSpec((rows, chunk), lambda i, c: (0, turn + far(i))),
                full, full, full,
            ],
            out_specs=[tall, tall, wide],
        ),
        out_shape=[
            jax.ShapeDtypeStruct((1, width, units), BF16),
            jax.ShapeDtypeStruct((1, width, units), BF16),
            jax.ShapeDtypeStruct((1, units, width), BF16),
        ],
        compiler_params=limit(20),
        name="weight_grads",
    )(core, own, other, own, other, hidden, gback, uback)


def combine_kernel(at, place, *refs):
    blocks, out = refs[:-1], refs[-1]
    cap = blocks[0].shape[0]
    total = None
    for n, block in enumerate(blocks):
        part = dot(place[n * cap : (n + 1) * cap, :], block[...], 0, 0)
        total = part if total is None else total + part
    out[...] = total.astype(BF16)


def base_kernel(at, g, part, out):
    out[...] = g[...].astype(F32) + part[...].astype(F32)


def base_sum(at, g, part):
    tokens, half = part.shape
    whole = lambda i, c: (0, 0)
    return pl.pallas_call(
        base_kernel,
        grid_spec=pltpu.PrefetchScalarGridSpec(
            num_scalar_prefetch=1,
            grid=(1,),
            in_specs=[
                pl.BlockSpec((tokens, half), lambda i, c: (0, c[0])),
                pl.BlockSpec((tokens, half), whole),
            ],
            out_specs=pl.BlockSpec((tokens, half), whole),
        ),
        out_shape=jax.ShapeDtypeStruct((tokens, half), F32),
        compiler_params=limit(4),
        name="base",
    )(at, in_hbm(g), part)


def decays(log_decay, head):
    span = log_decay.shape[-1]
    row = iota((span, span), 0)
    col = iota((span, span), 1)
    keep = row >= col
    lower = jnp.where(keep, 1.0, 0.0)
    own = log_decay[head : head + 1, :]
    down = jnp.sum(lower * own, axis=1, keepdims=True)
    across = jnp.sum(jnp.where(row <= col, 1.0, 0.0) * jnp.sum(
        jnp.where(row == col, own, 0.0), axis=1, keepdims=True), axis=0, keepdims=True)
    total = jnp.sum(own, axis=1, keepdims=True)
    table = jnp.where(keep, jnp.exp(jnp.where(keep, down - across, 0.0)), 0.0)
    return table, jnp.exp(down), jnp.exp(total - down), total


def mixed_kernel(at, q, k, v, log_decay, state, mixed):
    heads, _, size = q.shape
    width = v.shape[2]
    scale = size**-0.5
    for h in range(heads):
        table, lead, _, _ = decays(log_decay[...], h)
        scores = (dot(q[h], k[h], 1, 1) * (scale * table)).astype(BF16)
        out = dot(scores, v[h]) + lead * dot(q[h], state[h, 0].astype(BF16))
        mixed[:, h * width : (h + 1) * width] = out.astype(BF16)


PIECES = 16


def pieces(decay, shape):
    row = iota(shape, 0)
    high = decay.astype(BF16).astype(F32)
    rest = decay - high
    middle = rest.astype(BF16).astype(F32)
    low = rest - middle
    return jnp.where(row == 0, high, jnp.where(row == 1, middle, jnp.where(row == 2, low, 0.0)))


def put_message(ref, h, body, decay):
    size = body.shape[0]
    ref[h, :size, :] = body.astype(BF16)
    ref[h, size:, :] = pieces(decay, (PIECES, body.shape[1])).astype(BF16)


def get_message(ref, h):
    size = ref.shape[1] - PIECES
    decay = jnp.sum(ref[h, size:, :].astype(F32), axis=0, keepdims=True)[:, 0:1]
    return ref[h, :size, :].astype(F32), decay


def carry_kernel(at, ma, mb, wo, q, log_decay, hg, keep, send, stay, leave):
    heads, span, _ = q.shape
    turn, rows, size = stay.shape
    width = hg.shape[2]
    half = width // 2
    upper = (at[1] & 1) == 1
    lower = jnp.where(iota((span, span), 0) >= iota((span, span), 1), 1.0, 0.0)
    for h in range(heads):
        cut = slice(h * width, (h + 1) * width)
        h_grad = (dot(ma[...], wo[0, :, cut]) + dot(mb[...], wo[1, :, cut])).astype(BF16)
        hg[h] = h_grad
        own = log_decay[h : h + 1, :]
        lead = jnp.exp(jnp.sum(lower * own, axis=1, keepdims=True))
        total = jnp.exp(jnp.sum(own, axis=1, keepdims=True))
        part = dot((q[h].astype(F32) * lead).astype(BF16), h_grad, 0, 0)
        put_message(keep, h, jnp.where(upper, part[:, half:], part[:, :half]), total)
        put_message(send, h, jnp.where(upper, part[:, :half], part[:, half:]), total)
    mine = pl.ds(pl.multiple_of(at[0] * rows, rows), rows)
    side = at[0] ^ (at[1] // turn)

    def sort(near, far):
        for i in range(turn):
            n = i ^ (at[1] % turn)
            stay[n] = near[mine, i * size : (i + 1) * size]
            leave[n] = far[mine, i * size : (i + 1) * size]

    @pl.when(side == 0)
    def _():
        sort(ma, mb)

    @pl.when(side == 1)
    def _():
        sort(mb, ma)


def split_kernel(at, kept, came, stay, leave):
    sources, count = kept.shape[:2]
    for n, part in enumerate((kept, came)):
        for m in range(sources):
            stay[n * sources + m] = part[m, : count // 2]
            leave[n * sources + m] = part[m, count // 2 :]


def pair_kernel(at, keep, came, out):
    upper = (at[1] & 1) == 1
    for h in range(keep.shape[0]):
        mine, mine_decay = get_message(keep, h)
        theirs, their_decay = get_message(came, h)
        first = jnp.where(upper, theirs, mine)
        second = jnp.where(upper, mine, theirs)
        decay = jnp.where(upper, their_decay, mine_decay)
        put_message(out, h, first + decay * second, mine_decay * their_decay)


def join_kernel(at, group, came, later, reach, out, later_out, reach_out, *, bit):
    upper = (at[1] & bit) != 0
    for h in range(group.shape[0]):
        mine, mine_decay = get_message(group, h)
        theirs, their_decay = get_message(came, h)
        first = jnp.where(upper, theirs, mine)
        second = jnp.where(upper, mine, theirs)
        decay = jnp.where(upper, their_decay, mine_decay)
        put_message(out, h, first + decay * second, mine_decay * their_decay)
        old = reach[h : h + 1, :]
        later_out[h] = later[h] + jnp.where(upper, 0.0, old[:, 0:1]) * theirs
        reach_out[h : h + 1, :] = old * jnp.where(upper, 1.0, their_decay)


def close_kernel(at, came, later, reach, keep, first_came, own, send, *, bit):
    upper = (at[1] & bit) != 0
    right = (at[1] & 1) == 1
    for h in range(keep.shape[0]):
        theirs, _ = get_message(came, h)
        after = later[h] + jnp.where(upper, 0.0, reach[h : h + 1, 0:1]) * theirs
        mine, mine_decay = get_message(keep, h)
        pair, pair_decay = get_message(first_came, h)
        second = jnp.where(right, mine, pair)
        decay = jnp.where(right, mine_decay, pair_decay)
        through = second + decay * after
        own[h] = jnp.where(right, after, through).astype(BF16)
        send[h] = jnp.where(right, through, after).astype(BF16)


def small(kernel, outs, at, *operands, mib=8):
    spec = pl.BlockSpec()
    many = isinstance(outs, (list, tuple))
    return pl.pallas_call(
        kernel,
        in_specs=[pl.BlockSpec(memory_space=pltpu.SMEM)] + [spec] * len(operands),
        out_specs=[spec] * len(outs) if many else spec,
        out_shape=outs,
        compiler_params=limit(mib),
    )(at, *operands)


def local_kernel(at, q, k, v, log_decay, state, hg, q_grad, k_part, v_part, trails):
    heads, _, size = q.shape
    scale = size**-0.5
    for h in range(heads):
        table, lead, trail, _ = decays(log_decay[...], h)
        trails[h] = scale * trail
        scores = (dot(q[h], k[h], 1, 1) * (scale * table)).astype(BF16)
        back = (dot(hg[h], v[h], 1, 1) * table).astype(BF16)
        from_state = dot(hg[h], state[h, 0].astype(BF16), 1, 1)
        q_grad[h] = (scale * dot(back, k[h]) + lead * from_state).astype(BF16)
        k_part[h] = scale * dot(back, q[h], 0, 0)
        v_part[h] = dot(scores, hg[h], 0, 0)


def final_kernel(at, k, v, trails, own, came, k_part, v_part, k_grad, v_grad):
    heads = k.shape[0]
    half = v.shape[2] // 2
    right = (at[1] & 1) == 1
    for h in range(heads):
        low = jnp.where(right, came[h].astype(F32), own[h].astype(F32)).astype(BF16)
        high = jnp.where(right, own[h].astype(F32), came[h].astype(F32)).astype(BF16)
        back = dot(v[h, :, :half], low, 1, 1) + dot(v[h, :, half:], high, 1, 1)
        trail = trails[h]
        k_grad[h] = (k_part[h] + trail * back).astype(BF16)
        v_grad[h, :, :half] = (v_part[h, :, :half] + trail * dot(k[h], low)).astype(BF16)
        v_grad[h, :, half:] = (v_part[h, :, half:] + trail * dot(k[h], high)).astype(BF16)


def project_kernel(core, a0, a1, b0, b1, *refs):
    out, x = refs[-2:]
    turn, rows, size = a0.shape

    @pl.when(pl.program_id(0) == 0)
    def _():
        mine = pl.ds(pl.multiple_of(core[0] * rows, rows), rows)
        other = pl.ds(pl.multiple_of((1 - core[0]) * rows, rows), rows)
        for place, pair in ((mine, (a0, a1)), (other, (b0, b1))):
            x[:turn, place, :] = pair[0][...]
            x[turn:, place, :] = pair[1][...]

    total, at = None, 0
    for y in refs[:-2]:
        blocks, span, width = y.shape
        left = x[at : at + blocks].reshape(blocks * span, size)
        part = dot(left, y[...].reshape(blocks * span, width), 0, 0)
        total = part if total is None else total + part
        at += blocks
    out[...] = total


def project(at, slices, parts):
    turn, rows, size = slices[0].shape
    width = parts[0].shape[2]
    chunk = min(width, 512)
    piece = pl.BlockSpec((turn, rows, size), lambda i, *_: (0, 0, 0))
    return pl.pallas_call(
        project_kernel,
        grid_spec=pltpu.PrefetchScalarGridSpec(
            num_scalar_prefetch=1,
            grid=(width // chunk,),
            in_specs=[piece] * 4
            + [pl.BlockSpec(y.shape[:2] + (chunk,), lambda i, *_: (0, 0, i)) for y in parts],
            out_specs=pl.BlockSpec((size, chunk), lambda i, *_: (0, i)),
            scratch_shapes=[pltpu.VMEM((2 * turn, 2 * rows, size), BF16)],
        ),
        out_shape=jax.ShapeDtypeStruct((size, width), F32),
        compiler_params=limit(16),
        name="project",
    )(at, *slices, *parts)


def swap(a, axis, bit):
    count = lax.axis_size(axis)
    return lax.ppermute(a, axis, [(i, i ^ bit) for i in range(count)])


def far_first(count):
    return list(range(count // 2, count)) + list(range(count // 2 - 1, 0, -1))


def shared_far(count):
    return far_first(count)[: count // 2 - 1]


def bits_of(count):
    return [1 << i for i in range(count.bit_length() - 1)]


def step(
    moe_input,
    out_grad,
    routes,
    route_weight,
    w_gate,
    w_up,
    w_down,
    w_out,
    query_heads,
    key_heads,
    value_heads,
    log_decay,
    state_in,
):
    tokens, width = moe_input.shape
    half = width // 2
    sp = lax.axis_size("sp")
    tp = lax.axis_size("tp")
    place = lax.axis_index("sp").astype(jnp.int32)
    column = lax.axis_index("tp").astype(jnp.int32)
    core = column & 1
    at = jnp.stack([core, place, (column >> 1) & 1])
    experts = w_gate.shape[0] * sp
    cap = 5 * tokens * routes.shape[1] // (4 * experts)
    slots = experts * cap
    units = w_gate.shape[2]
    heads, _, size = query_heads.shape
    value_size = value_heads.shape[-1]

    picked, *sent = dispatch(at, routes.T, route_weight.T, moe_input, out_grad, experts, cap)
    came = {0: sent[0]}
    for n in far_first(sp):
        came[n] = swap(sent[n], "sp", n)
    wg, q, k, v, state, decay = stage(
        at, ("tall",) + ("plain",) * 5,
        (w_gate[0], query_heads, key_heads, value_heads, state_in, log_decay),
    )
    wu, wd = stage(at, ("tall", "wide"), (w_up[0], w_down[0]))
    (wo,) = stage(at, ("tall",), (w_out,))
    mixed = small(
        mixed_kernel, jax.ShapeDtypeStruct((tokens, heads * value_size), BF16),
        at, q, k, v, decay, state,
    )
    blocks, homes = [], []
    for n in range(sp):
        blocks.append(came[n])
        homes.append((n, 0 if n in shared_far(sp) else None))
        if n in shared_far(sp):
            blocks.append(swap(came[n], "tp", 2))
            homes.append((n, 1))
    own = gather(at, blocks, tuple(homes), experts, cap, width)
    other = swap(own, "tp", 1)
    hidden, gate_back, up_back, part_b = small(
        expert_kernel,
        [jax.ShapeDtypeStruct((slots, units), BF16)] * 3
        + [jax.ShapeDtypeStruct((slots, half), BF16)],
        at, own, other, wg, wu, wd, mib=16,
    )
    part_came = swap(part_b, "tp", 1)
    part_a = small(
        partial_kernel, jax.ShapeDtypeStruct((slots, half), BF16),
        at, gate_back, up_back, wg, wu,
    )
    parts_out = small(
        add_blocks_kernel, [jax.ShapeDtypeStruct((cap, half), BF16)] * sp,
        at, part_a, part_came,
    )
    back = {0: parts_out[0]}
    for n in far_first(sp):
        back[n] = swap(parts_out[n], "sp", n)
    gate_grad, up_grad, down_grad = weight_grads(at, own, other, hidden, gate_back, up_back)

    blocks = mixed[None]
    parts = []
    for bit in reversed(bits_of(sp)):
        if not parts:
            parts = [jnp.concatenate([blocks, swap(blocks, "sp", bit)], axis=0)]
        else:
            came = []
            for piece in parts:
                came.append(swap(piece, "sp", bit))
            parts = parts + came

    token_shape = jax.ShapeDtypeStruct((tokens, half), BF16)
    token_part = small(combine_kernel, token_shape, at, picked, *[back[n] for n in range(sp)])
    for bit in bits_of(tp)[1:]:
        came = swap(token_part, "tp", bit)
        if bit * 2 < tp:
            token_part = (token_part.astype(F32) + came.astype(F32)).astype(BF16)
    base = base_sum(at, out_grad, token_part)
    mixed_a = small(add_kernel, token_shape, at, base, came)
    mixed_b = swap(mixed_a, "tp", 1)

    message = jax.ShapeDtypeStruct((heads, size + PIECES, value_size // 2), BF16)
    turn = sp // 2
    block = (tokens // 2, width // sp)
    head_grad, keep, send, stay, leave = small(
        carry_kernel,
        [jax.ShapeDtypeStruct((heads, tokens, value_size), BF16), message, message]
        + [jax.ShapeDtypeStruct((turn,) + block, BF16)] * 2,
        at, mixed_a, mixed_b, wo, q, decay,
    )
    sources, slices = 1, []
    for bit in reversed(bits_of(sp)):
        came_slices = swap(leave, "sp", bit)
        if bit > 1:
            grid = (sources, bit) + block
            out = jax.ShapeDtypeStruct((2 * sources, bit // 2) + block, BF16)
            stay, leave = small(
                split_kernel, [out, out], at,
                stay.reshape(grid), came_slices.reshape(grid),
            )
            sources *= 2
        stay, leave = stay.reshape((turn,) + block), leave.reshape((turn,) + block)
    slices = [stay, came_slices.reshape((turn,) + block)]
    for n in range(2):
        slices.append(swap(slices[n], "tp", 1))
    first_came = swap(send, "sp", 1)
    q_grad, k_part, v_part, trails = small(
        local_kernel,
        [
            jax.ShapeDtypeStruct(query_heads.shape, BF16),
            jax.ShapeDtypeStruct(key_heads.shape, F32),
            jax.ShapeDtypeStruct(value_heads.shape, F32),
            jax.ShapeDtypeStruct((heads, tokens, 1), F32),
        ],
        at,
        q, k, v, decay, state, head_grad, mib=12,
    )
    state_shape = (heads, size, value_size // 2)
    group = small(pair_kernel, message, at, keep, first_came)
    later = jnp.zeros(state_shape, F32)
    reach = jnp.ones((heads, 128), F32)
    for bit in bits_of(sp)[1:]:
        came_state = swap(group, "sp", bit)
        if bit * 2 < sp:
            group, later, reach = small(
                functools.partial(join_kernel, bit=bit),
                [message, jax.ShapeDtypeStruct(state_shape, F32),
                 jax.ShapeDtypeStruct((heads, 128), F32)],
                at, group, came_state, later, reach,
            )
    state_out = jax.ShapeDtypeStruct(state_shape, BF16)
    own_state, send_state = small(
        functools.partial(close_kernel, bit=bit),
        [state_out, state_out], at, came_state, later, reach, keep, first_came,
    )
    other_state = swap(send_state, "sp", 1)
    out_proj_grad = project(at, slices, parts)
    k_grad, v_grad = small(
        final_kernel,
        [jax.ShapeDtypeStruct(key_heads.shape, BF16),
         jax.ShapeDtypeStruct(value_heads.shape, BF16)],
        at, k, v, trails, own_state, other_state, k_part, v_part,
    )
    return gate_grad, up_grad, down_grad, out_proj_grad, q_grad, k_grad, v_grad


def solution(mesh):
    return jax.shard_map(
        step,
        mesh=mesh,
        in_specs=(
            P("sp", None),
            P("sp", None),
            P("sp", None),
            P("sp", None),
            P("sp", None, "tp"),
            P("sp", None, "tp"),
            P("sp", "tp", None),
            P(None, "tp"),
            P("tp", "sp", None),
            P("tp", "sp", None),
            P("tp", "sp", None),
            P("tp", "sp"),
            P("tp", "sp", None, None),
        ),
        out_specs=(
            P("sp", None, "tp"),
            P("sp", None, "tp"),
            P("sp", "tp", None),
            P("sp", "tp"),
            P("tp", "sp", None),
            P("tp", "sp", None),
            P("tp", "sp", None),
        ),
        check_vma=False,
    )
```

time: 155 us -> 135 us (0.87)
  waiting for transfers between devices: 50.3 us -> 33.7 us
  starting transfers between devices: 48.9 us -> 58.8 us
  local copies, waits for them, and re-layouts: 9.19 us -> 0.02 us
  Pallas kernels: 44.9 us -> 40.8 us
    ppermute x27 -> x34, waiting for transfers between devices: 50.3 us -> 33.7 us  [swap(): return lax.ppermute(a, axis, [(i, i ^ bit) for i in range(count)])]
    ppermute x27 -> x34, starting transfers between devices: 43.2 us -> 58.8 us  [swap(): return lax.ppermute(a, axis, [(i, i ^ bit) for i in range(count)])]
    unnamed x64 -> x0, local copies, waits for them, and re-layouts: 9.17 us -> none
    all_to_all x1 -> x0, starting transfers between devices: 5.7 us -> none  [step(): lax.all_to_all(slices, 'sp', split_axis=0, concat_axis=0, tiled=True)]
    pallas_call x4, Pallas kernels: 15.1 us -> 10 us  [the longest x3 8.02 us: stage(): pl.pallas_call(functools.partial(stage_kernel, kinds=kinds), in_specs=[pl...]
    pallas_call x9 -> x14, Pallas kernels: 13.5 us -> 18 us  [small(): pl.pallas_call(kernel, in_specs=[pl.BlockSpec(memory_space=pltpu.SMEM)] +...]
  transfers between devices with their start and end apart: 28 -> 34, of which waited for: 13 -> 9; matrix products, arithmetic and copies ran while one was open for 0% -> 0% of each run, Pallas kernels for 19% -> 23%
where the time goes in v5:
time: 135 us; the launch traced here: 134 us
  starting transfers between devices  58.8 us (44%)
  Pallas kernels  40.8 us (30%)
  waiting for transfers between devices  33.7 us (25%)
    ppermute x34, starting transfers between devices, swap(): return lax.ppermute(a, axis, [(i, i ^ bit) for i in range(count)])  58.8 us
    ppermute x34, waiting for transfers between devices, swap(): return lax.ppermute(a, axis, [(i, i ^ bit) for i in range(count)])  33.7 us
    pallas_call x14, Pallas kernels, small(): pl.pallas_call(kernel, in_specs=[pl.BlockSpec(memory_space=pltpu.SMEM)] +...  18 us
    pallas_call x3, Pallas kernels, stage(): pl.pallas_call(functools.partial(stage_kernel, kinds=kinds), in_specs=[pl...  8.02 us
    pallas_call x1, Pallas kernels, weight_grads(): pl.pallas_call(weights_kernel, grid_spec=pltpu.PrefetchScalarGridSpec(num...  6.29 us
  transfers between devices with their start and end apart: 34, of which 9 were waited for; matrix products, arithmetic and copies ran while one was open for 0% of the time, Pallas kernels for 23%

profile of v5, /device:TPU:0, one launch (start us, length us, event | category | flops | bytes accessed | tf_op | source)
XLA Modules:
  0.0 134.3 jit_solution(890112708030666675)
XLA Ops:
  0.7 2.4 %dispatch.1 = (bf16[320,128]{1,0:T(8,128)(2,1)S(1)}, bf16[40,2048]{1,0:T(8,128)(2,1)S(1)}, bf16[40,2048]{1,0:T(8,128)(2,1)S(1)}, bf16[40,2048]{1,0:T(8,128)(2,1)...) custom-call(s32[3]{0:T(128)S(1)} %pad_add_fusion.at.core, ...), custom_call_target="tpu_custom_call" | custom-call | tf_op jit(solution)/shard_map/dispatch/pallas_call | solution.py:78
  3.1 4.1 %collective-permute-start.3 = (bf16[40,1024]{1,0:T(8,128)(2,1)S(1)}, bf16[40,1024]{1,0:T(8,128)(2,1)S(1)}, u32[]{:S(2)}, u32[]{:S(2)}) collective-permute-start(bf16[40,1024]{1,0:T(8,128)(2,1)S(1)} %get-tuple-element.63), channel_id=1, source_target_pairs={{0,16},{4,20},{8,24},{12,28},{16,0},{20,4},{24,8},{28,12},{1,17},{... | collective-permute-start | bytes 245768 | tf_op jit(solution)/shard_map/ppermute | solution.py:517
  7.2 1.3 collective-permute-start.5
  8.5 3.6 %collective-permute-start.7 = (bf16[40,1024]{1,0:T(8,128)(2,1)S(1)}, bf16[40,1024]{1,0:T(8,128)(2,1)S(1)}, u32[]{:S(2)}, u32[]{:S(2)}) collective-permute-start(bf16[40,1024]{1,0:T(8,128)(2,1)S(1)} %get-tuple-element.65), channel_id=1, source_target_pairs={{0,24},{4,28},{8,16},{12,20},{16,8},{20,12},{24,0},{28,4},{1,25},{... | collective-permute-start | bytes 245768 | tf_op jit(solution)/shard_map/ppermute | solution.py:517
  12.1 1.5 %collective-permute-start.4 = (bf16[40,1024]{1,0:T(8,128)(2,1)S(1)}, bf16[40,1024]{1,0:T(8,128)(2,1)S(1)}, u32[]{:S(2)}, u32[]{:S(2)}) collective-permute-start(bf16[40,1024]{1,0:T(8,128)(2,1)S(1)} %collective-permute-done.3.refs_4_), channel_id=1, source_target_pairs={{0,2},{1,3},{2,0},{3,1},{4,6},{5,7},{6,4},{7,5},{8,10},{9,11},{10,... | collective-permute-start | bytes 245768 | tf_op jit(solution)/shard_map/ppermute | solution.py:517
  13.6 5.1 %collective-permute-start = (bf16[40,2048]{1,0:T(8,128)(2,1)S(1)}, bf16[40,2048]{1,0:T(8,128)(2,1)S(1)}, u32[]{:S(2)}, u32[]{:S(2)}) collective-permute-start(bf16[40,2048]{1,0:T(8,128)(2,1)S(1)} %get-tuple-element.60), channel_id=1, source_target_pairs={{0,4},{4,0},{8,12},{12,8},{16,20},{20,16},{24,28},{28,24},{1,5},{5... | collective-permute-start | bytes 491528 | tf_op jit(solution)/shard_map/ppermute | solution.py:517
  18.8 1.2 collective-permute-start.6
  20.0 0.8 collective-permute-start.2
  20.8 4.3 %collective-permute-start.9 = (bf16[40,2048]{1,0:T(8,128)(2,1)S(1)}, bf16[40,2048]{1,0:T(8,128)(2,1)S(1)}, u32[]{:S(2)}, u32[]{:S(2)}) collective-permute-start(bf16[40,2048]{1,0:T(8,128)(2,1)S(1)} %get-tuple-element.66), channel_id=1, source_target_pairs={{0,28},{4,24},{8,20},{12,16},{16,12},{20,8},{24,4},{28,0},{1,29},{... | collective-permute-start | bytes 491528 | tf_op jit(solution)/shard_map/ppermute | solution.py:517
  25.0 1.5 %collective-permute-start.8 = (bf16[40,1024]{1,0:T(8,128)(2,1)S(1)}, bf16[40,1024]{1,0:T(8,128)(2,1)S(1)}, u32[]{:S(2)}, u32[]{:S(2)}) collective-permute-start(bf16[40,1024]{1,0:T(8,128)(2,1)S(1)} %collective-permute-done.7.refs_8_), channel_id=1, source_target_pairs={{0,2},{1,3},{2,0},{3,1},{4,6},{5,7},{6,4},{7,5},{8,10},{9,11},{10,... | collective-permute-start | bytes 245768 | tf_op jit(solution)/shard_map/ppermute | solution.py:517
  26.6 2.9 %collective-permute-done.8.refs_9_ = bf16[40,1024]{1,0:T(8,128)(2,1)S(1)} collective-permute-done((bf16[40,1024]{1,0:T(8,128)(2,1)S(1)}, bf16[40,1024]{1,0:T(8,128)(2,1)S(1)}, u32[]{:S(2)}, u32[]{:S(2)}) %collective-permute-start.8) | collective-permute-done | bytes 81952 | tf_op jit(solution)/shard_map/ppermute | solution.py:517
  29.5 2.9 %collective-permute-done.9.refs_10_ = bf16[40,2048]{1,0:T(8,128)(2,1)S(1)} collective-permute-done((bf16[40,2048]{1,0:T(8,128)(2,1)S(1)}, bf16[40,2048]{1,0:T(8,128)(2,1)S(1)}, u32[]{:S(2)}, u32[]{:S(2)}) %collective-permute-start.9) | collective-permute-done | bytes 163872 | tf_op jit(solution)/shard_map/ppermute | solution.py:517
  32.4 2.0 %gather.1 = bf16[8,40,2048]{2,1,0:T(8,128)(2,1)S(1)} custom-call(s32[3]{0:T(128)S(1)} %pad_add_fusion.at.core, bf16[40,2048]{1,0:T(8,128)(2,1)S(1)} %get-tuple-element.59.refs_0_, bf16[40,2048]{1,0:T(8,128)(2,1)S(1)} %collective-permute-done.refs_1_, bf16[40,2048]{1,0:T(8,128)(2,1)S(1)} %collective-permute-done.1.refs_2_, ...), custom_call_target="tpu_custom_call" | custom-call | tf_op jit(solution)/shard_map/gather/pallas_call | solution.py:122
  34.5 2.8 %stage.4 = (bf16[2,1024,512]{2,1,0:T(8,128)(2,1)S(1)}, bf16[2,512,1024]{2,1,0:T(8,128)(2,1)S(1)}) custom-call(s32[3]{0:T(128)S(1)} %pad_add_fusion.at.core, bf16[2048,512]{1,0:T(8,128)(2,1)} %bitcast.30, bf16[512,2048]{1,0:T(8,128)(2,1)} %bitcast.31), custom_call_target="tpu_custom_call" | custom-call | tf_op jit(solution)/shard_map/stage/pallas_call | solution.py:167
  37.3 2.5 %stage.3 = (bf16[2,1024,512]{2,1,0:T(8,128)(2,1)S(1)}, bf16[4,128,128]{2,1,0:T(8,128)(2,1)S(1)}, bf16[4,128,128]{2,1,0:T(8,128)(2,1)S(1)}, bf16[4,128,256]{2,1,0...) custom-call(s32[3]{0:T(128)S(1)} %pad_add_fusion.at.core, bf16[2048,512]{1,0:T(8,128)(2,1)} %bitcast.29, ...), custom_call_target="tpu_custom_call" | custom-call | tf_op jit(solution)/shard_map/stage/pallas_call | solution.py:167
  39.8 3.6 %shard_map.180 = (bf16[320,512]{1,0:T(8,128)(2,1)S(1)}, bf16[320,512]{1,0:T(8,128)(2,1)S(1)}, bf16[320,512]{1,0:T(8,128)(2,1)S(1)}, bf16[320,1024]{1,0:T(8,128)(2,1)S(1)}) custom-call(s32[3]{0:T(128)S(1)} %pad_add_fusion.at.core, bf16[320,2048]{1,0:T(8,128)(2,1)S(1)} %bitcast.17, bf16[320,2048]{1,0:T(8,128)(2,1)S(1)} %collective-permute-done.10.other.rb.gb, ...), custom_call_target="tpu_custom_call" | custom-call | tf_op jit(solution)/shard_map/pallas_call | solution.py:435
  43.9 1.1 shard_map.188
  45.0 1.0 collective-permute-start.26
  46.0 1.4 %shard_map.181.a = bf16[320,1024]{1,0:T(8,128)(2,1)S(1)} custom-call(s32[3]{0:T(128)S(1)} %pad_add_fusion.at.core, bf16[320,512]{1,0:T(8,128)(2,1)S(1)} %get-tuple-element.71.gback, bf16[320,512]{1,0:T(8,128)(2,1)S(1)} %get-tuple-element.72.uback, bf16[2,1024,512]{2,1,0:T(8,128)(2,1)S(1)} %get-tuple-element.67.wg, bf16[2,1024,512]{2,1,0:T(8,128)(2,1)S(1)} %get-tuple-element.68.wu), custom_call_target="tpu_custom_call" | custom-call | tf_op jit(solution)/shard_map/pallas_call | solution.py:435
  48.1 1.3 %collective-permute-start.12 = (bf16[40,1024]{1,0:T(8,128)(2,1)S(1)}, bf16[40,1024]{1,0:T(8,128)(2,1)S(1)}, u32[]{:S(2)}, u32[]{:S(2)}) collective-permute-start(bf16[40,1024]{1,0:T(8,128)(2,1)S(1)} %get-tuple-element.79), channel_id=1, source_target_pairs={{0,4},{4,0},{8,12},{12,8},{16,20},{20,16},{24,28},{28,24},{1,5},{5... | collective-permute-start | bytes 245768 | tf_op jit(solution)/shard_map/ppermute | solution.py:517
  49.5 1.4 %collective-permute-start.13 = (bf16[40,1024]{1,0:T(8,128)(2,1)S(1)}, bf16[40,1024]{1,0:T(8,128)(2,1)S(1)}, u32[]{:S(2)}, u32[]{:S(2)}) collective-permute-start(bf16[40,1024]{1,0:T(8,128)(2,1)S(1)} %get-tuple-element.80), channel_id=1, source_target_pairs={{0,8},{4,12},{8,0},{12,4},{16,24},{20,28},{24,16},{28,20},{1,9},{5... | collective-permute-start | bytes 245768 | tf_op jit(solution)/shard_map/ppermute | solution.py:517
  50.9 0.8 collective-permute-start.14
  51.7 2.0 %collective-permute-start.15 = (bf16[40,1024]{1,0:T(8,128)(2,1)S(1)}, bf16[40,1024]{1,0:T(8,128)(2,1)S(1)}, u32[]{:S(2)}, u32[]{:S(2)}) collective-permute-start(bf16[40,1024]{1,0:T(8,128)(2,1)S(1)} %get-tuple-element.82), channel_id=1, source_target_pairs={{0,16},{4,20},{8,24},{12,28},{16,0},{20,4},{24,8},{28,12},{1,17},{... | collective-permute-start | bytes 245768 | tf_op jit(solution)/shard_map/ppermute | solution.py:517
  53.7 2.2 %collective-permute-start.16 = (bf16[40,1024]{1,0:T(8,128)(2,1)S(1)}, bf16[40,1024]{1,0:T(8,128)(2,1)S(1)}, u32[]{:S(2)}, u32[]{:S(2)}) collective-permute-start(bf16[40,1024]{1,0:T(8,128)(2,1)S(1)} %get-tuple-element.83), channel_id=1, source_target_pairs={{0,20},{4,16},{8,28},{12,24},{16,4},{20,0},{24,12},{28,8},{1,21},{... | collective-permute-start | bytes 245768 | tf_op jit(solution)/shard_map/ppermute | solution.py:517
  55.8 1.8 %collective-permute-done.13.refs_2_ = bf16[40,1024]{1,0:T(8,128)(2,1)S(1)} collective-permute-done((bf16[40,1024]{1,0:T(8,128)(2,1)S(1)}, bf16[40,1024]{1,0:T(8,128)(2,1)S(1)}, u32[]{:S(2)}, u32[]{:S(2)}) %collective-permute-start.13) | collective-permute-done | bytes 81952 | tf_op jit(solution)/shard_map/ppermute | solution.py:517
  57.7 2.0 %collective-permute-start.17 = (bf16[40,1024]{1,0:T(8,128)(2,1)S(1)}, bf16[40,1024]{1,0:T(8,128)(2,1)S(1)}, u32[]{:S(2)}, u32[]{:S(2)}) collective-permute-start(bf16[40,1024]{1,0:T(8,128)(2,1)S(1)} %get-tuple-element.84), channel_id=1, source_target_pairs={{0,24},{4,28},{8,16},{12,20},{16,8},{20,12},{24,0},{28,4},{1,25},{... | collective-permute-start | bytes 245768 | tf_op jit(solution)/shard_map/ppermute | solution.py:517
  59.7 2.4 %collective-permute-start.18 = (bf16[40,1024]{1,0:T(8,128)(2,1)S(1)}, bf16[40,1024]{1,0:T(8,128)(2,1)S(1)}, u32[]{:S(2)}, u32[]{:S(2)}) collective-permute-start(bf16[40,1024]{1,0:T(8,128)(2,1)S(1)} %get-tuple-element.85), channel_id=1, source_target_pairs={{0,28},{4,24},{8,20},{12,16},{16,12},{20,8},{24,4},{28,0},{1,29},{... | collective-permute-start | bytes 245768 | tf_op jit(solution)/shard_map/ppermute | solution.py:517
  62.0 5.6 %collective-permute-done.15.refs_4_ = bf16[40,1024]{1,0:T(8,128)(2,1)S(1)} collective-permute-done((bf16[40,1024]{1,0:T(8,128)(2,1)S(1)}, bf16[40,1024]{1,0:T(8,128)(2,1)S(1)}, u32[]{:S(2)}, u32[]{:S(2)}) %collective-permute-start.15) | collective-permute-done | bytes 81952 | tf_op jit(solution)/shard_map/ppermute | solution.py:517
  67.6 2.8 %collective-permute-done.16.refs_5_ = bf16[40,1024]{1,0:T(8,128)(2,1)S(1)} collective-permute-done((bf16[40,1024]{1,0:T(8,128)(2,1)S(1)}, bf16[40,1024]{1,0:T(8,128)(2,1)S(1)}, u32[]{:S(2)}, u32[]{:S(2)}) %collective-permute-start.16) | collective-permute-done | bytes 81952 | tf_op jit(solution)/shard_map/ppermute | solution.py:517
  70.4 1.3 shard_map.183.part
  71.6 0.8 collective-permute-start.19
  72.5 4.0 %collective-permute-start.27 = (bf16[2,128,1024]{2,1,0:T(8,128)(2,1)S(1)}, bf16[2,128,1024]{2,1,0:T(8,128)(2,1)S(1)}, u32[]{:S(2)}, u32[]{:S(2)}) collective-permute-start(bf16[2,128,1024]{2,1,0:T(8,128)(2,1)S(1)} %pad_maximum_fusion.refs_0_), channel_id=1, source_target_pairs={{0,8},{4,12},{8,0},{12,4},{16,24},{20,28},{24,16},{28,20},{1,9},{5... | collective-permute-start | bytes 1572872 | tf_op jit(solution)/shard_map/ppermute | solution.py:517
  76.5 1.6 %base.1.a = f32[128,1024]{1,0:T(8,128)S(1)} custom-call(s32[3]{0:T(128)S(1)} %pad_add_fusion.at.core, bf16[128,2048]{1,0:T(8,128)(2,1)} %g.3, bf16[128,1024]{1,0:T(8,128)(2,1)S(1)} %shard_map.183.part), custom_call_target="tpu_custom_call" | custom-call | tf_op jit(solution)/shard_map/base/pallas_call | solution.py:282
  78.1 1.8 %collective-permute-done.19.b = bf16[128,1024]{1,0:T(8,128)(2,1)S(1)} collective-permute-done((bf16[128,1024]{1,0:T(8,128)(2,1)S(1)}, bf16[128,1024]{1,0:T(8,128)(2,1)S(1)}, u32[]{:S(2)}, u32[]{:S(2)}) %collective-permute-start.19) | collective-permute-done | bytes 262176 | tf_op jit(solution)/shard_map/ppermute | solution.py:517
  80.5 2.8 %stage.5.wo = bf16[2,1024,1024]{2,1,0:T(8,128)(2,1)S(1)} custom-call(s32[3]{0:T(128)S(1)} %pad_add_fusion.at.core, bf16[2048,1024]{1,0:T(8,128)(2,1)} %refs_0_.1), custom_call_target="tpu_custom_call" | custom-call | tf_op jit(solution)/shard_map/stage/pallas_call | solution.py:167
  83.3 2.4 %shard_map.185 = (bf16[4,128,256]{2,1,0:T(8,128)(2,1)S(1)}, bf16[4,144,128]{2,1,0:T(8,128)(2,1)S(1)}, bf16[4,144,128]{2,1,0:T(8,128)(2,1)S(1)}, bf16[4,64,256]{2,1,0:T(8,128)(2,1)S(1)}, bf16[4,64,256]{2,1,0:T(8,128)(2,1)S(1)}) custom-call(s32[3]{0:T(128)S(1)} %pad_add_fusion.at.core, bf16[128,1024]{1,0:T(8,128)(2,1)S(1)} %shard_map.184.ma, ...), custom_call_target="tpu_custom_call" | custom-call | tf_op jit(solution)/shard_map/pallas_call | solution.py:435
  86.3 4.9 %collective-permute-start.21 = (bf16[4,64,256]{2,1,0:T(8,128)(2,1)S(1)}, bf16[4,64,256]{2,1,0:T(8,128)(2,1)S(1)}, u32[]{:S(2)}, u32[]{:S(2)}) collective-permute-start(bf16[4,64,256]{2,1,0:T(8,128)(2,1)S(1)} %get-tuple-element.89), channel_id=1, source_target_pairs={{0,16},{4,20},{8,24},{12,28},{16,0},{20,4},{24,8},{28,12},{1,17},{... | collective-permute-start | bytes 393224 | tf_op jit(solution)/shard_map/ppermute | solution.py:517
  91.1 1.9 %collective-permute-start.28 = (bf16[2,128,1024]{2,1,0:T(8,128)(2,1)S(1)}, bf16[2,128,1024]{2,1,0:T(8,128)(2,1)S(1)}, u32[]{:S(2)}, u32[]{:S(2)}) collective-permute-start(bf16[2,128,1024]{2,1,0:T(8,128)(2,1)S(1)} %pad_maximum_fusion.refs_0_), channel_id=1, source_target_pairs={{0,4},{4,0},{8,12},{12,8},{16,20},{20,16},{24,28},{28,24},{1,5},{5... | collective-permute-start | bytes 1572872 | tf_op jit(solution)/shard_map/ppermute | solution.py:517
  93.8 3.5 %collective-permute-start.31 = (bf16[4,144,128]{2,1,0:T(8,128)(2,1)S(1)}, bf16[4,144,128]{2,1,0:T(8,128)(2,1)S(1)}, u32[]{:S(2)}, u32[]{:S(2)}) collective-permute-start(bf16[4,144,128]{2,1,0:T(8,128)(2,1)S(1)} %shard_map.190.group), channel_id=1, source_target_pairs={{0,8},{4,12},{8,0},{12,4},{16,24},{20,28},{24,16},{28,20},{1,9},{5... | collective-permute-start | bytes 442376 | tf_op jit(solution)/shard_map/ppermute | solution.py:517
  97.3 0.8 collective-permute-done.21
  98.8 2.5 %collective-permute-done.31.came = bf16[4,144,128]{2,1,0:T(8,128)(2,1)S(1)} collective-permute-done((bf16[4,144,128]{2,1,0:T(8,128)(2,1)S(1)}, bf16[4,144,128]{2,1,0:T(8,128)(2,1)S(1)}, u32[]{:S(2)}, u32[]{:S(2)}) %collective-permute-start.31) | collective-permute-done | bytes 147488 | tf_op jit(solution)/shard_map/ppermute | solution.py:517
  102.0 3.6 %collective-permute-start.32 = (bf16[4,144,128]{2,1,0:T(8,128)(2,1)S(1)}, bf16[4,144,128]{2,1,0:T(8,128)(2,1)S(1)}, u32[]{:S(2)}, u32[]{:S(2)}) collective-permute-start(bf16[4,144,128]{2,1,0:T(8,128)(2,1)S(1)} %get-tuple-element.102), channel_id=1, source_target_pairs={{0,16},{4,20},{8,24},{12,28},{16,0},{20,4},{24,8},{28,12},{1,17},{... | collective-permute-start | bytes 442376 | tf_op jit(solution)/shard_map/ppermute | solution.py:517
  106.6 12.5 %collective-permute-done.23.a1 = bf16[4,64,256]{2,1,0:T(8,128)(2,1)S(1)} collective-permute-done((bf16[4,64,256]{2,1,0:T(8,128)(2,1)S(1)}, bf16[4,64,256]{2,1,0:T(8,128)(2,1)S(1)}, u32[]{:S(2)}, u32[]{:S(2)}) %collective-permute-start.23) | collective-permute-done | bytes 131104 | tf_op jit(solution)/shard_map/ppermute | solution.py:517
  119.9 1.7 %collective-permute-start.33 = (bf16[4,128,128]{2,1,0:T(8,128)(2,1)S(1)}, bf16[4,128,128]{2,1,0:T(8,128)(2,1)S(1)}, u32[]{:S(2)}, u32[]{:S(2)}) collective-permute-start(bf16[4,128,128]{2,1,0:T(8,128)(2,1)S(1)} %get-tuple-element.106), channel_id=1, source_target_pairs={{0,4},{4,0},{8,12},{12,8},{16,20},{20,16},{24,28},{28,24},{1,5},{5... | collective-permute-start | bytes 393224 | tf_op jit(solution)/shard_map/ppermute | solution.py:517
  121.6 6.3 %weight_grads.1 = (bf16[1,2048,512]{2,1,0:T(8,128)(2,1)}, bf16[1,2048,512]{2,1,0:T(8,128)(2,1)}, bf16[1,512,2048]{2,1,0:T(8,128)(2,1)}) custom-call(s32[3]{0:T(128)S(1)} %pad_add_fusion.at.core, bf16[320,2048]{1,0:T(8,128)(2,1)S(1)} %bitcast.18, bf16[320,2048]{1,0:T(8,128)(2,1)S(1)} %collective-permute-done.10.other.rb.gb, bf16[320,2048]{1,0:T(8,128)(2,1)S(1)} %bitcast.19, ...), custom_call_target="tpu_custom_call" | custom-call | tf_op jit(solution)/shard_map/weight_grads/pallas_call | solution.py:241
  127.9 2.2 %shard_map.189 = (bf16[4,128,128]{2,1,0:T(8,128)(2,1)}, f32[4,128,128]{2,1,0:T(8,128)S(1)}, f32[4,128,256]{2,1,0:T(8,128)S(1)}, f32[4,128,1]{2,1,0:T(8,128)S(1)}) custom-call(s32[3]{0:T(128)S(1)} %pad_add_fusion.at.core, bf16[4,128,128]{2,1,0:T(8,128)(2,1)S(1)} %get-tuple-element.86.q, bf16[4,128,128]{2,1,0:T(8,128)(2,1)S(1)} %get-tuple-element.94.k, ...), custom_call_target="tpu_custom_call" | custom-call | tf_op jit(solution)/shard_map/pallas_call | solution.py:435
  130.1 2.5 %project.1 = f32[256,1024]{1,0:T(8,128)} custom-call(s32[3]{0:T(128)S(1)} %pad_add_fusion.at.core, bf16[4,64,256]{2,1,0:T(8,128)(2,1)S(1)} %bitcast.23, bf16[4,64,256]{2,1,0:T(8,128)(2,1)S(1)} %collective-permute-done.23.a1, bf16[4,64,256]{2,1,0:T(8,128)(2,1)S(1)} %collective-permute-done.24.b0, bf16[4,64,256]{2,1,0:T(8,128)(2,1)S(1)} %collective-permute-done.25.b1, ...), custom_call_target="tpu_custom_call" | custom-call | tf_op jit(solution)/shard_map/project/pallas_call | solution.py:499
  132.7 1.7 %shard_map.193 = (bf16[4,128,128]{2,1,0:T(8,128)(2,1)}, bf16[4,128,256]{2,1,0:T(8,128)(2,1)}) custom-call(s32[3]{0:T(128)S(1)} %pad_add_fusion.at.core, bf16[4,128,128]{2,1,0:T(8,128)(2,1)S(1)} %get-tuple-element.94.k, bf16[4,128,256]{2,1,0:T(8,128)(2,1)S(1)} %get-tuple-element.95.v, f32[4,128,1]{2,1,0:T(8,128)S(1)} %get-tuple-element.99.trails, ...), custom_call_target="tpu_custom_call" | custom-call | tf_op jit(solution)/shard_map/pallas_call | solution.py:435
  (46 shorter events, 6.5 us)
Async XLA Ops:
  3.1 9.0 %collective-permute-start.3 = (bf16[40,1024]{1,0:T(8,128)(2,1)S(1)}, bf16[40,1024]{1,0:T(8,128)(2,1)S(1)}, u32[]{:S(2)}, u32[]{:S(2)}) collective-permute-start(bf16[40,1024]{1,0:T(8,128)(2,1)S(1)} %get-tuple-element.63), channel_id=1, source_target_pairs={{0,16},{4,20},{8,24},{12,28},{16,0},{20,4},{24,8},{28,12},{1,17},{... | collective-permute-start | bytes 245768 | tf_op jit(solution)/shard_map/ppermute | solution.py:517
  7.2 11.5 %collective-permute-start.5 = (bf16[40,1024]{1,0:T(8,128)(2,1)S(1)}, bf16[40,1024]{1,0:T(8,128)(2,1)S(1)}, u32[]{:S(2)}, u32[]{:S(2)}) collective-permute-start(bf16[40,1024]{1,0:T(8,128)(2,1)S(1)} %get-tuple-element.64), channel_id=1, source_target_pairs={{0,20},{4,16},{8,28},{12,24},{16,4},{20,0},{24,12},{28,8},{1,21},{... | collective-permute-start | bytes 245768 | tf_op jit(solution)/shard_map/ppermute | solution.py:517
  8.5 11.5 %collective-permute-start.7 = (bf16[40,1024]{1,0:T(8,128)(2,1)S(1)}, bf16[40,1024]{1,0:T(8,128)(2,1)S(1)}, u32[]{:S(2)}, u32[]{:S(2)}) collective-permute-start(bf16[40,1024]{1,0:T(8,128)(2,1)S(1)} %get-tuple-element.65), channel_id=1, source_target_pairs={{0,24},{4,28},{8,16},{12,20},{16,8},{20,12},{24,0},{28,4},{1,25},{... | collective-permute-start | bytes 245768 | tf_op jit(solution)/shard_map/ppermute | solution.py:517
  12.1 8.6 %collective-permute-start.4 = (bf16[40,1024]{1,0:T(8,128)(2,1)S(1)}, bf16[40,1024]{1,0:T(8,128)(2,1)S(1)}, u32[]{:S(2)}, u32[]{:S(2)}) collective-permute-start(bf16[40,1024]{1,0:T(8,128)(2,1)S(1)} %collective-permute-done.3.refs_4_), channel_id=1, source_target_pairs={{0,2},{1,3},{2,0},{3,1},{4,6},{5,7},{6,4},{7,5},{8,10},{9,11},{10,... | collective-permute-start | bytes 245768 | tf_op jit(solution)/shard_map/ppermute | solution.py:517
  13.6 15.9 %collective-permute-start = (bf16[40,2048]{1,0:T(8,128)(2,1)S(1)}, bf16[40,2048]{1,0:T(8,128)(2,1)S(1)}, u32[]{:S(2)}, u32[]{:S(2)}) collective-permute-start(bf16[40,2048]{1,0:T(8,128)(2,1)S(1)} %get-tuple-element.60), channel_id=1, source_target_pairs={{0,4},{4,0},{8,12},{12,8},{16,20},{20,16},{24,28},{28,24},{1,5},{5... | collective-permute-start | bytes 491528 | tf_op jit(solution)/shard_map/ppermute | solution.py:517
  18.8 10.7 %collective-permute-start.1 = (bf16[40,2048]{1,0:T(8,128)(2,1)S(1)}, bf16[40,2048]{1,0:T(8,128)(2,1)S(1)}, u32[]{:S(2)}, u32[]{:S(2)}) collective-permute-start(bf16[40,2048]{1,0:T(8,128)(2,1)S(1)} %get-tuple-element.61), channel_id=1, source_target_pairs={{0,8},{4,12},{8,0},{12,4},{16,24},{20,28},{24,16},{28,20},{1,9},{5... | collective-permute-start | bytes 491528 | tf_op jit(solution)/shard_map/ppermute | solution.py:517
  18.8 6.3 %collective-permute-start.6 = (bf16[40,1024]{1,0:T(8,128)(2,1)S(1)}, bf16[40,1024]{1,0:T(8,128)(2,1)S(1)}, u32[]{:S(2)}, u32[]{:S(2)}) collective-permute-start(bf16[40,1024]{1,0:T(8,128)(2,1)S(1)} %collective-permute-done.5.refs_6_), channel_id=1, source_target_pairs={{0,2},{1,3},{2,0},{3,1},{4,6},{5,7},{6,4},{7,5},{8,10},{9,11},{10,... | collective-permute-start | bytes 245768 | tf_op jit(solution)/shard_map/ppermute | solution.py:517
  20.0 9.5 %collective-permute-start.2 = (bf16[40,2048]{1,0:T(8,128)(2,1)S(1)}, bf16[40,2048]{1,0:T(8,128)(2,1)S(1)}, u32[]{:S(2)}, u32[]{:S(2)}) collective-permute-start(bf16[40,2048]{1,0:T(8,128)(2,1)S(1)} %get-tuple-element.62), channel_id=1, source_target_pairs={{0,12},{4,8},{8,4},{12,0},{16,28},{20,24},{24,20},{28,16},{1,13},{... | collective-permute-start | bytes 491528 | tf_op jit(solution)/shard_map/ppermute | solution.py:517
  20.8 11.7 %collective-permute-start.9 = (bf16[40,2048]{1,0:T(8,128)(2,1)S(1)}, bf16[40,2048]{1,0:T(8,128)(2,1)S(1)}, u32[]{:S(2)}, u32[]{:S(2)}) collective-permute-start(bf16[40,2048]{1,0:T(8,128)(2,1)S(1)} %get-tuple-element.66), channel_id=1, source_target_pairs={{0,28},{4,24},{8,20},{12,16},{16,12},{20,8},{24,4},{28,0},{1,29},{... | collective-permute-start | bytes 491528 | tf_op jit(solution)/shard_map/ppermute | solution.py:517
  25.0 4.4 %collective-permute-start.8 = (bf16[40,1024]{1,0:T(8,128)(2,1)S(1)}, bf16[40,1024]{1,0:T(8,128)(2,1)S(1)}, u32[]{:S(2)}, u32[]{:S(2)}) collective-permute-start(bf16[40,1024]{1,0:T(8,128)(2,1)S(1)} %collective-permute-done.7.refs_8_), channel_id=1, source_target_pairs={{0,2},{1,3},{2,0},{3,1},{4,6},{5,7},{6,4},{7,5},{8,10},{9,11},{10,... | collective-permute-start | bytes 245768 | tf_op jit(solution)/shard_map/ppermute | solution.py:517
  34.4 5.3 %collective-permute-start.10 = (bf16[320,2048]{1,0:T(8,128)(2,1)S(1)}, bf16[320,2048]{1,0:T(8,128)(2,1)S(1)}, u32[]{:S(2)}, u32[]{:S(2)}) collective-permute-start(bf16[320,2048]{1,0:T(8,128)(2,1)S(1)} %bitcast.16), channel_id=1, source_target_pairs={{0,1},{1,0},{2,3},{3,2},{4,5},{5,4},{6,7},{7,6},{8,9},{9,8},{10,11... | collective-permute-start | bytes 3932168 | tf_op jit(solution)/shard_map/ppermute | solution.py:517
  43.3 4.1 %collective-permute-start.11 = (bf16[320,1024]{1,0:T(8,128)(2,1)S(1)}, bf16[320,1024]{1,0:T(8,128)(2,1)S(1)}, u32[]{:S(2)}, u32[]{:S(2)}) collective-permute-start(bf16[320,1024]{1,0:T(8,128)(2,1)S(1)} %get-tuple-element.77), channel_id=1, source_target_pairs={{0,1},{1,0},{2,3},{3,2},{4,5},{5,4},{6,7},{7,6},{8,9},{9,8},{10,11... | collective-permute-start | bytes 1966088 | tf_op jit(solution)/shard_map/ppermute | solution.py:517
  45.0 27.4 %collective-permute-start.26 = (bf16[1,128,1024]{2,1,0:T(8,128)(2,1)S(1)}, bf16[1,128,1024]{2,1,0:T(8,128)(2,1)S(1)}, u32[]{:S(2)}, u32[]{:S(2)}) collective-permute-start(bf16[1,128,1024]{2,1,0:T(8,128)(2,1)S(1)} %bitcast.20), channel_id=1, source_target_pairs={{0,16},{4,20},{8,24},{12,28},{16,0},{20,4},{24,8},{28,12},{1,17},{... | collective-permute-start | bytes 786440 | tf_op jit(solution)/shard_map/ppermute | solution.py:517
  48.1 5.5 %collective-permute-start.12 = (bf16[40,1024]{1,0:T(8,128)(2,1)S(1)}, bf16[40,1024]{1,0:T(8,128)(2,1)S(1)}, u32[]{:S(2)}, u32[]{:S(2)}) collective-permute-start(bf16[40,1024]{1,0:T(8,128)(2,1)S(1)} %get-tuple-element.79), channel_id=1, source_target_pairs={{0,4},{4,0},{8,12},{12,8},{16,20},{20,16},{24,28},{28,24},{1,5},{5... | collective-permute-start | bytes 245768 | tf_op jit(solution)/shard_map/ppermute | solution.py:517
  49.5 8.2 %collective-permute-start.13 = (bf16[40,1024]{1,0:T(8,128)(2,1)S(1)}, bf16[40,1024]{1,0:T(8,128)(2,1)S(1)}, u32[]{:S(2)}, u32[]{:S(2)}) collective-permute-start(bf16[40,1024]{1,0:T(8,128)(2,1)S(1)} %get-tuple-element.80), channel_id=1, source_target_pairs={{0,8},{4,12},{8,0},{12,4},{16,24},{20,28},{24,16},{28,20},{1,9},{5... | collective-permute-start | bytes 245768 | tf_op jit(solution)/shard_map/ppermute | solution.py:517
  50.9 8.7 %collective-permute-start.14 = (bf16[40,1024]{1,0:T(8,128)(2,1)S(1)}, bf16[40,1024]{1,0:T(8,128)(2,1)S(1)}, u32[]{:S(2)}, u32[]{:S(2)}) collective-permute-start(bf16[40,1024]{1,0:T(8,128)(2,1)S(1)} %get-tuple-element.81), channel_id=1, source_target_pairs={{0,12},{4,8},{8,4},{12,0},{16,28},{20,24},{24,20},{28,16},{1,13},{... | collective-permute-start | bytes 245768 | tf_op jit(solution)/shard_map/ppermute | solution.py:517
  51.7 15.9 %collective-permute-start.15 = (bf16[40,1024]{1,0:T(8,128)(2,1)S(1)}, bf16[40,1024]{1,0:T(8,128)(2,1)S(1)}, u32[]{:S(2)}, u32[]{:S(2)}) collective-permute-start(bf16[40,1024]{1,0:T(8,128)(2,1)S(1)} %get-tuple-element.82), channel_id=1, source_target_pairs={{0,16},{4,20},{8,24},{12,28},{16,0},{20,4},{24,8},{28,12},{1,17},{... | collective-permute-start | bytes 245768 | tf_op jit(solution)/shard_map/ppermute | solution.py:517
  53.7 16.7 %collective-permute-start.16 = (bf16[40,1024]{1,0:T(8,128)(2,1)S(1)}, bf16[40,1024]{1,0:T(8,128)(2,1)S(1)}, u32[]{:S(2)}, u32[]{:S(2)}) collective-permute-start(bf16[40,1024]{1,0:T(8,128)(2,1)S(1)} %get-tuple-element.83), channel_id=1, source_target_pairs={{0,20},{4,16},{8,28},{12,24},{16,4},{20,0},{24,12},{28,8},{1,21},{... | collective-permute-start | bytes 245768 | tf_op jit(solution)/shard_map/ppermute | solution.py:517
  57.7 12.7 %collective-permute-start.17 = (bf16[40,1024]{1,0:T(8,128)(2,1)S(1)}, bf16[40,1024]{1,0:T(8,128)(2,1)S(1)}, u32[]{:S(2)}, u32[]{:S(2)}) collective-permute-start(bf16[40,1024]{1,0:T(8,128)(2,1)S(1)} %get-tuple-element.84), channel_id=1, source_target_pairs={{0,24},{4,28},{8,16},{12,20},{16,8},{20,12},{24,0},{28,4},{1,25},{... | collective-permute-start | bytes 245768 | tf_op jit(solution)/shard_map/ppermute | solution.py:517
  59.7 10.7 %collective-permute-start.18 = (bf16[40,1024]{1,0:T(8,128)(2,1)S(1)}, bf16[40,1024]{1,0:T(8,128)(2,1)S(1)}, u32[]{:S(2)}, u32[]{:S(2)}) collective-permute-start(bf16[40,1024]{1,0:T(8,128)(2,1)S(1)} %get-tuple-element.85), channel_id=1, source_target_pairs={{0,28},{4,24},{8,20},{12,16},{16,12},{20,8},{24,4},{28,0},{1,29},{... | collective-permute-start | bytes 245768 | tf_op jit(solution)/shard_map/ppermute | solution.py:517
  71.6 8.2 %collective-permute-start.19 = (bf16[128,1024]{1,0:T(8,128)(2,1)S(1)}, bf16[128,1024]{1,0:T(8,128)(2,1)S(1)}, u32[]{:S(2)}, u32[]{:S(2)}) collective-permute-start(bf16[128,1024]{1,0:T(8,128)(2,1)S(1)} %shard_map.183.part), channel_id=1, source_target_pairs={{0,2},{1,3},{2,0},{3,1},{4,6},{5,7},{6,4},{7,5},{8,10},{9,11},{10,... | collective-permute-start | bytes 786440 | tf_op jit(solution)/shard_map/ppermute | solution.py:517
  72.5 20.6 %collective-permute-start.27 = (bf16[2,128,1024]{2,1,0:T(8,128)(2,1)S(1)}, bf16[2,128,1024]{2,1,0:T(8,128)(2,1)S(1)}, u32[]{:S(2)}, u32[]{:S(2)}) collective-permute-start(bf16[2,128,1024]{2,1,0:T(8,128)(2,1)S(1)} %pad_maximum_fusion.refs_0_), channel_id=1, source_target_pairs={{0,8},{4,12},{8,0},{12,4},{16,24},{20,28},{24,16},{28,20},{1,9},{5... | collective-permute-start | bytes 1572872 | tf_op jit(solution)/shard_map/ppermute | solution.py:517
  80.4 2.9 %collective-permute-start.20 = (bf16[128,1024]{1,0:T(8,128)(2,1)S(1)}, bf16[128,1024]{1,0:T(8,128)(2,1)S(1)}, u32[]{:S(2)}, u32[]{:S(2)}) collective-permute-start(bf16[128,1024]{1,0:T(8,128)(2,1)S(1)} %shard_map.184.ma), channel_id=1, source_target_pairs={{0,1},{1,0},{2,3},{3,2},{4,5},{5,4},{6,7},{7,6},{8,9},{9,8},{10,11... | collective-permute-start | bytes 786440 | tf_op jit(solution)/shard_map/ppermute | solution.py:517
  85.8 7.4 %collective-permute-start.30 = (bf16[4,144,128]{2,1,0:T(8,128)(2,1)S(1)}, bf16[4,144,128]{2,1,0:T(8,128)(2,1)S(1)}, u32[]{:S(2)}, u32[]{:S(2)}) collective-permute-start(bf16[4,144,128]{2,1,0:T(8,128)(2,1)S(1)} %get-tuple-element.101), channel_id=1, source_target_pairs={{0,4},{4,0},{8,12},{12,8},{16,20},{20,16},{24,28},{28,24},{1,5},{5... | collective-permute-start | bytes 442376 | tf_op jit(solution)/shard_map/ppermute | solution.py:517
  86.3 11.9 %collective-permute-start.21 = (bf16[4,64,256]{2,1,0:T(8,128)(2,1)S(1)}, bf16[4,64,256]{2,1,0:T(8,128)(2,1)S(1)}, u32[]{:S(2)}, u32[]{:S(2)}) collective-permute-start(bf16[4,64,256]{2,1,0:T(8,128)(2,1)S(1)} %get-tuple-element.89), channel_id=1, source_target_pairs={{0,16},{4,20},{8,24},{12,28},{16,0},{20,4},{24,8},{28,12},{1,17},{... | collective-permute-start | bytes 393224 | tf_op jit(solution)/shard_map/ppermute | solution.py:517
  91.1 39.0 %collective-permute-start.28 = (bf16[2,128,1024]{2,1,0:T(8,128)(2,1)S(1)}, bf16[2,128,1024]{2,1,0:T(8,128)(2,1)S(1)}, u32[]{:S(2)}, u32[]{:S(2)}) collective-permute-start(bf16[2,128,1024]{2,1,0:T(8,128)(2,1)S(1)} %pad_maximum_fusion.refs_0_), channel_id=1, source_target_pairs={{0,4},{4,0},{8,12},{12,8},{16,20},{20,16},{24,28},{28,24},{1,5},{5... | collective-permute-start | bytes 1572872 | tf_op jit(solution)/shard_map/ppermute | solution.py:517
  93.0 37.1 %collective-permute-start.29 = (bf16[2,128,1024]{2,1,0:T(8,128)(2,1)S(1)}, bf16[2,128,1024]{2,1,0:T(8,128)(2,1)S(1)}, u32[]{:S(2)}, u32[]{:S(2)}) collective-permute-start(bf16[2,128,1024]{2,1,0:T(8,128)(2,1)S(1)} %collective-permute-done.27.refs_1_), channel_id=1, source_target_pairs={{0,4},{4,0},{8,12},{12,8},{16,20},{20,16},{24,28},{28,24},{1,5},{5... | collective-permute-start | bytes 1572872 | tf_op jit(solution)/shard_map/ppermute | solution.py:517
  93.8 7.5 %collective-permute-start.31 = (bf16[4,144,128]{2,1,0:T(8,128)(2,1)S(1)}, bf16[4,144,128]{2,1,0:T(8,128)(2,1)S(1)}, u32[]{:S(2)}, u32[]{:S(2)}) collective-permute-start(bf16[4,144,128]{2,1,0:T(8,128)(2,1)S(1)} %shard_map.190.group), channel_id=1, source_target_pairs={{0,8},{4,12},{8,0},{12,4},{16,24},{20,28},{24,16},{28,20},{1,9},{5... | collective-permute-start | bytes 442376 | tf_op jit(solution)/shard_map/ppermute | solution.py:517
  98.7 6.8 %collective-permute-start.22 = (bf16[4,64,256]{2,1,0:T(8,128)(2,1)S(1)}, bf16[4,64,256]{2,1,0:T(8,128)(2,1)S(1)}, u32[]{:S(2)}, u32[]{:S(2)}) collective-permute-start(bf16[4,64,256]{2,1,0:T(8,128)(2,1)S(1)} %bitcast.27), channel_id=1, source_target_pairs={{0,8},{4,12},{8,0},{12,4},{16,24},{20,28},{24,16},{28,20},{1,9},{5... | collective-permute-start | bytes 393224 | tf_op jit(solution)/shard_map/ppermute | solution.py:517
  102.0 17.2 %collective-permute-start.32 = (bf16[4,144,128]{2,1,0:T(8,128)(2,1)S(1)}, bf16[4,144,128]{2,1,0:T(8,128)(2,1)S(1)}, u32[]{:S(2)}, u32[]{:S(2)}) collective-permute-start(bf16[4,144,128]{2,1,0:T(8,128)(2,1)S(1)} %get-tuple-element.102), channel_id=1, source_target_pairs={{0,16},{4,20},{8,24},{12,28},{16,0},{20,4},{24,8},{28,12},{1,17},{... | collective-permute-start | bytes 442376 | tf_op jit(solution)/shard_map/ppermute | solution.py:517
  106.1 13.1 %collective-permute-start.23 = (bf16[4,64,256]{2,1,0:T(8,128)(2,1)S(1)}, bf16[4,64,256]{2,1,0:T(8,128)(2,1)S(1)}, u32[]{:S(2)}, u32[]{:S(2)}) collective-permute-start(bf16[4,64,256]{2,1,0:T(8,128)(2,1)S(1)} %bitcast.28), channel_id=1, source_target_pairs={{0,4},{4,0},{8,12},{12,8},{16,20},{20,16},{24,28},{28,24},{1,5},{5... | collective-permute-start | bytes 393224 | tf_op jit(solution)/shard_map/ppermute | solution.py:517
  106.6 23.5 %collective-permute-start.24 = (bf16[4,64,256]{2,1,0:T(8,128)(2,1)S(1)}, bf16[4,64,256]{2,1,0:T(8,128)(2,1)S(1)}, u32[]{:S(2)}, u32[]{:S(2)}) collective-permute-start(bf16[4,64,256]{2,1,0:T(8,128)(2,1)S(1)} %bitcast.22), channel_id=1, source_target_pairs={{0,1},{1,0},{2,3},{3,2},{4,5},{5,4},{6,7},{7,6},{8,9},{9,8},{10,11... | collective-permute-start | bytes 393224 | tf_op jit(solution)/shard_map/ppermute | solution.py:517
  119.2 10.9 %collective-permute-start.25 = (bf16[4,64,256]{2,1,0:T(8,128)(2,1)S(1)}, bf16[4,64,256]{2,1,0:T(8,128)(2,1)S(1)}, u32[]{:S(2)}, u32[]{:S(2)}) collective-permute-start(bf16[4,64,256]{2,1,0:T(8,128)(2,1)S(1)} %collective-permute-done.23.a1), channel_id=1, source_target_pairs={{0,1},{1,0},{2,3},{3,2},{4,5},{5,4},{6,7},{7,6},{8,9},{9,8},{10,11... | collective-permute-start | bytes 393224 | tf_op jit(solution)/shard_map/ppermute | solution.py:517
  119.9 12.8 %collective-permute-start.33 = (bf16[4,128,128]{2,1,0:T(8,128)(2,1)S(1)}, bf16[4,128,128]{2,1,0:T(8,128)(2,1)S(1)}, u32[]{:S(2)}, u32[]{:S(2)}) collective-permute-start(bf16[4,128,128]{2,1,0:T(8,128)(2,1)S(1)} %get-tuple-element.106), channel_id=1, source_target_pairs={{0,4},{4,0},{8,12},{12,8},{16,20},{20,16},{24,28},{28,24},{1,5},{5... | collective-permute-start | bytes 393224 | tf_op jit(solution)/shard_map/ppermute | solution.py:517

commit v6 on v5

--- a/solution.py
+++ b/solution.py
@@ -11,6 +11,8 @@
 F32 = jnp.float32
 BF16 = jnp.bfloat16
 EXACT = lax.Precision.HIGHEST
+SP, TP = "sp", "tp"
+TALL, WIDE, PLAIN = range(3)
 
 
 def dot(a, b, ca=1, cb=0, precision=None):
@@ -94,42 +96,28 @@
 
 
 def gather_kernel(at, *refs, homes):
-    blocks, out, sems = refs[:-2], refs[-2], refs[-1]
+    blocks, out = refs[:-1], refs[-1]
     half = out.shape[2] // 2
     quarter = half // 2
-    copies = []
-
-    def copy(source, target):
-        copies.append(pltpu.make_async_copy(source, target, sems.at[len(copies)]))
-        copies[-1].start()
+
+    def put(low):
+        for block, (n, side) in zip(blocks, homes):
+            if side is not None:
+                for m in range(2):
+                    begin = m * half + (0 if (side == 0) == low else quarter)
+                    out[n, :, begin : begin + quarter] = block[:, m * quarter : (m + 1) * quarter]
 
     for block, (n, side) in zip(blocks, homes):
         if side is None:
-            copy(block, out.at[n])
-        else:
-            place = at[2] if side == 0 else 1 - at[2]
-            for m in range(2):
-                begin = pl.multiple_of(m * half + place * quarter, quarter)
-                copy(
-                    block.at[:, m * quarter : (m + 1) * quarter],
-                    out.at[n, :, pl.ds(begin, quarter)],
-                )
-    for each in copies:
-        each.wait()
-
-
-def gather(at, blocks, homes, experts, cap, width):
-    out = pl.pallas_call(
-        functools.partial(gather_kernel, homes=homes),
-        in_specs=[pl.BlockSpec(memory_space=pltpu.SMEM)]
-        + [pl.BlockSpec(memory_space=pl.ANY)] * len(blocks),
-        out_specs=pl.BlockSpec(memory_space=pltpu.VMEM),
-        out_shape=jax.ShapeDtypeStruct((experts, cap, width), BF16),
-        scratch_shapes=[pltpu.SemaphoreType.DMA((2 * len(blocks),))],
-        compiler_params=limit(4),
-        name="gather",
-    )(at, *blocks)
-    return out.reshape(experts * cap, width)
+            out[n] = block[...]
+
+    @pl.when(at[2] == 0)
+    def _():
+        put(True)
+
+    @pl.when(at[2] == 1)
+    def _():
+        put(False)
 
 
 def stage_kernel(at, *refs, kinds):
@@ -142,14 +130,14 @@
         copies[-1].start()
 
     for source, target, kind in zip(sources, outs, kinds):
-        if kind == "plain":
+        if kind == PLAIN:
             copy(source, target)
             continue
-        half = target.shape[1] if kind == "tall" else target.shape[2]
+        half = target.shape[1] if kind == TALL else target.shape[2]
         for side in range(2):
             begin = pl.multiple_of((at[0] if side == 0 else 1 - at[0]) * half, half)
             cut = pl.ds(begin, half)
-            copy(source.at[cut, :] if kind == "tall" else source.at[:, cut], target.at[side])
+            copy(source.at[cut, :] if kind == TALL else source.at[:, cut], target.at[side])
     for each in copies:
         each.wait()
 
@@ -157,9 +145,9 @@
 def stage(at, kinds, arrays):
     shapes = []
     for a, kind in zip(arrays, kinds):
-        if kind == "tall":
+        if kind == TALL:
             shapes.append(pltpu.VMEM((2, a.shape[0] // 2, a.shape[1]), a.dtype))
-        elif kind == "wide":
+        elif kind == WIDE:
             shapes.append(pltpu.VMEM((2, a.shape[0], a.shape[1] // 2), a.dtype))
         else:
             shapes.append(pltpu.VMEM(a.shape, a.dtype))
@@ -204,62 +192,86 @@
         block[...] = (a[cut, :].astype(F32) + b[cut, :].astype(F32)).astype(BF16)
 
 
-def add_kernel(at, a, b, out):
-    out[...] = (a[...].astype(F32) + b[...].astype(F32)).astype(out.dtype)
-
-
-def weights_kernel(core, ra, rb, ga, gb, hidden, gback, uback, gate_out, up_out, down_out):
+def weights_kernel(core, ra, rb, gback, uback, gate_out, up_out):
     step = pl.program_id(0)
     turn = pl.num_programs(0) // 2
 
-    def write(r, g):
+    def write(r):
         gate_out[...] = dot(r[...], gback[...], 0, 0).astype(BF16)
         up_out[...] = dot(r[...], uback[...], 0, 0).astype(BF16)
-        down_out[...] = dot(hidden[...], g[...], 0, 0).astype(BF16)
 
     @pl.when(step < turn)
     def _():
-        write(ra, ga)
+        write(ra)
 
     @pl.when(step >= turn)
     def _():
-        write(rb, gb)
-
-
-def weight_grads(core, own, other, hidden, gback, uback):
+        write(rb)
+
+
+def down_kernel(core, ga, gb, hidden, out):
+    step = pl.program_id(0)
+    turn = pl.num_programs(0) // 2
+
+    @pl.when(step < turn)
+    def _():
+        out[...] = dot(hidden[...], ga[...], 0, 0).astype(BF16)
+
+    @pl.when(step >= turn)
+    def _():
+        out[...] = dot(hidden[...], gb[...], 0, 0).astype(BF16)
+
+
+def weight_grads(core, own, other, gback, uback):
     rows, width = own.shape
     half = width // 2
-    units = hidden.shape[1]
+    units = gback.shape[1]
     chunk = min(half, 512)
     turn = half // chunk
-    near = lambda i: jnp.minimum(i, turn - 1)
-    far = lambda i: jnp.maximum(i - turn, 0)
     at = lambda i, c: jnp.where(i < turn, c[0] * turn + i, (1 - c[0]) * turn + i - turn)
     full = pl.BlockSpec((rows, units), lambda i, c: (0, 0))
     tall = pl.BlockSpec((None, chunk, units), lambda i, c: (0, at(i, c), 0))
-    wide = pl.BlockSpec((None, units, chunk), lambda i, c: (0, 0, at(i, c)))
     return pl.pallas_call(
         weights_kernel,
         grid_spec=pltpu.PrefetchScalarGridSpec(
             num_scalar_prefetch=1,
             grid=(2 * turn,),
             in_specs=[
-                pl.BlockSpec((rows, chunk), lambda i, c: (0, near(i))),
-                pl.BlockSpec((rows, chunk), lambda i, c: (0, far(i))),
-                pl.BlockSpec((rows, chunk), lambda i, c: (0, turn + near(i))),
-                pl.BlockSpec((rows, chunk), lambda i, c: (0, turn + far(i))),
-                full, full, full,
+                pl.BlockSpec((rows, chunk), lambda i, c: (0, jnp.minimum(i, turn - 1))),
+                pl.BlockSpec((rows, chunk), lambda i, c: (0, jnp.maximum(i - turn, 0))),
+                full, full,
             ],
-            out_specs=[tall, tall, wide],
+            out_specs=[tall, tall],
         ),
-        out_shape=[
-            jax.ShapeDtypeStruct((1, width, units), BF16),
-            jax.ShapeDtypeStruct((1, width, units), BF16),
-            jax.ShapeDtypeStruct((1, units, width), BF16),
-        ],
-        compiler_params=limit(20),
-        name="weight_grads",
-    )(core, own, other, own, other, hidden, gback, uback)
+        out_shape=[jax.ShapeDtypeStruct((1, width, units), BF16)] * 2,
+        compiler_params=limit(16),
+        name="weights",
+    )(core, own, other, gback, uback)
+
+
+def down_grads(core, own, other, hidden):
+    rows, width = own.shape
+    half = width // 2
+    units = hidden.shape[1]
+    chunk = min(half, 512)
+    turn = half // chunk
+    at = lambda i, c: jnp.where(i < turn, c[0] * turn + i, (1 - c[0]) * turn + i - turn)
+    return pl.pallas_call(
+        down_kernel,
+        grid_spec=pltpu.PrefetchScalarGridSpec(
+            num_scalar_prefetch=1,
+            grid=(2 * turn,),
+            in_specs=[
+                pl.BlockSpec((rows, chunk), lambda i, c: (0, turn + jnp.minimum(i, turn - 1))),
+                pl.BlockSpec((rows, chunk), lambda i, c: (0, turn + jnp.maximum(i - turn, 0))),
+                pl.BlockSpec((rows, units), lambda i, c: (0, 0)),
+            ],
+            out_specs=pl.BlockSpec((None, units, chunk), lambda i, c: (0, 0, at(i, c))),
+        ),
+        out_shape=jax.ShapeDtypeStruct((1, units, width), BF16),
+        compiler_params=limit(12),
+        name="down",
+    )(core, own, other, hidden)
 
 
 def combine_kernel(at, place, *refs):
@@ -272,28 +284,9 @@
     out[...] = total.astype(BF16)
 
 
-def base_kernel(at, g, part, out):
-    out[...] = g[...].astype(F32) + part[...].astype(F32)
-
-
-def base_sum(at, g, part):
-    tokens, half = part.shape
-    whole = lambda i, c: (0, 0)
-    return pl.pallas_call(
-        base_kernel,
-        grid_spec=pltpu.PrefetchScalarGridSpec(
-            num_scalar_prefetch=1,
-            grid=(1,),
-            in_specs=[
-                pl.BlockSpec((tokens, half), lambda i, c: (0, c[0])),
-                pl.BlockSpec((tokens, half), whole),
-            ],
-            out_specs=pl.BlockSpec((tokens, half), whole),
-        ),
-        out_shape=jax.ShapeDtypeStruct((tokens, half), F32),
-        compiler_params=limit(4),
-        name="base",
-    )(at, in_hbm(g), part)
+def sum_kernel(at, g, own, came, out):
+    total = own[...].astype(F32) + came[...].astype(F32)
+    out[...] = (g[0].astype(F32) + total).astype(BF16)
 
 
 def decays(log_decay, head):
@@ -521,8 +514,12 @@
     return list(range(count // 2, count)) + list(range(count // 2 - 1, 0, -1))
 
 
+def way_back(count):
+    return list(range(count - 1, 0, -1))
+
+
 def shared_far(count):
-    return far_first(count)[: count // 2 - 1]
+    return far_first(count)[: count // 2]
 
 
 def bits_of(count):
@@ -546,10 +543,10 @@
 ):
     tokens, width = moe_input.shape
     half = width // 2
-    sp = lax.axis_size("sp")
-    tp = lax.axis_size("tp")
-    place = lax.axis_index("sp").astype(jnp.int32)
-    column = lax.axis_index("tp").astype(jnp.int32)
+    sp = lax.axis_size(SP)
+    tp = lax.axis_size(TP)
+    place = lax.axis_index(SP).astype(jnp.int32)
+    column = lax.axis_index(TP).astype(jnp.int32)
     core = column & 1
     at = jnp.stack([core, place, (column >> 1) & 1])
     experts = w_gate.shape[0] * sp
@@ -562,13 +559,13 @@
     picked, *sent = dispatch(at, routes.T, route_weight.T, moe_input, out_grad, experts, cap)
     came = {0: sent[0]}
     for n in far_first(sp):
-        came[n] = swap(sent[n], "sp", n)
-    wg, q, k, v, state, decay = stage(
-        at, ("tall",) + ("plain",) * 5,
-        (w_gate[0], query_heads, key_heads, value_heads, state_in, log_decay),
-    )
-    wu, wd = stage(at, ("tall", "wide"), (w_up[0], w_down[0]))
-    (wo,) = stage(at, ("tall",), (w_out,))
+        came[n] = swap(sent[n], SP, n)
+    wg, grad, q, k, v, state, decay = stage(
+        at, (TALL, WIDE) + (PLAIN,) * 5,
+        (w_gate[0], out_grad, query_heads, key_heads, value_heads, state_in, log_decay),
+    )
+    wu, wd = stage(at, (TALL, WIDE), (w_up[0], w_down[0]))
+    (wo,) = stage(at, (TALL,), (w_out,))
     mixed = small(
         mixed_kernel, jax.ShapeDtypeStruct((tokens, heads * value_size), BF16),
         at, q, k, v, decay, state,
@@ -578,17 +575,20 @@
         blocks.append(came[n])
         homes.append((n, 0 if n in shared_far(sp) else None))
         if n in shared_far(sp):
-            blocks.append(swap(came[n], "tp", 2))
+            blocks.append(swap(came[n], TP, 2))
             homes.append((n, 1))
-    own = gather(at, blocks, tuple(homes), experts, cap, width)
-    other = swap(own, "tp", 1)
+    own = small(
+        functools.partial(gather_kernel, homes=tuple(homes)),
+        jax.ShapeDtypeStruct((experts, cap, width), BF16), at, *blocks,
+    ).reshape(slots, width)
+    other = swap(own, TP, 1)
     hidden, gate_back, up_back, part_b = small(
         expert_kernel,
         [jax.ShapeDtypeStruct((slots, units), BF16)] * 3
         + [jax.ShapeDtypeStruct((slots, half), BF16)],
         at, own, other, wg, wu, wd, mib=16,
     )
-    part_came = swap(part_b, "tp", 1)
+    part_came = swap(part_b, TP, 1)
     part_a = small(
         partial_kernel, jax.ShapeDtypeStruct((slots, half), BF16),
         at, gate_back, up_back, wg, wu,
@@ -598,30 +598,30 @@
         at, part_a, part_came,
     )
     back = {0: parts_out[0]}
-    for n in far_first(sp):
-        back[n] = swap(parts_out[n], "sp", n)
-    gate_grad, up_grad, down_grad = weight_grads(at, own, other, hidden, gate_back, up_back)
+    for n in way_back(sp):
+        back[n] = swap(parts_out[n], SP, n)
+    gate_grad, up_grad = weight_grads(at, own, other, gate_back, up_back)
+    down_grad = down_grads(at, own, other, hidden)
 
     blocks = mixed[None]
     parts = []
     for bit in reversed(bits_of(sp)):
         if not parts:
-            parts = [jnp.concatenate([blocks, swap(blocks, "sp", bit)], axis=0)]
+            parts = [jnp.concatenate([blocks, swap(blocks, SP, bit)], axis=0)]
         else:
             came = []
             for piece in parts:
-                came.append(swap(piece, "sp", bit))
+                came.append(swap(piece, SP, bit))
             parts = parts + came
 
     token_shape = jax.ShapeDtypeStruct((tokens, half), BF16)
     token_part = small(combine_kernel, token_shape, at, picked, *[back[n] for n in range(sp)])
     for bit in bits_of(tp)[1:]:
-        came = swap(token_part, "tp", bit)
+        came = swap(token_part, TP, bit)
         if bit * 2 < tp:
             token_part = (token_part.astype(F32) + came.astype(F32)).astype(BF16)
-    base = base_sum(at, out_grad, token_part)
-    mixed_a = small(add_kernel, token_shape, at, base, came)
-    mixed_b = swap(mixed_a, "tp", 1)
+    mixed_a = small(sum_kernel, token_shape, at, grad, token_part, came)
+    mixed_b = swap(mixed_a, TP, 1)
 
     message = jax.ShapeDtypeStruct((heads, size + PIECES, value_size // 2), BF16)
     turn = sp // 2
@@ -634,7 +634,7 @@
     )
     sources, slices = 1, []
     for bit in reversed(bits_of(sp)):
-        came_slices = swap(leave, "sp", bit)
+        came_slices = swap(leave, SP, bit)
         if bit > 1:
             grid = (sources, bit) + block
             out = jax.ShapeDtypeStruct((2 * sources, bit // 2) + block, BF16)
@@ -646,8 +646,8 @@
         stay, leave = stay.reshape((turn,) + block), leave.reshape((turn,) + block)
     slices = [stay, came_slices.reshape((turn,) + block)]
     for n in range(2):
-        slices.append(swap(slices[n], "tp", 1))
-    first_came = swap(send, "sp", 1)
+        slices.append(swap(slices[n], TP, 1))
+    first_came = swap(send, SP, 1)
     q_grad, k_part, v_part, trails = small(
         local_kernel,
         [
@@ -664,7 +664,7 @@
     later = jnp.zeros(state_shape, F32)
     reach = jnp.ones((heads, 128), F32)
     for bit in bits_of(sp)[1:]:
-        came_state = swap(group, "sp", bit)
+        came_state = swap(group, SP, bit)
         if bit * 2 < sp:
             group, later, reach = small(
                 functools.partial(join_kernel, bit=bit),
@@ -677,7 +677,7 @@
         functools.partial(close_kernel, bit=bit),
         [state_out, state_out], at, came_state, later, reach, keep, first_came,
     )
-    other_state = swap(send_state, "sp", 1)
+    other_state = swap(send_state, SP, 1)
     out_proj_grad = project(at, slices, parts)
     k_grad, v_grad = small(
         final_kernel,
@@ -693,28 +693,28 @@
         step,
         mesh=mesh,
         in_specs=(
-            P("sp", None),
-            P("sp", None),
-            P("sp", None),
-            P("sp", None),
-            P("sp", None, "tp"),
-            P("sp", None, "tp"),
-            P("sp", "tp", None),
-            P(None, "tp"),
-            P("tp", "sp", None),
-            P("tp", "sp", None),
-            P("tp", "sp", None),
-            P("tp", "sp"),
-            P("tp", "sp", None, None),
+            P(SP, None),
+            P(SP, None),
+            P(SP, None),
+            P(SP, None),
+            P(SP, None, TP),
+            P(SP, None, TP),
+            P(SP, TP, None),
+            P(None, TP),
+            P(TP, SP, None),
+            P(TP, SP, None),
+            P(TP, SP, None),
+            P(TP, SP),
+            P(TP, SP, None, None),
         ),
         out_specs=(
-            P("sp", None, "tp"),
-            P("sp", None, "tp"),
-            P("sp", "tp", None),
-            P("sp", "tp"),
-            P("tp", "sp", None),
-            P("tp", "sp", None),
-            P("tp", "sp", None),
+            P(SP, None, TP),
+            P(SP, None, TP),
+            P(SP, TP, None),
+            P(SP, TP),
+            P(TP, SP, None),
+            P(TP, SP, None),
+            P(TP, SP, None),
         ),
         check_vma=False,
     )

time: 135 us -> 134 us (level)
  waiting for transfers between devices: 33.7 us -> 39.3 us
  starting transfers between devices: 58.8 us -> 53.4 us
    ppermute x34 -> x35, waiting for transfers between devices: 33.7 us -> 39.3 us  [swap(): return lax.ppermute(a, axis, [(i, i ^ bit) for i in range(count)])]
    ppermute x34 -> x35, starting transfers between devices: 58.8 us -> 53.4 us  [swap(): return lax.ppermute(a, axis, [(i, i ^ bit) for i in range(count)])]
    pallas_call x1, Pallas kernels: 6.29 us -> 4.93 us  [weight_grads(): pl.pallas_call(weights_kernel, grid_spec=pltpu.PrefetchScalarGridSpec(num...]
    pallas_call x14 -> x15, Pallas kernels: 18 us -> 18.7 us  [small(): pl.pallas_call(kernel, in_specs=[pl.BlockSpec(memory_space=pltpu.SMEM)] +...]
    pallas_call x2 -> x1, Pallas kernels: 3.55 us -> 3.77 us  [down_grads(): pl.pallas_call(down_kernel, grid_spec=pltpu.PrefetchScalarGridSpec(num_sc...]
  transfers between devices with their start and end apart: 34 -> 35, of which waited for: 9 -> 12; matrix products, arithmetic and copies ran while one was open for 0% -> 0% of each run, Pallas kernels for 23% -> 24%
where the time goes in v6:
time: 134 us
  starting transfers between devices  53.4 us (40%)
  Pallas kernels  40.5 us (30%)
  waiting for transfers between devices  39.3 us (29%)
    ppermute x35, starting transfers between devices, swap(): return lax.ppermute(a, axis, [(i, i ^ bit) for i in range(count)])  53.4 us
    ppermute x35, waiting for transfers between devices, swap(): return lax.ppermute(a, axis, [(i, i ^ bit) for i in range(count)])  39.3 us
    pallas_call x15, Pallas kernels, small(): pl.pallas_call(kernel, in_specs=[pl.BlockSpec(memory_space=pltpu.SMEM)] +...  18.7 us
    pallas_call x3, Pallas kernels, stage(): pl.pallas_call(functools.partial(stage_kernel, kinds=kinds), in_specs=[pl...  8.2 us
    pallas_call x1, Pallas kernels, weight_grads(): pl.pallas_call(weights_kernel, grid_spec=pltpu.PrefetchScalarGridSpec(num...  4.93 us
    pallas_call x1, Pallas kernels, down_grads(): pl.pallas_call(down_kernel, grid_spec=pltpu.PrefetchScalarGridSpec(num_sc...  3.77 us
  transfers between devices with their start and end apart: 35, of which 12 were waited for; matrix products, arithmetic and copies ran while one was open for 0% of the time, Pallas kernels for 24%

profile of v6, /device:TPU:0, one launch (start us, length us, event | category | flops | bytes accessed | tf_op | source)
XLA Modules:
  0.0 134.2 jit_solution(16802222976341536782)
XLA Ops:
  0.7 2.4 %dispatch.1 = (bf16[320,128]{1,0:T(8,128)(2,1)S(1)}, bf16[40,2048]{1,0:T(8,128)(2,1)S(1)}, bf16[40,2048]{1,0:T(8,128)(2,1)S(1)}, bf16[40,2048]{1,0:T(8,128)(2,1)...) custom-call(s32[3]{0:T(128)S(1)} %pad_add_fusion.at.core, ...), custom_call_target="tpu_custom_call" | custom-call | tf_op jit(solution)/shard_map/dispatch/pallas_call | solution.py:80
  3.1 6.1 %collective-permute-start.9 = (bf16[40,1024]{1,0:T(8,128)(2,1)S(1)}, bf16[40,1024]{1,0:T(8,128)(2,1)S(1)}, u32[]{:S(2)}, u32[]{:S(2)}) collective-permute-start(bf16[40,1024]{1,0:T(8,128)(2,1)S(1)} %get-tuple-element.66), channel_id=1, source_target_pairs={{0,28},{4,24},{8,20},{12,16},{16,12},{20,8},{24,4},{28,0},{1,29},{... | collective-permute-start | bytes 245768 | tf_op jit(solution)/shard_map/ppermute | solution.py:510
  9.2 2.9 %collective-permute-start.5 = (bf16[40,1024]{1,0:T(8,128)(2,1)S(1)}, bf16[40,1024]{1,0:T(8,128)(2,1)S(1)}, u32[]{:S(2)}, u32[]{:S(2)}) collective-permute-start(bf16[40,1024]{1,0:T(8,128)(2,1)S(1)} %get-tuple-element.64), channel_id=1, source_target_pairs={{0,20},{4,16},{8,28},{12,24},{16,4},{20,0},{24,12},{28,8},{1,21},{... | collective-permute-start | bytes 245768 | tf_op jit(solution)/shard_map/ppermute | solution.py:510
  12.2 1.6 %collective-permute-start = (bf16[40,2048]{1,0:T(8,128)(2,1)S(1)}, bf16[40,2048]{1,0:T(8,128)(2,1)S(1)}, u32[]{:S(2)}, u32[]{:S(2)}) collective-permute-start(bf16[40,2048]{1,0:T(8,128)(2,1)S(1)} %get-tuple-element.60), channel_id=1, source_target_pairs={{0,4},{4,0},{8,12},{12,8},{16,20},{20,16},{24,28},{28,24},{1,5},{5... | collective-permute-start | bytes 491528 | tf_op jit(solution)/shard_map/ppermute | solution.py:510
  13.8 1.5 %collective-permute-start.10 = (bf16[40,1024]{1,0:T(8,128)(2,1)S(1)}, bf16[40,1024]{1,0:T(8,128)(2,1)S(1)}, u32[]{:S(2)}, u32[]{:S(2)}) collective-permute-start(bf16[40,1024]{1,0:T(8,128)(2,1)S(1)} %collective-permute-done.9.refs_10_), channel_id=1, source_target_pairs={{0,2},{1,3},{2,0},{3,1},{4,6},{5,7},{6,4},{7,5},{8,10},{9,11},{10,... | collective-permute-start | bytes 245768 | tf_op jit(solution)/shard_map/ppermute | solution.py:510
  15.3 5.0 %collective-permute-done.3.refs_4_ = bf16[40,1024]{1,0:T(8,128)(2,1)S(1)} collective-permute-done((bf16[40,1024]{1,0:T(8,128)(2,1)S(1)}, bf16[40,1024]{1,0:T(8,128)(2,1)S(1)}, u32[]{:S(2)}, u32[]{:S(2)}) %collective-permute-start.3) | collective-permute-done | bytes 81952 | tf_op jit(solution)/shard_map/ppermute | solution.py:510
  20.3 1.5 %collective-permute-start.4 = (bf16[40,1024]{1,0:T(8,128)(2,1)S(1)}, bf16[40,1024]{1,0:T(8,128)(2,1)S(1)}, u32[]{:S(2)}, u32[]{:S(2)}) collective-permute-start(bf16[40,1024]{1,0:T(8,128)(2,1)S(1)} %collective-permute-done.3.refs_4_), channel_id=1, source_target_pairs={{0,2},{1,3},{2,0},{3,1},{4,6},{5,7},{6,4},{7,5},{8,10},{9,11},{10,... | collective-permute-start | bytes 245768 | tf_op jit(solution)/shard_map/ppermute | solution.py:510
  22.1 2.9 %collective-permute-start.2 = (bf16[40,2048]{1,0:T(8,128)(2,1)S(1)}, bf16[40,2048]{1,0:T(8,128)(2,1)S(1)}, u32[]{:S(2)}, u32[]{:S(2)}) collective-permute-start(bf16[40,2048]{1,0:T(8,128)(2,1)S(1)} %get-tuple-element.62), channel_id=1, source_target_pairs={{0,12},{4,8},{8,4},{12,0},{16,28},{20,24},{24,20},{28,16},{1,13},{... | collective-permute-start | bytes 491528 | tf_op jit(solution)/shard_map/ppermute | solution.py:510
  25.0 1.5 %collective-permute-start.6 = (bf16[40,1024]{1,0:T(8,128)(2,1)S(1)}, bf16[40,1024]{1,0:T(8,128)(2,1)S(1)}, u32[]{:S(2)}, u32[]{:S(2)}) collective-permute-start(bf16[40,1024]{1,0:T(8,128)(2,1)S(1)} %collective-permute-done.5.refs_6_), channel_id=1, source_target_pairs={{0,2},{1,3},{2,0},{3,1},{4,6},{5,7},{6,4},{7,5},{8,10},{9,11},{10,... | collective-permute-start | bytes 245768 | tf_op jit(solution)/shard_map/ppermute | solution.py:510
  27.0 2.4 %collective-permute-done.6.refs_7_ = bf16[40,1024]{1,0:T(8,128)(2,1)S(1)} collective-permute-done((bf16[40,1024]{1,0:T(8,128)(2,1)S(1)}, bf16[40,1024]{1,0:T(8,128)(2,1)S(1)}, u32[]{:S(2)}, u32[]{:S(2)}) %collective-permute-start.6) | collective-permute-done | bytes 81952 | tf_op jit(solution)/shard_map/ppermute | solution.py:510
  29.4 1.5 %collective-permute-done.8.refs_9_ = bf16[40,1024]{1,0:T(8,128)(2,1)S(1)} collective-permute-done((bf16[40,1024]{1,0:T(8,128)(2,1)S(1)}, bf16[40,1024]{1,0:T(8,128)(2,1)S(1)}, u32[]{:S(2)}, u32[]{:S(2)}) %collective-permute-start.8) | collective-permute-done | bytes 81952 | tf_op jit(solution)/shard_map/ppermute | solution.py:510
  32.0 2.8 %stage.4 = (bf16[2,1024,512]{2,1,0:T(8,128)(2,1)S(1)}, bf16[2,512,1024]{2,1,0:T(8,128)(2,1)S(1)}) custom-call(s32[3]{0:T(128)S(1)} %pad_add_fusion.at.core, bf16[2048,512]{1,0:T(8,128)(2,1)} %bitcast.30, bf16[512,2048]{1,0:T(8,128)(2,1)} %bitcast.31), custom_call_target="tpu_custom_call" | custom-call | tf_op jit(solution)/shard_map/stage/pallas_call | solution.py:155
  34.7 2.7 %stage.3 = (bf16[2,1024,512]{2,1,0:T(8,128)(2,1)S(1)}, bf16[2,128,1024]{2,1,0:T(8,128)(2,1)S(1)}, bf16[4,128,128]{2,1,0:T(8,128)(2,1)S(1)}, bf16[4,128,128]{2,1,...) custom-call(s32[3]{0:T(128)S(1)} %pad_add_fusion.at.core, ...), custom_call_target="tpu_custom_call" | custom-call | tf_op jit(solution)/shard_map/stage/pallas_call | solution.py:155
  37.4 3.6 %shard_map.181 = (bf16[320,512]{1,0:T(8,128)(2,1)S(1)}, bf16[320,512]{1,0:T(8,128)(2,1)S(1)}, bf16[320,512]{1,0:T(8,128)(2,1)S(1)}, bf16[320,1024]{1,0:T(8,128)(2,1)S(1)}) custom-call(s32[3]{0:T(128)S(1)} %pad_add_fusion.at.core, bf16[320,2048]{1,0:T(8,128)(2,1)S(1)} %bitcast.17, bf16[320,2048]{1,0:T(8,128)(2,1)S(1)} %collective-permute-done.11.other.rb.gb, ...), custom_call_target="tpu_custom_call" | custom-call | tf_op jit(solution)/shard_map/pallas_call | solution.py:428
  41.6 1.1 shard_map.189
  42.6 1.0 collective-permute-start.27
  43.7 1.4 %shard_map.182.a = bf16[320,1024]{1,0:T(8,128)(2,1)S(1)} custom-call(s32[3]{0:T(128)S(1)} %pad_add_fusion.at.core, bf16[320,512]{1,0:T(8,128)(2,1)S(1)} %get-tuple-element.70.gback, bf16[320,512]{1,0:T(8,128)(2,1)S(1)} %get-tuple-element.71.uback, bf16[2,1024,512]{2,1,0:T(8,128)(2,1)S(1)} %get-tuple-element.67.wg, bf16[2,1024,512]{2,1,0:T(8,128)(2,1)S(1)} %get-tuple-element.68.wu), custom_call_target="tpu_custom_call" | custom-call | tf_op jit(solution)/shard_map/pallas_call | solution.py:428
  45.8 1.0 collective-permute-start.13
  46.8 1.8 %collective-permute-start.14 = (bf16[40,1024]{1,0:T(8,128)(2,1)S(1)}, bf16[40,1024]{1,0:T(8,128)(2,1)S(1)}, u32[]{:S(2)}, u32[]{:S(2)}) collective-permute-start(bf16[40,1024]{1,0:T(8,128)(2,1)S(1)} %get-tuple-element.80), channel_id=1, source_target_pairs={{0,8},{4,12},{8,0},{12,4},{16,24},{20,28},{24,16},{28,20},{1,9},{5... | collective-permute-start | bytes 245768 | tf_op jit(solution)/shard_map/ppermute | solution.py:510
  49.3 1.9 %collective-permute-start.16 = (bf16[40,1024]{1,0:T(8,128)(2,1)S(1)}, bf16[40,1024]{1,0:T(8,128)(2,1)S(1)}, u32[]{:S(2)}, u32[]{:S(2)}) collective-permute-start(bf16[40,1024]{1,0:T(8,128)(2,1)S(1)} %get-tuple-element.82), channel_id=1, source_target_pairs={{0,16},{4,20},{8,24},{12,28},{16,0},{20,4},{24,8},{28,12},{1,17},{... | collective-permute-start | bytes 245768 | tf_op jit(solution)/shard_map/ppermute | solution.py:510
  51.3 1.3 collective-permute-start.17
  52.6 2.2 %collective-permute-start.18 = (bf16[40,1024]{1,0:T(8,128)(2,1)S(1)}, bf16[40,1024]{1,0:T(8,128)(2,1)S(1)}, u32[]{:S(2)}, u32[]{:S(2)}) collective-permute-start(bf16[40,1024]{1,0:T(8,128)(2,1)S(1)} %get-tuple-element.84), channel_id=1, source_target_pairs={{0,24},{4,28},{8,16},{12,20},{16,8},{20,12},{24,0},{28,4},{1,25},{... | collective-permute-start | bytes 245768 | tf_op jit(solution)/shard_map/ppermute | solution.py:510
  54.8 2.2 %collective-permute-done.15.refs_3_ = bf16[40,1024]{1,0:T(8,128)(2,1)S(1)} collective-permute-done((bf16[40,1024]{1,0:T(8,128)(2,1)S(1)}, bf16[40,1024]{1,0:T(8,128)(2,1)S(1)}, u32[]{:S(2)}, u32[]{:S(2)}) %collective-permute-start.15) | collective-permute-done | bytes 81952 | tf_op jit(solution)/shard_map/ppermute | solution.py:510
  57.0 2.2 %collective-permute-start.19 = (bf16[40,1024]{1,0:T(8,128)(2,1)S(1)}, bf16[40,1024]{1,0:T(8,128)(2,1)S(1)}, u32[]{:S(2)}, u32[]{:S(2)}) collective-permute-start(bf16[40,1024]{1,0:T(8,128)(2,1)S(1)} %get-tuple-element.85), channel_id=1, source_target_pairs={{0,28},{4,24},{8,20},{12,16},{16,12},{20,8},{24,4},{28,0},{1,29},{... | collective-permute-start | bytes 245768 | tf_op jit(solution)/shard_map/ppermute | solution.py:510
  59.2 7.1 %collective-permute-done.16.refs_4_ = bf16[40,1024]{1,0:T(8,128)(2,1)S(1)} collective-permute-done((bf16[40,1024]{1,0:T(8,128)(2,1)S(1)}, bf16[40,1024]{1,0:T(8,128)(2,1)S(1)}, u32[]{:S(2)}, u32[]{:S(2)}) %collective-permute-start.16) | collective-permute-done | bytes 81952 | tf_op jit(solution)/shard_map/ppermute | solution.py:510
  66.3 1.8 %collective-permute-done.17.refs_5_ = bf16[40,1024]{1,0:T(8,128)(2,1)S(1)} collective-permute-done((bf16[40,1024]{1,0:T(8,128)(2,1)S(1)}, bf16[40,1024]{1,0:T(8,128)(2,1)S(1)}, u32[]{:S(2)}, u32[]{:S(2)}) %collective-permute-start.17) | collective-permute-done | bytes 81952 | tf_op jit(solution)/shard_map/ppermute | solution.py:510
  68.1 1.3 shard_map.184.own
  69.4 1.5 %collective-permute-start.20 = (bf16[128,1024]{1,0:T(8,128)(2,1)S(1)}, bf16[128,1024]{1,0:T(8,128)(2,1)S(1)}, u32[]{:S(2)}, u32[]{:S(2)}) collective-permute-start(bf16[128,1024]{1,0:T(8,128)(2,1)S(1)} %shard_map.184.own), channel_id=1, source_target_pairs={{0,2},{1,3},{2,0},{3,1},{4,6},{5,7},{6,4},{7,5},{8,10},{9,11},{10,... | collective-permute-start | bytes 786440 | tf_op jit(solution)/shard_map/ppermute | solution.py:510
  70.9 4.1 %collective-permute-start.28 = (bf16[2,128,1024]{2,1,0:T(8,128)(2,1)S(1)}, bf16[2,128,1024]{2,1,0:T(8,128)(2,1)S(1)}, u32[]{:S(2)}, u32[]{:S(2)}) collective-permute-start(bf16[2,128,1024]{2,1,0:T(8,128)(2,1)S(1)} %pad_maximum_fusion.refs_0_), channel_id=1, source_target_pairs={{0,8},{4,12},{8,0},{12,4},{16,24},{20,28},{24,16},{28,20},{1,9},{5... | collective-permute-start | bytes 1572872 | tf_op jit(solution)/shard_map/ppermute | solution.py:510
  75.0 2.4 %collective-permute-done.20.came = bf16[128,1024]{1,0:T(8,128)(2,1)S(1)} collective-permute-done((bf16[128,1024]{1,0:T(8,128)(2,1)S(1)}, bf16[128,1024]{1,0:T(8,128)(2,1)S(1)}, u32[]{:S(2)}, u32[]{:S(2)}) %collective-permute-start.20) | collective-permute-done | bytes 262176 | tf_op jit(solution)/shard_map/ppermute | solution.py:510
  78.0 2.8 %stage.5.wo = bf16[2,1024,1024]{2,1,0:T(8,128)(2,1)S(1)} custom-call(s32[3]{0:T(128)S(1)} %pad_add_fusion.at.core, bf16[2048,1024]{1,0:T(8,128)(2,1)} %refs_0_.1), custom_call_target="tpu_custom_call" | custom-call | tf_op jit(solution)/shard_map/stage/pallas_call | solution.py:155
  80.9 2.4 %shard_map.186 = (bf16[4,128,256]{2,1,0:T(8,128)(2,1)S(1)}, bf16[4,144,128]{2,1,0:T(8,128)(2,1)S(1)}, bf16[4,144,128]{2,1,0:T(8,128)(2,1)S(1)}, bf16[4,64,256]{2,1,0:T(8,128)(2,1)S(1)}, bf16[4,64,256]{2,1,0:T(8,128)(2,1)S(1)}) custom-call(s32[3]{0:T(128)S(1)} %pad_add_fusion.at.core, bf16[128,1024]{1,0:T(8,128)(2,1)S(1)} %shard_map.185.ma, ...), custom_call_target="tpu_custom_call" | custom-call | tf_op jit(solution)/shard_map/pallas_call | solution.py:428
  83.3 1.7 %collective-permute-start.31 = (bf16[4,144,128]{2,1,0:T(8,128)(2,1)S(1)}, bf16[4,144,128]{2,1,0:T(8,128)(2,1)S(1)}, u32[]{:S(2)}, u32[]{:S(2)}) collective-permute-start(bf16[4,144,128]{2,1,0:T(8,128)(2,1)S(1)} %get-tuple-element.101), channel_id=1, source_target_pairs={{0,4},{4,0},{8,12},{12,8},{16,20},{20,16},{24,28},{28,24},{1,5},{5... | collective-permute-start | bytes 442376 | tf_op jit(solution)/shard_map/ppermute | solution.py:510
  85.0 4.5 %collective-permute-start.22 = (bf16[4,64,256]{2,1,0:T(8,128)(2,1)S(1)}, bf16[4,64,256]{2,1,0:T(8,128)(2,1)S(1)}, u32[]{:S(2)}, u32[]{:S(2)}) collective-permute-start(bf16[4,64,256]{2,1,0:T(8,128)(2,1)S(1)} %get-tuple-element.89), channel_id=1, source_target_pairs={{0,16},{4,20},{8,24},{12,28},{16,0},{20,4},{24,8},{28,12},{1,17},{... | collective-permute-start | bytes 393224 | tf_op jit(solution)/shard_map/ppermute | solution.py:510
  89.6 0.9 collective-permute-start.29
  90.5 1.1 collective-permute-start.30
  92.3 2.6 %collective-permute-start.32 = (bf16[4,144,128]{2,1,0:T(8,128)(2,1)S(1)}, bf16[4,144,128]{2,1,0:T(8,128)(2,1)S(1)}, u32[]{:S(2)}, u32[]{:S(2)}) collective-permute-start(bf16[4,144,128]{2,1,0:T(8,128)(2,1)S(1)} %shard_map.191.group), channel_id=1, source_target_pairs={{0,8},{4,12},{8,0},{12,4},{16,24},{20,28},{24,16},{28,20},{1,9},{5... | collective-permute-start | bytes 442376 | tf_op jit(solution)/shard_map/ppermute | solution.py:510
  94.9 1.5 %collective-permute-done.22 = bf16[4,64,256]{2,1,0:T(8,128)(2,1)S(1)} collective-permute-done((bf16[4,64,256]{2,1,0:T(8,128)(2,1)S(1)}, bf16[4,64,256]{2,1,0:T(8,128)(2,1)S(1)}, u32[]{:S(2)}, u32[]{:S(2)}) %collective-permute-start.22) | collective-permute-done | bytes 131104 | tf_op jit(solution)/shard_map/ppermute | solution.py:510
  97.0 2.2 %collective-permute-done.32.came = bf16[4,144,128]{2,1,0:T(8,128)(2,1)S(1)} collective-permute-done((bf16[4,144,128]{2,1,0:T(8,128)(2,1)S(1)}, bf16[4,144,128]{2,1,0:T(8,128)(2,1)S(1)}, u32[]{:S(2)}, u32[]{:S(2)}) %collective-permute-start.32) | collective-permute-done | bytes 147488 | tf_op jit(solution)/shard_map/ppermute | solution.py:510
  99.9 3.1 %collective-permute-start.33 = (bf16[4,144,128]{2,1,0:T(8,128)(2,1)S(1)}, bf16[4,144,128]{2,1,0:T(8,128)(2,1)S(1)}, u32[]{:S(2)}, u32[]{:S(2)}) collective-permute-start(bf16[4,144,128]{2,1,0:T(8,128)(2,1)S(1)} %get-tuple-element.102), channel_id=1, source_target_pairs={{0,16},{4,20},{8,24},{12,28},{16,0},{20,4},{24,8},{28,12},{1,17},{... | collective-permute-start | bytes 442376 | tf_op jit(solution)/shard_map/ppermute | solution.py:510
  103.6 1.2 collective-permute-start.24
  104.7 12.6 %collective-permute-done.24.a1 = bf16[4,64,256]{2,1,0:T(8,128)(2,1)S(1)} collective-permute-done((bf16[4,64,256]{2,1,0:T(8,128)(2,1)S(1)}, bf16[4,64,256]{2,1,0:T(8,128)(2,1)S(1)}, u32[]{:S(2)}, u32[]{:S(2)}) %collective-permute-start.24) | collective-permute-done | bytes 131104 | tf_op jit(solution)/shard_map/ppermute | solution.py:510
  118.1 1.0 collective-permute-start.34
  119.0 4.9 %weights.1 = (bf16[1,2048,512]{2,1,0:T(8,128)(2,1)}, bf16[1,2048,512]{2,1,0:T(8,128)(2,1)}) custom-call(s32[3]{0:T(128)S(1)} %pad_add_fusion.at.core, bf16[320,2048]{1,0:T(8,128)(2,1)S(1)} %bitcast.18, bf16[320,2048]{1,0:T(8,128)(2,1)S(1)} %collective-permute-done.11.other.rb.gb, bf16[320,512]{1,0:T(8,128)(2,1)S(1)} %get-tuple-element.70.gback, ...), custom_call_target="tpu_custom_call" | custom-call | tf_op jit(solution)/shard_map/weights/pallas_call | solution.py:234
  124.0 3.8 %down.1 = bf16[1,512,2048]{2,1,0:T(8,128)(2,1)} custom-call(s32[3]{0:T(128)S(1)} %pad_add_fusion.at.core, bf16[320,2048]{1,0:T(8,128)(2,1)S(1)} %bitcast.19, bf16[320,2048]{1,0:T(8,128)(2,1)S(1)} %collective-permute-done.11.other.rb.gb, bf16[320,512]{1,0:T(8,128)(2,1)S(1)} %get-tuple-element.74.hidden), custom_call_target="tpu_custom_call" | custom-call | tf_op jit(solution)/shard_map/down/pallas_call | solution.py:259
  127.7 2.2 %shard_map.190 = (bf16[4,128,128]{2,1,0:T(8,128)(2,1)}, f32[4,128,128]{2,1,0:T(8,128)S(1)}, f32[4,128,256]{2,1,0:T(8,128)S(1)}, f32[4,128,1]{2,1,0:T(8,128)S(1)}) custom-call(s32[3]{0:T(128)S(1)} %pad_add_fusion.at.core, bf16[4,128,128]{2,1,0:T(8,128)(2,1)S(1)} %get-tuple-element.86.q, bf16[4,128,128]{2,1,0:T(8,128)(2,1)S(1)} %get-tuple-element.94.k, ...), custom_call_target="tpu_custom_call" | custom-call | tf_op jit(solution)/shard_map/pallas_call | solution.py:428
  130.0 2.5 %project.1 = f32[256,1024]{1,0:T(8,128)} custom-call(s32[3]{0:T(128)S(1)} %pad_add_fusion.at.core, bf16[4,64,256]{2,1,0:T(8,128)(2,1)S(1)} %bitcast.23, bf16[4,64,256]{2,1,0:T(8,128)(2,1)S(1)} %collective-permute-done.24.a1, bf16[4,64,256]{2,1,0:T(8,128)(2,1)S(1)} %collective-permute-done.25.b0, bf16[4,64,256]{2,1,0:T(8,128)(2,1)S(1)} %collective-permute-done.26.b1, ...), custom_call_target="tpu_custom_call" | custom-call | tf_op jit(solution)/shard_map/project/pallas_call | solution.py:492
  132.5 1.7 %shard_map.194 = (bf16[4,128,128]{2,1,0:T(8,128)(2,1)}, bf16[4,128,256]{2,1,0:T(8,128)(2,1)}) custom-call(s32[3]{0:T(128)S(1)} %pad_add_fusion.at.core, bf16[4,128,128]{2,1,0:T(8,128)(2,1)S(1)} %get-tuple-element.94.k, bf16[4,128,256]{2,1,0:T(8,128)(2,1)S(1)} %get-tuple-element.95.v, f32[4,128,1]{2,1,0:T(8,128)S(1)} %get-tuple-element.99.trails, ...), custom_call_target="tpu_custom_call" | custom-call | tf_op jit(solution)/shard_map/pallas_call | solution.py:428
  (48 shorter events, 8.1 us)
Async XLA Ops:
  3.1 10.7 %collective-permute-start.9 = (bf16[40,1024]{1,0:T(8,128)(2,1)S(1)}, bf16[40,1024]{1,0:T(8,128)(2,1)S(1)}, u32[]{:S(2)}, u32[]{:S(2)}) collective-permute-start(bf16[40,1024]{1,0:T(8,128)(2,1)S(1)} %get-tuple-element.66), channel_id=1, source_target_pairs={{0,28},{4,24},{8,20},{12,16},{16,12},{20,8},{24,4},{28,0},{1,29},{... | collective-permute-start | bytes 245768 | tf_op jit(solution)/shard_map/ppermute | solution.py:510
  9.2 11.1 %collective-permute-start.3 = (bf16[40,1024]{1,0:T(8,128)(2,1)S(1)}, bf16[40,1024]{1,0:T(8,128)(2,1)S(1)}, u32[]{:S(2)}, u32[]{:S(2)}) collective-permute-start(bf16[40,1024]{1,0:T(8,128)(2,1)S(1)} %get-tuple-element.63), channel_id=1, source_target_pairs={{0,16},{4,20},{8,24},{12,28},{16,0},{20,4},{24,8},{28,12},{1,17},{... | collective-permute-start | bytes 245768 | tf_op jit(solution)/shard_map/ppermute | solution.py:510
  9.2 12.9 %collective-permute-start.5 = (bf16[40,1024]{1,0:T(8,128)(2,1)S(1)}, bf16[40,1024]{1,0:T(8,128)(2,1)S(1)}, u32[]{:S(2)}, u32[]{:S(2)}) collective-permute-start(bf16[40,1024]{1,0:T(8,128)(2,1)S(1)} %get-tuple-element.64), channel_id=1, source_target_pairs={{0,20},{4,16},{8,28},{12,24},{16,4},{20,0},{24,12},{28,8},{1,21},{... | collective-permute-start | bytes 245768 | tf_op jit(solution)/shard_map/ppermute | solution.py:510
  12.1 10.0 %collective-permute-start.7 = (bf16[40,1024]{1,0:T(8,128)(2,1)S(1)}, bf16[40,1024]{1,0:T(8,128)(2,1)S(1)}, u32[]{:S(2)}, u32[]{:S(2)}) collective-permute-start(bf16[40,1024]{1,0:T(8,128)(2,1)S(1)} %get-tuple-element.65), channel_id=1, source_target_pairs={{0,24},{4,28},{8,16},{12,20},{16,8},{20,12},{24,0},{28,4},{1,25},{... | collective-permute-start | bytes 245768 | tf_op jit(solution)/shard_map/ppermute | solution.py:510
  12.2 18.8 %collective-permute-start = (bf16[40,2048]{1,0:T(8,128)(2,1)S(1)}, bf16[40,2048]{1,0:T(8,128)(2,1)S(1)}, u32[]{:S(2)}, u32[]{:S(2)}) collective-permute-start(bf16[40,2048]{1,0:T(8,128)(2,1)S(1)} %get-tuple-element.60), channel_id=1, source_target_pairs={{0,4},{4,0},{8,12},{12,8},{16,20},{20,16},{24,28},{28,24},{1,5},{5... | collective-permute-start | bytes 491528 | tf_op jit(solution)/shard_map/ppermute | solution.py:510
  13.8 11.2 %collective-permute-start.10 = (bf16[40,1024]{1,0:T(8,128)(2,1)S(1)}, bf16[40,1024]{1,0:T(8,128)(2,1)S(1)}, u32[]{:S(2)}, u32[]{:S(2)}) collective-permute-start(bf16[40,1024]{1,0:T(8,128)(2,1)S(1)} %collective-permute-done.9.refs_10_), channel_id=1, source_target_pairs={{0,2},{1,3},{2,0},{3,1},{4,6},{5,7},{6,4},{7,5},{8,10},{9,11},{10,... | collective-permute-start | bytes 245768 | tf_op jit(solution)/shard_map/ppermute | solution.py:510
  20.3 6.2 %collective-permute-start.4 = (bf16[40,1024]{1,0:T(8,128)(2,1)S(1)}, bf16[40,1024]{1,0:T(8,128)(2,1)S(1)}, u32[]{:S(2)}, u32[]{:S(2)}) collective-permute-start(bf16[40,1024]{1,0:T(8,128)(2,1)S(1)} %collective-permute-done.3.refs_4_), channel_id=1, source_target_pairs={{0,2},{1,3},{2,0},{3,1},{4,6},{5,7},{6,4},{7,5},{8,10},{9,11},{10,... | collective-permute-start | bytes 245768 | tf_op jit(solution)/shard_map/ppermute | solution.py:510
  22.1 8.9 %collective-permute-start.1 = (bf16[40,2048]{1,0:T(8,128)(2,1)S(1)}, bf16[40,2048]{1,0:T(8,128)(2,1)S(1)}, u32[]{:S(2)}, u32[]{:S(2)}) collective-permute-start(bf16[40,2048]{1,0:T(8,128)(2,1)S(1)} %get-tuple-element.61), channel_id=1, source_target_pairs={{0,8},{4,12},{8,0},{12,4},{16,24},{20,28},{24,16},{28,20},{1,9},{5... | collective-permute-start | bytes 491528 | tf_op jit(solution)/shard_map/ppermute | solution.py:510
  22.1 9.2 %collective-permute-start.2 = (bf16[40,2048]{1,0:T(8,128)(2,1)S(1)}, bf16[40,2048]{1,0:T(8,128)(2,1)S(1)}, u32[]{:S(2)}, u32[]{:S(2)}) collective-permute-start(bf16[40,2048]{1,0:T(8,128)(2,1)S(1)} %get-tuple-element.62), channel_id=1, source_target_pairs={{0,12},{4,8},{8,4},{12,0},{16,28},{20,24},{24,20},{28,16},{1,13},{... | collective-permute-start | bytes 491528 | tf_op jit(solution)/shard_map/ppermute | solution.py:510
  25.0 4.4 %collective-permute-start.6 = (bf16[40,1024]{1,0:T(8,128)(2,1)S(1)}, bf16[40,1024]{1,0:T(8,128)(2,1)S(1)}, u32[]{:S(2)}, u32[]{:S(2)}) collective-permute-start(bf16[40,1024]{1,0:T(8,128)(2,1)S(1)} %collective-permute-done.5.refs_6_), channel_id=1, source_target_pairs={{0,2},{1,3},{2,0},{3,1},{4,6},{5,7},{6,4},{7,5},{8,10},{9,11},{10,... | collective-permute-start | bytes 245768 | tf_op jit(solution)/shard_map/ppermute | solution.py:510
  26.5 4.4 %collective-permute-start.8 = (bf16[40,1024]{1,0:T(8,128)(2,1)S(1)}, bf16[40,1024]{1,0:T(8,128)(2,1)S(1)}, u32[]{:S(2)}, u32[]{:S(2)}) collective-permute-start(bf16[40,1024]{1,0:T(8,128)(2,1)S(1)} %collective-permute-done.7.refs_8_), channel_id=1, source_target_pairs={{0,2},{1,3},{2,0},{3,1},{4,6},{5,7},{6,4},{7,5},{8,10},{9,11},{10,... | collective-permute-start | bytes 245768 | tf_op jit(solution)/shard_map/ppermute | solution.py:510
  31.9 5.5 %collective-permute-start.11 = (bf16[320,2048]{1,0:T(8,128)(2,1)S(1)}, bf16[320,2048]{1,0:T(8,128)(2,1)S(1)}, u32[]{:S(2)}, u32[]{:S(2)}) collective-permute-start(bf16[320,2048]{1,0:T(8,128)(2,1)S(1)} %bitcast.16), channel_id=1, source_target_pairs={{0,1},{1,0},{2,3},{3,2},{4,5},{5,4},{6,7},{7,6},{8,9},{9,8},{10,11... | collective-permute-start | bytes 3932168 | tf_op jit(solution)/shard_map/ppermute | solution.py:510
  41.0 4.1 %collective-permute-start.12 = (bf16[320,1024]{1,0:T(8,128)(2,1)S(1)}, bf16[320,1024]{1,0:T(8,128)(2,1)S(1)}, u32[]{:S(2)}, u32[]{:S(2)}) collective-permute-start(bf16[320,1024]{1,0:T(8,128)(2,1)S(1)} %get-tuple-element.77), channel_id=1, source_target_pairs={{0,1},{1,0},{2,3},{3,2},{4,5},{5,4},{6,7},{7,6},{8,9},{9,8},{10,11... | collective-permute-start | bytes 1966088 | tf_op jit(solution)/shard_map/ppermute | solution.py:510
  42.6 28.2 %collective-permute-start.27 = (bf16[1,128,1024]{2,1,0:T(8,128)(2,1)S(1)}, bf16[1,128,1024]{2,1,0:T(8,128)(2,1)S(1)}, u32[]{:S(2)}, u32[]{:S(2)}) collective-permute-start(bf16[1,128,1024]{2,1,0:T(8,128)(2,1)S(1)} %bitcast.20), channel_id=1, source_target_pairs={{0,16},{4,20},{8,24},{12,28},{16,0},{20,4},{24,8},{28,12},{1,17},{... | collective-permute-start | bytes 786440 | tf_op jit(solution)/shard_map/ppermute | solution.py:510
  45.8 5.5 %collective-permute-start.13 = (bf16[40,1024]{1,0:T(8,128)(2,1)S(1)}, bf16[40,1024]{1,0:T(8,128)(2,1)S(1)}, u32[]{:S(2)}, u32[]{:S(2)}) collective-permute-start(bf16[40,1024]{1,0:T(8,128)(2,1)S(1)} %get-tuple-element.79), channel_id=1, source_target_pairs={{0,4},{4,0},{8,12},{12,8},{16,20},{20,16},{24,28},{28,24},{1,5},{5... | collective-permute-start | bytes 245768 | tf_op jit(solution)/shard_map/ppermute | solution.py:510
  46.8 5.9 %collective-permute-start.14 = (bf16[40,1024]{1,0:T(8,128)(2,1)S(1)}, bf16[40,1024]{1,0:T(8,128)(2,1)S(1)}, u32[]{:S(2)}, u32[]{:S(2)}) collective-permute-start(bf16[40,1024]{1,0:T(8,128)(2,1)S(1)} %get-tuple-element.80), channel_id=1, source_target_pairs={{0,8},{4,12},{8,0},{12,4},{16,24},{20,28},{24,16},{28,20},{1,9},{5... | collective-permute-start | bytes 245768 | tf_op jit(solution)/shard_map/ppermute | solution.py:510
  48.5 8.5 %collective-permute-start.15 = (bf16[40,1024]{1,0:T(8,128)(2,1)S(1)}, bf16[40,1024]{1,0:T(8,128)(2,1)S(1)}, u32[]{:S(2)}, u32[]{:S(2)}) collective-permute-start(bf16[40,1024]{1,0:T(8,128)(2,1)S(1)} %get-tuple-element.81), channel_id=1, source_target_pairs={{0,12},{4,8},{8,4},{12,0},{16,28},{20,24},{24,20},{28,16},{1,13},{... | collective-permute-start | bytes 245768 | tf_op jit(solution)/shard_map/ppermute | solution.py:510
  49.3 16.9 %collective-permute-start.16 = (bf16[40,1024]{1,0:T(8,128)(2,1)S(1)}, bf16[40,1024]{1,0:T(8,128)(2,1)S(1)}, u32[]{:S(2)}, u32[]{:S(2)}) collective-permute-start(bf16[40,1024]{1,0:T(8,128)(2,1)S(1)} %get-tuple-element.82), channel_id=1, source_target_pairs={{0,16},{4,20},{8,24},{12,28},{16,0},{20,4},{24,8},{28,12},{1,17},{... | collective-permute-start | bytes 245768 | tf_op jit(solution)/shard_map/ppermute | solution.py:510
  51.3 16.8 %collective-permute-start.17 = (bf16[40,1024]{1,0:T(8,128)(2,1)S(1)}, bf16[40,1024]{1,0:T(8,128)(2,1)S(1)}, u32[]{:S(2)}, u32[]{:S(2)}) collective-permute-start(bf16[40,1024]{1,0:T(8,128)(2,1)S(1)} %get-tuple-element.83), channel_id=1, source_target_pairs={{0,20},{4,16},{8,28},{12,24},{16,4},{20,0},{24,12},{28,8},{1,21},{... | collective-permute-start | bytes 245768 | tf_op jit(solution)/shard_map/ppermute | solution.py:510
  52.6 15.5 %collective-permute-start.18 = (bf16[40,1024]{1,0:T(8,128)(2,1)S(1)}, bf16[40,1024]{1,0:T(8,128)(2,1)S(1)}, u32[]{:S(2)}, u32[]{:S(2)}) collective-permute-start(bf16[40,1024]{1,0:T(8,128)(2,1)S(1)} %get-tuple-element.84), channel_id=1, source_target_pairs={{0,24},{4,28},{8,16},{12,20},{16,8},{20,12},{24,0},{28,4},{1,25},{... | collective-permute-start | bytes 245768 | tf_op jit(solution)/shard_map/ppermute | solution.py:510
  57.0 11.1 %collective-permute-start.19 = (bf16[40,1024]{1,0:T(8,128)(2,1)S(1)}, bf16[40,1024]{1,0:T(8,128)(2,1)S(1)}, u32[]{:S(2)}, u32[]{:S(2)}) collective-permute-start(bf16[40,1024]{1,0:T(8,128)(2,1)S(1)} %get-tuple-element.85), channel_id=1, source_target_pairs={{0,28},{4,24},{8,20},{12,16},{16,12},{20,8},{24,4},{28,0},{1,29},{... | collective-permute-start | bytes 245768 | tf_op jit(solution)/shard_map/ppermute | solution.py:510
  69.4 8.0 %collective-permute-start.20 = (bf16[128,1024]{1,0:T(8,128)(2,1)S(1)}, bf16[128,1024]{1,0:T(8,128)(2,1)S(1)}, u32[]{:S(2)}, u32[]{:S(2)}) collective-permute-start(bf16[128,1024]{1,0:T(8,128)(2,1)S(1)} %shard_map.184.own), channel_id=1, source_target_pairs={{0,2},{1,3},{2,0},{3,1},{4,6},{5,7},{6,4},{7,5},{8,10},{9,11},{10,... | collective-permute-start | bytes 786440 | tf_op jit(solution)/shard_map/ppermute | solution.py:510
  70.9 19.6 %collective-permute-start.28 = (bf16[2,128,1024]{2,1,0:T(8,128)(2,1)S(1)}, bf16[2,128,1024]{2,1,0:T(8,128)(2,1)S(1)}, u32[]{:S(2)}, u32[]{:S(2)}) collective-permute-start(bf16[2,128,1024]{2,1,0:T(8,128)(2,1)S(1)} %pad_maximum_fusion.refs_0_), channel_id=1, source_target_pairs={{0,8},{4,12},{8,0},{12,4},{16,24},{20,28},{24,16},{28,20},{1,9},{5... | collective-permute-start | bytes 1572872 | tf_op jit(solution)/shard_map/ppermute | solution.py:510
  78.0 2.9 %collective-permute-start.21 = (bf16[128,1024]{1,0:T(8,128)(2,1)S(1)}, bf16[128,1024]{1,0:T(8,128)(2,1)S(1)}, u32[]{:S(2)}, u32[]{:S(2)}) collective-permute-start(bf16[128,1024]{1,0:T(8,128)(2,1)S(1)} %shard_map.185.ma), channel_id=1, source_target_pairs={{0,1},{1,0},{2,3},{3,2},{4,5},{5,4},{6,7},{7,6},{8,9},{9,8},{10,11... | collective-permute-start | bytes 786440 | tf_op jit(solution)/shard_map/ppermute | solution.py:510
  83.3 8.3 %collective-permute-start.31 = (bf16[4,144,128]{2,1,0:T(8,128)(2,1)S(1)}, bf16[4,144,128]{2,1,0:T(8,128)(2,1)S(1)}, u32[]{:S(2)}, u32[]{:S(2)}) collective-permute-start(bf16[4,144,128]{2,1,0:T(8,128)(2,1)S(1)} %get-tuple-element.101), channel_id=1, source_target_pairs={{0,4},{4,0},{8,12},{12,8},{16,20},{20,16},{24,28},{28,24},{1,5},{5... | collective-permute-start | bytes 442376 | tf_op jit(solution)/shard_map/ppermute | solution.py:510
  85.0 11.3 %collective-permute-start.22 = (bf16[4,64,256]{2,1,0:T(8,128)(2,1)S(1)}, bf16[4,64,256]{2,1,0:T(8,128)(2,1)S(1)}, u32[]{:S(2)}, u32[]{:S(2)}) collective-permute-start(bf16[4,64,256]{2,1,0:T(8,128)(2,1)S(1)} %get-tuple-element.89), channel_id=1, source_target_pairs={{0,16},{4,20},{8,24},{12,28},{16,0},{20,4},{24,8},{28,12},{1,17},{... | collective-permute-start | bytes 393224 | tf_op jit(solution)/shard_map/ppermute | solution.py:510
  89.6 40.4 %collective-permute-start.29 = (bf16[2,128,1024]{2,1,0:T(8,128)(2,1)S(1)}, bf16[2,128,1024]{2,1,0:T(8,128)(2,1)S(1)}, u32[]{:S(2)}, u32[]{:S(2)}) collective-permute-start(bf16[2,128,1024]{2,1,0:T(8,128)(2,1)S(1)} %pad_maximum_fusion.refs_0_), channel_id=1, source_target_pairs={{0,4},{4,0},{8,12},{12,8},{16,20},{20,16},{24,28},{28,24},{1,5},{5... | collective-permute-start | bytes 1572872 | tf_op jit(solution)/shard_map/ppermute | solution.py:510
  90.5 39.5 %collective-permute-start.30 = (bf16[2,128,1024]{2,1,0:T(8,128)(2,1)S(1)}, bf16[2,128,1024]{2,1,0:T(8,128)(2,1)S(1)}, u32[]{:S(2)}, u32[]{:S(2)}) collective-permute-start(bf16[2,128,1024]{2,1,0:T(8,128)(2,1)S(1)} %collective-permute-done.28.refs_1_), channel_id=1, source_target_pairs={{0,4},{4,0},{8,12},{12,8},{16,20},{20,16},{24,28},{28,24},{1,5},{5... | collective-permute-start | bytes 1572872 | tf_op jit(solution)/shard_map/ppermute | solution.py:510
  92.3 6.9 %collective-permute-start.32 = (bf16[4,144,128]{2,1,0:T(8,128)(2,1)S(1)}, bf16[4,144,128]{2,1,0:T(8,128)(2,1)S(1)}, u32[]{:S(2)}, u32[]{:S(2)}) collective-permute-start(bf16[4,144,128]{2,1,0:T(8,128)(2,1)S(1)} %shard_map.191.group), channel_id=1, source_target_pairs={{0,8},{4,12},{8,0},{12,4},{16,24},{20,28},{24,16},{28,20},{1,9},{5... | collective-permute-start | bytes 442376 | tf_op jit(solution)/shard_map/ppermute | solution.py:510
  96.9 6.1 %collective-permute-start.23 = (bf16[4,64,256]{2,1,0:T(8,128)(2,1)S(1)}, bf16[4,64,256]{2,1,0:T(8,128)(2,1)S(1)}, u32[]{:S(2)}, u32[]{:S(2)}) collective-permute-start(bf16[4,64,256]{2,1,0:T(8,128)(2,1)S(1)} %bitcast.27), channel_id=1, source_target_pairs={{0,8},{4,12},{8,0},{12,4},{16,24},{20,28},{24,16},{28,20},{1,9},{5... | collective-permute-start | bytes 393224 | tf_op jit(solution)/shard_map/ppermute | solution.py:510
  99.9 17.5 %collective-permute-start.33 = (bf16[4,144,128]{2,1,0:T(8,128)(2,1)S(1)}, bf16[4,144,128]{2,1,0:T(8,128)(2,1)S(1)}, u32[]{:S(2)}, u32[]{:S(2)}) collective-permute-start(bf16[4,144,128]{2,1,0:T(8,128)(2,1)S(1)} %get-tuple-element.102), channel_id=1, source_target_pairs={{0,16},{4,20},{8,24},{12,28},{16,0},{20,4},{24,8},{28,12},{1,17},{... | collective-permute-start | bytes 442376 | tf_op jit(solution)/shard_map/ppermute | solution.py:510
  103.6 13.8 %collective-permute-start.24 = (bf16[4,64,256]{2,1,0:T(8,128)(2,1)S(1)}, bf16[4,64,256]{2,1,0:T(8,128)(2,1)S(1)}, u32[]{:S(2)}, u32[]{:S(2)}) collective-permute-start(bf16[4,64,256]{2,1,0:T(8,128)(2,1)S(1)} %bitcast.28), channel_id=1, source_target_pairs={{0,4},{4,0},{8,12},{12,8},{16,20},{20,16},{24,28},{28,24},{1,5},{5... | collective-permute-start | bytes 393224 | tf_op jit(solution)/shard_map/ppermute | solution.py:510
  104.7 25.2 %collective-permute-start.25 = (bf16[4,64,256]{2,1,0:T(8,128)(2,1)S(1)}, bf16[4,64,256]{2,1,0:T(8,128)(2,1)S(1)}, u32[]{:S(2)}, u32[]{:S(2)}) collective-permute-start(bf16[4,64,256]{2,1,0:T(8,128)(2,1)S(1)} %bitcast.22), channel_id=1, source_target_pairs={{0,1},{1,0},{2,3},{3,2},{4,5},{5,4},{6,7},{7,6},{8,9},{9,8},{10,11... | collective-permute-start | bytes 393224 | tf_op jit(solution)/shard_map/ppermute | solution.py:510
  117.4 12.6 %collective-permute-start.26 = (bf16[4,64,256]{2,1,0:T(8,128)(2,1)S(1)}, bf16[4,64,256]{2,1,0:T(8,128)(2,1)S(1)}, u32[]{:S(2)}, u32[]{:S(2)}) collective-permute-start(bf16[4,64,256]{2,1,0:T(8,128)(2,1)S(1)} %collective-permute-done.24.a1), channel_id=1, source_target_pairs={{0,1},{1,0},{2,3},{3,2},{4,5},{5,4},{6,7},{7,6},{8,9},{9,8},{10,11... | collective-permute-start | bytes 393224 | tf_op jit(solution)/shard_map/ppermute | solution.py:510
  118.1 14.4 %collective-permute-start.34 = (bf16[4,128,128]{2,1,0:T(8,128)(2,1)S(1)}, bf16[4,128,128]{2,1,0:T(8,128)(2,1)S(1)}, u32[]{:S(2)}, u32[]{:S(2)}) collective-permute-start(bf16[4,128,128]{2,1,0:T(8,128)(2,1)S(1)} %get-tuple-element.106), channel_id=1, source_target_pairs={{0,4},{4,0},{8,12},{12,8},{16,20},{20,16},{24,28},{28,24},{1,5},{5... | collective-permute-start | bytes 393224 | tf_op jit(solution)/shard_map/ppermute | solution.py:510

commit v7 on v6

--- a/solution.py
+++ b/solution.py
@@ -330,7 +330,8 @@
 def put_message(ref, h, body, decay):
     size = body.shape[0]
     ref[h, :size, :] = body.astype(BF16)
-    ref[h, size:, :] = pieces(decay, (PIECES, body.shape[1])).astype(BF16)
+    if ref.shape[1] > size:
+        ref[h, size:, :] = pieces(decay, (PIECES, body.shape[1])).astype(BF16)
 
 
 def get_message(ref, h):
@@ -411,7 +412,7 @@
     upper = (at[1] & bit) != 0
     right = (at[1] & 1) == 1
     for h in range(keep.shape[0]):
-        theirs, _ = get_message(came, h)
+        theirs = came[h, : later.shape[1], :].astype(F32)
         after = later[h] + jnp.where(upper, 0.0, reach[h : h + 1, 0:1]) * theirs
         mine, mine_decay = get_message(keep, h)
         pair, pair_decay = get_message(first_came, h)
@@ -462,47 +463,46 @@
         v_grad[h, :, half:] = (v_part[h, :, half:] + trail * dot(k[h], high)).astype(BF16)
 
 
-def project_kernel(core, a0, a1, b0, b1, *refs):
+def project_kernel(core, a, b, *refs, held):
     out, x = refs[-2:]
-    turn, rows, size = a0.shape
+    _, rows, size = a.shape
 
     @pl.when(pl.program_id(0) == 0)
     def _():
-        mine = pl.ds(pl.multiple_of(core[0] * rows, rows), rows)
-        other = pl.ds(pl.multiple_of((1 - core[0]) * rows, rows), rows)
-        for place, pair in ((mine, (a0, a1)), (other, (b0, b1))):
-            x[:turn, place, :] = pair[0][...]
-            x[turn:, place, :] = pair[1][...]
-
-    total, at = None, 0
-    for y in refs[:-2]:
-        blocks, span, width = y.shape
-        left = x[at : at + blocks].reshape(blocks * span, size)
-        part = dot(left, y[...].reshape(blocks * span, width), 0, 0)
+        x[:, pl.ds(pl.multiple_of(core[0] * rows, rows), rows), :] = a[...]
+        x[:, pl.ds(pl.multiple_of((1 - core[0]) * rows, rows), rows), :] = b[...]
+
+    total, at = (refs[0][...] if held else None), 0
+    for y in refs[1 if held else 0 : -2]:
+        count, span, width = y.shape
+        left = x[at : at + count].reshape(count * span, size)
+        part = dot(left, y[...].reshape(count * span, width), 0, 0)
         total = part if total is None else total + part
-        at += blocks
+        at += count
     out[...] = total
 
 
-def project(at, slices, parts):
-    turn, rows, size = slices[0].shape
+def project(at, slices, parts, held=()):
+    blocks, rows, size = slices[0].shape
     width = parts[0].shape[2]
     chunk = min(width, 512)
-    piece = pl.BlockSpec((turn, rows, size), lambda i, *_: (0, 0, 0))
+    piece = pl.BlockSpec((blocks, rows, size), lambda i, *_: (0, 0, 0))
+    result = pl.BlockSpec((size, chunk), lambda i, *_: (0, i))
     return pl.pallas_call(
-        project_kernel,
+        functools.partial(project_kernel, held=len(held) > 0),
         grid_spec=pltpu.PrefetchScalarGridSpec(
             num_scalar_prefetch=1,
             grid=(width // chunk,),
-            in_specs=[piece] * 4
+            in_specs=[piece] * 2
+            + [result] * len(held)
             + [pl.BlockSpec(y.shape[:2] + (chunk,), lambda i, *_: (0, 0, i)) for y in parts],
-            out_specs=pl.BlockSpec((size, chunk), lambda i, *_: (0, i)),
-            scratch_shapes=[pltpu.VMEM((2 * turn, 2 * rows, size), BF16)],
+            out_specs=result,
+            scratch_shapes=[pltpu.VMEM((blocks, 2 * rows, size), BF16)],
         ),
         out_shape=jax.ShapeDtypeStruct((size, width), F32),
         compiler_params=limit(16),
         name="project",
-    )(at, *slices, *parts)
+    )(at, *slices, *held, *parts)
 
 
 def swap(a, axis, bit):
@@ -668,7 +668,8 @@
         if bit * 2 < sp:
             group, later, reach = small(
                 functools.partial(join_kernel, bit=bit),
-                [message, jax.ShapeDtypeStruct(state_shape, F32),
+                [message if bit * 4 < sp else jax.ShapeDtypeStruct(state_shape, BF16),
+                 jax.ShapeDtypeStruct(state_shape, F32),
                  jax.ShapeDtypeStruct((heads, 128), F32)],
                 at, group, came_state, later, reach,
             )
@@ -678,7 +679,9 @@
         [state_out, state_out], at, came_state, later, reach, keep, first_came,
     )
     other_state = swap(send_state, SP, 1)
-    out_proj_grad = project(at, slices, parts)
+    middle = len(parts) // 2
+    held = project(at, slices[0::2], parts[:middle])
+    out_proj_grad = project(at, slices[1::2], parts[middle:], (held,))
     k_grad, v_grad = small(
         final_kernel,
         [jax.ShapeDtypeStruct(key_heads.shape, BF16),

time: 134 us -> 135 us (level)
  waiting for transfers between devices: 39.3 us -> 40.7 us
  starting transfers between devices: 53.4 us -> 52 us
    ppermute x35, waiting for transfers between devices: 39.3 us -> 40.7 us  [swap(): return lax.ppermute(a, axis, [(i, i ^ bit) for i in range(count)])]
    ppermute x35, starting transfers between devices: 53.4 us -> 52 us  [swap(): return lax.ppermute(a, axis, [(i, i ^ bit) for i in range(count)])]
    pallas_call x1 -> x2, Pallas kernels: 2.53 us -> 3.63 us  [project(): pl.pallas_call(functools.partial(project_kernel, held=len(held) > 0), gri...]
  transfers between devices with their start and end apart: 35 -> 35, of which waited for: 12 -> 12; matrix products, arithmetic and copies ran while one was open for 0% -> 0% of each run, Pallas kernels for 24% -> 25%
where the time goes in v7:
time: 135 us
  starting transfers between devices  52 us (39%)
  Pallas kernels  41.6 us (31%)
  waiting for transfers between devices  40.7 us (30%)
    ppermute x35, starting transfers between devices, swap(): return lax.ppermute(a, axis, [(i, i ^ bit) for i in range(count)])  52 us
    ppermute x35, waiting for transfers between devices, swap(): return lax.ppermute(a, axis, [(i, i ^ bit) for i in range(count)])  40.7 us
    pallas_call x15, Pallas kernels, small(): pl.pallas_call(kernel, in_specs=[pl.BlockSpec(memory_space=pltpu.SMEM)] +...  18.7 us
    pallas_call x3, Pallas kernels, stage(): pl.pallas_call(functools.partial(stage_kernel, kinds=kinds), in_specs=[pl...  8.2 us
    pallas_call x1, Pallas kernels, weight_grads(): pl.pallas_call(weights_kernel, grid_spec=pltpu.PrefetchScalarGridSpec(num...  4.93 us
    pallas_call x1, Pallas kernels, down_grads(): pl.pallas_call(down_kernel, grid_spec=pltpu.PrefetchScalarGridSpec(num_sc...  3.77 us
    pallas_call x2, Pallas kernels, project(): pl.pallas_call(functools.partial(project_kernel, held=len(held) > 0), gri...  3.63 us
  transfers between devices with their start and end apart: 35, of which 12 were waited for; matrix products, arithmetic and copies ran while one was open for 0% of the time, Pallas kernels for 25%

profile of v7, /device:TPU:0, one launch (start us, length us, event | category | flops | bytes accessed | tf_op | source)
XLA Modules:
  0.0 135.3 jit_solution(4201717369097189836)
XLA Ops:
  0.7 2.4 %dispatch.1 = (bf16[320,128]{1,0:T(8,128)(2,1)S(1)}, bf16[40,2048]{1,0:T(8,128)(2,1)S(1)}, bf16[40,2048]{1,0:T(8,128)(2,1)S(1)}, bf16[40,2048]{1,0:T(8,128)(2,1)...) custom-call(s32[3]{0:T(128)S(1)} %pad_add_fusion.at.core, ...), custom_call_target="tpu_custom_call" | custom-call | tf_op jit(solution)/shard_map/dispatch/pallas_call | solution.py:80
  3.1 6.1 %collective-permute-start.9 = (bf16[40,1024]{1,0:T(8,128)(2,1)S(1)}, bf16[40,1024]{1,0:T(8,128)(2,1)S(1)}, u32[]{:S(2)}, u32[]{:S(2)}) collective-permute-start(bf16[40,1024]{1,0:T(8,128)(2,1)S(1)} %get-tuple-element.66), channel_id=1, source_target_pairs={{0,28},{4,24},{8,20},{12,16},{16,12},{20,8},{24,4},{28,0},{1,29},{... | collective-permute-start | bytes 245768 | tf_op jit(solution)/shard_map/ppermute | solution.py:510
  9.2 2.9 %collective-permute-start.5 = (bf16[40,1024]{1,0:T(8,128)(2,1)S(1)}, bf16[40,1024]{1,0:T(8,128)(2,1)S(1)}, u32[]{:S(2)}, u32[]{:S(2)}) collective-permute-start(bf16[40,1024]{1,0:T(8,128)(2,1)S(1)} %get-tuple-element.64), channel_id=1, source_target_pairs={{0,20},{4,16},{8,28},{12,24},{16,4},{20,0},{24,12},{28,8},{1,21},{... | collective-permute-start | bytes 245768 | tf_op jit(solution)/shard_map/ppermute | solution.py:510
  12.2 1.6 %collective-permute-start = (bf16[40,2048]{1,0:T(8,128)(2,1)S(1)}, bf16[40,2048]{1,0:T(8,128)(2,1)S(1)}, u32[]{:S(2)}, u32[]{:S(2)}) collective-permute-start(bf16[40,2048]{1,0:T(8,128)(2,1)S(1)} %get-tuple-element.60), channel_id=1, source_target_pairs={{0,4},{4,0},{8,12},{12,8},{16,20},{20,16},{24,28},{28,24},{1,5},{5... | collective-permute-start | bytes 491528 | tf_op jit(solution)/shard_map/ppermute | solution.py:510
  13.8 1.5 %collective-permute-start.10 = (bf16[40,1024]{1,0:T(8,128)(2,1)S(1)}, bf16[40,1024]{1,0:T(8,128)(2,1)S(1)}, u32[]{:S(2)}, u32[]{:S(2)}) collective-permute-start(bf16[40,1024]{1,0:T(8,128)(2,1)S(1)} %collective-permute-done.9.refs_10_), channel_id=1, source_target_pairs={{0,2},{1,3},{2,0},{3,1},{4,6},{5,7},{6,4},{7,5},{8,10},{9,11},{10,... | collective-permute-start | bytes 245768 | tf_op jit(solution)/shard_map/ppermute | solution.py:510
  15.3 5.0 %collective-permute-done.3.refs_4_ = bf16[40,1024]{1,0:T(8,128)(2,1)S(1)} collective-permute-done((bf16[40,1024]{1,0:T(8,128)(2,1)S(1)}, bf16[40,1024]{1,0:T(8,128)(2,1)S(1)}, u32[]{:S(2)}, u32[]{:S(2)}) %collective-permute-start.3) | collective-permute-done | bytes 81952 | tf_op jit(solution)/shard_map/ppermute | solution.py:510
  20.3 1.5 %collective-permute-start.4 = (bf16[40,1024]{1,0:T(8,128)(2,1)S(1)}, bf16[40,1024]{1,0:T(8,128)(2,1)S(1)}, u32[]{:S(2)}, u32[]{:S(2)}) collective-permute-start(bf16[40,1024]{1,0:T(8,128)(2,1)S(1)} %collective-permute-done.3.refs_4_), channel_id=1, source_target_pairs={{0,2},{1,3},{2,0},{3,1},{4,6},{5,7},{6,4},{7,5},{8,10},{9,11},{10,... | collective-permute-start | bytes 245768 | tf_op jit(solution)/shard_map/ppermute | solution.py:510
  22.1 2.9 %collective-permute-start.2 = (bf16[40,2048]{1,0:T(8,128)(2,1)S(1)}, bf16[40,2048]{1,0:T(8,128)(2,1)S(1)}, u32[]{:S(2)}, u32[]{:S(2)}) collective-permute-start(bf16[40,2048]{1,0:T(8,128)(2,1)S(1)} %get-tuple-element.62), channel_id=1, source_target_pairs={{0,12},{4,8},{8,4},{12,0},{16,28},{20,24},{24,20},{28,16},{1,13},{... | collective-permute-start | bytes 491528 | tf_op jit(solution)/shard_map/ppermute | solution.py:510
  25.0 1.5 %collective-permute-start.6 = (bf16[40,1024]{1,0:T(8,128)(2,1)S(1)}, bf16[40,1024]{1,0:T(8,128)(2,1)S(1)}, u32[]{:S(2)}, u32[]{:S(2)}) collective-permute-start(bf16[40,1024]{1,0:T(8,128)(2,1)S(1)} %collective-permute-done.5.refs_6_), channel_id=1, source_target_pairs={{0,2},{1,3},{2,0},{3,1},{4,6},{5,7},{6,4},{7,5},{8,10},{9,11},{10,... | collective-permute-start | bytes 245768 | tf_op jit(solution)/shard_map/ppermute | solution.py:510
  27.0 2.4 %collective-permute-done.6.refs_7_ = bf16[40,1024]{1,0:T(8,128)(2,1)S(1)} collective-permute-done((bf16[40,1024]{1,0:T(8,128)(2,1)S(1)}, bf16[40,1024]{1,0:T(8,128)(2,1)S(1)}, u32[]{:S(2)}, u32[]{:S(2)}) %collective-permute-start.6) | collective-permute-done | bytes 81952 | tf_op jit(solution)/shard_map/ppermute | solution.py:510
  29.4 1.5 %collective-permute-done.8.refs_9_ = bf16[40,1024]{1,0:T(8,128)(2,1)S(1)} collective-permute-done((bf16[40,1024]{1,0:T(8,128)(2,1)S(1)}, bf16[40,1024]{1,0:T(8,128)(2,1)S(1)}, u32[]{:S(2)}, u32[]{:S(2)}) %collective-permute-start.8) | collective-permute-done | bytes 81952 | tf_op jit(solution)/shard_map/ppermute | solution.py:510
  32.0 2.8 %stage.4 = (bf16[2,1024,512]{2,1,0:T(8,128)(2,1)S(1)}, bf16[2,512,1024]{2,1,0:T(8,128)(2,1)S(1)}) custom-call(s32[3]{0:T(128)S(1)} %pad_add_fusion.at.core, bf16[2048,512]{1,0:T(8,128)(2,1)} %bitcast.30, bf16[512,2048]{1,0:T(8,128)(2,1)} %bitcast.31), custom_call_target="tpu_custom_call" | custom-call | tf_op jit(solution)/shard_map/stage/pallas_call | solution.py:155
  34.7 2.7 %stage.3 = (bf16[2,1024,512]{2,1,0:T(8,128)(2,1)S(1)}, bf16[2,128,1024]{2,1,0:T(8,128)(2,1)S(1)}, bf16[4,128,128]{2,1,0:T(8,128)(2,1)S(1)}, bf16[4,128,128]{2,1,...) custom-call(s32[3]{0:T(128)S(1)} %pad_add_fusion.at.core, ...), custom_call_target="tpu_custom_call" | custom-call | tf_op jit(solution)/shard_map/stage/pallas_call | solution.py:155
  37.4 3.6 %shard_map.181 = (bf16[320,512]{1,0:T(8,128)(2,1)S(1)}, bf16[320,512]{1,0:T(8,128)(2,1)S(1)}, bf16[320,512]{1,0:T(8,128)(2,1)S(1)}, bf16[320,1024]{1,0:T(8,128)(2,1)S(1)}) custom-call(s32[3]{0:T(128)S(1)} %pad_add_fusion.at.core, bf16[320,2048]{1,0:T(8,128)(2,1)S(1)} %bitcast.17, bf16[320,2048]{1,0:T(8,128)(2,1)S(1)} %collective-permute-done.11.other.rb.gb, ...), custom_call_target="tpu_custom_call" | custom-call | tf_op jit(solution)/shard_map/pallas_call | solution.py:429
  41.6 1.1 shard_map.189
  42.6 1.0 collective-permute-start.27
  43.7 1.4 %shard_map.182.a = bf16[320,1024]{1,0:T(8,128)(2,1)S(1)} custom-call(s32[3]{0:T(128)S(1)} %pad_add_fusion.at.core, bf16[320,512]{1,0:T(8,128)(2,1)S(1)} %get-tuple-element.70.gback, bf16[320,512]{1,0:T(8,128)(2,1)S(1)} %get-tuple-element.71.uback, bf16[2,1024,512]{2,1,0:T(8,128)(2,1)S(1)} %get-tuple-element.67.wg, bf16[2,1024,512]{2,1,0:T(8,128)(2,1)S(1)} %get-tuple-element.68.wu), custom_call_target="tpu_custom_call" | custom-call | tf_op jit(solution)/shard_map/pallas_call | solution.py:429
  45.8 1.0 collective-permute-start.13
  46.8 1.8 %collective-permute-start.14 = (bf16[40,1024]{1,0:T(8,128)(2,1)S(1)}, bf16[40,1024]{1,0:T(8,128)(2,1)S(1)}, u32[]{:S(2)}, u32[]{:S(2)}) collective-permute-start(bf16[40,1024]{1,0:T(8,128)(2,1)S(1)} %get-tuple-element.80), channel_id=1, source_target_pairs={{0,8},{4,12},{8,0},{12,4},{16,24},{20,28},{24,16},{28,20},{1,9},{5... | collective-permute-start | bytes 245768 | tf_op jit(solution)/shard_map/ppermute | solution.py:510
  49.3 1.9 %collective-permute-start.16 = (bf16[40,1024]{1,0:T(8,128)(2,1)S(1)}, bf16[40,1024]{1,0:T(8,128)(2,1)S(1)}, u32[]{:S(2)}, u32[]{:S(2)}) collective-permute-start(bf16[40,1024]{1,0:T(8,128)(2,1)S(1)} %get-tuple-element.82), channel_id=1, source_target_pairs={{0,16},{4,20},{8,24},{12,28},{16,0},{20,4},{24,8},{28,12},{1,17},{... | collective-permute-start | bytes 245768 | tf_op jit(solution)/shard_map/ppermute | solution.py:510
  51.3 1.3 collective-permute-start.17
  52.6 2.2 %collective-permute-start.18 = (bf16[40,1024]{1,0:T(8,128)(2,1)S(1)}, bf16[40,1024]{1,0:T(8,128)(2,1)S(1)}, u32[]{:S(2)}, u32[]{:S(2)}) collective-permute-start(bf16[40,1024]{1,0:T(8,128)(2,1)S(1)} %get-tuple-element.84), channel_id=1, source_target_pairs={{0,24},{4,28},{8,16},{12,20},{16,8},{20,12},{24,0},{28,4},{1,25},{... | collective-permute-start | bytes 245768 | tf_op jit(solution)/shard_map/ppermute | solution.py:510
  54.8 2.2 %collective-permute-done.15.refs_3_ = bf16[40,1024]{1,0:T(8,128)(2,1)S(1)} collective-permute-done((bf16[40,1024]{1,0:T(8,128)(2,1)S(1)}, bf16[40,1024]{1,0:T(8,128)(2,1)S(1)}, u32[]{:S(2)}, u32[]{:S(2)}) %collective-permute-start.15) | collective-permute-done | bytes 81952 | tf_op jit(solution)/shard_map/ppermute | solution.py:510
  57.0 2.2 %collective-permute-start.19 = (bf16[40,1024]{1,0:T(8,128)(2,1)S(1)}, bf16[40,1024]{1,0:T(8,128)(2,1)S(1)}, u32[]{:S(2)}, u32[]{:S(2)}) collective-permute-start(bf16[40,1024]{1,0:T(8,128)(2,1)S(1)} %get-tuple-element.85), channel_id=1, source_target_pairs={{0,28},{4,24},{8,20},{12,16},{16,12},{20,8},{24,4},{28,0},{1,29},{... | collective-permute-start | bytes 245768 | tf_op jit(solution)/shard_map/ppermute | solution.py:510
  59.2 7.1 %collective-permute-done.16.refs_4_ = bf16[40,1024]{1,0:T(8,128)(2,1)S(1)} collective-permute-done((bf16[40,1024]{1,0:T(8,128)(2,1)S(1)}, bf16[40,1024]{1,0:T(8,128)(2,1)S(1)}, u32[]{:S(2)}, u32[]{:S(2)}) %collective-permute-start.16) | collective-permute-done | bytes 81952 | tf_op jit(solution)/shard_map/ppermute | solution.py:510
  66.3 1.8 %collective-permute-done.17.refs_5_ = bf16[40,1024]{1,0:T(8,128)(2,1)S(1)} collective-permute-done((bf16[40,1024]{1,0:T(8,128)(2,1)S(1)}, bf16[40,1024]{1,0:T(8,128)(2,1)S(1)}, u32[]{:S(2)}, u32[]{:S(2)}) %collective-permute-start.17) | collective-permute-done | bytes 81952 | tf_op jit(solution)/shard_map/ppermute | solution.py:510
  68.1 1.3 shard_map.184.own
  69.4 1.5 %collective-permute-start.20 = (bf16[128,1024]{1,0:T(8,128)(2,1)S(1)}, bf16[128,1024]{1,0:T(8,128)(2,1)S(1)}, u32[]{:S(2)}, u32[]{:S(2)}) collective-permute-start(bf16[128,1024]{1,0:T(8,128)(2,1)S(1)} %shard_map.184.own), channel_id=1, source_target_pairs={{0,2},{1,3},{2,0},{3,1},{4,6},{5,7},{6,4},{7,5},{8,10},{9,11},{10,... | collective-permute-start | bytes 786440 | tf_op jit(solution)/shard_map/ppermute | solution.py:510
  70.9 4.1 %collective-permute-start.28 = (bf16[2,128,1024]{2,1,0:T(8,128)(2,1)S(1)}, bf16[2,128,1024]{2,1,0:T(8,128)(2,1)S(1)}, u32[]{:S(2)}, u32[]{:S(2)}) collective-permute-start(bf16[2,128,1024]{2,1,0:T(8,128)(2,1)S(1)} %pad_maximum_fusion.refs_0_), channel_id=1, source_target_pairs={{0,8},{4,12},{8,0},{12,4},{16,24},{20,28},{24,16},{28,20},{1,9},{5... | collective-permute-start | bytes 1572872 | tf_op jit(solution)/shard_map/ppermute | solution.py:510
  75.0 2.4 %collective-permute-done.20.came = bf16[128,1024]{1,0:T(8,128)(2,1)S(1)} collective-permute-done((bf16[128,1024]{1,0:T(8,128)(2,1)S(1)}, bf16[128,1024]{1,0:T(8,128)(2,1)S(1)}, u32[]{:S(2)}, u32[]{:S(2)}) %collective-permute-start.20) | collective-permute-done | bytes 262176 | tf_op jit(solution)/shard_map/ppermute | solution.py:510
  78.0 2.8 %stage.5.wo = bf16[2,1024,1024]{2,1,0:T(8,128)(2,1)S(1)} custom-call(s32[3]{0:T(128)S(1)} %pad_add_fusion.at.core, bf16[2048,1024]{1,0:T(8,128)(2,1)} %refs_0_.1), custom_call_target="tpu_custom_call" | custom-call | tf_op jit(solution)/shard_map/stage/pallas_call | solution.py:155
  80.9 2.4 %shard_map.186 = (bf16[4,128,256]{2,1,0:T(8,128)(2,1)S(1)}, bf16[4,144,128]{2,1,0:T(8,128)(2,1)S(1)}, bf16[4,144,128]{2,1,0:T(8,128)(2,1)S(1)}, bf16[4,64,256]{2,1,0:T(8,128)(2,1)S(1)}, bf16[4,64,256]{2,1,0:T(8,128)(2,1)S(1)}) custom-call(s32[3]{0:T(128)S(1)} %pad_add_fusion.at.core, bf16[128,1024]{1,0:T(8,128)(2,1)S(1)} %shard_map.185.ma, ...), custom_call_target="tpu_custom_call" | custom-call | tf_op jit(solution)/shard_map/pallas_call | solution.py:429
  83.3 1.7 %collective-permute-start.31 = (bf16[4,144,128]{2,1,0:T(8,128)(2,1)S(1)}, bf16[4,144,128]{2,1,0:T(8,128)(2,1)S(1)}, u32[]{:S(2)}, u32[]{:S(2)}) collective-permute-start(bf16[4,144,128]{2,1,0:T(8,128)(2,1)S(1)} %get-tuple-element.101), channel_id=1, source_target_pairs={{0,4},{4,0},{8,12},{12,8},{16,20},{20,16},{24,28},{28,24},{1,5},{5... | collective-permute-start | bytes 442376 | tf_op jit(solution)/shard_map/ppermute | solution.py:510
  85.0 4.5 %collective-permute-start.22 = (bf16[4,64,256]{2,1,0:T(8,128)(2,1)S(1)}, bf16[4,64,256]{2,1,0:T(8,128)(2,1)S(1)}, u32[]{:S(2)}, u32[]{:S(2)}) collective-permute-start(bf16[4,64,256]{2,1,0:T(8,128)(2,1)S(1)} %get-tuple-element.89), channel_id=1, source_target_pairs={{0,16},{4,20},{8,24},{12,28},{16,0},{20,4},{24,8},{28,12},{1,17},{... | collective-permute-start | bytes 393224 | tf_op jit(solution)/shard_map/ppermute | solution.py:510
  90.5 1.1 collective-permute-start.30
  92.3 2.6 %collective-permute-start.32 = (bf16[4,144,128]{2,1,0:T(8,128)(2,1)S(1)}, bf16[4,144,128]{2,1,0:T(8,128)(2,1)S(1)}, u32[]{:S(2)}, u32[]{:S(2)}) collective-permute-start(bf16[4,144,128]{2,1,0:T(8,128)(2,1)S(1)} %shard_map.191.group), channel_id=1, source_target_pairs={{0,8},{4,12},{8,0},{12,4},{16,24},{20,28},{24,16},{28,20},{1,9},{5... | collective-permute-start | bytes 442376 | tf_op jit(solution)/shard_map/ppermute | solution.py:510
  94.9 1.5 %collective-permute-done.22 = bf16[4,64,256]{2,1,0:T(8,128)(2,1)S(1)} collective-permute-done((bf16[4,64,256]{2,1,0:T(8,128)(2,1)S(1)}, bf16[4,64,256]{2,1,0:T(8,128)(2,1)S(1)}, u32[]{:S(2)}, u32[]{:S(2)}) %collective-permute-start.22) | collective-permute-done | bytes 131104 | tf_op jit(solution)/shard_map/ppermute | solution.py:510
  97.0 5.0 %collective-permute-done.23 = bf16[4,64,256]{2,1,0:T(8,128)(2,1)S(1)} collective-permute-done((bf16[4,64,256]{2,1,0:T(8,128)(2,1)S(1)}, bf16[4,64,256]{2,1,0:T(8,128)(2,1)S(1)}, u32[]{:S(2)}, u32[]{:S(2)}) %collective-permute-start.23) | collective-permute-done | bytes 131104 | tf_op jit(solution)/shard_map/ppermute | solution.py:510
  102.5 1.2 collective-permute-start.24
  104.5 1.7 %collective-permute-start.33 = (bf16[4,128,128]{2,1,0:T(8,128)(2,1)S(1)}, bf16[4,128,128]{2,1,0:T(8,128)(2,1)S(1)}, u32[]{:S(2)}, u32[]{:S(2)}) collective-permute-start(bf16[4,128,128]{2,1,0:T(8,128)(2,1)S(1)} %get-tuple-element.102), channel_id=1, source_target_pairs={{0,16},{4,20},{8,24},{12,28},{16,0},{20,4},{24,8},{28,12},{1,17},{... | collective-permute-start | bytes 393224 | tf_op jit(solution)/shard_map/ppermute | solution.py:510
  106.1 11.2 %collective-permute-done.24.a = bf16[4,64,256]{2,1,0:T(8,128)(2,1)S(1)} collective-permute-done((bf16[4,64,256]{2,1,0:T(8,128)(2,1)S(1)}, bf16[4,64,256]{2,1,0:T(8,128)(2,1)S(1)}, u32[]{:S(2)}, u32[]{:S(2)}) %collective-permute-start.24) | collective-permute-done | bytes 131104 | tf_op jit(solution)/shard_map/ppermute | solution.py:510
  118.1 1.0 collective-permute-start.34
  119.0 4.9 %weights.1 = (bf16[1,2048,512]{2,1,0:T(8,128)(2,1)}, bf16[1,2048,512]{2,1,0:T(8,128)(2,1)}) custom-call(s32[3]{0:T(128)S(1)} %pad_add_fusion.at.core, bf16[320,2048]{1,0:T(8,128)(2,1)S(1)} %bitcast.18, bf16[320,2048]{1,0:T(8,128)(2,1)S(1)} %collective-permute-done.11.other.rb.gb, bf16[320,512]{1,0:T(8,128)(2,1)S(1)} %get-tuple-element.70.gback, ...), custom_call_target="tpu_custom_call" | custom-call | tf_op jit(solution)/shard_map/weights/pallas_call | solution.py:234
  124.0 3.8 %down.1 = bf16[1,512,2048]{2,1,0:T(8,128)(2,1)} custom-call(s32[3]{0:T(128)S(1)} %pad_add_fusion.at.core, bf16[320,2048]{1,0:T(8,128)(2,1)S(1)} %bitcast.19, bf16[320,2048]{1,0:T(8,128)(2,1)S(1)} %collective-permute-done.11.other.rb.gb, bf16[320,512]{1,0:T(8,128)(2,1)S(1)} %get-tuple-element.74.hidden), custom_call_target="tpu_custom_call" | custom-call | tf_op jit(solution)/shard_map/down/pallas_call | solution.py:259
  127.7 2.2 %shard_map.190 = (bf16[4,128,128]{2,1,0:T(8,128)(2,1)}, f32[4,128,128]{2,1,0:T(8,128)S(1)}, f32[4,128,256]{2,1,0:T(8,128)S(1)}, f32[4,128,1]{2,1,0:T(8,128)S(1)}) custom-call(s32[3]{0:T(128)S(1)} %pad_add_fusion.at.core, bf16[4,128,128]{2,1,0:T(8,128)(2,1)S(1)} %get-tuple-element.86.q, bf16[4,128,128]{2,1,0:T(8,128)(2,1)S(1)} %get-tuple-element.94.k, ...), custom_call_target="tpu_custom_call" | custom-call | tf_op jit(solution)/shard_map/pallas_call | solution.py:429
  129.9 1.4 %project.2.refs_0_ = f32[256,1024]{1,0:T(8,128)S(1)} custom-call(s32[3]{0:T(128)S(1)} %pad_add_fusion.at.core, bf16[4,64,256]{2,1,0:T(8,128)(2,1)S(1)} %bitcast.23, bf16[4,64,256]{2,1,0:T(8,128)(2,1)S(1)} %collective-permute-done.26.b, bf16[2,128,1024]{2,1,0:T(8,128)(2,1)S(1)} %pad_maximum_fusion.refs_0_, ...), custom_call_target="tpu_custom_call" | custom-call | tf_op jit(solution)/shard_map/project/pallas_call | solution.py:491
  131.4 2.2 %project.3 = f32[256,1024]{1,0:T(8,128)} custom-call(s32[3]{0:T(128)S(1)} %pad_add_fusion.at.core, bf16[4,64,256]{2,1,0:T(8,128)(2,1)S(1)} %collective-permute-done.24.a, bf16[4,64,256]{2,1,0:T(8,128)(2,1)S(1)} %collective-permute-done.25.b, f32[256,1024]{1,0:T(8,128)S(1)} %project.2.refs_0_, bf16[2,128,1024]{2,1,0:T(8,128)(2,1)S(1)} %collective-permute-done.29.refs_1_, ...), custom_call_target="tpu_custom_call" | custom-call | tf_op jit(solution)/shard_map/project/pallas_call | solution.py:491
  133.6 1.7 %shard_map.194 = (bf16[4,128,128]{2,1,0:T(8,128)(2,1)}, bf16[4,128,256]{2,1,0:T(8,128)(2,1)}) custom-call(s32[3]{0:T(128)S(1)} %pad_add_fusion.at.core, bf16[4,128,128]{2,1,0:T(8,128)(2,1)S(1)} %get-tuple-element.94.k, bf16[4,128,256]{2,1,0:T(8,128)(2,1)S(1)} %get-tuple-element.95.v, f32[4,128,1]{2,1,0:T(8,128)S(1)} %get-tuple-element.99.trails, ...), custom_call_target="tpu_custom_call" | custom-call | tf_op jit(solution)/shard_map/pallas_call | solution.py:429
  (49 shorter events, 9.0 us)
Async XLA Ops:
  3.1 10.7 %collective-permute-start.9 = (bf16[40,1024]{1,0:T(8,128)(2,1)S(1)}, bf16[40,1024]{1,0:T(8,128)(2,1)S(1)}, u32[]{:S(2)}, u32[]{:S(2)}) collective-permute-start(bf16[40,1024]{1,0:T(8,128)(2,1)S(1)} %get-tuple-element.66), channel_id=1, source_target_pairs={{0,28},{4,24},{8,20},{12,16},{16,12},{20,8},{24,4},{28,0},{1,29},{... | collective-permute-start | bytes 245768 | tf_op jit(solution)/shard_map/ppermute | solution.py:510
  9.2 11.1 %collective-permute-start.3 = (bf16[40,1024]{1,0:T(8,128)(2,1)S(1)}, bf16[40,1024]{1,0:T(8,128)(2,1)S(1)}, u32[]{:S(2)}, u32[]{:S(2)}) collective-permute-start(bf16[40,1024]{1,0:T(8,128)(2,1)S(1)} %get-tuple-element.63), channel_id=1, source_target_pairs={{0,16},{4,20},{8,24},{12,28},{16,0},{20,4},{24,8},{28,12},{1,17},{... | collective-permute-start | bytes 245768 | tf_op jit(solution)/shard_map/ppermute | solution.py:510
  9.2 12.9 %collective-permute-start.5 = (bf16[40,1024]{1,0:T(8,128)(2,1)S(1)}, bf16[40,1024]{1,0:T(8,128)(2,1)S(1)}, u32[]{:S(2)}, u32[]{:S(2)}) collective-permute-start(bf16[40,1024]{1,0:T(8,128)(2,1)S(1)} %get-tuple-element.64), channel_id=1, source_target_pairs={{0,20},{4,16},{8,28},{12,24},{16,4},{20,0},{24,12},{28,8},{1,21},{... | collective-permute-start | bytes 245768 | tf_op jit(solution)/shard_map/ppermute | solution.py:510
  12.1 10.0 %collective-permute-start.7 = (bf16[40,1024]{1,0:T(8,128)(2,1)S(1)}, bf16[40,1024]{1,0:T(8,128)(2,1)S(1)}, u32[]{:S(2)}, u32[]{:S(2)}) collective-permute-start(bf16[40,1024]{1,0:T(8,128)(2,1)S(1)} %get-tuple-element.65), channel_id=1, source_target_pairs={{0,24},{4,28},{8,16},{12,20},{16,8},{20,12},{24,0},{28,4},{1,25},{... | collective-permute-start | bytes 245768 | tf_op jit(solution)/shard_map/ppermute | solution.py:510
  12.2 18.8 %collective-permute-start = (bf16[40,2048]{1,0:T(8,128)(2,1)S(1)}, bf16[40,2048]{1,0:T(8,128)(2,1)S(1)}, u32[]{:S(2)}, u32[]{:S(2)}) collective-permute-start(bf16[40,2048]{1,0:T(8,128)(2,1)S(1)} %get-tuple-element.60), channel_id=1, source_target_pairs={{0,4},{4,0},{8,12},{12,8},{16,20},{20,16},{24,28},{28,24},{1,5},{5... | collective-permute-start | bytes 491528 | tf_op jit(solution)/shard_map/ppermute | solution.py:510
  13.8 11.2 %collective-permute-start.10 = (bf16[40,1024]{1,0:T(8,128)(2,1)S(1)}, bf16[40,1024]{1,0:T(8,128)(2,1)S(1)}, u32[]{:S(2)}, u32[]{:S(2)}) collective-permute-start(bf16[40,1024]{1,0:T(8,128)(2,1)S(1)} %collective-permute-done.9.refs_10_), channel_id=1, source_target_pairs={{0,2},{1,3},{2,0},{3,1},{4,6},{5,7},{6,4},{7,5},{8,10},{9,11},{10,... | collective-permute-start | bytes 245768 | tf_op jit(solution)/shard_map/ppermute | solution.py:510
  20.3 6.2 %collective-permute-start.4 = (bf16[40,1024]{1,0:T(8,128)(2,1)S(1)}, bf16[40,1024]{1,0:T(8,128)(2,1)S(1)}, u32[]{:S(2)}, u32[]{:S(2)}) collective-permute-start(bf16[40,1024]{1,0:T(8,128)(2,1)S(1)} %collective-permute-done.3.refs_4_), channel_id=1, source_target_pairs={{0,2},{1,3},{2,0},{3,1},{4,6},{5,7},{6,4},{7,5},{8,10},{9,11},{10,... | collective-permute-start | bytes 245768 | tf_op jit(solution)/shard_map/ppermute | solution.py:510
  22.1 8.9 %collective-permute-start.1 = (bf16[40,2048]{1,0:T(8,128)(2,1)S(1)}, bf16[40,2048]{1,0:T(8,128)(2,1)S(1)}, u32[]{:S(2)}, u32[]{:S(2)}) collective-permute-start(bf16[40,2048]{1,0:T(8,128)(2,1)S(1)} %get-tuple-element.61), channel_id=1, source_target_pairs={{0,8},{4,12},{8,0},{12,4},{16,24},{20,28},{24,16},{28,20},{1,9},{5... | collective-permute-start | bytes 491528 | tf_op jit(solution)/shard_map/ppermute | solution.py:510
  22.1 9.2 %collective-permute-start.2 = (bf16[40,2048]{1,0:T(8,128)(2,1)S(1)}, bf16[40,2048]{1,0:T(8,128)(2,1)S(1)}, u32[]{:S(2)}, u32[]{:S(2)}) collective-permute-start(bf16[40,2048]{1,0:T(8,128)(2,1)S(1)} %get-tuple-element.62), channel_id=1, source_target_pairs={{0,12},{4,8},{8,4},{12,0},{16,28},{20,24},{24,20},{28,16},{1,13},{... | collective-permute-start | bytes 491528 | tf_op jit(solution)/shard_map/ppermute | solution.py:510
  25.0 4.4 %collective-permute-start.6 = (bf16[40,1024]{1,0:T(8,128)(2,1)S(1)}, bf16[40,1024]{1,0:T(8,128)(2,1)S(1)}, u32[]{:S(2)}, u32[]{:S(2)}) collective-permute-start(bf16[40,1024]{1,0:T(8,128)(2,1)S(1)} %collective-permute-done.5.refs_6_), channel_id=1, source_target_pairs={{0,2},{1,3},{2,0},{3,1},{4,6},{5,7},{6,4},{7,5},{8,10},{9,11},{10,... | collective-permute-start | bytes 245768 | tf_op jit(solution)/shard_map/ppermute | solution.py:510
  26.5 4.4 %collective-permute-start.8 = (bf16[40,1024]{1,0:T(8,128)(2,1)S(1)}, bf16[40,1024]{1,0:T(8,128)(2,1)S(1)}, u32[]{:S(2)}, u32[]{:S(2)}) collective-permute-start(bf16[40,1024]{1,0:T(8,128)(2,1)S(1)} %collective-permute-done.7.refs_8_), channel_id=1, source_target_pairs={{0,2},{1,3},{2,0},{3,1},{4,6},{5,7},{6,4},{7,5},{8,10},{9,11},{10,... | collective-permute-start | bytes 245768 | tf_op jit(solution)/shard_map/ppermute | solution.py:510
  31.9 5.5 %collective-permute-start.11 = (bf16[320,2048]{1,0:T(8,128)(2,1)S(1)}, bf16[320,2048]{1,0:T(8,128)(2,1)S(1)}, u32[]{:S(2)}, u32[]{:S(2)}) collective-permute-start(bf16[320,2048]{1,0:T(8,128)(2,1)S(1)} %bitcast.16), channel_id=1, source_target_pairs={{0,1},{1,0},{2,3},{3,2},{4,5},{5,4},{6,7},{7,6},{8,9},{9,8},{10,11... | collective-permute-start | bytes 3932168 | tf_op jit(solution)/shard_map/ppermute | solution.py:510
  41.0 4.1 %collective-permute-start.12 = (bf16[320,1024]{1,0:T(8,128)(2,1)S(1)}, bf16[320,1024]{1,0:T(8,128)(2,1)S(1)}, u32[]{:S(2)}, u32[]{:S(2)}) collective-permute-start(bf16[320,1024]{1,0:T(8,128)(2,1)S(1)} %get-tuple-element.77), channel_id=1, source_target_pairs={{0,1},{1,0},{2,3},{3,2},{4,5},{5,4},{6,7},{7,6},{8,9},{9,8},{10,11... | collective-permute-start | bytes 1966088 | tf_op jit(solution)/shard_map/ppermute | solution.py:510
  42.6 28.2 %collective-permute-start.27 = (bf16[1,128,1024]{2,1,0:T(8,128)(2,1)S(1)}, bf16[1,128,1024]{2,1,0:T(8,128)(2,1)S(1)}, u32[]{:S(2)}, u32[]{:S(2)}) collective-permute-start(bf16[1,128,1024]{2,1,0:T(8,128)(2,1)S(1)} %bitcast.20), channel_id=1, source_target_pairs={{0,16},{4,20},{8,24},{12,28},{16,0},{20,4},{24,8},{28,12},{1,17},{... | collective-permute-start | bytes 786440 | tf_op jit(solution)/shard_map/ppermute | solution.py:510
  45.8 5.5 %collective-permute-start.13 = (bf16[40,1024]{1,0:T(8,128)(2,1)S(1)}, bf16[40,1024]{1,0:T(8,128)(2,1)S(1)}, u32[]{:S(2)}, u32[]{:S(2)}) collective-permute-start(bf16[40,1024]{1,0:T(8,128)(2,1)S(1)} %get-tuple-element.79), channel_id=1, source_target_pairs={{0,4},{4,0},{8,12},{12,8},{16,20},{20,16},{24,28},{28,24},{1,5},{5... | collective-permute-start | bytes 245768 | tf_op jit(solution)/shard_map/ppermute | solution.py:510
  46.8 5.9 %collective-permute-start.14 = (bf16[40,1024]{1,0:T(8,128)(2,1)S(1)}, bf16[40,1024]{1,0:T(8,128)(2,1)S(1)}, u32[]{:S(2)}, u32[]{:S(2)}) collective-permute-start(bf16[40,1024]{1,0:T(8,128)(2,1)S(1)} %get-tuple-element.80), channel_id=1, source_target_pairs={{0,8},{4,12},{8,0},{12,4},{16,24},{20,28},{24,16},{28,20},{1,9},{5... | collective-permute-start | bytes 245768 | tf_op jit(solution)/shard_map/ppermute | solution.py:510
  48.5 8.5 %collective-permute-start.15 = (bf16[40,1024]{1,0:T(8,128)(2,1)S(1)}, bf16[40,1024]{1,0:T(8,128)(2,1)S(1)}, u32[]{:S(2)}, u32[]{:S(2)}) collective-permute-start(bf16[40,1024]{1,0:T(8,128)(2,1)S(1)} %get-tuple-element.81), channel_id=1, source_target_pairs={{0,12},{4,8},{8,4},{12,0},{16,28},{20,24},{24,20},{28,16},{1,13},{... | collective-permute-start | bytes 245768 | tf_op jit(solution)/shard_map/ppermute | solution.py:510
  49.3 16.9 %collective-permute-start.16 = (bf16[40,1024]{1,0:T(8,128)(2,1)S(1)}, bf16[40,1024]{1,0:T(8,128)(2,1)S(1)}, u32[]{:S(2)}, u32[]{:S(2)}) collective-permute-start(bf16[40,1024]{1,0:T(8,128)(2,1)S(1)} %get-tuple-element.82), channel_id=1, source_target_pairs={{0,16},{4,20},{8,24},{12,28},{16,0},{20,4},{24,8},{28,12},{1,17},{... | collective-permute-start | bytes 245768 | tf_op jit(solution)/shard_map/ppermute | solution.py:510
  51.3 16.8 %collective-permute-start.17 = (bf16[40,1024]{1,0:T(8,128)(2,1)S(1)}, bf16[40,1024]{1,0:T(8,128)(2,1)S(1)}, u32[]{:S(2)}, u32[]{:S(2)}) collective-permute-start(bf16[40,1024]{1,0:T(8,128)(2,1)S(1)} %get-tuple-element.83), channel_id=1, source_target_pairs={{0,20},{4,16},{8,28},{12,24},{16,4},{20,0},{24,12},{28,8},{1,21},{... | collective-permute-start | bytes 245768 | tf_op jit(solution)/shard_map/ppermute | solution.py:510
  52.6 15.5 %collective-permute-start.18 = (bf16[40,1024]{1,0:T(8,128)(2,1)S(1)}, bf16[40,1024]{1,0:T(8,128)(2,1)S(1)}, u32[]{:S(2)}, u32[]{:S(2)}) collective-permute-start(bf16[40,1024]{1,0:T(8,128)(2,1)S(1)} %get-tuple-element.84), channel_id=1, source_target_pairs={{0,24},{4,28},{8,16},{12,20},{16,8},{20,12},{24,0},{28,4},{1,25},{... | collective-permute-start | bytes 245768 | tf_op jit(solution)/shard_map/ppermute | solution.py:510
  57.0 11.1 %collective-permute-start.19 = (bf16[40,1024]{1,0:T(8,128)(2,1)S(1)}, bf16[40,1024]{1,0:T(8,128)(2,1)S(1)}, u32[]{:S(2)}, u32[]{:S(2)}) collective-permute-start(bf16[40,1024]{1,0:T(8,128)(2,1)S(1)} %get-tuple-element.85), channel_id=1, source_target_pairs={{0,28},{4,24},{8,20},{12,16},{16,12},{20,8},{24,4},{28,0},{1,29},{... | collective-permute-start | bytes 245768 | tf_op jit(solution)/shard_map/ppermute | solution.py:510
  69.4 8.0 %collective-permute-start.20 = (bf16[128,1024]{1,0:T(8,128)(2,1)S(1)}, bf16[128,1024]{1,0:T(8,128)(2,1)S(1)}, u32[]{:S(2)}, u32[]{:S(2)}) collective-permute-start(bf16[128,1024]{1,0:T(8,128)(2,1)S(1)} %shard_map.184.own), channel_id=1, source_target_pairs={{0,2},{1,3},{2,0},{3,1},{4,6},{5,7},{6,4},{7,5},{8,10},{9,11},{10,... | collective-permute-start | bytes 786440 | tf_op jit(solution)/shard_map/ppermute | solution.py:510
  70.9 19.6 %collective-permute-start.28 = (bf16[2,128,1024]{2,1,0:T(8,128)(2,1)S(1)}, bf16[2,128,1024]{2,1,0:T(8,128)(2,1)S(1)}, u32[]{:S(2)}, u32[]{:S(2)}) collective-permute-start(bf16[2,128,1024]{2,1,0:T(8,128)(2,1)S(1)} %pad_maximum_fusion.refs_0_), channel_id=1, source_target_pairs={{0,8},{4,12},{8,0},{12,4},{16,24},{20,28},{24,16},{28,20},{1,9},{5... | collective-permute-start | bytes 1572872 | tf_op jit(solution)/shard_map/ppermute | solution.py:510
  78.0 2.9 %collective-permute-start.21 = (bf16[128,1024]{1,0:T(8,128)(2,1)S(1)}, bf16[128,1024]{1,0:T(8,128)(2,1)S(1)}, u32[]{:S(2)}, u32[]{:S(2)}) collective-permute-start(bf16[128,1024]{1,0:T(8,128)(2,1)S(1)} %shard_map.185.ma), channel_id=1, source_target_pairs={{0,1},{1,0},{2,3},{3,2},{4,5},{5,4},{6,7},{7,6},{8,9},{9,8},{10,11... | collective-permute-start | bytes 786440 | tf_op jit(solution)/shard_map/ppermute | solution.py:510
  83.3 8.3 %collective-permute-start.31 = (bf16[4,144,128]{2,1,0:T(8,128)(2,1)S(1)}, bf16[4,144,128]{2,1,0:T(8,128)(2,1)S(1)}, u32[]{:S(2)}, u32[]{:S(2)}) collective-permute-start(bf16[4,144,128]{2,1,0:T(8,128)(2,1)S(1)} %get-tuple-element.101), channel_id=1, source_target_pairs={{0,4},{4,0},{8,12},{12,8},{16,20},{20,16},{24,28},{28,24},{1,5},{5... | collective-permute-start | bytes 442376 | tf_op jit(solution)/shard_map/ppermute | solution.py:510
  85.0 11.3 %collective-permute-start.22 = (bf16[4,64,256]{2,1,0:T(8,128)(2,1)S(1)}, bf16[4,64,256]{2,1,0:T(8,128)(2,1)S(1)}, u32[]{:S(2)}, u32[]{:S(2)}) collective-permute-start(bf16[4,64,256]{2,1,0:T(8,128)(2,1)S(1)} %get-tuple-element.89), channel_id=1, source_target_pairs={{0,16},{4,20},{8,24},{12,28},{16,0},{20,4},{24,8},{28,12},{1,17},{... | collective-permute-start | bytes 393224 | tf_op jit(solution)/shard_map/ppermute | solution.py:510
  89.6 41.8 %collective-permute-start.29 = (bf16[2,128,1024]{2,1,0:T(8,128)(2,1)S(1)}, bf16[2,128,1024]{2,1,0:T(8,128)(2,1)S(1)}, u32[]{:S(2)}, u32[]{:S(2)}) collective-permute-start(bf16[2,128,1024]{2,1,0:T(8,128)(2,1)S(1)} %pad_maximum_fusion.refs_0_), channel_id=1, source_target_pairs={{0,4},{4,0},{8,12},{12,8},{16,20},{20,16},{24,28},{28,24},{1,5},{5... | collective-permute-start | bytes 1572872 | tf_op jit(solution)/shard_map/ppermute | solution.py:510
  90.5 40.9 %collective-permute-start.30 = (bf16[2,128,1024]{2,1,0:T(8,128)(2,1)S(1)}, bf16[2,128,1024]{2,1,0:T(8,128)(2,1)S(1)}, u32[]{:S(2)}, u32[]{:S(2)}) collective-permute-start(bf16[2,128,1024]{2,1,0:T(8,128)(2,1)S(1)} %collective-permute-done.28.refs_1_), channel_id=1, source_target_pairs={{0,4},{4,0},{8,12},{12,8},{16,20},{20,16},{24,28},{28,24},{1,5},{5... | collective-permute-start | bytes 1572872 | tf_op jit(solution)/shard_map/ppermute | solution.py:510
  92.3 11.5 %collective-permute-start.32 = (bf16[4,144,128]{2,1,0:T(8,128)(2,1)S(1)}, bf16[4,144,128]{2,1,0:T(8,128)(2,1)S(1)}, u32[]{:S(2)}, u32[]{:S(2)}) collective-permute-start(bf16[4,144,128]{2,1,0:T(8,128)(2,1)S(1)} %shard_map.191.group), channel_id=1, source_target_pairs={{0,8},{4,12},{8,0},{12,4},{16,24},{20,28},{24,16},{28,20},{1,9},{5... | collective-permute-start | bytes 442376 | tf_op jit(solution)/shard_map/ppermute | solution.py:510
  96.9 5.0 %collective-permute-start.23 = (bf16[4,64,256]{2,1,0:T(8,128)(2,1)S(1)}, bf16[4,64,256]{2,1,0:T(8,128)(2,1)S(1)}, u32[]{:S(2)}, u32[]{:S(2)}) collective-permute-start(bf16[4,64,256]{2,1,0:T(8,128)(2,1)S(1)} %bitcast.28), channel_id=1, source_target_pairs={{0,8},{4,12},{8,0},{12,4},{16,24},{20,28},{24,16},{28,20},{1,9},{5... | collective-permute-start | bytes 393224 | tf_op jit(solution)/shard_map/ppermute | solution.py:510
  102.5 14.9 %collective-permute-start.24 = (bf16[4,64,256]{2,1,0:T(8,128)(2,1)S(1)}, bf16[4,64,256]{2,1,0:T(8,128)(2,1)S(1)}, u32[]{:S(2)}, u32[]{:S(2)}) collective-permute-start(bf16[4,64,256]{2,1,0:T(8,128)(2,1)S(1)} %bitcast.27), channel_id=1, source_target_pairs={{0,4},{4,0},{8,12},{12,8},{16,20},{20,16},{24,28},{28,24},{1,5},{5... | collective-permute-start | bytes 393224 | tf_op jit(solution)/shard_map/ppermute | solution.py:510
  104.5 12.9 %collective-permute-start.33 = (bf16[4,128,128]{2,1,0:T(8,128)(2,1)S(1)}, bf16[4,128,128]{2,1,0:T(8,128)(2,1)S(1)}, u32[]{:S(2)}, u32[]{:S(2)}) collective-permute-start(bf16[4,128,128]{2,1,0:T(8,128)(2,1)S(1)} %get-tuple-element.102), channel_id=1, source_target_pairs={{0,16},{4,20},{8,24},{12,28},{16,0},{20,4},{24,8},{28,12},{1,17},{... | collective-permute-start | bytes 393224 | tf_op jit(solution)/shard_map/ppermute | solution.py:510
  106.1 23.8 %collective-permute-start.26 = (bf16[4,64,256]{2,1,0:T(8,128)(2,1)S(1)}, bf16[4,64,256]{2,1,0:T(8,128)(2,1)S(1)}, u32[]{:S(2)}, u32[]{:S(2)}) collective-permute-start(bf16[4,64,256]{2,1,0:T(8,128)(2,1)S(1)} %bitcast.22), channel_id=1, source_target_pairs={{0,1},{1,0},{2,3},{3,2},{4,5},{5,4},{6,7},{7,6},{8,9},{9,8},{10,11... | collective-permute-start | bytes 393224 | tf_op jit(solution)/shard_map/ppermute | solution.py:510
  117.4 14.0 %collective-permute-start.25 = (bf16[4,64,256]{2,1,0:T(8,128)(2,1)S(1)}, bf16[4,64,256]{2,1,0:T(8,128)(2,1)S(1)}, u32[]{:S(2)}, u32[]{:S(2)}) collective-permute-start(bf16[4,64,256]{2,1,0:T(8,128)(2,1)S(1)} %collective-permute-done.24.a), channel_id=1, source_target_pairs={{0,1},{1,0},{2,3},{3,2},{4,5},{5,4},{6,7},{7,6},{8,9},{9,8},{10,11... | collective-permute-start | bytes 393224 | tf_op jit(solution)/shard_map/ppermute | solution.py:510
  118.1 15.5 %collective-permute-start.34 = (bf16[4,128,128]{2,1,0:T(8,128)(2,1)S(1)}, bf16[4,128,128]{2,1,0:T(8,128)(2,1)S(1)}, u32[]{:S(2)}, u32[]{:S(2)}) collective-permute-start(bf16[4,128,128]{2,1,0:T(8,128)(2,1)S(1)} %get-tuple-element.106), channel_id=1, source_target_pairs={{0,4},{4,0},{8,12},{12,8},{16,20},{20,16},{24,28},{28,24},{1,5},{5... | collective-permute-start | bytes 393224 | tf_op jit(solution)/shard_map/ppermute | solution.py:510
